TPU v7x, 256 devices: a whole 4x4x8 slice. The times are simulated.
256 devices in a mesh: sp: 32 (over z, y), tp: 4 (over x), dp: 2 (over core).
Axes of the slice: x: 4, y: 4, z: 8, core: 2. Of those that a mesh axis runs over, the one named last changes fastest.
Arguments:
- latent: bfloat16 [2, 32768, 2048], P('dp', 'sp'), may hold values from -4 to 4
- context: bfloat16 [2, 768, 2048], P('dp', 'sp'), may hold values from -6 to 6
- cond: float32 [2, 2048], P('dp'), may hold values from -6 to 6
- ctx_cond: float32 [2048], replicated, may hold values from -6 to 6
- norm_gain: float32 [2048], replicated, may hold values from 0.1 to 1.9
- mod_shift: bfloat16 [2048, 2048], P('sp', 'tp'), may hold values from -0.125 to 0.125
- mod_scale: bfloat16 [2048, 2048], P('sp', 'tp'), may hold values from -0.125 to 0.125
- mod_gate: bfloat16 [2048, 2048], P('sp', 'tp'), may hold values from -0.125 to 0.125
- w_query: bfloat16 [2048, 2048], P(None, 'tp'), may hold values from -0.125 to 0.125
- w_key: bfloat16 [2048, 512], P(None, 'tp'), may hold values from -0.125 to 0.125
- w_value: bfloat16 [2048, 512], P(None, 'tp'), may hold values from -0.125 to 0.125
- w_out: bfloat16 [2048, 2048], P('tp'), may hold values from -2 to 2
- q_gain: float32 [128], replicated, may hold values from 0.1 to 1.9
- k_gain: float32 [128], replicated, may hold values from 0.1 to 1.9
- sinks: float32 [16], P('tp'), may hold values from 3 to 8
Outputs:
- result: bfloat16 [2, 32768, 2048], P('dp', ('sp', 'tp'))
All inputs are finite; a program needn't handle non-finite values.
Results may differ from a plain program's by a relative error of at most 0.013.
Values may be sent and summed in bfloat16 or wider, within the bound.
No kernel may reach another device: no remote copies, remote signals or barrier semaphores. Data moves between devices by JAX's collectives and lax.ppermute only.
A program may use at most 128 MiB of HBM per device.

v0:
```python
import jax
import jax.numpy as jnp
from jax import lax
from jax.sharding import PartitionSpec as P

HEAD_DIM = 128
WINDOW = 128
GRID_W = 64


NORM_EPSILON = 1e-06
ROPE_BASE = 10000.0


def from_everyone(array, axis):
    peers = lax.axis_size(axis)
    return lax.all_to_all(
        jnp.broadcast_to(array[None], (peers, *array.shape)), axis, 0, 0, tiled=True
    )


def taken_together(array, axis):
    return from_everyone(array, axis).sum(axis=0)


def in_order(pieces, dim):
    lengths = list(pieces.shape[1:])
    lengths[dim] *= pieces.shape[0]
    return jnp.moveaxis(pieces, 0, dim).reshape(lengths)


def gather_directly(array, axis, dim):
    pieces = from_everyone(array, axis)
    return in_order(pieces, dim)


def extended(array, sides, width):
    for axis, dim in sides:
        peers, length = (lax.axis_size(axis), array.shape[dim])
        up = [(i, (i + 1) % peers) for i in range(peers - 1)]
        down = [(j, i) for i, j in up]
        last = lax.slice_in_dim(array, length - width, length, axis=dim)
        first = lax.slice_in_dim(array, 0, width, axis=dim)
        before = lax.ppermute(last, axis, up)
        after = lax.ppermute(first, axis, down)
        array = jnp.concatenate([before, array, after], axis=dim)
    return array


def split_up(array, dim, peers):
    before, after = (array.shape[:dim], array.shape[dim + 1 :])
    return jnp.moveaxis(array.reshape(*before, peers, -1, *after), dim, 0)


def summed_on_arrival(array, axis, dim):
    peers = lax.axis_size(axis)
    pieces = lax.all_to_all(split_up(array, dim, peers), axis, 0, 0, tiled=True)
    return jnp.sum(pieces.astype(jnp.float32), axis=0)


def head_norm(vectors, gain_row):
    return (
        vectors
        * lax.rsqrt(jnp.mean(vectors * vectors, axis=-1, keepdims=True) + NORM_EPSILON)
        * gain_row
    )


def modulated(rows_in, gain_row, shift_row, scale_row):
    values = rows_in.astype(jnp.float32)
    normed = (
        values
        * lax.rsqrt(jnp.mean(values * values, axis=-1, keepdims=True) + NORM_EPSILON)
        * gain_row
    )
    return (normed * (1.0 + scale_row) + shift_row).astype(jnp.bfloat16)


def rotate_half(halves, coords):
    quarter = halves.shape[-1] // 2
    frequency = ROPE_BASE ** (-jnp.arange(quarter, dtype=jnp.float32) / quarter)
    angles = coords.astype(jnp.float32)[:, None] * frequency
    cosine_part = jnp.cos(angles)[:, None, :]
    sine_part = jnp.sin(angles)[:, None, :]
    first_part = halves[..., :quarter]
    second_part = halves[..., quarter:]
    return jnp.concatenate(
        [
            first_part * cosine_part - second_part * sine_part,
            second_part * cosine_part + first_part * sine_part,
        ],
        axis=-1,
    )


def rotate(vectors, positions):
    half_dim = vectors.shape[-1] // 2
    return jnp.concatenate(
        [
            rotate_half(vectors[..., :half_dim], positions // GRID_W),
            rotate_half(vectors[..., half_dim:], positions % GRID_W),
        ],
        axis=-1,
    )


def per_device(
    latent,
    context,
    cond,
    ctx_cond,
    norm_gain,
    mod_shift,
    mod_scale,
    mod_gate,
    w_query,
    w_key,
    w_value,
    w_out,
    q_gain,
    k_gain,
    sinks,
):
    tok_count = latent.shape[1]
    part_rows = mod_shift.shape[0]
    sp_index = lax.axis_index("sp")
    tp_index = lax.axis_index("tp")
    cond_rows = jnp.stack([cond[0], ctx_cond])
    own_cond = lax.dynamic_slice_in_dim(cond_rows, sp_index * part_rows, part_rows, 1)
    active = jax.nn.silu(own_cond).astype(jnp.bfloat16)
    shifts = jnp.dot(active, mod_shift, preferred_element_type=jnp.float32)
    scales = jnp.dot(active, mod_scale, preferred_element_type=jnp.float32)
    gate_rows = jnp.dot(active[0:1], mod_gate, preferred_element_type=jnp.float32)
    partial_value = jnp.concatenate([shifts, scales, gate_rows], axis=0)
    summed = taken_together(partial_value, "sp")
    modulation = gather_directly(summed, "tp", 1)
    lat_in = modulated(latent[0], norm_gain, modulation[0], modulation[2])
    ctx_in = modulated(context[0], norm_gain, modulation[1], modulation[3])
    gate_row = modulation[4]
    kv_local = w_key.shape[1] // HEAD_DIM
    q_local = w_query.shape[1] // HEAD_DIM
    group_size = q_local // kv_local
    kv_width = kv_local * HEAD_DIM
    score_scale = HEAD_DIM ** (-0.5)
    positions = sp_index * tok_count + jnp.arange(tok_count, dtype=jnp.int32)
    lat_queries = rotate(
        head_norm(
            jnp.dot(lat_in, w_query, preferred_element_type=jnp.float32).reshape(
                tok_count, q_local, HEAD_DIM
            ),
            q_gain,
        ),
        positions,
    ).astype(jnp.bfloat16)
    lat_keys = rotate(
        head_norm(
            jnp.dot(lat_in, w_key, preferred_element_type=jnp.float32).reshape(
                tok_count, kv_local, HEAD_DIM
            ),
            k_gain,
        ),
        positions,
    ).astype(jnp.bfloat16)
    lat_values = jnp.dot(lat_in, w_value, preferred_element_type=jnp.float32).astype(jnp.bfloat16)
    lat_both = jnp.concatenate([lat_keys.reshape(tok_count, kv_width), lat_values], axis=1)
    padded = extended(lat_both, (("sp", 0),), WINDOW)
    piece_keys = head_norm(
        jnp.dot(ctx_in, w_key, preferred_element_type=jnp.float32).reshape(
            ctx_in.shape[0], kv_local, HEAD_DIM
        ),
        k_gain,
    ).astype(jnp.bfloat16)
    piece_values = jnp.dot(ctx_in, w_value, preferred_element_type=jnp.float32).astype(jnp.bfloat16)
    context_both = gather_directly(
        jnp.concatenate([piece_keys.reshape(ctx_in.shape[0], kv_width), piece_values], axis=1),
        "sp",
        0,
    )
    ctx_count = context_both.shape[0]
    ctx_keys = context_both[:, :kv_width].reshape(ctx_count, kv_local, HEAD_DIM)
    ctx_values = context_both[:, kv_width:].reshape(ctx_count, kv_local, HEAD_DIM)
    block_count = tok_count // WINDOW
    padded_blocks = padded.reshape(block_count + 2, WINDOW, 2 * kv_width)
    window_both = jnp.concatenate(
        [
            padded_blocks[0:block_count],
            padded_blocks[1 : block_count + 1],
            padded_blocks[2 : block_count + 2],
        ],
        axis=1,
    )
    window_keys = window_both[..., :kv_width].reshape(block_count, 3 * WINDOW, kv_local, HEAD_DIM)
    window_values = window_both[..., kv_width:].reshape(block_count, 3 * WINDOW, kv_local, HEAD_DIM)
    query_blocks = lat_queries.reshape(block_count, WINDOW, kv_local, group_size, HEAD_DIM)
    key_rows = jnp.arange(3 * WINDOW, dtype=jnp.int32)
    query_rows = jnp.arange(WINDOW, dtype=jnp.int32)
    offset_rows = key_rows[None, :] - query_rows[:, None]
    in_band = (offset_rows >= 0) & (offset_rows <= 2 * WINDOW)
    key_pos = (
        sp_index * tok_count
        - WINDOW
        + jnp.arange(block_count, dtype=jnp.int32)[:, None] * WINDOW
        + key_rows[None, :]
    )
    seq_total = tok_count * lax.axis_size("sp")
    in_range = (key_pos >= 0) & (key_pos < seq_total)
    in_window = in_band[None, :, :] & in_range[:, None, :]
    scores = (
        jnp.einsum(
            "nqhgd,nkhd->hgnqk", query_blocks, window_keys, preferred_element_type=jnp.float32
        )
        * score_scale
    )
    weights = jnp.where(in_window[None, None], jnp.exp(scores), 0.0)
    flat_queries = lat_queries.reshape(tok_count, kv_local, group_size, HEAD_DIM)
    ctx_weights = jnp.exp(
        jnp.einsum("thgd,chd->hgtc", flat_queries, ctx_keys, preferred_element_type=jnp.float32)
        * score_scale
    )
    sink_exp = jnp.exp(sinks).reshape(kv_local, group_size)
    denominator = (
        jnp.sum(weights, axis=-1).reshape(kv_local, group_size, tok_count)
        + jnp.sum(ctx_weights, axis=-1)
        + sink_exp[:, :, None]
    )
    local_probs = (
        weights / denominator.reshape(kv_local, group_size, block_count, WINDOW)[..., None]
    ).astype(jnp.bfloat16)
    ctx_probs = (ctx_weights / denominator[..., None]).astype(jnp.bfloat16)
    local_part = jnp.einsum(
        "hgnqk,nkhd->nqhgd", local_probs, window_values, preferred_element_type=jnp.float32
    )
    ctx_part = jnp.einsum(
        "hgtc,chd->thgd", ctx_probs, ctx_values, preferred_element_type=jnp.float32
    )
    attended = (local_part.reshape(tok_count, kv_local, group_size, HEAD_DIM) + ctx_part).astype(
        jnp.bfloat16
    )
    attended = attended.reshape(tok_count, q_local * HEAD_DIM)
    sub_rows = tok_count // lax.axis_size("tp")
    mixed_rows = summed_on_arrival(
        jnp.dot(attended, w_out, preferred_element_type=jnp.float32).astype(jnp.bfloat16), "tp", 0
    )
    own_rows = lax.dynamic_slice_in_dim(latent[0], tp_index * sub_rows, sub_rows, 0).astype(
        jnp.float32
    )
    result = (own_rows + gate_row * mixed_rows).astype(jnp.bfloat16)
    return result[None]


def solution(mesh):
    in_specs = (
        P("dp", "sp", None),
        P("dp", "sp", None),
        P("dp", None),
        P(),
        P(),
        P("sp", "tp"),
        P("sp", "tp"),
        P("sp", "tp"),
        P(None, "tp"),
        P(None, "tp"),
        P(None, "tp"),
        P("tp", None),
        P(),
        P(),
        P("tp"),
    )
    out_specs = P("dp", ("sp", "tp"), None)
    return jax.shard_map(
        per_device, mesh=mesh, in_specs=in_specs, out_specs=out_specs, check_vma=False
    )
```

profile of v0, /device:TPU:32, one launch (start us, length us, event | category | flops | bytes accessed | tf_op | source)
XLA Modules:
  0.0 184.0 jit_solution(10324458758093356720)
XLA Ops:
  4.7 11.4 %all-to-all-start = ((f32[32,5,512]{2,1,0:T(8,128)}), f32[32,5,512]{2,1,0:T(8,128)S(1)}, u32[]{:S(2)}, u32[]{:S(2)}) async-start(f32[32,5,512]{2,1,0:T(8,128)} %broadcast_in_dim.14), calls=%async_computation | async-start | bytes 1048576 | tf_op jit(solution)/shard_map/all_to_all | solution.py:17
  16.2 3.1 %fusion.3 = f32[1024]{0:T(1024)S(1)} fusion(bf16[1,1024,2048]{2,1,0:T(8,128)(2,1)} %param.15), kind=kLoop, calls=%fused_computation.8 | loop fusion | flops 6290432 | bytes 4198400 | tf_op jit(solution)/shard_map/reduce_sum | solution.py:73
  22.5 10.8 %all-to-all-done = f32[32,5,512]{2,1,0:T(8,128)S(1)} async-done(((f32[32,5,512]{2,1,0:T(8,128)}), f32[32,5,512]{2,1,0:T(8,128)S(1)}, u32[]{:S(2)}, u32[]{:S(2)}) %all-to-all-start) | async-done | bytes 327712 | tf_op jit(solution)/shard_map/all_to_all | solution.py:17
  34.0 4.3 %all-to-all-start.1 = ((f32[4,5,512]{2,1,0:T(8,128)}), f32[4,5,512]{2,1,0:T(8,128)S(1)}, u32[]{:S(2)}, u32[]{:S(2)}) async-start(f32[4,5,512]{2,1,0:T(8,128)} %broadcast_in_dim.15), calls=%async_computation.1 | async-start | bytes 131072 | tf_op jit(solution)/shard_map/all_to_all | solution.py:17
  38.3 4.0 %copy.80 = bf16[512,2048]{1,0:T(8,128)(2,1)} copy(bf16[512,2048]{0,1:T(8,128)(2,1)} %bitcast.186) | data formatting | bytes 4194304 | tf_op jit(solution)/shard_map/dot_general | solution.py:148
  45.5 5.2 %all-to-all-start.2 = ((bf16[32,24,256]{2,1,0:T(8,128)(2,1)}), bf16[32,24,256]{2,1,0:T(8,128)(2,1)}, u32[]{:S(2)}, u32[]{:S(2)}) async-start(bf16[32,24,256]{2,1,0:T(8,128)(2,1)} %broadcast_in_dim.18), calls=%async_computation.2 | async-start | bytes 786432 | tf_op jit(solution)/shard_map/all_to_all | solution.py:17
  50.7 4.2 %multiply_reduce_fusion.1 = (f32[1024]{0:T(1024)S(1)}, f32[1024,128]{0,1:T(8,128)S(1)}) fusion(bf16[2048,128]{1,0:T(8,128)(2,1)S(1)} %copy-done.10, bf16[1,1024,2048]{2,1,0:T(8,128)(2,1)} %param.15, f32[2048]{0:T(1024)S(1)} %bitcast.201, f32[2048]{0:T(1024)S(1)} %bitcast.204, f32[2048]{0:T(1024)S(1)} %copy-done.14, f32[1024]{0:T(1024)S(1)} %add_rsqrt_fusion.2), kind=kOutput, calls=%fused_computation.72 | convolution fusion | flops 549714944 | bytes 5275648 | tf_op jit(solution)/shard_map/dot_general | solution.py:157
  59.8 3.4 %collective-permute-start = (bf16[128,256]{0,1:T(8,128)(2,1)}, bf16[128,256]{0,1:T(8,128)(2,1)}, u32[]{:S(2)}, u32[]{:S(2)}) collective-permute-start(bf16[128,256]{0,1:T(8,128)(2,1)} %get-tuple-element.13), channel_id=1, source_target_pairs={{0,8},{8,16},{16,24},{24,32},{32,40},{40,48},{48,56},{56,64},{64,7... | collective-permute-start | bytes 196616 | tf_op jit(solution)/shard_map/ppermute | solution.py:44
  63.2 4.8 %collective-permute-start.1 = (bf16[128,256]{0,1:T(8,128)(2,1)}, bf16[128,256]{0,1:T(8,128)(2,1)}, u32[]{:S(2)}, u32[]{:S(2)}) collective-permute-start(bf16[128,256]{0,1:T(8,128)(2,1)} %get-tuple-element.14), channel_id=1, source_target_pairs={{8,0},{16,8},{24,16},{32,24},{40,32},{48,40},{56,48},{64,56},{72,6... | collective-permute-start | bytes 196616 | tf_op jit(solution)/shard_map/ppermute | solution.py:45
  68.0 2.6 %multiply_reduce_fusion = (f32[1024,4]{0,1:T(4,128)S(1)}, f32[1024,4,128]{0,2,1:T(8,128)S(1)}) fusion(bf16[4,128,2048]{2,1,0:T(8,128)(2,1)S(1)} %bitcast.187, bf16[1,1024,2048]{2,1,0:T(8,128)(2,1)S(1)} %copy-done.1, f32[2048]{0:T(1024)S(1)} %bitcast.203, f32[2048]{0:T(1024)S(1)} %bitcast.206, f32[2048]{0:T(1024)S(1)} %copy-done.14, ...), kind=kOutput, calls=%fused_computation.40 | convolution fusion | flops 2161111040 | bytes 8433664 | tf_op jit(solution)/shard_map/dot_general | solution.py:148
  77.7 2.3 %copy.61 = bf16[8,128,4,32]{3,1,2,0:T(8,128)(2,1)} copy(bf16[8,128,4,32]{1,0,3,2:T(8,128)(2,1)} %bitcast.194) | data formatting | bytes 524288 | tf_op jit(solution)/shard_map/concatenate | solution.py:98
  80.0 2.3 %copy.62 = bf16[8,128,4,32]{3,1,2,0:T(8,128)(2,1)} copy(bf16[8,128,4,32]{1,0,3,2:T(8,128)(2,1)} %bitcast.193) | data formatting | bytes 524288 | tf_op jit(solution)/shard_map/concatenate | solution.py:98
  82.3 2.3 %copy.64 = bf16[8,128,4,32]{3,1,2,0:T(8,128)(2,1)} copy(bf16[8,128,4,32]{1,0,3,2:T(8,128)(2,1)} %bitcast.192) | data formatting | bytes 524288 | tf_op jit(solution)/shard_map/concatenate | solution.py:98
  84.6 2.3 %copy.63 = bf16[8,128,4,32]{3,1,2,0:T(8,128)(2,1)} copy(bf16[8,128,4,32]{1,0,3,2:T(8,128)(2,1)} %bitcast.191) | data formatting | bytes 524288 | tf_op jit(solution)/shard_map/concatenate | solution.py:98
  94.7 7.4 %fusion.16 = (f32[4,8,128]{2,0,1:T(4,128)S(1)}, f32[8,384,128,4]{2,1,3,0:T(8,128)}) fusion(pred[8,128,384]{1,2,0:T(8,128)(4,1)} %broadcast_and_fusion, bf16[8,128,4,32]{3,1,2,0:T(8,128)(2,1)} %copy.64, bf16[8,128,4,32]{3,1,2,0:T(8,128)(2,1)} %copy.63, bf16[8,128,4,32]{3,1,2,0:T(8,128)(2,1)} %copy.62, bf16[8,128,4,32]{3,1,2,0:T(8,128)(2,1)} %copy.61, ...), kind=kOutput, calls=%fused_computation.23 | convolution fusion | flops 411561984 | bytes 8536064 | tf_op jit(solution)/shard_map/nqhgd,nkhd->hgnqk/dot_general | solution.py:209
  102.1 6.9 %bitcast_reduce_fusion = (f32[4,1024]{1,0:T(4,128)S(1)}, f32[768,1024,4]{1,0,2:T(8,128)}) fusion(bf16[1024,4,32]{0,2,1:T(8,128)(2,1)S(1)} %get-tuple-element.9, bf16[1024,4,32]{0,2,1:T(8,128)(2,1)S(1)} %copy-done.2, bf16[1024,4,32]{0,2,1:T(8,128)(2,1)S(1)} %get-tuple-element.6, bf16[1024,4,32]{0,2,1:T(8,128)(2,1)S(1)} %get-tuple-element.5, ...), kind=kOutput, calls=%fused_computation.1 | convolution fusion | flops 815788032 | bytes 13844480 | tf_op jit(solution)/shard_map/thgd,chd->hgtc/dot_general | solution.py:217
  109.1 2.0 %fusion.30 = f32[8,128,1,4,128]{4,1,3,0,2:T(8,128)S(1)} fusion(f32[4,8,128]{2,0,1:T(4,128)S(1)} %fusion.80, f32[8,384,128,4]{2,1,3,0:T(8,128)S(1)} %copy-done.18, pred[8,128,384]{1,2,0:T(8,128)(4,1)S(1)} %copy-done.13, bf16[8,384,256]{2,1,0:T(8,128)(2,1)S(1)} %copy-done.5), kind=kOutput, calls=%fused_computation.41 | convolution fusion | flops 408944640 | bytes 9584640 | tf_op jit(solution)/shard_map/hgnqk,nkhd->nqhgd/dot_general | solution.py:230
  112.6 2.9 %copy.70 = f32[1024,1,4,128]{0,3,2,1:T(8,128)} copy(f32[1024,1,4,128]{3,0,2,1:T(8,128)} %bitcast.180) | data formatting | bytes 4194304 | tf_op jit(solution)/shard_map/reshape | solution.py:236
  115.5 7.7 %fusion.27 = bf16[1024,1,4,128]{0,3,2,1:T(8,128)(2,1)S(1)} fusion(f32[1024,1,4,128]{0,3,2,1:T(8,128)} %copy.70, f32[4,1024]{1,0:T(4,128)S(1)} %fusion.79, f32[768,1024,4]{1,0,2:T(8,128)} %get-tuple-element.35, bf16[768,256]{1,0:T(8,128)(2,1)} %bitcast.31), kind=kOutput, calls=%fused_computation.35 | convolution fusion | flops 815792128 | bytes 15941632 | tf_op jit(solution)/shard_map/hgtc,chd->thgd/dot_general | solution.py:233
  123.3 4.4 %convolution_convert_fusion = bf16[1024,2048]{1,0:T(8,128)(2,1)} fusion(bf16[1024,512]{0,1:T(8,128)(2,1)S(1)} %bitcast.208, bf16[512,2048]{1,0:T(8,128)(2,1)S(1)} %copy-done), kind=kOutput, calls=%fused_computation.30 | convolution fusion | flops 2149580800 | bytes 7340032 | tf_op jit(solution)/shard_map/dot_general | solution.py:242
  127.6 4.8 %all-to-all-start.3 = ((bf16[4,256,2048]{2,1,0:T(8,128)(2,1)}), bf16[4,256,2048]{2,1,0:T(8,128)(2,1)}, u32[]{:S(2)}, u32[]{:S(2)}) async-start(bf16[4,256,2048]{2,1,0:T(8,128)(2,1)} %bitcast.181), calls=%async_computation.3 | async-start | bytes 8388608 | tf_op jit(solution)/shard_map/all_to_all | solution.py:57
  132.5 45.7 %all-to-all-done.3 = bf16[4,256,2048]{2,1,0:T(8,128)(2,1)} async-done(((bf16[4,256,2048]{2,1,0:T(8,128)(2,1)}), bf16[4,256,2048]{2,1,0:T(8,128)(2,1)}, u32[]{:S(2)}, u32[]{:S(2)}) %all-to-all-start.3) | async-done | bytes 4194336 | tf_op jit(solution)/shard_map/all_to_all | solution.py:57
  178.2 3.3 %convert_reduce_fusion = f32[256,2048]{1,0:T(8,128)S(1)} fusion(bf16[4,256,2048]{2,1,0:T(8,128)(2,1)} %all-to-all-done.3), kind=kLoop, calls=%fused_computation.17 | loop fusion | flops 3670016 | bytes 6291456 | tf_op jit(solution)/shard_map/reduce_sum | solution.py:58
  181.5 2.6 %fusion.29 = bf16[1,256,2048]{2,1,0:T(8,128)(2,1)} fusion(f32[256,2048]{1,0:T(8,128)S(1)} %convert_reduce_fusion, f32[2048]{0:T(1024)S(1)} %bitcast.200, bf16[1,1024,2048]{2,1,0:T(8,128)(2,1)} %param.15, s32[]{:T(128)S(6)} %select_n.33), kind=kLoop, calls=%fused_computation.38 | loop fusion | flops 2097152 | bytes 4202500 | tf_op jit(solution)/shard_map/convert_element_type | solution.py:247
  (91 shorter events, 33.0 us)
Async XLA Ops:
  0.0 123.3 %copy-start = (bf16[512,2048]{1,0:T(8,128)(2,1)S(1)}, bf16[512,2048]{1,0:T(8,128)(2,1)}, u32[]{:S(2)}) copy-start(bf16[512,2048]{1,0:T(8,128)(2,1)} %param.26) | copy-start | bytes 6291460
  0.0 19.4 %copy-start.6 = (bf16[1,24,2048]{2,1,0:T(8,128)(2,1)S(1)}, bf16[1,24,2048]{2,1,0:T(8,128)(2,1)}, u32[]{:S(2)}) copy-start(bf16[1,24,2048]{2,1,0:T(8,128)(2,1)} %param.16) | copy-start | bytes 294916
  0.0 38.3 %copy-start.17 = (f32[4]{0:T(128)S(1)}, f32[4]{0:T(128)}, u32[]{:S(2)}) copy-start(f32[4]{0:T(128)} %param.29) | copy-start | bytes 52
  4.7 28.6 %all-to-all-start = ((f32[32,5,512]{2,1,0:T(8,128)}), f32[32,5,512]{2,1,0:T(8,128)S(1)}, u32[]{:S(2)}, u32[]{:S(2)}) async-start(f32[32,5,512]{2,1,0:T(8,128)} %broadcast_in_dim.14), calls=%async_computation | async-start | bytes 1048576 | tf_op jit(solution)/shard_map/all_to_all | solution.py:17
  16.2 27.7 %copy-start.14 = (f32[2048]{0:T(1024)S(1)}, f32[2048]{0:T(1024)}, u32[]{:S(2)}) copy-start(f32[2048]{0:T(1024)} %param.19) | copy-start | bytes 24580
  19.3 24.9 %copy-start.10 = (bf16[2048,128]{1,0:T(8,128)(2,1)S(1)}, bf16[2048,128]{1,0:T(8,128)(2,1)}, u32[]{:S(2)}) copy-start(bf16[2048,128]{1,0:T(8,128)(2,1)} %param.24) | copy-start | bytes 1572868
  19.3 25.3 %copy-start.15 = (f32[128]{0:T(128)S(1)}, f32[128]{0:T(128)}, u32[]{:S(2)}) copy-start(f32[128]{0:T(128)} %param.28) | copy-start | bytes 1540
  33.3 10.6 %copy-start.11 = (bf16[2048,128]{1,0:T(8,128)(2,1)S(1)}, bf16[2048,128]{1,0:T(8,128)(2,1)}, u32[]{:S(2)}) copy-start(bf16[2048,128]{1,0:T(8,128)(2,1)} %param.25) | copy-start | bytes 1572868
  34.0 9.9 %all-to-all-start.1 = ((f32[4,5,512]{2,1,0:T(8,128)}), f32[4,5,512]{2,1,0:T(8,128)S(1)}, u32[]{:S(2)}, u32[]{:S(2)}) async-start(f32[4,5,512]{2,1,0:T(8,128)} %broadcast_in_dim.15), calls=%async_computation.1 | async-start | bytes 131072 | tf_op jit(solution)/shard_map/all_to_all | solution.py:17
  45.5 56.6 %all-to-all-start.2 = ((bf16[32,24,256]{2,1,0:T(8,128)(2,1)}), bf16[32,24,256]{2,1,0:T(8,128)(2,1)}, u32[]{:S(2)}, u32[]{:S(2)}) async-start(bf16[32,24,256]{2,1,0:T(8,128)(2,1)} %broadcast_in_dim.18), calls=%async_computation.2 | async-start | bytes 786432 | tf_op jit(solution)/shard_map/all_to_all | solution.py:17
  50.7 6.5 %copy-start.1 = (bf16[1,1024,2048]{2,1,0:T(8,128)(2,1)S(1)}, bf16[1,1024,2048]{2,1,0:T(8,128)(2,1)}, u32[]{:S(2)}) copy-start(bf16[1,1024,2048]{2,1,0:T(8,128)(2,1)} %param.15) | copy-start | bytes 12582916
  50.7 6.5 %copy-start.12 = (bf16[2048,128]{1,0:T(8,128)(2,1)S(1)}, bf16[2048,128]{1,0:T(8,128)(2,1)}, u32[]{:S(2)}) copy-start(bf16[2048,128]{1,0:T(8,128)(2,1)} %param.25) | copy-start | bytes 1572868
  57.3 10.7 %copy-start.3 = (bf16[512,2048]{1,0:T(8,128)(2,1)S(1)}, bf16[512,2048]{1,0:T(8,128)(2,1)}, u32[]{:S(2)}) copy-start(bf16[512,2048]{1,0:T(8,128)(2,1)} %copy.80) | copy-start | bytes 6291460
  59.8 27.1 %collective-permute-start = (bf16[128,256]{0,1:T(8,128)(2,1)}, bf16[128,256]{0,1:T(8,128)(2,1)}, u32[]{:S(2)}, u32[]{:S(2)}) collective-permute-start(bf16[128,256]{0,1:T(8,128)(2,1)} %get-tuple-element.13), channel_id=1, source_target_pairs={{0,8},{8,16},{16,24},{24,32},{32,40},{40,48},{48,56},{56,64},{64,7... | collective-permute-start | bytes 196616 | tf_op jit(solution)/shard_map/ppermute | solution.py:44
  63.2 23.8 %collective-permute-start.1 = (bf16[128,256]{0,1:T(8,128)(2,1)}, bf16[128,256]{0,1:T(8,128)(2,1)}, u32[]{:S(2)}, u32[]{:S(2)}) collective-permute-start(bf16[128,256]{0,1:T(8,128)(2,1)} %get-tuple-element.14), channel_id=1, source_target_pairs={{8,0},{16,8},{24,16},{32,24},{40,32},{48,40},{56,48},{64,56},{72,6... | collective-permute-start | bytes 196616 | tf_op jit(solution)/shard_map/ppermute | solution.py:45
  68.0 2.7 %copy-start.16 = (f32[128]{0:T(128)S(1)}, f32[128]{0:T(128)}, u32[]{:S(2)}) copy-start(f32[128]{0:T(128)} %param.27) | copy-start | bytes 1540
  70.6 1.0 copy-start.8
  70.6 1.0 copy-start.9
  93.5 1.2 copy-start.4
  94.7 7.4 %copy-start.2 = (bf16[1024,4,32]{0,2,1:T(8,128)(2,1)S(1)}, bf16[1024,4,32]{0,2,1:T(8,128)(2,1)}, u32[]{:S(2)}) copy-start(bf16[1024,4,32]{0,2,1:T(8,128)(2,1)} %get-tuple-element.10) | copy-start | bytes 786436
  102.1 7.0 %copy-start.5 = (bf16[8,384,256]{2,1,0:T(8,128)(2,1)S(1)}, bf16[8,384,256]{2,1,0:T(8,128)(2,1)}, u32[]{:S(2)}) copy-start(bf16[8,384,256]{2,1,0:T(8,128)(2,1)} %copy-done.4) | copy-start | bytes 4718596
  102.1 7.0 %copy-start.13 = (pred[8,128,384]{1,2,0:T(8,128)(4,1)S(1)}, pred[8,128,384]{1,2,0:T(8,128)(4,1)}, u32[]{:S(2)}) copy-start(pred[8,128,384]{1,2,0:T(8,128)(4,1)} %broadcast_and_fusion) | copy-start | bytes 1179652
  102.1 7.0 %copy-start.18 = (f32[8,384,128,4]{2,1,3,0:T(8,128)S(1)}, f32[8,384,128,4]{2,1,3,0:T(8,128)}, u32[]{:S(2)}) copy-start(f32[8,384,128,4]{2,1,3,0:T(8,128)} %get-tuple-element.31) | copy-start | bytes 18874372
  127.6 50.6 %all-to-all-start.3 = ((bf16[4,256,2048]{2,1,0:T(8,128)(2,1)}), bf16[4,256,2048]{2,1,0:T(8,128)(2,1)}, u32[]{:S(2)}, u32[]{:S(2)}) async-start(bf16[4,256,2048]{2,1,0:T(8,128)(2,1)} %bitcast.181), calls=%async_computation.3 | async-start | bytes 8388608 | tf_op jit(solution)/shard_map/all_to_all | solution.py:57
  (1 other events, 0.9 us)
where the time goes:
time: 185 us; the launch traced here: 184 us
  waiting for transfers between devices  58.1 us (31%)
  matrix products  40.6 us (22%)
  starting transfers between devices  33.9 us (18%)
  local copies, waits for them, and re-layouts  30.6 us (17%)
  other arithmetic  20.5 us (11%)
    all_to_all x1, waiting for transfers between devices, summed_on_arrival(): pieces = lax.all_to_all(split_up(array, dim, peers), axis, 0, 0, tiled=True)  45.7 us
    all_to_all x3, starting transfers between devices, from_everyone(): lax.all_to_all(jnp.broadcast_to(array[None], (peers, *array.shape)), axis...  20.9 us
    all_to_all x3, waiting for transfers between devices, from_everyone(): lax.all_to_all(jnp.broadcast_to(array[None], (peers, *array.shape)), axis...  12.4 us
    concatenate x4, local copies, waits for them, and re-layouts, rotate(): jnp.concatenate([rotate_half(vectors[..., :half_dim], positions // GRID_W...  9.27 us
    dot_general x1, matrix products, per_device(): jnp.einsum('hgtc,chd->thgd', ctx_probs, ctx_values, preferred_element_typ...  7.74 us
    dot_general x1, matrix products, per_device(): jnp.einsum('nqhgd,nkhd->hgnqk', query_blocks, window_keys, preferred_elem...  7.4 us
    dot_general x1, matrix products, per_device(): jnp.einsum('thgd,chd->hgtc', flat_queries, ctx_keys, preferred_element_ty...  6.85 us
    unnamed x42, local copies, waits for them, and re-layouts  5.73 us
  transfers between devices with their start and end apart: 6, of which 3 were waited for; matrix products, arithmetic and copies ran while one was open for 28% of the time, Pallas kernels for 0%

commit v1 on v0

v1 whole, which is shorter than its diff:
```python
import math

import jax
import jax.numpy as jnp
from jax import lax
from jax.experimental import pallas as pl
from jax.experimental.pallas import tpu as pltpu
from jax.sharding import Mesh, PartitionSpec as P

HEAD_DIM = 128
WINDOW = 128
GRID_W = 64
NORM_EPSILON = 1e-06
ROPE_BASE = 10000.0
D = 2048
ROWS = 24
NZ, NY, NX = 8, 4, 4
SP = ("z", "y")

F32 = jnp.float32
BF16 = jnp.bfloat16
QUERY_SCALE = HEAD_DIM ** (-0.5) * math.log2(math.e)


def sp_index():
    return lax.axis_index("z") * NY + lax.axis_index("y")


def params(vmem_mib=48):
    return pltpu.CompilerParams(vmem_limit_bytes=vmem_mib * 1024 * 1024)


def cost(flops, nbytes, trans=0):
    return pl.CostEstimate(flops=flops, bytes_accessed=nbytes, transcendentals=trans)


def partial_kernel(cond_ref, ctx_ref, shift_ref, scale_ref, gate_ref, out_ref):
    sp = sp_index()
    start = pl.multiple_of((sp // 2) * 128, 128)
    row = lax.broadcasted_iota(jnp.int32, (8, 128), 0)
    lane = lax.broadcasted_iota(jnp.int32, (8, 128), 1)
    rows = jnp.where(
        row == 0,
        cond_ref[:, pl.ds(start, 128)],
        jnp.where(row == 1, ctx_ref[:, pl.ds(start, 128)], 0.0),
    )
    active = rows / (1.0 + jnp.exp(-rows))
    active = jnp.where((lane // 64) == (sp % 2), active, 0.0).astype(BF16)

    def times(ref):
        matrix = ref[...]
        return jnp.dot(
            active, jnp.concatenate([matrix, matrix], axis=0), preferred_element_type=F32
        )

    shifts, scales, gates = times(shift_ref), times(scale_ref), times(gate_ref)
    pieces = []
    for values, at in ((shifts, 0), (scales, 0), (shifts, 1), (scales, 1), (gates, 0)):
        for i in range(4):
            pieces.append(values[at : at + 1, i * 128 : (i + 1) * 128])
    pieces.append(jnp.zeros((4, 128), F32))
    stacked = jnp.concatenate(pieces, axis=0).astype(BF16)
    out_ref[...] = jnp.broadcast_to(stacked[None], out_ref.shape)


def resum_kernel(in_ref, out_ref):
    total = jnp.sum(in_ref[...].astype(F32), axis=0).astype(BF16)
    out_ref[...] = jnp.broadcast_to(total[None], out_ref.shape)


def vectors_of(mod_ref, wanted):
    found = []
    for v in wanted:
        pieces = []
        for t in range(NX):
            rows = None
            for y in range(NY):
                part = mod_ref[y * NX + t].astype(F32)
                rows = part if rows is None else rows + part
            for i in range(4):
                pieces.append(rows[v * 4 + i : v * 4 + i + 1, :])
        found.append(jnp.concatenate(pieces, axis=1))
    return found


def modulated(rows, factor, shift):
    values = rows.astype(F32)
    inverse = lax.rsqrt(jnp.mean(values * values, axis=-1, keepdims=True) + NORM_EPSILON)
    return (values * inverse * factor + shift).astype(BF16)


def head_norm(v, gain):
    return v * lax.rsqrt(jnp.mean(v * v, axis=-1, keepdims=True) + NORM_EPSILON) * gain


def rotated(v, cosine, sine):
    lane = lax.broadcasted_iota(jnp.int32, v.shape, 1)
    odd = ((lane // 32) % 2) == 1
    swapped = jnp.where(odd, pltpu.roll(v, 32, 1), pltpu.roll(v, 96, 1))
    return v * cosine + swapped * sine


def edge_kernel(
    mod_ref, ctx_ref, first_ref, last_ref, wk_ref, wv_ref, gain_ref, kgain_ref,
    cosf_ref, sinf_ref, cosl_ref, sinl_ref, ctxkv_ref, firstkv_ref, lastkv_ref,
):
    shift_lat, scale_lat, shift_ctx, scale_ctx = vectors_of(mod_ref, (0, 1, 2, 3))
    gain = gain_ref[...]
    lat_factor = gain * (1.0 + scale_lat)
    ctx_factor = gain * (1.0 + scale_ctx)
    kgain = kgain_ref[...]
    wk, wv = wk_ref[...], wv_ref[...]
    rows = jnp.concatenate(
        [
            modulated(ctx_ref[...], ctx_factor, shift_ctx),
            modulated(first_ref[...], lat_factor, shift_lat),
            modulated(last_ref[...], lat_factor, shift_lat),
        ],
        axis=0,
    )
    keys = head_norm(jnp.dot(rows, wk, preferred_element_type=F32), kgain)
    values = jnp.dot(rows, wv, preferred_element_type=F32).astype(BF16)
    n = ctx_ref.shape[0]
    for y in range(NY):
        ctxkv_ref[y, :, :HEAD_DIM] = keys[:n].astype(BF16)
        ctxkv_ref[y, :, HEAD_DIM:] = values[:n]
    firstkv_ref[:, :HEAD_DIM] = rotated(keys[n : n + WINDOW], cosf_ref[...], sinf_ref[...]).astype(BF16)
    firstkv_ref[:, HEAD_DIM:] = values[n : n + WINDOW]
    lastkv_ref[:, :HEAD_DIM] = rotated(keys[n + WINDOW :], cosl_ref[...], sinl_ref[...]).astype(BF16)
    lastkv_ref[:, HEAD_DIM:] = values[n + WINDOW :]


def qkv_kernel(
    mod_ref, lat_ref, wq_ref, wk_ref, wv_ref, gain_ref, qgain_ref, kgain_ref,
    cos_ref, sin_ref, q_ref, k_ref, v_ref,
):
    shift_lat, scale_lat = vectors_of(mod_ref, (0, 1))
    rows = modulated(lat_ref[...], gain_ref[...] * (1.0 + scale_lat), shift_lat)
    cosine, sine = cos_ref[...], sin_ref[...]
    qgain = qgain_ref[...] * QUERY_SCALE
    queries = jnp.dot(rows, wq_ref[...], preferred_element_type=F32)
    for h in range(4):
        at = slice(h * HEAD_DIM, (h + 1) * HEAD_DIM)
        q_ref[:, at] = rotated(head_norm(queries[:, at], qgain), cosine, sine).astype(BF16)
    keys = jnp.dot(rows, wk_ref[...], preferred_element_type=F32)
    k_ref[...] = rotated(head_norm(keys, kgain_ref[...]), cosine, sine).astype(BF16)
    v_ref[...] = jnp.dot(rows, wv_ref[...], preferred_element_type=F32).astype(BF16)


def contract_last(a, b):
    return lax.dot_general(a, b, (((1,), (1,)), ((), ())), preferred_element_type=F32)


def attend_kernel(at_ref, q_ref, k_ref, v_ref, before_ref, after_ref, ctx_ref, sink_ref, out_ref):
    quarter, sp = at_ref[0], at_ref[1]
    head = HEAD_DIM
    first = pl.multiple_of(quarter * 256, 256)
    low = pl.multiple_of(jnp.maximum(first - WINDOW, 0), WINDOW)
    high = pl.multiple_of(jnp.minimum(first + 256, 1024 - WINDOW), WINDOW)
    is_first, is_last = quarter == 0, quarter == 3

    def window(ref, edge):
        before, after = before_ref[:, edge], after_ref[:, edge]
        return jnp.concatenate(
            [
                jnp.where(is_first, before, ref[pl.ds(low, WINDOW), :]),
                ref[pl.ds(first, 256), :],
                jnp.where(is_last, after, ref[pl.ds(high, WINDOW), :]),
            ],
            axis=0,
        )

    keys = window(k_ref, slice(0, head))
    values = window(v_ref, slice(head, 2 * head))
    ctx_keys = ctx_ref[:, :head]
    ctx_values = ctx_ref[:, head:]
    no_before = is_first & (sp == 0)
    no_after = is_last & (sp == NZ * NY - 1)
    query_at = lax.broadcasted_iota(jnp.int32, (4 * WINDOW, WINDOW), 0) % WINDOW
    key_at = lax.broadcasted_iota(jnp.int32, (4 * WINDOW, WINDOW), 1)
    in_before, in_after = key_at >= query_at, key_at <= query_at
    sink = jnp.concatenate(
        [jnp.exp(jnp.full((WINDOW, 1), sink_ref[0, h], F32)) for h in range(4)], axis=0
    )
    for block in range(2):
        rows = slice(block * WINDOW, (block + 1) * WINDOW)
        queries = jnp.concatenate(
            [q_ref[rows, h * head : (h + 1) * head] for h in range(4)], axis=0
        )
        near = slice(block * WINDOW, (block + 3) * WINDOW)
        local = jnp.exp2(contract_last(queries, keys[near]))
        allow_before, allow_after = in_before, in_after
        if block == 0:
            allow_before = in_before & jnp.logical_not(no_before)
        else:
            allow_after = in_after & jnp.logical_not(no_after)
        local = jnp.concatenate(
            [
                jnp.where(allow_before, local[:, :WINDOW], 0.0),
                local[:, WINDOW : 2 * WINDOW],
                jnp.where(allow_after, local[:, 2 * WINDOW :], 0.0),
            ],
            axis=1,
        )
        far = jnp.exp2(contract_last(queries, ctx_keys))
        total = (
            jnp.sum(local, axis=-1, keepdims=True) + jnp.sum(far, axis=-1, keepdims=True) + sink
        )
        mixed = jnp.dot(local.astype(BF16), values[near], preferred_element_type=F32) + jnp.dot(
            far.astype(BF16), ctx_values, preferred_element_type=F32
        )
        mixed = (mixed * (1.0 / total)).astype(BF16)
        for h in range(4):
            out_ref[rows, h * head : (h + 1) * head] = mixed[h * WINDOW : (h + 1) * WINDOW]


def out_kernel(
    at_ref, mod_ref, a0_ref, a1_ref, a2_ref, a3_ref, w0_ref,
    m1_ref, m2_ref, m3_ref, o1_ref, o2_ref, o3_ref, lat_ref, out_ref, gate_ref,
):
    part, sub = pl.program_id(0), pl.program_id(1)

    @pl.when((part == 0) & (sub == 0))
    def _():
        gate_ref[...] = jnp.broadcast_to(vectors_of(mod_ref, (4,))[0], gate_ref.shape)

    column = jnp.where(part == 0, at_ref[1], 1 - at_ref[1]) * 2 + sub
    own = jnp.dot(a0_ref[...], w0_ref[...], preferred_element_type=F32)
    gate = gate_ref[0:1, pl.ds(pl.multiple_of(column * 512, 512), 512)]

    def finish(w1, w2, w3):
        mixed = own
        for a, w in ((a1_ref, w1), (a2_ref, w2), (a3_ref, w3)):
            mixed = mixed + jnp.dot(a[...], w[...], preferred_element_type=F32)
        out_ref[...] = (lat_ref[...].astype(F32) + gate * mixed).astype(BF16)

    @pl.when(part == 0)
    def _():
        finish(m1_ref, m2_ref, m3_ref)

    @pl.when(part == 1)
    def _():
        finish(o1_ref, o2_ref, o3_ref)


def copies(array, axis):
    peers = lax.axis_size(axis)
    return lax.all_to_all(
        jnp.broadcast_to(array[None], (peers, *array.shape)), axis, 0, 0, tiled=True
    )


def shifted(array, axis, by):
    peers = lax.axis_size(axis)
    return lax.ppermute(array, axis, [(i, (i + by) % peers) for i in range(peers)])


def full(shape):
    return pl.BlockSpec(shape, lambda *_: (0,) * len(shape))


def per_device(
    latent, context, cond, ctx_cond, norm_gain, mod_shift, mod_scale, mod_gate,
    w_query, w_key, w_value, w_out, q_gain, k_gain, sinks,
):
    lat = latent[0]
    tok = lat.shape[0]
    sp = sp_index()
    tp = lax.axis_index("tp")
    dp = lax.axis_index("dp")

    partial = pl.pallas_call(
        partial_kernel,
        out_shape=jax.ShapeDtypeStruct((NZ, ROWS, 128), BF16),
        cost_estimate=cost(3 * 2 * 128 * 512 * 8, 3 * 64 * 512 * 2),
        name="partial",
    )(cond, ctx_cond[None], mod_shift, mod_scale, mod_gate)
    over_z = lax.all_to_all(partial, "z", 0, 0, tiled=True)
    resummed = pl.pallas_call(
        resum_kernel,
        out_shape=jax.ShapeDtypeStruct((NY * NX, ROWS, 128), BF16),
        name="resum",
    )(over_z)
    mod = lax.all_to_all(resummed, ("y", "tp"), 0, 0, tiled=True)

    ctx_rows = copies(context[0], "z").reshape(-1, D)
    n_ctx = ctx_rows.shape[0]

    half = lax.dynamic_slice_in_dim(w_out, dp * (D // 2), D // 2, 1)
    mine = [shifted(half, "tp", s) for s in (1, 2, 3)]
    other = [shifted(w, "dp", 1) for w in mine]

    positions = sp * tok + jnp.arange(tok, dtype=jnp.int32)
    quarter = HEAD_DIM // 4
    frequency = ROPE_BASE ** (-jnp.arange(quarter, dtype=F32) / quarter)
    by_row = (positions // GRID_W).astype(F32)[:, None] * frequency
    by_col = (positions % GRID_W).astype(F32)[:, None] * frequency
    angles = jnp.concatenate([by_row, by_row, by_col, by_col], axis=1)
    signs = jnp.where((jnp.arange(HEAD_DIM) // quarter) % 2 == 0, -1.0, 1.0).astype(F32)
    cosine, sine = jnp.cos(angles), jnp.sin(angles) * signs

    gain, qgain, kgain = norm_gain[None], q_gain[None], k_gain[None]
    edge_last = tok // WINDOW - 1
    kv_piece = jax.ShapeDtypeStruct((WINDOW, 2 * HEAD_DIM), BF16)
    table_first = pl.BlockSpec((WINDOW, HEAD_DIM), lambda i: (0, 0))
    table_last = pl.BlockSpec((WINDOW, HEAD_DIM), lambda i: (edge_last, 0))
    ctx_kv, first_kv, last_kv = pl.pallas_call(
        edge_kernel,
        grid=(1,),
        in_specs=[
            full((NY * NX, ROWS, 128)), full((n_ctx, D)),
            pl.BlockSpec((WINDOW, D), lambda i: (0, 0)),
            pl.BlockSpec((WINDOW, D), lambda i: (edge_last, 0)),
            full((D, HEAD_DIM)), full((D, HEAD_DIM)), full((1, D)), full((1, HEAD_DIM)),
            table_first, table_first, table_last, table_last,
        ],
        out_specs=[
            full((NY, n_ctx, 2 * HEAD_DIM)), full((WINDOW, 2 * HEAD_DIM)),
            full((WINDOW, 2 * HEAD_DIM)),
        ],
        out_shape=[
            jax.ShapeDtypeStruct((NY, n_ctx, 2 * HEAD_DIM), BF16), kv_piece, kv_piece,
        ],
        compiler_params=params(),
        cost_estimate=cost(2 * (n_ctx + 256) * D * 256, (n_ctx + 256) * D * 2 + D * 512),
        name="edge",
    )(mod, ctx_rows, lat, lat, w_key, w_value, gain, kgain, cosine, sine, cosine, sine)
    ctx_all = lax.all_to_all(ctx_kv, "y", 0, 0, tiled=True).reshape(-1, 2 * HEAD_DIM)
    peers = NZ * NY
    up = [(i, i + 1) for i in range(peers - 1)]
    before = lax.ppermute(last_kv, SP, up)
    after = lax.ppermute(first_kv, SP, [(j, i) for i, j in up])

    block = 256
    queries, keys, values = pl.pallas_call(
        qkv_kernel,
        grid=(tok // block,),
        in_specs=[
            full((NY * NX, ROWS, 128)),
            pl.BlockSpec((block, D), lambda i: (i, 0)),
            full((D, 4 * HEAD_DIM)), full((D, HEAD_DIM)), full((D, HEAD_DIM)),
            full((1, D)), full((1, HEAD_DIM)), full((1, HEAD_DIM)),
            pl.BlockSpec((block, HEAD_DIM), lambda i: (i, 0)),
            pl.BlockSpec((block, HEAD_DIM), lambda i: (i, 0)),
        ],
        out_specs=[
            pl.BlockSpec((block, 4 * HEAD_DIM), lambda i: (i, 0)),
            pl.BlockSpec((block, HEAD_DIM), lambda i: (i, 0)),
            pl.BlockSpec((block, HEAD_DIM), lambda i: (i, 0)),
        ],
        out_shape=[
            jax.ShapeDtypeStruct((tok, 4 * HEAD_DIM), BF16),
            jax.ShapeDtypeStruct((tok, HEAD_DIM), BF16),
            jax.ShapeDtypeStruct((tok, HEAD_DIM), BF16),
        ],
        compiler_params=params(),
        cost_estimate=cost(2 * tok * D * 768, tok * D * 2 + D * 768 * 2),
        name="qkv",
    )(mod, lat, w_query, w_key, w_value, gain, qgain, kgain, cosine, sine)

    sub = tok // NX
    pieces = []
    for s in (2, 1, 3, 0):
        to = (tp + s) % NX
        piece = pl.pallas_call(
            attend_kernel,
            grid_spec=pltpu.PrefetchScalarGridSpec(
                num_scalar_prefetch=1,
                grid=(1,),
                in_specs=[
                    pl.BlockSpec((sub, 4 * HEAD_DIM), lambda i, at: (at[0], 0)),
                    full((tok, HEAD_DIM)), full((tok, HEAD_DIM)),
                    full((WINDOW, 2 * HEAD_DIM)), full((WINDOW, 2 * HEAD_DIM)),
                    full((NY * n_ctx, 2 * HEAD_DIM)),
                    pl.BlockSpec(memory_space=pltpu.SMEM),
                ],
                out_specs=full((sub, 4 * HEAD_DIM)),
            ),
            out_shape=jax.ShapeDtypeStruct((sub, 4 * HEAD_DIM), BF16),
            compiler_params=params(),
            cost_estimate=cost(4 * 4 * sub * 1152 * HEAD_DIM, 2 << 20, 4 * sub * 1152),
            name=f"attend{s}",
        )(
            jnp.stack([to, sp]).astype(jnp.int32), queries, keys, values,
            before, after, ctx_all, sinks[None],
        )
        pieces.append((s, piece if s == 0 else shifted(piece, "tp", s)))
    arrived = dict(pieces)

    col = 512
    wide = pl.BlockSpec((sub, 4 * HEAD_DIM), lambda p, j, at: (0, 0))
    from_mine = pl.BlockSpec((4 * HEAD_DIM, col), lambda p, j, at: (0, jnp.where(p == 0, j, 1)))
    from_other = pl.BlockSpec((4 * HEAD_DIM, col), lambda p, j, at: (0, jnp.where(p == 0, 0, j)))

    def column(p, j, at):
        return jnp.where(p == 0, at[1], 1 - at[1]) * 2 + j

    result = pl.pallas_call(
        out_kernel,
        grid_spec=pltpu.PrefetchScalarGridSpec(
            num_scalar_prefetch=1,
            grid=(2, 2),
            in_specs=[
                full((NY * NX, ROWS, 128)), wide, wide, wide, wide,
                pl.BlockSpec((4 * HEAD_DIM, col), lambda p, j, at: (0, column(p, j, at))),
                from_mine, from_mine, from_mine, from_other, from_other, from_other,
                pl.BlockSpec((sub, col), lambda p, j, at: (at[0], column(p, j, at))),
            ],
            out_specs=pl.BlockSpec((sub, col), lambda p, j, at: (0, column(p, j, at))),
            scratch_shapes=[pltpu.VMEM((8, D), F32)],
        ),
        out_shape=jax.ShapeDtypeStruct((sub, D), BF16),
        compiler_params=params(),
        cost_estimate=cost(2 * sub * D * D, D * D * 2),
        name="project",
    )(
        jnp.stack([tp, dp]).astype(jnp.int32), mod, arrived[0], arrived[1], arrived[2],
        arrived[3], w_out, *mine, *other, lat,
    )
    return result[None]


def solution(mesh):
    grid = Mesh(mesh.devices.reshape(NZ, NY, NX, 2), ("z", "y", "tp", "dp"))
    in_specs = (
        P("dp", SP, None),
        P("dp", SP, None),
        P("dp", None),
        P(),
        P(),
        P(SP, "tp"),
        P(SP, "tp"),
        P(SP, "tp"),
        P(None, "tp"),
        P(None, "tp"),
        P(None, "tp"),
        P("tp", None),
        P(),
        P(),
        P("tp"),
    )
    out_specs = P("dp", ("z", "y", "tp"), None)
    return jax.shard_map(
        per_device, mesh=grid, in_specs=in_specs, out_specs=out_specs, check_vma=False
    )
```

time: 185 us -> 149 us (0.81)
  matrix products: 40.6 us -> 0 us
  Pallas kernels: 0 us -> 33.9 us
  blocking collectives: 0 us -> 30.3 us
  local copies, waits for them, and re-layouts: 30.6 us -> 7.37 us
  other arithmetic: 20.5 us -> 3.04 us
  starting transfers between devices: 33.9 us -> 21.8 us
  waiting for transfers between devices: 58.1 us -> 51.8 us
    all_to_all x4 -> x2, waiting for transfers between devices: 58.1 us -> 0.01 us  [the longest x1 0.01 us: copies(): lax.all_to_all(jnp.broadcast_to(array[None], (peers, *array.shape)), axis...]
    ppermute x2 -> x11, waiting for transfers between devices: 0.01 us -> 51.8 us  [the longest x9 51.8 us: shifted(): lax.ppermute(array, axis, [(i, (i + by) % peers) for i in range(peers)])]
    dot_general x13 -> x0, matrix products: 40.6 us -> none  [the longest x1 7.74 us: per_device(): jnp.einsum('hgtc,chd->thgd', ctx_probs, ctx_values, preferred_element_typ...]
    pallas_call x0 -> x9, Pallas kernels: none -> 33.9 us  [the longest x4 12.3 us: per_device(): pl.pallas_call(attend_kernel, grid_spec=pltpu.PrefetchScalarGridSpec(num_...]
    all_to_all x0 -> x2, blocking collectives: none -> 30.3 us  [the longest x1 15.4 us: per_device(): over_z = lax.all_to_all(partial, 'z', 0, 0, tiled=True)]
    all_to_all x4 -> x2, starting transfers between devices: 25.7 us -> 8.37 us  [the longest x1 4.91 us: copies(): lax.all_to_all(jnp.broadcast_to(array[None], (peers, *array.shape)), axis...]
    concatenate x4 -> x0, local copies, waits for them, and re-layouts: 9.27 us -> none  [rotate(): jnp.concatenate([rotate_half(vectors[..., :half_dim], positions // GRID_W...]
    reduce_sum x4 -> x0, other arithmetic: 6.53 us -> none  [the longest x1 3.25 us: summed_on_arrival(): return jnp.sum(pieces.astype(jnp.float32), axis=0)]
  transfers between devices with their start and end apart: 6 -> 13, of which waited for: 3 -> 5; matrix products, arithmetic and copies ran while one was open for 28% -> 3% of each run, Pallas kernels for 0% -> 15%
where the time goes in v1:
time: 149 us; the launch traced here: 148 us
  waiting for transfers between devices  51.8 us (35%)
  Pallas kernels  33.9 us (23%)
  blocking collectives  30.3 us (20%)
  starting transfers between devices  21.8 us (15%)
  local copies, waits for them, and re-layouts  7.37 us (5%)
  other arithmetic  3.04 us (2%)
    ppermute x9, waiting for transfers between devices, shifted(): lax.ppermute(array, axis, [(i, (i + by) % peers) for i in range(peers)])  51.8 us
    all_to_all x1, blocking collectives, per_device(): over_z = lax.all_to_all(partial, 'z', 0, 0, tiled=True)  15.4 us
    all_to_all x1, blocking collectives, per_device(): mod = lax.all_to_all(resummed, ('y', 'tp'), 0, 0, tiled=True)  14.8 us
    pallas_call x4, Pallas kernels, per_device(): pl.pallas_call(attend_kernel, grid_spec=pltpu.PrefetchScalarGridSpec(num_...  12.3 us
    pallas_call x1, Pallas kernels, per_device(): pl.pallas_call(out_kernel, grid_spec=pltpu.PrefetchScalarGridSpec(num_sca...  7.89 us
    pallas_call x1, Pallas kernels, per_device(): pl.pallas_call(qkv_kernel, grid=(tok // block,), in_specs=[full((NY * NX,...  7.52 us
    ppermute x9, starting transfers between devices, shifted(): lax.ppermute(array, axis, [(i, (i + by) % peers) for i in range(peers)])  5.44 us
    all_to_all x1, starting transfers between devices, copies(): lax.all_to_all(jnp.broadcast_to(array[None], (peers, *array.shape)), axis...  4.91 us
  transfers between devices with their start and end apart: 13, of which 5 were waited for; matrix products, arithmetic and copies ran while one was open for 3% of the time, Pallas kernels for 15%

profile of v1, /device:TPU:32, one launch (start us, length us, event | category | flops | bytes accessed | tf_op | source)
XLA Modules:
  0.0 148.3 jit_solution(9626450934616235954)
XLA Ops:
  0.0 1.9 %partial.1 = bf16[8,24,128]{2,1,0:T(8,128)(2,1)} custom-call(f32[1,2048]{1,0:T(1,128)} %cond_ref.1, f32[1,2048]{1,0:T(1,128)} %bitcast.36, bf16[64,512]{1,0:T(8,128)(2,1)} %shift_ref.1, bf16[64,512]{1,0:T(8,128)(2,1)} %scale_ref.1, bf16[64,512]{1,0:T(8,128)(2,1)} %gate_ref.1), custom_call_target="tpu_custom_call" | custom-call | flops 3145728 | bytes 196608 | tf_op jit(solution)/shard_map/partial/pallas_call | solution.py:272
  1.9 15.4 %all_to_all.20.in_ref = bf16[8,24,128]{2,1,0:T(8,128)(2,1)} all-to-all(bf16[8,24,128]{2,1,0:T(8,128)(2,1)} %partial.1), channel_id=1, replica_groups=mesh['z'=8,'y'=4,'tp'=4,'dp'=2] {'z'}, dimensions={0} | all-to-all | bytes 98304 | tf_op jit(solution)/shard_map/all_to_all | solution.py:278
  18.8 14.8 %all_to_all.21.mod_ref = bf16[16,24,128]{2,1,0:T(8,128)(2,1)S(1)} all-to-all(bf16[16,24,128]{2,1,0:T(8,128)(2,1)} %resum.1), channel_id=1, replica_groups=mesh['z'=8,'y'=4,'tp'=4,'dp'=2] {'y','tp'}, dimensions={0} | all-to-all | bytes 196608 | tf_op jit(solution)/shard_map/all_to_all | solution.py:284
  33.6 1.9 %broadcast_in_dim.48 = bf16[8,24,2048]{2,1,0:T(8,128)(2,1)} broadcast(bf16[24,2048]{1,0:T(8,128)(2,1)} %bitcast.35), dimensions={1,2} | broadcast | bytes 884736 | tf_op jit(solution)/shard_map/broadcast_in_dim | solution.py:249
  35.5 4.9 %all-to-all-start.2 = ((bf16[8,24,2048]{2,1,0:T(8,128)(2,1)}), bf16[8,24,2048]{2,1,0:T(8,128)(2,1)S(1)}, u32[]{:S(2)}, u32[]{:S(2)}) async-start(bf16[8,24,2048]{2,1,0:T(8,128)(2,1)} %broadcast_in_dim.48), calls=%async_computation.2 | async-start | bytes 1572864 | tf_op jit(solution)/shard_map/all_to_all | solution.py:248
  42.6 1.6 %collective-permute-start.6 = (bf16[512,1024]{1,0:T(8,128)(2,1)}, bf16[512,1024]{1,0:T(8,128)(2,1)}, u32[]{:S(2)}, u32[]{:S(2)}) collective-permute-start(bf16[512,1024]{1,0:T(8,128)(2,1)} %constant_dynamic-slice_fusion), channel_id=1, source_target_pairs={{0,4},{2,6},{4,0},{6,2},{1,5},{3,7},{5,1},{7,3},{8,12},{10,14},{12... | collective-permute-start | bytes 3145736 | tf_op jit(solution)/shard_map/ppermute | solution.py:255
  44.6 2.3 %sine_multiply_fusion = (f32[1024,128]{1,0:T(8,128)S(1)}, f32[1024,128]{1,0:T(8,128)S(1)}) fusion(f32[128]{0:T(128)S(1)} %compare_select_fusion.2, f32[1024,32]{1,0:T(8,128)S(1)} %get-tuple-element.20, f32[1024,32]{1,0:T(8,128)S(1)} %get-tuple-element.19), kind=kLoop, calls=%fused_computation.1 | loop fusion | flops 524288 | bytes 1311232 | tf_op jit(solution)/shard_map/mul | solution.py:300
  46.9 21.0 %collective-permute-done.7.m3_ref = bf16[512,1024]{1,0:T(8,128)(2,1)} collective-permute-done((bf16[512,1024]{1,0:T(8,128)(2,1)}, bf16[512,1024]{1,0:T(8,128)(2,1)}, u32[]{:S(2)}, u32[]{:S(2)}) %collective-permute-start.7) | collective-permute-done | bytes 1048608 | tf_op jit(solution)/shard_map/ppermute | solution.py:255
  67.9 2.6 %collective-permute-done.6.m2_ref = bf16[512,1024]{1,0:T(8,128)(2,1)} collective-permute-done((bf16[512,1024]{1,0:T(8,128)(2,1)}, bf16[512,1024]{1,0:T(8,128)(2,1)}, u32[]{:S(2)}, u32[]{:S(2)}) %collective-permute-start.6) | collective-permute-done | bytes 1048608 | tf_op jit(solution)/shard_map/ppermute | solution.py:255
  70.5 17.9 %collective-permute-done.5.m1_ref = bf16[512,1024]{1,0:T(8,128)(2,1)} collective-permute-done((bf16[512,1024]{1,0:T(8,128)(2,1)}, bf16[512,1024]{1,0:T(8,128)(2,1)}, u32[]{:S(2)}, u32[]{:S(2)}) %collective-permute-start.5) | collective-permute-done | bytes 1048608 | tf_op jit(solution)/shard_map/ppermute | solution.py:255
  88.5 2.9 %edge.1 = (bf16[4,192,256]{2,1,0:T(8,128)(2,1)S(1)}, bf16[128,256]{1,0:T(8,128)(2,1)S(1)}, bf16[128,256]{1,0:T(8,128)(2,1)S(1)}) custom-call(bf16[16,24,128]{2,1,0:T(8,128)(2,1)S(1)} %all_to_all.21.mod_ref, bf16[192,2048]{1,0:T(8,128)(2,1)S(1)} %bitcast.21, bf16[1024,2048]{1,0:T(8,128)(2,1)} %bitcast.31, bf16[1024,2048]{1,0:T(8,128)(2,1)} %bitcast.32, ...), custom_call_target="tpu_custom_call" | custom-call | flops 469762048 | bytes 2883584 | tf_op jit(solution)/shard_map/edge/pallas_call | solution.py:307
  92.1 3.5 %all-to-all-start.3 = ((bf16[4,192,256]{2,1,0:T(8,128)(2,1)}), bf16[4,192,256]{2,1,0:T(8,128)(2,1)S(1)}, u32[]{:S(2)}, u32[]{:S(2)}) async-start(bf16[4,192,256]{2,1,0:T(8,128)(2,1)} %copy-done.4), calls=%async_computation.3 | async-start | bytes 786432 | tf_op jit(solution)/shard_map/all_to_all | solution.py:328
  95.6 3.9 %collective-permute-start = (bf16[128,256]{1,0:T(8,128)(2,1)S(1)}, bf16[128,256]{1,0:T(8,128)(2,1)S(1)}, u32[]{:S(2)}, u32[]{:S(2)}) collective-permute-start(bf16[128,256]{1,0:T(8,128)(2,1)S(1)} %get-tuple-element.14), channel_id=1, source_target_pairs={{0,8},{8,16},{16,24},{24,32},{32,40},{40,48},{48,56},{56,64},{64,7... | collective-permute-start | bytes 196616 | tf_op jit(solution)/shard_map/ppermute | solution.py:331
  99.5 4.1 %collective-permute-start.1 = (bf16[128,256]{1,0:T(8,128)(2,1)S(1)}, bf16[128,256]{1,0:T(8,128)(2,1)S(1)}, u32[]{:S(2)}, u32[]{:S(2)}) collective-permute-start(bf16[128,256]{1,0:T(8,128)(2,1)S(1)} %get-tuple-element.15), channel_id=1, source_target_pairs={{8,0},{16,8},{24,16},{32,24},{40,32},{48,40},{56,48},{64,56},{72,6... | collective-permute-start | bytes 196616 | tf_op jit(solution)/shard_map/ppermute | solution.py:332
  105.7 1.6 %copy-done.8 = bf16[2048,512]{1,0:T(8,128)(2,1)S(1)} copy-done((bf16[2048,512]{1,0:T(8,128)(2,1)S(1)}, bf16[2048,512]{1,0:T(8,128)(2,1)}, u32[]{:S(2)}) %copy-start.8) | copy-done | bytes 2097176
  107.3 7.5 %qkv.1 = (bf16[1024,512]{1,0:T(8,128)(2,1)S(1)}, bf16[1024,128]{1,0:T(8,128)(2,1)S(1)}, bf16[1024,128]{1,0:T(8,128)(2,1)S(1)}) custom-call(bf16[16,24,128]{2,1,0:T(8,128)(2,1)S(1)} %all_to_all.21.mod_ref, bf16[1024,2048]{1,0:T(8,128)(2,1)} %bitcast.33, bf16[2048,512]{1,0:T(8,128)(2,1)S(1)} %copy-done.8, bf16[2048,128]{1,0:T(8,128)(2,1)S(1)} %copy-done.1, ...), custom_call_target="tpu_custom_call" | custom-call | flops 3221225472 | bytes 7340032 | tf_op jit(solution)/shard_map/qkv/pallas_call | solution.py:335
  114.8 3.1 %attend1.1 = bf16[256,512]{1,0:T(8,128)(2,1)S(1)} custom-call(s32[2]{0:T(128)S(1)} %pad_add_fusion.2.at_ref, bf16[1024,512]{1,0:T(8,128)(2,1)S(1)} %get-tuple-element.11.q_ref, bf16[1024,128]{1,0:T(8,128)(2,1)S(1)} %get-tuple-element.12.k_ref, bf16[1024,128]{1,0:T(8,128)(2,1)S(1)} %get-tuple-element.13.v_ref, ...), custom_call_target="tpu_custom_call" | custom-call | flops 603979776 | bytes 2097152 | tf_op jit(solution)/shard_map/attend1/pallas_call | solution.py:365
  118.4 3.1 %attend2.1 = bf16[256,512]{1,0:T(8,128)(2,1)S(1)} custom-call(s32[2]{0:T(128)S(1)} %pad_add_fusion.3.at_ref, bf16[1024,512]{1,0:T(8,128)(2,1)S(1)} %get-tuple-element.11.q_ref, bf16[1024,128]{1,0:T(8,128)(2,1)S(1)} %get-tuple-element.12.k_ref, bf16[1024,128]{1,0:T(8,128)(2,1)S(1)} %get-tuple-element.13.v_ref, ...), custom_call_target="tpu_custom_call" | custom-call | flops 603979776 | bytes 2097152 | tf_op jit(solution)/shard_map/attend2/pallas_call | solution.py:365
  121.4 2.4 %collective-permute-start.3 = (bf16[256,512]{1,0:T(8,128)(2,1)S(1)}, bf16[256,512]{1,0:T(8,128)(2,1)S(1)}, u32[]{:S(2)}, u32[]{:S(2)}) collective-permute-start(bf16[256,512]{1,0:T(8,128)(2,1)S(1)} %attend2.1), channel_id=1, source_target_pairs={{0,4},{2,6},{4,0},{6,2},{1,5},{3,7},{5,1},{7,3},{8,12},{10,14},{12... | collective-permute-start | bytes 786440 | tf_op jit(solution)/shard_map/ppermute | solution.py:255
  123.8 3.1 %attend3.1 = bf16[256,512]{1,0:T(8,128)(2,1)S(1)} custom-call(s32[2]{0:T(128)S(1)} %pad_add_fusion.4.at_ref, bf16[1024,512]{1,0:T(8,128)(2,1)S(1)} %get-tuple-element.11.q_ref, bf16[1024,128]{1,0:T(8,128)(2,1)S(1)} %get-tuple-element.12.k_ref, bf16[1024,128]{1,0:T(8,128)(2,1)S(1)} %get-tuple-element.13.v_ref, ...), custom_call_target="tpu_custom_call" | custom-call | flops 603979776 | bytes 2097152 | tf_op jit(solution)/shard_map/attend3/pallas_call | solution.py:365
  126.8 6.3 %collective-permute-done.2.a1_ref = bf16[256,512]{1,0:T(8,128)(2,1)S(1)} collective-permute-done((bf16[256,512]{1,0:T(8,128)(2,1)S(1)}, bf16[256,512]{1,0:T(8,128)(2,1)S(1)}, u32[]{:S(2)}, u32[]{:S(2)}) %collective-permute-start.2) | collective-permute-done | bytes 262176 | tf_op jit(solution)/shard_map/ppermute | solution.py:255
  133.3 3.1 %attend0.1.a0_ref = bf16[256,512]{1,0:T(8,128)(2,1)S(1)} custom-call(s32[2]{0:T(128)S(1)} %pad_add_fusion.1.at_ref, bf16[1024,512]{1,0:T(8,128)(2,1)S(1)} %get-tuple-element.11.q_ref, bf16[1024,128]{1,0:T(8,128)(2,1)S(1)} %get-tuple-element.12.k_ref, bf16[1024,128]{1,0:T(8,128)(2,1)S(1)} %get-tuple-element.13.v_ref, ...), custom_call_target="tpu_custom_call" | custom-call | flops 603979776 | bytes 2097152 | tf_op jit(solution)/shard_map/attend0/pallas_call | solution.py:365
  136.3 4.1 %collective-permute-done.4.a3_ref = bf16[256,512]{1,0:T(8,128)(2,1)S(1)} collective-permute-done((bf16[256,512]{1,0:T(8,128)(2,1)S(1)}, bf16[256,512]{1,0:T(8,128)(2,1)S(1)}, u32[]{:S(2)}, u32[]{:S(2)}) %collective-permute-start.4) | collective-permute-done | bytes 262176 | tf_op jit(solution)/shard_map/ppermute | solution.py:255
  140.4 7.9 %project.1 = bf16[256,2048]{1,0:T(8,128)(2,1)} custom-call(s32[2]{0:T(128)S(1)} %pad_add_fusion.at_ref, bf16[16,24,128]{2,1,0:T(8,128)(2,1)S(1)} %all_to_all.21.mod_ref, bf16[256,512]{1,0:T(8,128)(2,1)S(1)} %attend0.1.a0_ref, bf16[256,512]{1,0:T(8,128)(2,1)S(1)} %collective-permute-done.2.a1_ref, bf16[256,512]{1,0:T(8,128)(2,1)S(1)} %collective-permute-done.3.a2_ref, ...), custom_call_target="tpu_custom_call" | custom-call | flops 2147483648 | bytes 8388608 | tf_op jit(solution)/shard_map/project/pallas_call | solution.py:398
  (47 shorter events, 7.6 us)
Async XLA Ops:
  0.0 40.4 %copy-start.10 = (bf16[512,2048]{1,0:T(8,128)(2,1)S(1)}, bf16[512,2048]{1,0:T(8,128)(2,1)}, u32[]{:S(2)}) copy-start(bf16[512,2048]{1,0:T(8,128)(2,1)} %w0_ref.1) | copy-start | bytes 6291460
  35.5 53.0 %all-to-all-start.2 = ((bf16[8,24,2048]{2,1,0:T(8,128)(2,1)}), bf16[8,24,2048]{2,1,0:T(8,128)(2,1)S(1)}, u32[]{:S(2)}, u32[]{:S(2)}) async-start(bf16[8,24,2048]{2,1,0:T(8,128)(2,1)} %broadcast_in_dim.48), calls=%async_computation.2 | async-start | bytes 1572864 | tf_op jit(solution)/shard_map/all_to_all | solution.py:248
  41.5 47.0 %copy-start = (bf16[2048,128]{1,0:T(8,128)(2,1)S(1)}, bf16[2048,128]{1,0:T(8,128)(2,1)}, u32[]{:S(2)}) copy-start(bf16[2048,128]{1,0:T(8,128)(2,1)} %wk_ref.3) | copy-start | bytes 1572868
  41.5 47.0 %copy-start.2 = (bf16[2048,128]{1,0:T(8,128)(2,1)S(1)}, bf16[2048,128]{1,0:T(8,128)(2,1)}, u32[]{:S(2)}) copy-start(bf16[2048,128]{1,0:T(8,128)(2,1)} %wv_ref.3) | copy-start | bytes 1572868
  41.5 47.0 %copy-start.5 = (f32[2048]{0:T(1024)S(1)}, f32[2048]{0:T(1024)}, u32[]{:S(2)}) copy-start(f32[2048]{0:T(1024)} %param.19) | copy-start | bytes 24580
  41.5 47.0 %copy-start.7 = (f32[128]{0:T(128)S(1)}, f32[128]{0:T(128)}, u32[]{:S(2)}) copy-start(f32[128]{0:T(128)} %param.28) | copy-start | bytes 1540
  41.5 26.4 %collective-permute-start.7 = (bf16[512,1024]{1,0:T(8,128)(2,1)}, bf16[512,1024]{1,0:T(8,128)(2,1)}, u32[]{:S(2)}, u32[]{:S(2)}) collective-permute-start(bf16[512,1024]{1,0:T(8,128)(2,1)} %constant_dynamic-slice_fusion), channel_id=1, source_target_pairs={{0,6},{2,0},{4,2},{6,4},{1,7},{3,1},{5,3},{7,5},{8,14},{10,8},{12,... | collective-permute-start | bytes 3145736 | tf_op jit(solution)/shard_map/ppermute | solution.py:255
  42.6 27.9 %collective-permute-start.6 = (bf16[512,1024]{1,0:T(8,128)(2,1)}, bf16[512,1024]{1,0:T(8,128)(2,1)}, u32[]{:S(2)}, u32[]{:S(2)}) collective-permute-start(bf16[512,1024]{1,0:T(8,128)(2,1)} %constant_dynamic-slice_fusion), channel_id=1, source_target_pairs={{0,4},{2,6},{4,0},{6,2},{1,5},{3,7},{5,1},{7,3},{8,12},{10,14},{12... | collective-permute-start | bytes 3145736 | tf_op jit(solution)/shard_map/ppermute | solution.py:255
  44.2 44.2 %collective-permute-start.5 = (bf16[512,1024]{1,0:T(8,128)(2,1)}, bf16[512,1024]{1,0:T(8,128)(2,1)}, u32[]{:S(2)}, u32[]{:S(2)}) collective-permute-start(bf16[512,1024]{1,0:T(8,128)(2,1)} %constant_dynamic-slice_fusion), channel_id=1, source_target_pairs={{0,2},{2,4},{4,6},{6,0},{1,3},{3,5},{5,7},{7,1},{8,10},{10,12},{12... | collective-permute-start | bytes 3145736 | tf_op jit(solution)/shard_map/ppermute | solution.py:255
  67.9 72.5 %collective-permute-start.10 = (bf16[512,1024]{1,0:T(8,128)(2,1)}, bf16[512,1024]{1,0:T(8,128)(2,1)}, u32[]{:S(2)}, u32[]{:S(2)}) collective-permute-start(bf16[512,1024]{1,0:T(8,128)(2,1)} %collective-permute-done.7.m3_ref), channel_id=1, source_target_pairs={{0,1},{1,0},{2,3},{3,2},{4,5},{5,4},{6,7},{7,6},{8,9},{9,8},{10,11... | collective-permute-start | bytes 3145736 | tf_op jit(solution)/shard_map/ppermute | solution.py:255
  70.5 69.9 %collective-permute-start.9 = (bf16[512,1024]{1,0:T(8,128)(2,1)}, bf16[512,1024]{1,0:T(8,128)(2,1)}, u32[]{:S(2)}, u32[]{:S(2)}) collective-permute-start(bf16[512,1024]{1,0:T(8,128)(2,1)} %collective-permute-done.6.m2_ref), channel_id=1, source_target_pairs={{0,1},{1,0},{2,3},{3,2},{4,5},{5,4},{6,7},{7,6},{8,9},{9,8},{10,11... | collective-permute-start | bytes 3145736 | tf_op jit(solution)/shard_map/ppermute | solution.py:255
  88.4 52.0 %collective-permute-start.8 = (bf16[512,1024]{1,0:T(8,128)(2,1)}, bf16[512,1024]{1,0:T(8,128)(2,1)}, u32[]{:S(2)}, u32[]{:S(2)}) collective-permute-start(bf16[512,1024]{1,0:T(8,128)(2,1)} %collective-permute-done.5.m1_ref), channel_id=1, source_target_pairs={{0,1},{1,0},{2,3},{3,2},{4,5},{5,4},{6,7},{7,6},{8,9},{9,8},{10,11... | collective-permute-start | bytes 3145736 | tf_op jit(solution)/shard_map/ppermute | solution.py:255
  88.5 15.1 %copy-start.9 = (f32[128]{0:T(128)S(1)}, f32[128]{0:T(128)}, u32[]{:S(2)}) copy-start(f32[128]{0:T(128)} %param.27) | copy-start | bytes 1540
  91.4 0.7 copy-start.4
  92.1 22.7 %all-to-all-start.3 = ((bf16[4,192,256]{2,1,0:T(8,128)(2,1)}), bf16[4,192,256]{2,1,0:T(8,128)(2,1)S(1)}, u32[]{:S(2)}, u32[]{:S(2)}) async-start(bf16[4,192,256]{2,1,0:T(8,128)(2,1)} %copy-done.4), calls=%async_computation.3 | async-start | bytes 786432 | tf_op jit(solution)/shard_map/all_to_all | solution.py:328
  95.6 19.2 %collective-permute-start = (bf16[128,256]{1,0:T(8,128)(2,1)S(1)}, bf16[128,256]{1,0:T(8,128)(2,1)S(1)}, u32[]{:S(2)}, u32[]{:S(2)}) collective-permute-start(bf16[128,256]{1,0:T(8,128)(2,1)S(1)} %get-tuple-element.14), channel_id=1, source_target_pairs={{0,8},{8,16},{16,24},{24,32},{32,40},{40,48},{48,56},{56,64},{64,7... | collective-permute-start | bytes 196616 | tf_op jit(solution)/shard_map/ppermute | solution.py:331
  99.5 15.3 %collective-permute-start.1 = (bf16[128,256]{1,0:T(8,128)(2,1)S(1)}, bf16[128,256]{1,0:T(8,128)(2,1)S(1)}, u32[]{:S(2)}, u32[]{:S(2)}) collective-permute-start(bf16[128,256]{1,0:T(8,128)(2,1)S(1)} %get-tuple-element.15), channel_id=1, source_target_pairs={{8,0},{16,8},{24,16},{32,24},{40,32},{48,40},{56,48},{64,56},{72,6... | collective-permute-start | bytes 196616 | tf_op jit(solution)/shard_map/ppermute | solution.py:332
  103.6 1.0 copy-start.1
  104.6 1.0 copy-start.3
  105.7 1.6 %copy-start.8 = (bf16[2048,512]{1,0:T(8,128)(2,1)S(1)}, bf16[2048,512]{1,0:T(8,128)(2,1)}, u32[]{:S(2)}) copy-start(bf16[2048,512]{1,0:T(8,128)(2,1)} %wq_ref.1) | copy-start | bytes 6291460
  107.3 7.6 %copy-start.6 = (f32[4]{0:T(128)S(1)}, f32[4]{0:T(128)}, u32[]{:S(2)}) copy-start(f32[4]{0:T(128)} %param.29) | copy-start | bytes 52
  117.9 15.2 %collective-permute-start.2 = (bf16[256,512]{1,0:T(8,128)(2,1)S(1)}, bf16[256,512]{1,0:T(8,128)(2,1)S(1)}, u32[]{:S(2)}, u32[]{:S(2)}) collective-permute-start(bf16[256,512]{1,0:T(8,128)(2,1)S(1)} %attend1.1), channel_id=1, source_target_pairs={{0,2},{2,4},{4,6},{6,0},{1,3},{3,5},{5,7},{7,1},{8,10},{10,12},{12... | collective-permute-start | bytes 786440 | tf_op jit(solution)/shard_map/ppermute | solution.py:255
  121.4 14.9 %collective-permute-start.3 = (bf16[256,512]{1,0:T(8,128)(2,1)S(1)}, bf16[256,512]{1,0:T(8,128)(2,1)S(1)}, u32[]{:S(2)}, u32[]{:S(2)}) collective-permute-start(bf16[256,512]{1,0:T(8,128)(2,1)S(1)} %attend2.1), channel_id=1, source_target_pairs={{0,4},{2,6},{4,0},{6,2},{1,5},{3,7},{5,1},{7,3},{8,12},{10,14},{12... | collective-permute-start | bytes 786440 | tf_op jit(solution)/shard_map/ppermute | solution.py:255
  133.1 7.3 %collective-permute-start.4 = (bf16[256,512]{1,0:T(8,128)(2,1)S(1)}, bf16[256,512]{1,0:T(8,128)(2,1)S(1)}, u32[]{:S(2)}, u32[]{:S(2)}) collective-permute-start(bf16[256,512]{1,0:T(8,128)(2,1)S(1)} %attend3.1), channel_id=1, source_target_pairs={{0,6},{2,0},{4,2},{6,4},{1,7},{3,1},{5,3},{7,5},{8,14},{10,8},{12,... | collective-permute-start | bytes 786440 | tf_op jit(solution)/shard_map/ppermute | solution.py:255

commit v2 on v1

v2 whole, which is shorter than its diff:
```python
import math

import jax
import jax.numpy as jnp
from jax import lax
from jax.experimental import pallas as pl
from jax.experimental.pallas import tpu as pltpu
from jax.sharding import Mesh, PartitionSpec as P


HEAD_DIM = 128
WINDOW = 128
GRID_W = 64
NORM_EPSILON = 1e-06
ROPE_BASE = 10000.0
D = 2048
VECS = 20
NZ, NY, NX = 8, 4, 4
SP = ("z", "y")

F32 = jnp.float32
BF16 = jnp.bfloat16
QUERY_SCALE = HEAD_DIM ** (-0.5) * math.log2(math.e)


def sp_index():
    return lax.axis_index("z") * NY + lax.axis_index("y")


def params(vmem_mib):
    return pltpu.CompilerParams(vmem_limit_bytes=vmem_mib * 1024 * 1024)


def cost(flops, nbytes, trans=0):
    return pl.CostEstimate(flops=flops, bytes_accessed=nbytes, transcendentals=trans)


def partial_kernel(cond_in, ctx_in, shift_in, scale_in, gate_in, out_ref,
                   cond_ref, ctx_ref, shift_ref, scale_ref, gate_ref, sems):
    moves = [
        pltpu.make_async_copy(source, to, sems.at[i])
        for i, (source, to) in enumerate(
            (
                (cond_in, cond_ref), (ctx_in, ctx_ref), (shift_in, shift_ref),
                (scale_in, scale_ref), (gate_in, gate_ref),
            )
        )
    ]
    for move in moves:
        move.start()
    for move in moves:
        move.wait()
    sp = sp_index()
    start = pl.multiple_of((sp // 2) * 128, 128)
    row = lax.broadcasted_iota(jnp.int32, (8, 128), 0)
    lane = lax.broadcasted_iota(jnp.int32, (8, 128), 1)
    rows = jnp.where(
        row == 0,
        cond_ref[:, pl.ds(start, 128)],
        jnp.where(row == 1, ctx_ref[:, pl.ds(start, 128)], 0.0),
    )
    active = rows / (1.0 + jnp.exp(-rows))
    active = jnp.where((lane // 64) == (sp % 2), active, 0.0).astype(BF16)

    def times(ref):
        matrix = ref[...]
        return jnp.dot(
            active, jnp.concatenate([matrix, matrix], axis=0), preferred_element_type=F32
        )

    shifts, scales, gates = times(shift_ref), times(scale_ref), times(gate_ref)
    pieces = []
    for values, at in ((shifts, 0), (scales, 0), (shifts, 1), (scales, 1), (gates, 0)):
        for i in range(4):
            pieces.append(values[at : at + 1, i * 128 : (i + 1) * 128])
    pieces.append(jnp.zeros((4, 128), F32))
    stacked = jnp.concatenate(pieces, axis=0).astype(BF16)
    out_ref[...] = jnp.broadcast_to(stacked[None], out_ref.shape)


def resum_kernel(in_ref, out_ref):
    pieces = []
    for t in range(NX):
        rows = None
        for y in range(NY):
            part = in_ref[y * NX + t].astype(F32)
            rows = part if rows is None else rows + part
        pieces.append(rows[:VECS])
    total = jnp.concatenate(pieces, axis=0).astype(BF16)
    out_ref[...] = jnp.broadcast_to(total[None], out_ref.shape)


def vectors_of(mod_ref):
    rows = None
    for z in range(NZ):
        part = mod_ref[z].astype(F32)
        rows = part if rows is None else rows + part
    found = []
    for v in range(5):
        pieces = []
        for t in range(NX):
            for i in range(4):
                at = t * VECS + v * 4 + i
                pieces.append(rows[at : at + 1, :])
        found.append(jnp.concatenate(pieces, axis=1))
    return found


def normed(values):
    values = values.astype(F32)
    return values * lax.rsqrt(jnp.mean(values * values, axis=-1, keepdims=True) + NORM_EPSILON)


def head_norm(v, gain):
    return v * lax.rsqrt(jnp.mean(v * v, axis=-1, keepdims=True) + NORM_EPSILON) * gain


def rotated(v, cosine, sine):
    lane = lax.broadcasted_iota(jnp.int32, v.shape, 1)
    odd = ((lane // 32) % 2) == 1
    swapped = jnp.where(odd, pltpu.roll(v, 32, 1), pltpu.roll(v, 96, 1))
    return v * cosine + swapped * sine


def prenorm_kernel(lat_ref, out_ref):
    step = 64

    def body(i, carry):
        at = pl.ds(pl.multiple_of(i * step, step), step)
        out_ref[at, :] = normed(lat_ref[at, :]).astype(BF16)
        return carry

    lax.fori_loop(0, lat_ref.shape[0] // step, body, 0)


def context_kernel(mod_ref, ctx_ref, wk_ref, wv_ref, gain_ref, kgain_ref, kv_ref, vec_ref):
    shift_lat, scale_lat, shift_ctx, scale_ctx, gate = vectors_of(mod_ref)
    gain = gain_ref[...]
    vec_ref[0:1, :] = gain * (1.0 + scale_lat)
    vec_ref[1:2, :] = shift_lat
    vec_ref[2:3, :] = gate
    rows = (normed(ctx_ref[...]) * (gain * (1.0 + scale_ctx)) + shift_ctx).astype(BF16)
    keys = head_norm(jnp.dot(rows, wk_ref[...], preferred_element_type=F32), kgain_ref[...])
    values = jnp.dot(rows, wv_ref[...], preferred_element_type=F32)
    both = jnp.concatenate([keys, values], axis=1).astype(BF16)
    kv_ref[...] = jnp.broadcast_to(both[None], kv_ref.shape)


def qkv_kernel(
    lat_in, before_in, after_in, wq_in, wk_in, wv_in,
    vec_ref, qgain_ref, kgain_ref, rcos_ref, rsin_ref, ccos_ref, csin_ref,
    q_ref, near_ref, sum_ref, lat_ref, halo_ref, wq_ref, wk_ref, wv_ref, k_ref, v_ref, sems,
):
    step = 256
    tok = lat_in.shape[0]
    steps = tok // step
    qgain = qgain_ref[...] * QUERY_SCALE
    kgain = kgain_ref[...]

    def rows_move(i):
        at = pl.ds(pl.multiple_of(i * step, step), step)
        return pltpu.make_async_copy(lat_in.at[at, :], lat_ref.at[at, :], sems.at[i])

    others = [
        pltpu.make_async_copy(source, to, sems.at[steps + i])
        for i, (source, to) in enumerate(
            (
                (wk_in, wk_ref), (wv_in, wv_ref), (wq_in, wq_ref),
                (before_in, halo_ref.at[:WINDOW]), (after_in, halo_ref.at[WINDOW:]),
            )
        )
    ]
    others[0].start()
    others[1].start()
    rows_move(0).start()
    others[2].start()
    for i in range(1, steps):
        rows_move(i).start()
    others[3].start()
    others[4].start()

    def table(group):
        cosine = rcos_ref[pl.ds(group, 1), :] + ccos_ref[...]
        sine = rsin_ref[pl.ds(group, 1), :] + csin_ref[...]
        return cosine, sine

    def tables(first, count):
        both = [table(first + g) for g in range(count)]
        return jnp.concatenate([c for c, _ in both]), jnp.concatenate([s for _, s in both])

    def modulated(values):
        return (values * vec_ref[0:1, :] + vec_ref[1:2, :]).astype(BF16)

    others[0].wait()
    others[1].wait()

    def body(i, carry):
        @pl.when(i == 0)
        def _():
            others[2].wait()

        rows_move(i).wait()
        at = pl.ds(pl.multiple_of(i * step, step), step)
        to = pl.ds(pl.multiple_of(i * step + WINDOW, WINDOW), step)
        rows = modulated(lat_ref[at, :].astype(F32))
        cosine, sine = tables(2 + i * (step // GRID_W), step // GRID_W)
        keys = jnp.dot(rows, wk_ref[...], preferred_element_type=F32)
        queries = jnp.dot(rows, wq_ref[...], preferred_element_type=F32)
        k_ref[to, :] = rotated(head_norm(keys, kgain), cosine, sine).astype(BF16)
        v_ref[to, :] = jnp.dot(rows, wv_ref[...], preferred_element_type=F32).astype(BF16)
        for h in range(4):
            head = slice(h * HEAD_DIM, (h + 1) * HEAD_DIM)
            turned = rotated(head_norm(queries[:, head], qgain), cosine, sine).astype(BF16)
            for half in range(2):
                q_ref[i * 2 + half, h * WINDOW : (h + 1) * WINDOW, :] = turned[
                    half * WINDOW : (half + 1) * WINDOW
                ]
        return carry

    lax.fori_loop(0, steps, body, 0)
    others[3].wait()
    others[4].wait()

    def halo(i, carry):
        at = pl.ds(pl.multiple_of(i * WINDOW, WINDOW), WINDOW)
        to = pl.ds(pl.multiple_of(i * (tok + WINDOW), WINDOW), WINDOW)
        rows = modulated(normed(halo_ref[at, :]))
        cosine, sine = tables(i * ((tok + WINDOW) // GRID_W), WINDOW // GRID_W)
        keys = head_norm(jnp.dot(rows, wk_ref[...], preferred_element_type=F32), kgain)
        k_ref[to, :] = rotated(keys, cosine, sine).astype(BF16)
        v_ref[to, :] = jnp.dot(rows, wv_ref[...], preferred_element_type=F32).astype(BF16)
        return carry

    lax.fori_loop(0, 2, halo, 0)
    local_pass(q_ref, k_ref, v_ref, near_ref, sum_ref)


def contract_last(a, b):
    return lax.dot_general(a, b, (((1,), (1,)), ((), ())), preferred_element_type=F32)


def lanes_summed(values):
    parts = [values[:, i : i + 128] for i in range(0, values.shape[1], 128)]
    while len(parts) > 1:
        parts = [sum(parts[i : i + 2]) for i in range(0, len(parts), 2)]
    return parts[0]


def local_pass(q_ref, k_ref, v_ref, out_ref, sum_ref):
    sp = sp_index()
    blocks = q_ref.shape[0]
    query_at = lax.broadcasted_iota(jnp.int32, (4 * WINDOW, WINDOW), 0) % WINDOW
    key_at = lax.broadcasted_iota(jnp.int32, (4 * WINDOW, WINDOW), 1)
    in_before, in_after = key_at >= query_at, key_at <= query_at

    sum_ref[...] = jnp.zeros(sum_ref.shape, F32)

    def body(block, carry):
        near = pl.ds(pl.multiple_of(block * WINDOW, WINDOW), 3 * WINDOW)
        no_before = (block == 0) & (sp == 0)
        no_after = (block == blocks - 1) & (sp == NZ * NY - 1)
        local = jnp.exp2(contract_last(q_ref[block], k_ref[near, :]))
        local = jnp.concatenate(
            [
                jnp.where(in_before & jnp.logical_not(no_before), local[:, :WINDOW], 0.0),
                local[:, WINDOW : 2 * WINDOW],
                jnp.where(in_after & jnp.logical_not(no_after), local[:, 2 * WINDOW :], 0.0),
            ],
            axis=1,
        )
        total = jnp.sum(lanes_summed(local), axis=-1, keepdims=True)
        sum_ref[...] = jnp.where(key_at == block, total, sum_ref[...])
        out_ref[block] = jnp.dot(local.astype(BF16), v_ref[near, :], preferred_element_type=F32)
        return carry

    lax.fori_loop(0, blocks, body, 0)


def attend_kernel(by, q_ref, near_ref, sum_ref, ctx_ref, sink_ref, out_ref):
    quarter = (lax.axis_index("tp") + by) % NX
    head = HEAD_DIM
    sink = jnp.concatenate(
        [jnp.exp(jnp.full((WINDOW, 1), sink_ref[0, h], F32)) for h in range(4)], axis=0
    )

    lane = lax.broadcasted_iota(jnp.int32, sum_ref.shape, 1)

    def body(i, carry):
        block = quarter * 2 + i
        base = pl.ds(pl.multiple_of(i * WINDOW, WINDOW), WINDOW)
        far = jnp.exp2(contract_last(q_ref[block], ctx_ref[:, :head]))
        near_sum = jnp.where(lane == block, sum_ref[...], 0.0)
        total = jnp.sum(lanes_summed(far) + near_sum, axis=-1, keepdims=True) + sink
        mixed = near_ref[block] + jnp.dot(
            far.astype(BF16), ctx_ref[:, head:], preferred_element_type=F32
        )
        mixed = (mixed * (1.0 / total)).astype(BF16)
        for h in range(4):
            out_ref[base, h * head : (h + 1) * head] = mixed[h * WINDOW : (h + 1) * WINDOW]
        return carry

    lax.fori_loop(0, 2, body, 0)


def project_kernel(
    vec_ref, a0_ref, a1_ref, a2_ref, a3_ref, w0_in,
    m1_in, m2_in, m3_in, o1_in, o2_in, o3_in, lat_in, out_ref,
    w_ref, lat_ref, done_ref, sems,
):
    dp = lax.axis_index("dp")
    col = 512
    deep = 4 * HEAD_DIM
    sub = lat_ref.shape[0]
    first = pl.multiple_of(lax.axis_index("tp") * sub, sub)
    rows_move = pltpu.make_async_copy(lat_in.at[pl.ds(first, sub), :], lat_ref, sems.at[16])
    halves = (dp, 1 - dp)

    def columns(slot):
        return pl.multiple_of(halves[slot // 2] * (D // 2) + (slot % 2) * col, col)

    def moves(slot):
        later = slice((slot % 2) * col, (slot % 2 + 1) * col)
        group = (m1_in, m2_in, m3_in) if slot < 2 else (o1_in, o2_in, o3_in)
        sources = [w0_in.at[:, pl.ds(columns(slot), col)]] + [w.at[:, later] for w in group]
        return [
            pltpu.make_async_copy(
                source, w_ref.at[slot, pl.ds(s * deep, deep), :], sems.at[slot * 4 + s]
            )
            for s, source in enumerate(sources)
        ]

    for slot in range(4):
        for move in moves(slot):
            move.start()
        if slot == 0:
            rows_move.start()
    left = jnp.concatenate([a0_ref[...], a1_ref[...], a2_ref[...], a3_ref[...]], axis=1)
    rows_move.wait()
    for slot in range(4):
        for move in moves(slot):
            move.wait()
        wide = pl.ds(columns(slot), col)
        mixed = jnp.dot(left, w_ref[slot], preferred_element_type=F32)
        result = lat_ref[:, wide].astype(F32) + vec_ref[2:3, wide] * mixed
        done_ref[slot] = result.astype(BF16)
        pltpu.make_async_copy(done_ref.at[slot], out_ref.at[:, wide], sems.at[17 + slot]).start()
    for slot in range(4):
        wide = pl.ds(columns(slot), col)
        pltpu.make_async_copy(done_ref.at[slot], out_ref.at[:, wide], sems.at[17 + slot]).wait()


def shifted(array, axis, by):
    peers = lax.axis_size(axis)
    return lax.ppermute(array, axis, [(i, (i + by) % peers) for i in range(peers)])


VMEM = pl.BlockSpec(memory_space=pltpu.VMEM)
SMEM = pl.BlockSpec(memory_space=pltpu.SMEM)
HBM = pl.BlockSpec(memory_space=pltpu.HBM)


def call(kernel, outs, args, estimate, limit, scratch=(), in_specs=None, out_specs=None):
    shapes = [jax.ShapeDtypeStruct(s, t) for s, t in outs]
    single = len(shapes) == 1
    return pl.pallas_call(
        kernel,
        in_specs=in_specs or [VMEM] * len(args),
        out_specs=out_specs or (VMEM if single else [VMEM] * len(shapes)),
        out_shape=shapes[0] if single else shapes,
        scratch_shapes=list(scratch),
        compiler_params=params(limit),
        cost_estimate=estimate,
    )(*args)


def per_device(
    latent, context, cond, ctx_cond, norm_gain, mod_shift, mod_scale, mod_gate,
    w_query, w_key, w_value, w_out, q_gain, k_gain, sinks,
):
    lat = latent[0]
    tok = lat.shape[0]
    sub = tok // NX
    sp = sp_index()
    dp = lax.axis_index("dp")
    width = 4 * HEAD_DIM

    part = call(
        partial_kernel, [((NY * NX, 24, 128), BF16)],
        (cond, ctx_cond[None], mod_shift, mod_scale, mod_gate), cost(1 << 20, 1 << 18), 62,
        scratch=[
            pltpu.VMEM((1, D), F32), pltpu.VMEM((1, D), F32), pltpu.VMEM((64, 512), BF16),
            pltpu.VMEM((64, 512), BF16), pltpu.VMEM((64, 512), BF16),
            pltpu.SemaphoreType.DMA((5,)),
        ],
        in_specs=[HBM] * 5,
    )
    part = lax.all_to_all(part, ("y", "tp"), 0, 0, tiled=True)
    part = call(resum_kernel, [((NZ, NX * VECS, 128), BF16)], (part,), cost(1 << 20, 1 << 18), 4)
    mod = lax.all_to_all(part, "z", 0, 0, tiled=True)

    peers = NZ * NY
    up = [(i, i + 1) for i in range(peers - 1)]
    before = lax.ppermute(lat[tok - WINDOW :], SP, up)
    after = lax.ppermute(lat[:WINDOW], SP, [(j, i) for i, j in up])

    half = lax.dynamic_slice_in_dim(w_out, dp * (D // 2), D // 2, 1)
    mine, other = {}, {}
    for s in (1, 3, 2):
        mine[s] = shifted(half, "tp", s)
        other[s] = shifted(mine[s], "dp", 1)

    quarter = HEAD_DIM // 4
    lane = jnp.arange(HEAD_DIM)
    frequency = ROPE_BASE ** (-(lane % quarter).astype(F32) / quarter)
    sign = jnp.where((lane // quarter) % 2 == 0, -1.0, 1.0).astype(F32)
    by_row = lane < HEAD_DIM // 2
    grid_row = (sp * tok - WINDOW) // GRID_W + jnp.arange(24, dtype=jnp.int32)
    row_angle = grid_row.astype(F32)[:, None] * frequency
    col_angle = jnp.arange(GRID_W, dtype=F32)[:, None] * frequency
    row_cos = jnp.where(by_row, jnp.cos(row_angle), 0.0)
    row_sin = jnp.where(by_row, jnp.sin(row_angle) * sign, 0.0)
    col_cos = jnp.where(by_row, 0.0, jnp.cos(col_angle))
    col_sin = jnp.where(by_row, 0.0, jnp.sin(col_angle) * sign)

    block = pl.BlockSpec((256, D), lambda i: (i, 0))
    scaled = pl.pallas_call(
        prenorm_kernel,
        grid=(tok // 256,),
        in_specs=[block],
        out_specs=block,
        out_shape=jax.ShapeDtypeStruct((tok, D), BF16),
        compiler_params=params(60),
        cost_estimate=cost(tok * D * 4, tok * D * 4),
        name="prenorm",
    )(lat)
    rows = tok + 2 * WINDOW
    gain, qgain, kgain = norm_gain[None], q_gain[None], k_gain[None]
    n_ctx = context.shape[1]
    ctx_kv, vec = call(
        context_kernel,
        [((peers, n_ctx, 2 * HEAD_DIM), BF16), ((8, D), F32)],
        (mod, context[0], w_key, w_value, gain, kgain),
        cost(2 * n_ctx * D * 256, D * 512), 4,
    )
    ctx_all = lax.all_to_all(ctx_kv, SP, 0, 0, tiled=True).reshape(-1, 2 * HEAD_DIM)

    queries, near, sums = call(
        qkv_kernel,
        [
            ((tok // WINDOW, 4 * WINDOW, HEAD_DIM), BF16),
            ((tok // WINDOW, 4 * WINDOW, HEAD_DIM), F32), ((4 * WINDOW, 128), F32),
        ],
        (
            scaled, before, after, w_query, w_key, w_value, vec, qgain, kgain,
            row_cos, row_sin, col_cos, col_sin,
        ),
        cost(2 * tok * D * 768 + 16 * tok * 384 * HEAD_DIM, tok * D * 2 + D * 768 * 2), 60,
        scratch=[
            pltpu.VMEM((tok, D), BF16), pltpu.VMEM((2 * WINDOW, D), BF16),
            pltpu.VMEM((D, width), BF16), pltpu.VMEM((D, HEAD_DIM), BF16),
            pltpu.VMEM((D, HEAD_DIM), BF16), pltpu.VMEM((rows, HEAD_DIM), BF16),
            pltpu.VMEM((rows, HEAD_DIM), BF16), pltpu.SemaphoreType.DMA((tok // 256 + 5,)),
        ],
        in_specs=[HBM] * 6 + [VMEM] * 7,
    )

    arrived = {}
    for s in (2, 1, 3, 0):
        piece = call(
            lambda *refs, s=s: attend_kernel(s, *refs), [((sub, width), BF16)],
            (queries, near, sums, ctx_all, sinks[None]),
            cost(4 * 4 * sub * 768 * HEAD_DIM, 2 << 20, 4 * sub * 768), 8,
            in_specs=[VMEM] * 4 + [SMEM],
        )
        if s == 0:
            arrived[s] = piece
        else:
            arrived[s] = shifted(piece, "tp", s)

    result = call(
        project_kernel, [((sub, D), BF16)],
        (
            vec, arrived[0], arrived[1], arrived[2], arrived[3], w_out,
            mine[1], mine[2], mine[3], other[1], other[2], other[3], lat,
        ),
        cost(2 * sub * D * D, D * D * 2), 61,
        scratch=[
            pltpu.VMEM((4, D, 512), BF16), pltpu.VMEM((sub, D), BF16),
            pltpu.VMEM((4, sub, 512), BF16), pltpu.SemaphoreType.DMA((21,)),
        ],
        in_specs=[VMEM] * 5 + [HBM] * 8,
        out_specs=HBM,
    )
    return result[None]


def solution(mesh):
    grid = Mesh(mesh.devices.reshape(NZ, NY, NX, 2), ("z", "y", "tp", "dp"))
    in_specs = (
        P("dp", SP, None),
        P("dp", SP, None),
        P("dp", None),
        P(),
        P(),
        P(SP, "tp"),
        P(SP, "tp"),
        P(SP, "tp"),
        P(None, "tp"),
        P(None, "tp"),
        P(None, "tp"),
        P("tp", None),
        P(),
        P(),
        P("tp"),
    )
    out_specs = P("dp", ("z", "y", "tp"), None)

    return jax.shard_map(
        per_device, mesh=grid, in_specs=in_specs, out_specs=out_specs, check_vma=False
    )
```

time: 149 us -> 117 us (0.79)
  blocking collectives: 30.3 us -> 0 us
  waiting for transfers between devices: 51.8 us -> 24.9 us
  starting transfers between devices: 21.8 us -> 38.6 us
  Pallas kernels: 33.9 us -> 40.8 us
  local copies, waits for them, and re-layouts: 7.37 us -> 10.5 us
  other arithmetic: 3.04 us -> 1.51 us
    all_to_all x2 -> x0, blocking collectives: 30.3 us -> none  [the longest x1 15.4 us: per_device(): over_z = lax.all_to_all(partial, 'z', 0, 0, tiled=True)]
    ppermute x9, waiting for transfers between devices: 51.8 us -> 24.9 us  [shifted(): lax.ppermute(array, axis, [(i, (i + by) % peers) for i in range(peers)])]
    all_to_all x2 -> x3, starting transfers between devices: 8.37 us -> 24.2 us  [the longest x1 8.58 us: per_device(): lax.all_to_all(ctx_kv, SP, 0, 0, tiled=True).reshape(-1, 2 * HEAD_DIM)]
    pallas_call x9 -> x10, Pallas kernels: 33.9 us -> 40.8 us  [the longest x9 35 us: call(): pl.pallas_call(kernel, in_specs=in_specs or [VMEM] * len(args), out_specs...]
    mul x2 -> x0, other arithmetic: 2.63 us -> none  [the longest x1 2.3 us: per_device(): cosine, sine = (jnp.cos(angles), jnp.sin(angles) * signs)]
    slice x0 -> x1, local copies, waits for them, and re-layouts: none -> 2.33 us  [per_device(): after = lax.ppermute(lat[:WINDOW], SP, [(j, i) for i, j in up])]
    broadcast_in_dim x1 -> x0, local copies, waits for them, and re-layouts: 1.86 us -> none  [copies(): jnp.broadcast_to(array[None], (peers, *array.shape))]
    select_n x1 -> x3, other arithmetic: 0.01 us -> 1.5 us  [the longest x1 0.77 us: per_device(): col_sin = jnp.where(by_row, 0.0, jnp.sin(col_angle) * sign)]
  transfers between devices with their start and end apart: 13 -> 14, of which waited for: 5 -> 5; matrix products, arithmetic and copies ran while one was open for 3% -> 5% of each run, Pallas kernels for 15% -> 28%
where the time goes in v2:
time: 117 us
  Pallas kernels  40.8 us (35%)
  starting transfers between devices  38.6 us (33%)
  waiting for transfers between devices  24.9 us (21%)
  local copies, waits for them, and re-layouts  10.5 us (9%)
  other arithmetic  1.51 us (1%)
    pallas_call x9, Pallas kernels, call(): pl.pallas_call(kernel, in_specs=in_specs or [VMEM] * len(args), out_specs...  35 us
    ppermute x9, waiting for transfers between devices, shifted(): lax.ppermute(array, axis, [(i, (i + by) % peers) for i in range(peers)])  24.9 us
    all_to_all x1, starting transfers between devices, per_device(): lax.all_to_all(ctx_kv, SP, 0, 0, tiled=True).reshape(-1, 2 * HEAD_DIM)  8.58 us
    all_to_all x1, starting transfers between devices, per_device(): mod = lax.all_to_all(part, 'z', 0, 0, tiled=True)  8.57 us
    all_to_all x1, starting transfers between devices, per_device(): part = lax.all_to_all(part, ('y', 'tp'), 0, 0, tiled=True)  7.05 us
    ppermute x9, starting transfers between devices, shifted(): lax.ppermute(array, axis, [(i, (i + by) % peers) for i in range(peers)])  6.51 us
    unnamed x32, local copies, waits for them, and re-layouts  5.85 us
    pallas_call x1, Pallas kernels, per_device(): pl.pallas_call(prenorm_kernel, grid=(tok // 256,), in_specs=[block], out_...  5.8 us
  transfers between devices with their start and end apart: 14, of which 5 were waited for; matrix products, arithmetic and copies ran while one was open for 5% of the time, Pallas kernels for 28%

profile of v2, /device:TPU:32, one launch (start us, length us, event | category | flops | bytes accessed | tf_op | source)
XLA Modules:
  0.0 116.8 jit_solution(9805227068406488071)
XLA Ops:
  0.0 1.8 %shard_map.145 = bf16[16,24,128]{2,1,0:T(8,128)(2,1)} custom-call(f32[1,2048]{1,0:T(1,128)} %cond_in.1, f32[1,2048]{1,0:T(1,128)} %bitcast.27, bf16[64,512]{1,0:T(8,128)(2,1)} %shift_in.1, bf16[64,512]{1,0:T(8,128)(2,1)} %scale_in.1, bf16[64,512]{1,0:T(8,128)(2,1)} %gate_in.1), custom_call_target="tpu_custom_call" | custom-call | flops 1048576 | bytes 262144 | tf_op jit(solution)/shard_map/pallas_call | solution.py:365
  1.8 7.0 %all-to-all-start = ((bf16[16,24,128]{2,1,0:T(8,128)(2,1)}), bf16[16,24,128]{2,1,0:T(8,128)(2,1)S(1)}, u32[]{:S(2)}, u32[]{:S(2)}) async-start(bf16[16,24,128]{2,1,0:T(8,128)(2,1)} %shard_map.145), calls=%async_computation | async-start | bytes 196608 | tf_op jit(solution)/shard_map/all_to_all | solution.py:397
  8.9 2.4 %constant_dynamic-slice_fusion = bf16[512,1024]{1,0:T(8,128)(2,1)} fusion(bf16[512,2048]{1,0:T(8,128)(2,1)} %w0_in.1, s32[]{:T(128)S(6)} %select_n.76), kind=kLoop, calls=%fused_computation.26 | loop fusion | bytes 2097156 | tf_op jit(solution)/shard_map/dynamic_slice | solution.py:406
  11.3 3.1 %collective-permute-start.7 = (bf16[512,1024]{1,0:T(8,128)(2,1)}, bf16[512,1024]{1,0:T(8,128)(2,1)S(1)}, u32[]{:S(2)}, u32[]{:S(2)}) collective-permute-start(bf16[512,1024]{1,0:T(8,128)(2,1)} %constant_dynamic-slice_fusion), channel_id=1, source_target_pairs={{0,6},{2,0},{4,2},{6,4},{1,7},{3,1},{5,3},{7,5},{8,14},{10,8},{12,... | collective-permute-start | bytes 3145736 | tf_op jit(solution)/shard_map/ppermute | solution.py:354
  14.4 2.3 %collective-permute-start.6 = (bf16[512,1024]{1,0:T(8,128)(2,1)}, bf16[512,1024]{1,0:T(8,128)(2,1)}, u32[]{:S(2)}, u32[]{:S(2)}) collective-permute-start(bf16[512,1024]{1,0:T(8,128)(2,1)} %constant_dynamic-slice_fusion), channel_id=1, source_target_pairs={{0,4},{2,6},{4,0},{6,2},{1,5},{3,7},{5,1},{7,3},{8,12},{10,14},{12... | collective-permute-start | bytes 3145736 | tf_op jit(solution)/shard_map/ppermute | solution.py:354
  17.4 8.6 %all-to-all-start.1 = ((bf16[8,80,128]{2,1,0:T(8,128)(2,1)}), bf16[8,80,128]{2,1,0:T(8,128)(2,1)S(1)}, u32[]{:S(2)}, u32[]{:S(2)}) async-start(bf16[8,80,128]{2,1,0:T(8,128)(2,1)} %shard_map.146), calls=%async_computation.1 | async-start | bytes 327680 | tf_op jit(solution)/shard_map/all_to_all | solution.py:399
  26.0 2.3 %slice_bitcast_fusion = (bf16[128,2048]{1,0:T(8,128)(2,1)}, bf16[128,2048]{1,0:T(8,128)(2,1)}) fusion(bf16[1,1024,2048]{2,1,0:T(8,128)(2,1)} %param.15), kind=kLoop, calls=%fused_computation | loop fusion | bytes 2097152 | tf_op jit(solution)/shard_map/slice | solution.py:404
  28.3 3.4 %collective-permute-start = (bf16[128,2048]{1,0:T(8,128)(2,1)}, bf16[128,2048]{1,0:T(8,128)(2,1)}, u32[]{:S(2)}, u32[]{:S(2)}) collective-permute-start(bf16[128,2048]{1,0:T(8,128)(2,1)} %get-tuple-element.16), channel_id=1, source_target_pairs={{0,8},{8,16},{16,24},{24,32},{32,40},{40,48},{48,56},{56,64},{64,7... | collective-permute-start | bytes 1572872 | tf_op jit(solution)/shard_map/ppermute | solution.py:403
  31.7 4.6 %collective-permute-start.1 = (bf16[128,2048]{1,0:T(8,128)(2,1)}, bf16[128,2048]{1,0:T(8,128)(2,1)}, u32[]{:S(2)}, u32[]{:S(2)}) collective-permute-start(bf16[128,2048]{1,0:T(8,128)(2,1)} %get-tuple-element.15), channel_id=1, source_target_pairs={{8,0},{16,8},{24,16},{32,24},{40,32},{48,40},{56,48},{64,56},{72,6... | collective-permute-start | bytes 1572872 | tf_op jit(solution)/shard_map/ppermute | solution.py:404
  38.2 8.6 %all-to-all-start.2 = ((bf16[32,24,256]{2,1,0:T(8,128)(2,1)}), bf16[32,24,256]{2,1,0:T(8,128)(2,1)S(1)}, u32[]{:S(2)}, u32[]{:S(2)}) async-start(bf16[32,24,256]{2,1,0:T(8,128)(2,1)} %get-tuple-element.14), calls=%async_computation.2 | async-start | bytes 786432 | tf_op jit(solution)/shard_map/all_to_all | solution.py:445
  47.5 11.5 %collective-permute-done.7.m3_in = bf16[512,1024]{1,0:T(8,128)(2,1)S(1)} collective-permute-done((bf16[512,1024]{1,0:T(8,128)(2,1)}, bf16[512,1024]{1,0:T(8,128)(2,1)S(1)}, u32[]{:S(2)}, u32[]{:S(2)}) %collective-permute-start.7) | collective-permute-done | bytes 1048608 | tf_op jit(solution)/shard_map/ppermute | solution.py:354
  59.1 3.3 %collective-permute-done.5.m1_in = bf16[512,1024]{1,0:T(8,128)(2,1)S(1)} collective-permute-done((bf16[512,1024]{1,0:T(8,128)(2,1)}, bf16[512,1024]{1,0:T(8,128)(2,1)S(1)}, u32[]{:S(2)}, u32[]{:S(2)}) %collective-permute-start.5) | collective-permute-done | bytes 1048608 | tf_op jit(solution)/shard_map/ppermute | solution.py:354
  63.6 5.8 %prenorm.1.lat_in = bf16[1024,2048]{1,0:T(8,128)(2,1)} custom-call(bf16[1024,2048]{1,0:T(8,128)(2,1)} %bitcast.25), custom_call_target="tpu_custom_call" | custom-call | flops 8388608 | bytes 8388608 | tf_op jit(solution)/shard_map/prenorm/pallas_call | solution.py:426
  69.4 15.2 %shard_map.148 = (bf16[8,512,128]{2,1,0:T(8,128)(2,1)}, f32[8,512,128]{2,1,0:T(8,128)}, f32[512,128]{1,0:T(8,128)}) custom-call(bf16[1024,2048]{1,0:T(8,128)(2,1)} %prenorm.1.lat_in, bf16[128,2048]{1,0:T(8,128)(2,1)} %collective-permute-done.before_in, bf16[128,2048]{1,0:T(8,128)(2,1)} %collective-permute-done.1.after_in, bf16[2048,512]{1,0:T(8,128)(2,1)} %wq_in.1, ...), custom_call_target="tpu_custom_call" | custom-call | flops 4026531840 | bytes 7340032 | tf_op jit(solution)/shard_map/pallas_call | solution.py:365
  84.7 1.6 %copy-done = f32[8,512,128]{2,1,0:T(8,128)S(1)} copy-done((f32[8,512,128]{2,1,0:T(8,128)S(1)}, f32[8,512,128]{2,1,0:T(8,128)}, u32[]{:S(2)}) %copy-start) | copy-done | bytes 2097176
  86.2 1.2 %copy-done.1 = bf16[8,512,128]{2,1,0:T(8,128)(2,1)S(1)} copy-done((bf16[8,512,128]{2,1,0:T(8,128)(2,1)S(1)}, bf16[8,512,128]{2,1,0:T(8,128)(2,1)}, u32[]{:S(2)}) %copy-start.1) | copy-done | bytes 1048600
  88.4 2.3 %shard_map.152 = bf16[256,512]{1,0:T(8,128)(2,1)S(1)} custom-call(bf16[8,512,128]{2,1,0:T(8,128)(2,1)S(1)} %copy-done.1, f32[8,512,128]{2,1,0:T(8,128)S(1)} %copy-done, f32[512,128]{1,0:T(8,128)S(1)} %copy-done.2, bf16[768,256]{1,0:T(8,128)(2,1)S(1)} %bitcast.13, f32[1,4]{1,0:T(1,128)S(1)} %bitcast.19), custom_call_target="tpu_custom_call" | custom-call | flops 402653184 | bytes 2097152 | tf_op jit(solution)/shard_map/pallas_call | solution.py:365
  91.2 2.3 %shard_map.151 = bf16[256,512]{1,0:T(8,128)(2,1)S(1)} custom-call(bf16[8,512,128]{2,1,0:T(8,128)(2,1)S(1)} %copy-done.1, f32[8,512,128]{2,1,0:T(8,128)S(1)} %copy-done, f32[512,128]{1,0:T(8,128)S(1)} %copy-done.2, bf16[768,256]{1,0:T(8,128)(2,1)S(1)} %bitcast.14, f32[1,4]{1,0:T(1,128)S(1)} %bitcast.20), custom_call_target="tpu_custom_call" | custom-call | flops 402653184 | bytes 2097152 | tf_op jit(solution)/shard_map/pallas_call | solution.py:365
  93.6 2.3 %shard_map.150 = bf16[256,512]{1,0:T(8,128)(2,1)S(1)} custom-call(bf16[8,512,128]{2,1,0:T(8,128)(2,1)S(1)} %copy-done.1, f32[8,512,128]{2,1,0:T(8,128)S(1)} %copy-done, f32[512,128]{1,0:T(8,128)S(1)} %copy-done.2, bf16[768,256]{1,0:T(8,128)(2,1)S(1)} %bitcast.15, f32[1,4]{1,0:T(1,128)S(1)} %bitcast.21), custom_call_target="tpu_custom_call" | custom-call | flops 402653184 | bytes 2097152 | tf_op jit(solution)/shard_map/pallas_call | solution.py:365
  96.0 4.0 %collective-permute-done.4.a3_ref = bf16[256,512]{1,0:T(8,128)(2,1)S(1)} collective-permute-done((bf16[256,512]{1,0:T(8,128)(2,1)S(1)}, bf16[256,512]{1,0:T(8,128)(2,1)S(1)}, u32[]{:S(2)}, u32[]{:S(2)}) %collective-permute-start.4) | collective-permute-done | bytes 262176 | tf_op jit(solution)/shard_map/ppermute | solution.py:354
  100.0 2.3 %shard_map.149.a0_ref = bf16[256,512]{1,0:T(8,128)(2,1)S(1)} custom-call(bf16[8,512,128]{2,1,0:T(8,128)(2,1)S(1)} %copy-done.1, f32[8,512,128]{2,1,0:T(8,128)S(1)} %copy-done, f32[512,128]{1,0:T(8,128)S(1)} %copy-done.2, bf16[768,256]{1,0:T(8,128)(2,1)S(1)} %bitcast.16, f32[1,4]{1,0:T(1,128)S(1)} %bitcast.22), custom_call_target="tpu_custom_call" | custom-call | flops 402653184 | bytes 2097152 | tf_op jit(solution)/shard_map/pallas_call | solution.py:365
  103.0 1.3 %collective-permute-done.3.a2_ref = bf16[256,512]{1,0:T(8,128)(2,1)S(1)} collective-permute-done((bf16[256,512]{1,0:T(8,128)(2,1)S(1)}, bf16[256,512]{1,0:T(8,128)(2,1)S(1)}, u32[]{:S(2)}, u32[]{:S(2)}) %collective-permute-start.3) | collective-permute-done | bytes 262176 | tf_op jit(solution)/shard_map/ppermute | solution.py:354
  104.3 4.7 %collective-permute-done.2.a1_ref = bf16[256,512]{1,0:T(8,128)(2,1)S(1)} collective-permute-done((bf16[256,512]{1,0:T(8,128)(2,1)S(1)}, bf16[256,512]{1,0:T(8,128)(2,1)S(1)}, u32[]{:S(2)}, u32[]{:S(2)}) %collective-permute-start.2) | collective-permute-done | bytes 262176 | tf_op jit(solution)/shard_map/ppermute | solution.py:354
  109.8 6.8 %shard_map.153 = bf16[256,2048]{1,0:T(8,128)(2,1)} custom-call(f32[8,2048]{1,0:T(8,128)} %copy-done.7, bf16[256,512]{1,0:T(8,128)(2,1)} %copy-done.3, bf16[256,512]{1,0:T(8,128)(2,1)} %copy-done.15, bf16[256,512]{1,0:T(8,128)(2,1)} %copy-done.14, bf16[256,512]{1,0:T(8,128)(2,1)} %copy-done.13, bf16[512,2048]{1,0:T(8,128)(2,1)} %w0_in.1, ...), custom_call_target="tpu_custom_call" | custom-call | flops 2147483648 | bytes 8388608 | tf_op jit(solution)/shard_map/pallas_call | solution.py:365
  (53 shorter events, 7.5 us)
Async XLA Ops:
  1.8 14.9 %all-to-all-start = ((bf16[16,24,128]{2,1,0:T(8,128)(2,1)}), bf16[16,24,128]{2,1,0:T(8,128)(2,1)S(1)}, u32[]{:S(2)}, u32[]{:S(2)}) async-start(bf16[16,24,128]{2,1,0:T(8,128)(2,1)} %shard_map.145), calls=%async_computation | async-start | bytes 196608 | tf_op jit(solution)/shard_map/all_to_all | solution.py:397
  8.9 27.5 %copy-start.4 = (bf16[2048,128]{1,0:T(8,128)(2,1)S(1)}, bf16[2048,128]{1,0:T(8,128)(2,1)}, u32[]{:S(2)}) copy-start(bf16[2048,128]{1,0:T(8,128)(2,1)} %wk_in.1) | copy-start | bytes 1572868
  8.9 27.5 %copy-start.5 = (bf16[2048,128]{1,0:T(8,128)(2,1)S(1)}, bf16[2048,128]{1,0:T(8,128)(2,1)}, u32[]{:S(2)}) copy-start(bf16[2048,128]{1,0:T(8,128)(2,1)} %wv_in.1) | copy-start | bytes 1572868
  8.9 27.5 %copy-start.6 = (bf16[1,24,2048]{2,1,0:T(8,128)(2,1)S(1)}, bf16[1,24,2048]{2,1,0:T(8,128)(2,1)}, u32[]{:S(2)}) copy-start(bf16[1,24,2048]{2,1,0:T(8,128)(2,1)} %param.16) | copy-start | bytes 294916
  8.9 27.5 %copy-start.8 = (f32[2048]{0:T(1024)S(1)}, f32[2048]{0:T(1024)}, u32[]{:S(2)}) copy-start(f32[2048]{0:T(1024)} %param.19) | copy-start | bytes 24580
  8.9 27.5 %copy-start.10 = (f32[128]{0:T(128)S(1)}, f32[128]{0:T(128)}, u32[]{:S(2)}) copy-start(f32[128]{0:T(128)} %param.28) | copy-start | bytes 1540
  11.3 47.8 %collective-permute-start.7 = (bf16[512,1024]{1,0:T(8,128)(2,1)}, bf16[512,1024]{1,0:T(8,128)(2,1)S(1)}, u32[]{:S(2)}, u32[]{:S(2)}) collective-permute-start(bf16[512,1024]{1,0:T(8,128)(2,1)} %constant_dynamic-slice_fusion), channel_id=1, source_target_pairs={{0,6},{2,0},{4,2},{6,4},{1,7},{3,1},{5,3},{7,5},{8,14},{10,8},{12,... | collective-permute-start | bytes 3145736 | tf_op jit(solution)/shard_map/ppermute | solution.py:354
  14.4 48.0 %collective-permute-start.5 = (bf16[512,1024]{1,0:T(8,128)(2,1)}, bf16[512,1024]{1,0:T(8,128)(2,1)S(1)}, u32[]{:S(2)}, u32[]{:S(2)}) collective-permute-start(bf16[512,1024]{1,0:T(8,128)(2,1)} %constant_dynamic-slice_fusion), channel_id=1, source_target_pairs={{0,2},{2,4},{4,6},{6,0},{1,3},{3,5},{5,7},{7,1},{8,10},{10,12},{12... | collective-permute-start | bytes 3145736 | tf_op jit(solution)/shard_map/ppermute | solution.py:354
  14.4 48.0 %collective-permute-start.6 = (bf16[512,1024]{1,0:T(8,128)(2,1)}, bf16[512,1024]{1,0:T(8,128)(2,1)}, u32[]{:S(2)}, u32[]{:S(2)}) collective-permute-start(bf16[512,1024]{1,0:T(8,128)(2,1)} %constant_dynamic-slice_fusion), channel_id=1, source_target_pairs={{0,4},{2,6},{4,0},{6,2},{1,5},{3,7},{5,1},{7,3},{8,12},{10,14},{12... | collective-permute-start | bytes 3145736 | tf_op jit(solution)/shard_map/ppermute | solution.py:354
  17.4 18.9 %all-to-all-start.1 = ((bf16[8,80,128]{2,1,0:T(8,128)(2,1)}), bf16[8,80,128]{2,1,0:T(8,128)(2,1)S(1)}, u32[]{:S(2)}, u32[]{:S(2)}) async-start(bf16[8,80,128]{2,1,0:T(8,128)(2,1)} %shard_map.146), calls=%async_computation.1 | async-start | bytes 327680 | tf_op jit(solution)/shard_map/all_to_all | solution.py:399
  28.3 41.1 %collective-permute-start = (bf16[128,2048]{1,0:T(8,128)(2,1)}, bf16[128,2048]{1,0:T(8,128)(2,1)}, u32[]{:S(2)}, u32[]{:S(2)}) collective-permute-start(bf16[128,2048]{1,0:T(8,128)(2,1)} %get-tuple-element.16), channel_id=1, source_target_pairs={{0,8},{8,16},{16,24},{24,32},{32,40},{40,48},{48,56},{56,64},{64,7... | collective-permute-start | bytes 1572872 | tf_op jit(solution)/shard_map/ppermute | solution.py:403
  31.7 37.7 %collective-permute-start.1 = (bf16[128,2048]{1,0:T(8,128)(2,1)}, bf16[128,2048]{1,0:T(8,128)(2,1)}, u32[]{:S(2)}, u32[]{:S(2)}) collective-permute-start(bf16[128,2048]{1,0:T(8,128)(2,1)} %get-tuple-element.15), channel_id=1, source_target_pairs={{8,0},{16,8},{24,16},{32,24},{40,32},{48,40},{56,48},{64,56},{72,6... | collective-permute-start | bytes 1572872 | tf_op jit(solution)/shard_map/ppermute | solution.py:404
  38.2 46.5 %all-to-all-start.2 = ((bf16[32,24,256]{2,1,0:T(8,128)(2,1)}), bf16[32,24,256]{2,1,0:T(8,128)(2,1)S(1)}, u32[]{:S(2)}, u32[]{:S(2)}) async-start(bf16[32,24,256]{2,1,0:T(8,128)(2,1)} %get-tuple-element.14), calls=%async_computation.2 | async-start | bytes 786432 | tf_op jit(solution)/shard_map/all_to_all | solution.py:445
  59.1 10.4 %copy-start.11 = (bf16[512,1024]{1,0:T(8,128)(2,1)}, bf16[512,1024]{1,0:T(8,128)(2,1)S(1)}, u32[]{:S(2)}) copy-start(bf16[512,1024]{1,0:T(8,128)(2,1)S(1)} %collective-permute-done.7.m3_in) | copy-start | bytes 3145732
  59.1 50.0 %collective-permute-start.10 = (bf16[512,1024]{1,0:T(8,128)(2,1)S(1)}, bf16[512,1024]{1,0:T(8,128)(2,1)}, u32[]{:S(2)}, u32[]{:S(2)}) collective-permute-start(bf16[512,1024]{1,0:T(8,128)(2,1)S(1)} %collective-permute-done.7.m3_in), channel_id=1, source_target_pairs={{0,1},{1,0},{2,3},{3,2},{4,5},{5,4},{6,7},{7,6},{8,9},{9,8},{10,11... | collective-permute-start | bytes 3145736 | tf_op jit(solution)/shard_map/ppermute | solution.py:354
  62.4 7.0 %copy-start.12 = (bf16[512,1024]{1,0:T(8,128)(2,1)}, bf16[512,1024]{1,0:T(8,128)(2,1)S(1)}, u32[]{:S(2)}) copy-start(bf16[512,1024]{1,0:T(8,128)(2,1)S(1)} %collective-permute-done.5.m1_in) | copy-start | bytes 3145732
  62.4 46.7 %collective-permute-start.8 = (bf16[512,1024]{1,0:T(8,128)(2,1)S(1)}, bf16[512,1024]{1,0:T(8,128)(2,1)}, u32[]{:S(2)}, u32[]{:S(2)}) collective-permute-start(bf16[512,1024]{1,0:T(8,128)(2,1)S(1)} %collective-permute-done.5.m1_in), channel_id=1, source_target_pairs={{0,1},{1,0},{2,3},{3,2},{4,5},{5,4},{6,7},{7,6},{8,9},{9,8},{10,11... | collective-permute-start | bytes 3145736 | tf_op jit(solution)/shard_map/ppermute | solution.py:354
  62.4 47.4 %collective-permute-start.9 = (bf16[512,1024]{1,0:T(8,128)(2,1)}, bf16[512,1024]{1,0:T(8,128)(2,1)}, u32[]{:S(2)}, u32[]{:S(2)}) collective-permute-start(bf16[512,1024]{1,0:T(8,128)(2,1)} %collective-permute-done.6.m2_in), channel_id=1, source_target_pairs={{0,1},{1,0},{2,3},{3,2},{4,5},{5,4},{6,7},{7,6},{8,9},{9,8},{10,11... | collective-permute-start | bytes 3145736 | tf_op jit(solution)/shard_map/ppermute | solution.py:354
  69.4 15.2 %copy-start.9 = (f32[4]{0:T(128)S(1)}, f32[4]{0:T(128)}, u32[]{:S(2)}) copy-start(f32[4]{0:T(128)} %param.29) | copy-start | bytes 52
  90.8 9.2 %collective-permute-start.4 = (bf16[256,512]{1,0:T(8,128)(2,1)S(1)}, bf16[256,512]{1,0:T(8,128)(2,1)S(1)}, u32[]{:S(2)}, u32[]{:S(2)}) collective-permute-start(bf16[256,512]{1,0:T(8,128)(2,1)S(1)} %shard_map.152), channel_id=1, source_target_pairs={{0,6},{2,0},{4,2},{6,4},{1,7},{3,1},{5,3},{7,5},{8,14},{10,8},{12,... | collective-permute-start | bytes 786440 | tf_op jit(solution)/shard_map/ppermute | solution.py:354
  93.6 10.7 %collective-permute-start.3 = (bf16[256,512]{1,0:T(8,128)(2,1)S(1)}, bf16[256,512]{1,0:T(8,128)(2,1)S(1)}, u32[]{:S(2)}, u32[]{:S(2)}) collective-permute-start(bf16[256,512]{1,0:T(8,128)(2,1)S(1)} %shard_map.151), channel_id=1, source_target_pairs={{0,4},{2,6},{4,0},{6,2},{1,5},{3,7},{5,1},{7,3},{8,12},{10,14},{12... | collective-permute-start | bytes 786440 | tf_op jit(solution)/shard_map/ppermute | solution.py:354
  100.0 9.8 %copy-start.13 = (bf16[256,512]{1,0:T(8,128)(2,1)}, bf16[256,512]{1,0:T(8,128)(2,1)S(1)}, u32[]{:S(2)}) copy-start(bf16[256,512]{1,0:T(8,128)(2,1)S(1)} %collective-permute-done.4.a3_ref) | copy-start | bytes 786436
  100.0 9.1 %collective-permute-start.2 = (bf16[256,512]{1,0:T(8,128)(2,1)S(1)}, bf16[256,512]{1,0:T(8,128)(2,1)S(1)}, u32[]{:S(2)}, u32[]{:S(2)}) collective-permute-start(bf16[256,512]{1,0:T(8,128)(2,1)S(1)} %shard_map.150), channel_id=1, source_target_pairs={{0,2},{2,4},{4,6},{6,0},{1,3},{3,5},{5,7},{7,1},{8,10},{10,12},{12... | collective-permute-start | bytes 786440 | tf_op jit(solution)/shard_map/ppermute | solution.py:354
  104.3 5.5 %copy-start.14 = (bf16[256,512]{1,0:T(8,128)(2,1)}, bf16[256,512]{1,0:T(8,128)(2,1)S(1)}, u32[]{:S(2)}) copy-start(bf16[256,512]{1,0:T(8,128)(2,1)S(1)} %collective-permute-done.3.a2_ref) | copy-start | bytes 786436
  (6 other events, 5.8 us)

commit v3 on v2

--- a/solution.py
+++ b/solution.py
@@ -122,15 +122,21 @@
     return v * cosine + swapped * sine
 
 
-def prenorm_kernel(lat_ref, out_ref):
-    step = 64
-
-    def body(i, carry):
-        at = pl.ds(pl.multiple_of(i * step, step), step)
-        out_ref[at, :] = normed(lat_ref[at, :]).astype(BF16)
-        return carry
-
-    lax.fori_loop(0, lat_ref.shape[0] // step, body, 0)
+def stage_kernel(w_in, lat_in, half_ref, first_ref, last_ref, own_ref, sems):
+    tok = lat_in.shape[0]
+    start = pl.multiple_of(lax.axis_index("dp") * (D // 2), D // 2)
+    sub = own_ref.shape[0]
+    first = pl.multiple_of(lax.axis_index("tp") * sub, sub)
+    moves = [
+        pltpu.make_async_copy(w_in.at[:, pl.ds(start, D // 2)], half_ref, sems.at[0]),
+        pltpu.make_async_copy(lat_in.at[:WINDOW, :], first_ref, sems.at[1]),
+        pltpu.make_async_copy(lat_in.at[tok - WINDOW :, :], last_ref, sems.at[2]),
+        pltpu.make_async_copy(lat_in.at[pl.ds(first, sub), :], own_ref, sems.at[3]),
+    ]
+    for move in moves:
+        move.start()
+    for move in moves:
+        move.wait()
 
 
 def context_kernel(mod_ref, ctx_ref, wk_ref, wv_ref, gain_ref, kgain_ref, kv_ref, vec_ref):
@@ -149,7 +155,8 @@
 def qkv_kernel(
     lat_in, before_in, after_in, wq_in, wk_in, wv_in,
     vec_ref, qgain_ref, kgain_ref, rcos_ref, rsin_ref, ccos_ref, csin_ref,
-    q_ref, near_ref, sum_ref, lat_ref, halo_ref, wq_ref, wk_ref, wv_ref, k_ref, v_ref, sems,
+    q_ref, near_ref, sum_ref,
+    lat_ref, wq_ref, wk_ref, wv_ref, k_ref, v_ref, even_ref, odd_ref, sems,
 ):
     step = 256
     tok = lat_in.shape[0]
@@ -157,57 +164,42 @@
     qgain = qgain_ref[...] * QUERY_SCALE
     kgain = kgain_ref[...]
 
-    def rows_move(i):
-        at = pl.ds(pl.multiple_of(i * step, step), step)
-        return pltpu.make_async_copy(lat_in.at[at, :], lat_ref.at[at, :], sems.at[i])
-
-    others = [
-        pltpu.make_async_copy(source, to, sems.at[steps + i])
-        for i, (source, to) in enumerate(
-            (
-                (wk_in, wk_ref), (wv_in, wv_ref), (wq_in, wq_ref),
-                (before_in, halo_ref.at[:WINDOW]), (after_in, halo_ref.at[WINDOW:]),
-            )
-        )
+    def at(i, size=step):
+        return pl.ds(pl.multiple_of(i * step, step), size)
+
+    sources = [(lat_in.at[at(i), :], lat_ref.at[at(i), :]) for i in range(steps)]
+    sources += [
+        (before_in, lat_ref.at[pl.ds(tok, WINDOW), :]),
+        (after_in, lat_ref.at[pl.ds(tok + WINDOW, WINDOW), :]),
+        (wk_in, wk_ref), (wv_in, wv_ref), (wq_in, wq_ref),
     ]
-    others[0].start()
-    others[1].start()
-    rows_move(0).start()
-    others[2].start()
-    for i in range(1, steps):
-        rows_move(i).start()
-    others[3].start()
-    others[4].start()
-
-    def table(group):
-        cosine = rcos_ref[pl.ds(group, 1), :] + ccos_ref[...]
-        sine = rsin_ref[pl.ds(group, 1), :] + csin_ref[...]
-        return cosine, sine
-
-    def tables(first, count):
-        both = [table(first + g) for g in range(count)]
-        return jnp.concatenate([c for c, _ in both]), jnp.concatenate([s for _, s in both])
-
-    def modulated(values):
-        return (values * vec_ref[0:1, :] + vec_ref[1:2, :]).astype(BF16)
-
-    others[0].wait()
-    others[1].wait()
-
-    def body(i, carry):
-        @pl.when(i == 0)
-        def _():
-            others[2].wait()
-
-        rows_move(i).wait()
-        at = pl.ds(pl.multiple_of(i * step, step), step)
+    moves = [
+        pltpu.make_async_copy(source, to, sems.at[i]) for i, (source, to) in enumerate(sources)
+    ]
+    for i in (0, steps + 2, steps + 3, steps + 4, *range(1, steps + 2)):
+        moves[i].start()
+
+    def tables(groups):
+        cosines = [rcos_ref[pl.ds(g, 1), :] + ccos_ref[...] for g in groups]
+        sines = [rsin_ref[pl.ds(g, 1), :] + csin_ref[...] for g in groups]
+        return jnp.concatenate(cosines), jnp.concatenate(sines)
+
+    def fill(i, to):
+        values = lat_ref[at(i), :].astype(F32)
+        inverse = lax.rsqrt(jnp.mean(values * values, axis=-1, keepdims=True) + NORM_EPSILON)
+        to[...] = (values * inverse * vec_ref[0:1, :] + vec_ref[1:2, :]).astype(BF16)
+
+    def keys_of(rows_ref, cosine, sine):
+        keys = jnp.dot(rows_ref[...], wk_ref[...], preferred_element_type=F32)
+        keys = rotated(head_norm(keys, kgain), cosine, sine).astype(BF16)
+        return keys, jnp.dot(rows_ref[...], wv_ref[...], preferred_element_type=F32).astype(BF16)
+
+    def project(i, rows_ref):
         to = pl.ds(pl.multiple_of(i * step + WINDOW, WINDOW), step)
-        rows = modulated(lat_ref[at, :].astype(F32))
-        cosine, sine = tables(2 + i * (step // GRID_W), step // GRID_W)
-        keys = jnp.dot(rows, wk_ref[...], preferred_element_type=F32)
-        queries = jnp.dot(rows, wq_ref[...], preferred_element_type=F32)
-        k_ref[to, :] = rotated(head_norm(keys, kgain), cosine, sine).astype(BF16)
-        v_ref[to, :] = jnp.dot(rows, wv_ref[...], preferred_element_type=F32).astype(BF16)
+        first = 2 + i * (step // GRID_W)
+        cosine, sine = tables([first + g for g in range(step // GRID_W)])
+        queries = jnp.dot(rows_ref[...], wq_ref[...], preferred_element_type=F32)
+        k_ref[to, :], v_ref[to, :] = keys_of(rows_ref, cosine, sine)
         for h in range(4):
             head = slice(h * HEAD_DIM, (h + 1) * HEAD_DIM)
             turned = rotated(head_norm(queries[:, head], qgain), cosine, sine).astype(BF16)
@@ -215,23 +207,39 @@
                 q_ref[i * 2 + half, h * WINDOW : (h + 1) * WINDOW, :] = turned[
                     half * WINDOW : (half + 1) * WINDOW
                 ]
+
+    moves[0].wait()
+    fill(0, even_ref)
+    for i in range(steps + 2, steps + 5):
+        moves[i].wait()
+
+    def wait_rows(i):
+        pltpu.make_async_copy(lat_in.at[at(0), :], lat_ref.at[at(i), :], sems.at[i]).wait()
+
+    def body(j, carry):
+        wait_rows(2 * j + 1)
+
+        @pl.when(j == 0)
+        def _():
+            wait_rows(2)
+
+        @pl.when(j == 1)
+        def _():
+            moves[steps].wait()
+            moves[steps + 1].wait()
+
+        fill(2 * j + 1, odd_ref)
+        project(2 * j, even_ref)
+        fill(2 * j + 2, even_ref)
+        project(2 * j + 1, odd_ref)
         return carry
 
-    lax.fori_loop(0, steps, body, 0)
-    others[3].wait()
-    others[4].wait()
-
-    def halo(i, carry):
-        at = pl.ds(pl.multiple_of(i * WINDOW, WINDOW), WINDOW)
-        to = pl.ds(pl.multiple_of(i * (tok + WINDOW), WINDOW), WINDOW)
-        rows = modulated(normed(halo_ref[at, :]))
-        cosine, sine = tables(i * ((tok + WINDOW) // GRID_W), WINDOW // GRID_W)
-        keys = head_norm(jnp.dot(rows, wk_ref[...], preferred_element_type=F32), kgain)
-        k_ref[to, :] = rotated(keys, cosine, sine).astype(BF16)
-        v_ref[to, :] = jnp.dot(rows, wv_ref[...], preferred_element_type=F32).astype(BF16)
-        return carry
-
-    lax.fori_loop(0, 2, halo, 0)
+    lax.fori_loop(0, steps // 2, body, 0)
+    beyond = (tok + WINDOW) // GRID_W
+    keys, values = keys_of(even_ref, *tables([0, 1, beyond, beyond + 1]))
+    for ref, rows in ((k_ref, keys), (v_ref, values)):
+        ref[:WINDOW, :] = rows[:WINDOW]
+        ref[tok + WINDOW :, :] = rows[WINDOW:]
     local_pass(q_ref, k_ref, v_ref, near_ref, sum_ref)
 
 
@@ -270,7 +278,8 @@
         )
         total = jnp.sum(lanes_summed(local), axis=-1, keepdims=True)
         sum_ref[...] = jnp.where(key_at == block, total, sum_ref[...])
-        out_ref[block] = jnp.dot(local.astype(BF16), v_ref[near, :], preferred_element_type=F32)
+        mixed = jnp.dot(local.astype(BF16), v_ref[near, :], preferred_element_type=F32)
+        out_ref[block] = mixed.astype(BF16)
         return carry
 
     lax.fori_loop(0, blocks, body, 0)
@@ -291,7 +300,7 @@
         far = jnp.exp2(contract_last(q_ref[block], ctx_ref[:, :head]))
         near_sum = jnp.where(lane == block, sum_ref[...], 0.0)
         total = jnp.sum(lanes_summed(far) + near_sum, axis=-1, keepdims=True) + sink
-        mixed = near_ref[block] + jnp.dot(
+        mixed = near_ref[block].astype(F32) + jnp.dot(
             far.astype(BF16), ctx_ref[:, head:], preferred_element_type=F32
         )
         mixed = (mixed * (1.0 / total)).astype(BF16)
@@ -303,50 +312,36 @@
 
 
 def project_kernel(
-    vec_ref, a0_ref, a1_ref, a2_ref, a3_ref, w0_in,
-    m1_in, m2_in, m3_in, o1_in, o2_in, o3_in, lat_in, out_ref,
-    w_ref, lat_ref, done_ref, sems,
+    vec_ref, a0_ref, a1_ref, a2_ref, a3_ref, w0_ref,
+    m1_ref, m2_ref, m3_ref, o1_ref, o2_ref, o3_ref, lat_ref, out_ref, done_ref, sems,
 ):
     dp = lax.axis_index("dp")
     col = 512
-    deep = 4 * HEAD_DIM
-    sub = lat_ref.shape[0]
-    first = pl.multiple_of(lax.axis_index("tp") * sub, sub)
-    rows_move = pltpu.make_async_copy(lat_in.at[pl.ds(first, sub), :], lat_ref, sems.at[16])
-    halves = (dp, 1 - dp)
-
-    def columns(slot):
-        return pl.multiple_of(halves[slot // 2] * (D // 2) + (slot % 2) * col, col)
-
-    def moves(slot):
-        later = slice((slot % 2) * col, (slot % 2 + 1) * col)
-        group = (m1_in, m2_in, m3_in) if slot < 2 else (o1_in, o2_in, o3_in)
-        sources = [w0_in.at[:, pl.ds(columns(slot), col)]] + [w.at[:, later] for w in group]
-        return [
-            pltpu.make_async_copy(
-                source, w_ref.at[slot, pl.ds(s * deep, deep), :], sems.at[slot * 4 + s]
-            )
-            for s, source in enumerate(sources)
-        ]
-
+
+    def copy(slot, column):
+        return pltpu.make_async_copy(
+            done_ref.at[slot], out_ref.at[:, pl.ds(column, col)], sems.at[slot]
+        )
+
+    for part, weights in enumerate(((m1_ref, m2_ref, m3_ref), (o1_ref, o2_ref, o3_ref))):
+        half = dp if part == 0 else 1 - dp
+
+        def body(j, carry, part=part, weights=weights, half=half):
+            column = pl.multiple_of(half * (D // 2) + j * col, col)
+            wide = pl.ds(column, col)
+            sub = pl.ds(pl.multiple_of(j * col, col), col)
+            mixed = jnp.dot(a0_ref[...], w0_ref[:, wide], preferred_element_type=F32)
+            for a, w in zip((a1_ref, a2_ref, a3_ref), weights):
+                mixed = mixed + jnp.dot(a[...], w[:, sub], preferred_element_type=F32)
+            slot = part * 2 + j
+            result = lat_ref[:, wide].astype(F32) + vec_ref[2:3, wide] * mixed
+            done_ref[slot] = result.astype(BF16)
+            copy(slot, column).start()
+            return carry
+
+        lax.fori_loop(0, 2, body, 0)
     for slot in range(4):
-        for move in moves(slot):
-            move.start()
-        if slot == 0:
-            rows_move.start()
-    left = jnp.concatenate([a0_ref[...], a1_ref[...], a2_ref[...], a3_ref[...]], axis=1)
-    rows_move.wait()
-    for slot in range(4):
-        for move in moves(slot):
-            move.wait()
-        wide = pl.ds(columns(slot), col)
-        mixed = jnp.dot(left, w_ref[slot], preferred_element_type=F32)
-        result = lat_ref[:, wide].astype(F32) + vec_ref[2:3, wide] * mixed
-        done_ref[slot] = result.astype(BF16)
-        pltpu.make_async_copy(done_ref.at[slot], out_ref.at[:, wide], sems.at[17 + slot]).start()
-    for slot in range(4):
-        wide = pl.ds(columns(slot), col)
-        pltpu.make_async_copy(done_ref.at[slot], out_ref.at[:, wide], sems.at[17 + slot]).wait()
+        copy(slot, 0).wait()
 
 
 def shifted(array, axis, by):
@@ -381,7 +376,6 @@
     tok = lat.shape[0]
     sub = tok // NX
     sp = sp_index()
-    dp = lax.axis_index("dp")
     width = 4 * HEAD_DIM
 
     part = call(
@@ -398,12 +392,17 @@
     part = call(resum_kernel, [((NZ, NX * VECS, 128), BF16)], (part,), cost(1 << 20, 1 << 18), 4)
     mod = lax.all_to_all(part, "z", 0, 0, tiled=True)
 
+    half, first_rows, last_rows, own = call(
+        stage_kernel,
+        [((width, D // 2), BF16), ((WINDOW, D), BF16), ((WINDOW, D), BF16), ((sub, D), BF16)],
+        (w_out, lat), cost(1 << 24, 4 << 20), 60,
+        scratch=[pltpu.SemaphoreType.DMA((4,))], in_specs=[HBM] * 2,
+    )
     peers = NZ * NY
     up = [(i, i + 1) for i in range(peers - 1)]
-    before = lax.ppermute(lat[tok - WINDOW :], SP, up)
-    after = lax.ppermute(lat[:WINDOW], SP, [(j, i) for i, j in up])
-
-    half = lax.dynamic_slice_in_dim(w_out, dp * (D // 2), D // 2, 1)
+    before = lax.ppermute(last_rows, SP, up)
+    after = lax.ppermute(first_rows, SP, [(j, i) for i, j in up])
+
     mine, other = {}, {}
     for s in (1, 3, 2):
         mine[s] = shifted(half, "tp", s)
@@ -422,17 +421,6 @@
     col_cos = jnp.where(by_row, 0.0, jnp.cos(col_angle))
     col_sin = jnp.where(by_row, 0.0, jnp.sin(col_angle) * sign)
 
-    block = pl.BlockSpec((256, D), lambda i: (i, 0))
-    scaled = pl.pallas_call(
-        prenorm_kernel,
-        grid=(tok // 256,),
-        in_specs=[block],
-        out_specs=block,
-        out_shape=jax.ShapeDtypeStruct((tok, D), BF16),
-        compiler_params=params(60),
-        cost_estimate=cost(tok * D * 4, tok * D * 4),
-        name="prenorm",
-    )(lat)
     rows = tok + 2 * WINDOW
     gain, qgain, kgain = norm_gain[None], q_gain[None], k_gain[None]
     n_ctx = context.shape[1]
@@ -440,7 +428,7 @@
         context_kernel,
         [((peers, n_ctx, 2 * HEAD_DIM), BF16), ((8, D), F32)],
         (mod, context[0], w_key, w_value, gain, kgain),
-        cost(2 * n_ctx * D * 256, D * 512), 4,
+        cost(2 * n_ctx * D * 256, D * 512), 63,
     )
     ctx_all = lax.all_to_all(ctx_kv, SP, 0, 0, tiled=True).reshape(-1, 2 * HEAD_DIM)
 
@@ -448,18 +436,19 @@
         qkv_kernel,
         [
             ((tok // WINDOW, 4 * WINDOW, HEAD_DIM), BF16),
-            ((tok // WINDOW, 4 * WINDOW, HEAD_DIM), F32), ((4 * WINDOW, 128), F32),
+            ((tok // WINDOW, 4 * WINDOW, HEAD_DIM), BF16), ((4 * WINDOW, 128), F32),
         ],
         (
-            scaled, before, after, w_query, w_key, w_value, vec, qgain, kgain,
+            lat, before, after, w_query, w_key, w_value, vec, qgain, kgain,
             row_cos, row_sin, col_cos, col_sin,
         ),
         cost(2 * tok * D * 768 + 16 * tok * 384 * HEAD_DIM, tok * D * 2 + D * 768 * 2), 60,
         scratch=[
-            pltpu.VMEM((tok, D), BF16), pltpu.VMEM((2 * WINDOW, D), BF16),
-            pltpu.VMEM((D, width), BF16), pltpu.VMEM((D, HEAD_DIM), BF16),
-            pltpu.VMEM((D, HEAD_DIM), BF16), pltpu.VMEM((rows, HEAD_DIM), BF16),
-            pltpu.VMEM((rows, HEAD_DIM), BF16), pltpu.SemaphoreType.DMA((tok // 256 + 5,)),
+            pltpu.VMEM((rows, D), BF16), pltpu.VMEM((D, width), BF16),
+            pltpu.VMEM((D, HEAD_DIM), BF16), pltpu.VMEM((D, HEAD_DIM), BF16),
+            pltpu.VMEM((rows, HEAD_DIM), BF16), pltpu.VMEM((rows, HEAD_DIM), BF16),
+            pltpu.VMEM((256, D), BF16), pltpu.VMEM((256, D), BF16),
+            pltpu.SemaphoreType.DMA((tok // 256 + 5,)),
         ],
         in_specs=[HBM] * 6 + [VMEM] * 7,
     )
@@ -481,14 +470,12 @@
         project_kernel, [((sub, D), BF16)],
         (
             vec, arrived[0], arrived[1], arrived[2], arrived[3], w_out,
-            mine[1], mine[2], mine[3], other[1], other[2], other[3], lat,
+            mine[1], mine[2], mine[3], other[1], other[2], other[3], own,
         ),
-        cost(2 * sub * D * D, D * D * 2), 61,
+        cost(2 * sub * D * D, D * D * 2), 8,
         scratch=[
-            pltpu.VMEM((4, D, 512), BF16), pltpu.VMEM((sub, D), BF16),
-            pltpu.VMEM((4, sub, 512), BF16), pltpu.SemaphoreType.DMA((21,)),
+            pltpu.VMEM((4, sub, 512), BF16), pltpu.SemaphoreType.DMA((4,)),
         ],
-        in_specs=[VMEM] * 5 + [HBM] * 8,
         out_specs=HBM,
     )
     return result[None]

time: 117 us -> 137 us (1.17)
  the two profiles are of different devices: /device:TPU:32 before, /device:TPU:120 now
where the time goes in v3:
time: 137 us
  blocking collectives  46 us (34%)
  Pallas kernels  38.3 us (28%)
  starting transfers between devices  35.1 us (26%)
  waiting for transfers between devices  11.5 us (8%)
  local copies, waits for them, and re-layouts  4.08 us (3%)
  other arithmetic  1.52 us (1%)
    all_to_all x1, blocking collectives, per_device(): part = lax.all_to_all(part, ('y', 'tp'), 0, 0, tiled=True)  46 us
    pallas_call x10, Pallas kernels, call(): pl.pallas_call(kernel, in_specs=in_specs or [VMEM] * len(args), out_specs...  38.3 us
    all_to_all x1, starting transfers between devices, per_device(): lax.all_to_all(ctx_kv, SP, 0, 0, tiled=True).reshape(-1, 2 * HEAD_DIM)  10 us
    ppermute x9, starting transfers between devices, shifted(): lax.ppermute(array, axis, [(i, (i + by) % peers) for i in range(peers)])  9.32 us
    ppermute x9, waiting for transfers between devices, shifted(): lax.ppermute(array, axis, [(i, (i + by) % peers) for i in range(peers)])  8.48 us
    all_to_all x1, starting transfers between devices, per_device(): mod = lax.all_to_all(part, 'z', 0, 0, tiled=True)  7.66 us
    ppermute x1, starting transfers between devices, per_device(): before = lax.ppermute(last_rows, SP, up)  6.19 us
    unnamed x16, local copies, waits for them, and re-layouts  4.08 us
  transfers between devices with their start and end apart: 13, of which 4 were waited for; matrix products, arithmetic and copies ran while one was open for 1% of the time, Pallas kernels for 21%

profile of v3, /device:TPU:120, one launch (start us, length us, event | category | flops | bytes accessed | tf_op | source)
XLA Modules:
  0.0 136.8 jit_solution(9381907054366595608)
XLA Ops:
  0.0 3.5 %shard_map.148 = (bf16[512,1024]{1,0:T(8,128)(2,1)}, bf16[128,2048]{1,0:T(8,128)(2,1)}, bf16[128,2048]{1,0:T(8,128)(2,1)}, bf16[256,2048]{1,0:T(8,128)(2,1)}) custom-call(bf16[512,2048]{1,0:T(8,128)(2,1)} %w0_ref.1, bf16[1024,2048]{1,0:T(8,128)(2,1)} %bitcast.17), custom_call_target="tpu_custom_call" | custom-call | flops 16777216 | bytes 4194304 | tf_op jit(solution)/shard_map/pallas_call | solution.py:360
  3.5 2.8 %collective-permute-start.7 = (bf16[512,1024]{1,0:T(8,128)(2,1)}, bf16[512,1024]{1,0:T(8,128)(2,1)}, u32[]{:S(2)}, u32[]{:S(2)}) collective-permute-start(bf16[512,1024]{1,0:T(8,128)(2,1)} %get-tuple-element.21), channel_id=1, source_target_pairs={{0,6},{2,0},{4,2},{6,4},{1,7},{3,1},{5,3},{7,5},{8,14},{10,8},{12,... | collective-permute-start | bytes 3145736 | tf_op jit(solution)/shard_map/ppermute | solution.py:349
  6.4 2.3 %collective-permute-start.6 = (bf16[512,1024]{1,0:T(8,128)(2,1)}, bf16[512,1024]{1,0:T(8,128)(2,1)}, u32[]{:S(2)}, u32[]{:S(2)}) collective-permute-start(bf16[512,1024]{1,0:T(8,128)(2,1)} %get-tuple-element.21), channel_id=1, source_target_pairs={{0,4},{2,6},{4,0},{6,2},{1,5},{3,7},{5,1},{7,3},{8,12},{10,14},{12... | collective-permute-start | bytes 3145736 | tf_op jit(solution)/shard_map/ppermute | solution.py:349
  8.7 1.8 %shard_map.145 = bf16[16,24,128]{2,1,0:T(8,128)(2,1)} custom-call(f32[1,2048]{1,0:T(1,128)} %cond_in.1, f32[1,2048]{1,0:T(1,128)} %bitcast.21, bf16[64,512]{1,0:T(8,128)(2,1)} %shift_in.1, bf16[64,512]{1,0:T(8,128)(2,1)} %scale_in.1, bf16[64,512]{1,0:T(8,128)(2,1)} %gate_in.1), custom_call_target="tpu_custom_call" | custom-call | flops 1048576 | bytes 262144 | tf_op jit(solution)/shard_map/pallas_call | solution.py:360
  10.5 46.0 %all_to_all.15.in_ref = bf16[16,24,128]{2,1,0:T(8,128)(2,1)S(1)} all-to-all(bf16[16,24,128]{2,1,0:T(8,128)(2,1)} %shard_map.145), channel_id=1, replica_groups=mesh['z'=8,'y'=4,'tp'=4,'dp'=2] {'y','tp'}, dimensions={0} | all-to-all | bytes 196608 | tf_op jit(solution)/shard_map/all_to_all | solution.py:391
  57.2 7.7 %all-to-all-start.1 = ((bf16[8,80,128]{2,1,0:T(8,128)(2,1)}), bf16[8,80,128]{2,1,0:T(8,128)(2,1)S(1)}, u32[]{:S(2)}, u32[]{:S(2)}) async-start(bf16[8,80,128]{2,1,0:T(8,128)(2,1)} %shard_map.146), calls=%async_computation.1 | async-start | bytes 327680 | tf_op jit(solution)/shard_map/all_to_all | solution.py:393
  64.8 6.2 %collective-permute-start = (bf16[128,2048]{1,0:T(8,128)(2,1)}, bf16[128,2048]{1,0:T(8,128)(2,1)}, u32[]{:S(2)}, u32[]{:S(2)}) collective-permute-start(bf16[128,2048]{1,0:T(8,128)(2,1)} %get-tuple-element.15), channel_id=1, source_target_pairs={{0,8},{8,16},{16,24},{24,32},{32,40},{40,48},{48,56},{56,64},{64,7... | collective-permute-start | bytes 1572872 | tf_op jit(solution)/shard_map/ppermute | solution.py:403
  71.0 1.9 %collective-permute-start.1 = (bf16[128,2048]{1,0:T(8,128)(2,1)}, bf16[128,2048]{1,0:T(8,128)(2,1)}, u32[]{:S(2)}, u32[]{:S(2)}) collective-permute-start(bf16[128,2048]{1,0:T(8,128)(2,1)} %get-tuple-element.16), channel_id=1, source_target_pairs={{8,0},{16,8},{24,16},{32,24},{40,32},{48,40},{56,48},{64,56},{72,6... | collective-permute-start | bytes 1572872 | tf_op jit(solution)/shard_map/ppermute | solution.py:404
  73.7 2.5 %shard_map.147 = (bf16[32,24,256]{2,1,0:T(8,128)(2,1)}, f32[8,2048]{1,0:T(8,128)}) custom-call(bf16[8,80,128]{2,1,0:T(8,128)(2,1)} %copy-done.7, bf16[24,2048]{1,0:T(8,128)(2,1)} %bitcast.19, bf16[2048,128]{1,0:T(8,128)(2,1)} %wk_in.1, bf16[2048,128]{1,0:T(8,128)(2,1)} %wv_in.1, f32[1,2048]{1,0:T(1,128)} %bitcast.20, f32[1,128]{1,0:T(1,128)} %bitcast.22), custom_call_target="tpu_custom_call" | custom-call | flops 25165824 | bytes 1048576 | tf_op jit(solution)/shard_map/pallas_call | solution.py:360
  76.1 10.0 %all-to-all-start.2 = ((bf16[32,24,256]{2,1,0:T(8,128)(2,1)}), bf16[32,24,256]{2,1,0:T(8,128)(2,1)S(1)}, u32[]{:S(2)}, u32[]{:S(2)}) async-start(bf16[32,24,256]{2,1,0:T(8,128)(2,1)} %get-tuple-element.20), calls=%async_computation.2 | async-start | bytes 786432 | tf_op jit(solution)/shard_map/all_to_all | solution.py:433
  88.4 3.0 %collective-permute-done.1.after_in = bf16[128,2048]{1,0:T(8,128)(2,1)} collective-permute-done((bf16[128,2048]{1,0:T(8,128)(2,1)}, bf16[128,2048]{1,0:T(8,128)(2,1)}, u32[]{:S(2)}, u32[]{:S(2)}) %collective-permute-start.1) | collective-permute-done | bytes 524320 | tf_op jit(solution)/shard_map/ppermute | solution.py:404
  91.4 15.0 %shard_map.149 = (bf16[8,512,128]{2,1,0:T(8,128)(2,1)}, bf16[8,512,128]{2,1,0:T(8,128)(2,1)}, f32[512,128]{1,0:T(8,128)}) custom-call(bf16[1024,2048]{1,0:T(8,128)(2,1)} %bitcast.18, bf16[128,2048]{1,0:T(8,128)(2,1)} %collective-permute-done.before_in, bf16[128,2048]{1,0:T(8,128)(2,1)} %collective-permute-done.1.after_in, bf16[2048,512]{1,0:T(8,128)(2,1)} %wq_in.1, ...), custom_call_target="tpu_custom_call" | custom-call | flops 4026531840 | bytes 7340032 | tf_op jit(solution)/shard_map/pallas_call | solution.py:360
  106.5 1.2 copy-done
  107.7 1.2 copy-done.1
  108.9 0.9 copy-done.3
  109.9 2.3 %shard_map.153 = bf16[256,512]{1,0:T(8,128)(2,1)S(1)} custom-call(bf16[8,512,128]{2,1,0:T(8,128)(2,1)S(1)} %copy-done, bf16[8,512,128]{2,1,0:T(8,128)(2,1)S(1)} %copy-done.1, f32[512,128]{1,0:T(8,128)S(1)} %copy-done.3, bf16[768,256]{1,0:T(8,128)(2,1)S(1)} %bitcast.9, f32[1,4]{1,0:T(1,128)S(1)} %bitcast.13), custom_call_target="tpu_custom_call" | custom-call | flops 402653184 | bytes 2097152 | tf_op jit(solution)/shard_map/pallas_call | solution.py:360
  112.2 2.6 %collective-permute-start.4 = (bf16[256,512]{1,0:T(8,128)(2,1)S(1)}, bf16[256,512]{1,0:T(8,128)(2,1)S(1)}, u32[]{:S(2)}, u32[]{:S(2)}) collective-permute-start(bf16[256,512]{1,0:T(8,128)(2,1)S(1)} %shard_map.153), channel_id=1, source_target_pairs={{0,6},{2,0},{4,2},{6,4},{1,7},{3,1},{5,3},{7,5},{8,14},{10,8},{12,... | collective-permute-start | bytes 786440 | tf_op jit(solution)/shard_map/ppermute | solution.py:349
  114.8 2.3 %shard_map.152 = bf16[256,512]{1,0:T(8,128)(2,1)S(1)} custom-call(bf16[8,512,128]{2,1,0:T(8,128)(2,1)S(1)} %copy-done, bf16[8,512,128]{2,1,0:T(8,128)(2,1)S(1)} %copy-done.1, f32[512,128]{1,0:T(8,128)S(1)} %copy-done.3, bf16[768,256]{1,0:T(8,128)(2,1)S(1)} %bitcast.10, f32[1,4]{1,0:T(1,128)S(1)} %bitcast.14), custom_call_target="tpu_custom_call" | custom-call | flops 402653184 | bytes 2097152 | tf_op jit(solution)/shard_map/pallas_call | solution.py:360
  118.0 2.3 %shard_map.151 = bf16[256,512]{1,0:T(8,128)(2,1)S(1)} custom-call(bf16[8,512,128]{2,1,0:T(8,128)(2,1)S(1)} %copy-done, bf16[8,512,128]{2,1,0:T(8,128)(2,1)S(1)} %copy-done.1, f32[512,128]{1,0:T(8,128)S(1)} %copy-done.3, bf16[768,256]{1,0:T(8,128)(2,1)S(1)} %bitcast.11, f32[1,4]{1,0:T(1,128)S(1)} %bitcast.15), custom_call_target="tpu_custom_call" | custom-call | flops 402653184 | bytes 2097152 | tf_op jit(solution)/shard_map/pallas_call | solution.py:360
  120.4 2.8 %collective-permute-done.4.a3_ref = bf16[256,512]{1,0:T(8,128)(2,1)S(1)} collective-permute-done((bf16[256,512]{1,0:T(8,128)(2,1)S(1)}, bf16[256,512]{1,0:T(8,128)(2,1)S(1)}, u32[]{:S(2)}, u32[]{:S(2)}) %collective-permute-start.4) | collective-permute-done | bytes 262176 | tf_op jit(solution)/shard_map/ppermute | solution.py:349
  123.2 2.3 %shard_map.150.a0_ref = bf16[256,512]{1,0:T(8,128)(2,1)S(1)} custom-call(bf16[8,512,128]{2,1,0:T(8,128)(2,1)S(1)} %copy-done, bf16[8,512,128]{2,1,0:T(8,128)(2,1)S(1)} %copy-done.1, f32[512,128]{1,0:T(8,128)S(1)} %copy-done.3, bf16[768,256]{1,0:T(8,128)(2,1)S(1)} %bitcast.12, f32[1,4]{1,0:T(1,128)S(1)} %bitcast.16), custom_call_target="tpu_custom_call" | custom-call | flops 402653184 | bytes 2097152 | tf_op jit(solution)/shard_map/pallas_call | solution.py:360
  125.5 1.0 collective-permute-done.3.a2_ref
  126.5 4.7 %collective-permute-done.2.a1_ref = bf16[256,512]{1,0:T(8,128)(2,1)S(1)} collective-permute-done((bf16[256,512]{1,0:T(8,128)(2,1)S(1)}, bf16[256,512]{1,0:T(8,128)(2,1)S(1)}, u32[]{:S(2)}, u32[]{:S(2)}) %collective-permute-start.2) | collective-permute-done | bytes 262176 | tf_op jit(solution)/shard_map/ppermute | solution.py:349
  131.2 5.4 %shard_map.154 = bf16[256,2048]{1,0:T(8,128)(2,1)} custom-call(f32[8,2048]{1,0:T(8,128)S(1)} %copy-done.5, bf16[256,512]{1,0:T(8,128)(2,1)S(1)} %shard_map.150.a0_ref, bf16[256,512]{1,0:T(8,128)(2,1)S(1)} %collective-permute-done.2.a1_ref, bf16[256,512]{1,0:T(8,128)(2,1)S(1)} %collective-permute-done.3.a2_ref, ...), custom_call_target="tpu_custom_call" | custom-call | flops 2147483648 | bytes 8388608 | tf_op jit(solution)/shard_map/pallas_call | solution.py:360
  (34 shorter events, 4.5 us)
Async XLA Ops:
  3.5 83.4 %collective-permute-start.7 = (bf16[512,1024]{1,0:T(8,128)(2,1)}, bf16[512,1024]{1,0:T(8,128)(2,1)}, u32[]{:S(2)}, u32[]{:S(2)}) collective-permute-start(bf16[512,1024]{1,0:T(8,128)(2,1)} %get-tuple-element.21), channel_id=1, source_target_pairs={{0,6},{2,0},{4,2},{6,4},{1,7},{3,1},{5,3},{7,5},{8,14},{10,8},{12,... | collective-permute-start | bytes 3145736 | tf_op jit(solution)/shard_map/ppermute | solution.py:349
  6.4 80.7 %collective-permute-start.5 = (bf16[512,1024]{1,0:T(8,128)(2,1)}, bf16[512,1024]{1,0:T(8,128)(2,1)}, u32[]{:S(2)}, u32[]{:S(2)}) collective-permute-start(bf16[512,1024]{1,0:T(8,128)(2,1)} %get-tuple-element.21), channel_id=1, source_target_pairs={{0,2},{2,4},{4,6},{6,0},{1,3},{3,5},{5,7},{7,1},{8,10},{10,12},{12... | collective-permute-start | bytes 3145736 | tf_op jit(solution)/shard_map/ppermute | solution.py:349
  6.4 81.2 %collective-permute-start.6 = (bf16[512,1024]{1,0:T(8,128)(2,1)}, bf16[512,1024]{1,0:T(8,128)(2,1)}, u32[]{:S(2)}, u32[]{:S(2)}) collective-permute-start(bf16[512,1024]{1,0:T(8,128)(2,1)} %get-tuple-element.21), channel_id=1, source_target_pairs={{0,4},{2,6},{4,0},{6,2},{1,5},{3,7},{5,1},{7,3},{8,12},{10,14},{12... | collective-permute-start | bytes 3145736 | tf_op jit(solution)/shard_map/ppermute | solution.py:349
  57.2 15.8 %all-to-all-start.1 = ((bf16[8,80,128]{2,1,0:T(8,128)(2,1)}), bf16[8,80,128]{2,1,0:T(8,128)(2,1)S(1)}, u32[]{:S(2)}, u32[]{:S(2)}) async-start(bf16[8,80,128]{2,1,0:T(8,128)(2,1)} %shard_map.146), calls=%async_computation.1 | async-start | bytes 327680 | tf_op jit(solution)/shard_map/all_to_all | solution.py:393
  64.8 23.6 %collective-permute-start = (bf16[128,2048]{1,0:T(8,128)(2,1)}, bf16[128,2048]{1,0:T(8,128)(2,1)}, u32[]{:S(2)}, u32[]{:S(2)}) collective-permute-start(bf16[128,2048]{1,0:T(8,128)(2,1)} %get-tuple-element.15), channel_id=1, source_target_pairs={{0,8},{8,16},{16,24},{24,32},{32,40},{40,48},{48,56},{56,64},{64,7... | collective-permute-start | bytes 1572872 | tf_op jit(solution)/shard_map/ppermute | solution.py:403
  71.0 20.4 %collective-permute-start.1 = (bf16[128,2048]{1,0:T(8,128)(2,1)}, bf16[128,2048]{1,0:T(8,128)(2,1)}, u32[]{:S(2)}, u32[]{:S(2)}) collective-permute-start(bf16[128,2048]{1,0:T(8,128)(2,1)} %get-tuple-element.16), channel_id=1, source_target_pairs={{8,0},{16,8},{24,16},{32,24},{40,32},{48,40},{56,48},{64,56},{72,6... | collective-permute-start | bytes 1572872 | tf_op jit(solution)/shard_map/ppermute | solution.py:404
  73.0 0.7 copy-start.7
  76.1 30.3 %all-to-all-start.2 = ((bf16[32,24,256]{2,1,0:T(8,128)(2,1)}), bf16[32,24,256]{2,1,0:T(8,128)(2,1)S(1)}, u32[]{:S(2)}, u32[]{:S(2)}) async-start(bf16[32,24,256]{2,1,0:T(8,128)(2,1)} %get-tuple-element.20), calls=%async_computation.2 | async-start | bytes 786432 | tf_op jit(solution)/shard_map/all_to_all | solution.py:433
  87.0 44.2 %collective-permute-start.10 = (bf16[512,1024]{1,0:T(8,128)(2,1)}, bf16[512,1024]{1,0:T(8,128)(2,1)S(1)}, u32[]{:S(2)}, u32[]{:S(2)}) collective-permute-start(bf16[512,1024]{1,0:T(8,128)(2,1)} %collective-permute-done.7.m3_ref), channel_id=1, source_target_pairs={{0,1},{1,0},{2,3},{3,2},{4,5},{5,4},{6,7},{7,6},{8,9},{9,8},{10,11... | collective-permute-start | bytes 3145736 | tf_op jit(solution)/shard_map/ppermute | solution.py:349
  87.1 44.1 %collective-permute-start.8 = (bf16[512,1024]{1,0:T(8,128)(2,1)}, bf16[512,1024]{1,0:T(8,128)(2,1)S(1)}, u32[]{:S(2)}, u32[]{:S(2)}) collective-permute-start(bf16[512,1024]{1,0:T(8,128)(2,1)} %collective-permute-done.5.m1_ref), channel_id=1, source_target_pairs={{0,1},{1,0},{2,3},{3,2},{4,5},{5,4},{6,7},{7,6},{8,9},{9,8},{10,11... | collective-permute-start | bytes 3145736 | tf_op jit(solution)/shard_map/ppermute | solution.py:349
  87.6 43.6 %collective-permute-start.9 = (bf16[512,1024]{1,0:T(8,128)(2,1)}, bf16[512,1024]{1,0:T(8,128)(2,1)S(1)}, u32[]{:S(2)}, u32[]{:S(2)}) collective-permute-start(bf16[512,1024]{1,0:T(8,128)(2,1)} %collective-permute-done.6.m2_ref), channel_id=1, source_target_pairs={{0,1},{1,0},{2,3},{3,2},{4,5},{5,4},{6,7},{7,6},{8,9},{9,8},{10,11... | collective-permute-start | bytes 3145736 | tf_op jit(solution)/shard_map/ppermute | solution.py:349
  91.4 15.1 %copy-start.6 = (f32[4]{0:T(128)S(1)}, f32[4]{0:T(128)}, u32[]{:S(2)}) copy-start(f32[4]{0:T(128)} %param.29) | copy-start | bytes 52
  106.5 1.2 copy-start
  107.7 1.2 copy-start.1
  108.9 0.9 copy-start.3
  112.2 11.0 %collective-permute-start.4 = (bf16[256,512]{1,0:T(8,128)(2,1)S(1)}, bf16[256,512]{1,0:T(8,128)(2,1)S(1)}, u32[]{:S(2)}, u32[]{:S(2)}) collective-permute-start(bf16[256,512]{1,0:T(8,128)(2,1)S(1)} %shard_map.153), channel_id=1, source_target_pairs={{0,6},{2,0},{4,2},{6,4},{1,7},{3,1},{5,3},{7,5},{8,14},{10,8},{12,... | collective-permute-start | bytes 786440 | tf_op jit(solution)/shard_map/ppermute | solution.py:349
  117.1 9.3 %collective-permute-start.3 = (bf16[256,512]{1,0:T(8,128)(2,1)S(1)}, bf16[256,512]{1,0:T(8,128)(2,1)S(1)}, u32[]{:S(2)}, u32[]{:S(2)}) collective-permute-start(bf16[256,512]{1,0:T(8,128)(2,1)S(1)} %shard_map.152), channel_id=1, source_target_pairs={{0,4},{2,6},{4,0},{6,2},{1,5},{3,7},{5,1},{7,3},{8,12},{10,14},{12... | collective-permute-start | bytes 786440 | tf_op jit(solution)/shard_map/ppermute | solution.py:349
  118.0 13.2 %copy-start.4 = (bf16[256,2048]{1,0:T(8,128)(2,1)S(1)}, bf16[256,2048]{1,0:T(8,128)(2,1)}, u32[]{:S(2)}) copy-start(bf16[256,2048]{1,0:T(8,128)(2,1)} %get-tuple-element.22.lat_ref) | copy-start | bytes 3145732
  120.4 10.8 %copy-start.2 = (bf16[512,2048]{1,0:T(8,128)(2,1)S(1)}, bf16[512,2048]{1,0:T(8,128)(2,1)}, u32[]{:S(2)}) copy-start(bf16[512,2048]{1,0:T(8,128)(2,1)} %w0_ref.1) | copy-start | bytes 6291460
  120.4 10.8 %copy-start.5 = (f32[8,2048]{1,0:T(8,128)S(1)}, f32[8,2048]{1,0:T(8,128)}, u32[]{:S(2)}) copy-start(f32[8,2048]{1,0:T(8,128)} %get-tuple-element.14.vec_ref) | copy-start | bytes 196612
  123.2 8.0 %collective-permute-start.2 = (bf16[256,512]{1,0:T(8,128)(2,1)S(1)}, bf16[256,512]{1,0:T(8,128)(2,1)S(1)}, u32[]{:S(2)}, u32[]{:S(2)}) collective-permute-start(bf16[256,512]{1,0:T(8,128)(2,1)S(1)} %shard_map.151), channel_id=1, source_target_pairs={{0,2},{2,4},{4,6},{6,0},{1,3},{3,5},{5,7},{7,1},{8,10},{10,12},{12... | collective-permute-start | bytes 786440 | tf_op jit(solution)/shard_map/ppermute | solution.py:349

commit v4 on v3

--- a/solution.py
+++ b/solution.py
@@ -122,16 +122,13 @@
     return v * cosine + swapped * sine
 
 
-def stage_kernel(w_in, lat_in, half_ref, first_ref, last_ref, own_ref, sems):
+def stage_kernel(w_in, lat_in, half_ref, first_ref, last_ref, sems):
     tok = lat_in.shape[0]
     start = pl.multiple_of(lax.axis_index("dp") * (D // 2), D // 2)
-    sub = own_ref.shape[0]
-    first = pl.multiple_of(lax.axis_index("tp") * sub, sub)
     moves = [
         pltpu.make_async_copy(w_in.at[:, pl.ds(start, D // 2)], half_ref, sems.at[0]),
         pltpu.make_async_copy(lat_in.at[:WINDOW, :], first_ref, sems.at[1]),
         pltpu.make_async_copy(lat_in.at[tok - WINDOW :, :], last_ref, sems.at[2]),
-        pltpu.make_async_copy(lat_in.at[pl.ds(first, sub), :], own_ref, sems.at[3]),
     ]
     for move in moves:
         move.start()
@@ -139,24 +136,41 @@
         move.wait()
 
 
-def context_kernel(mod_ref, ctx_ref, wk_ref, wv_ref, gain_ref, kgain_ref, kv_ref, vec_ref):
+def own_kernel(lat_in, own_ref, sem):
+    sub = own_ref.shape[0]
+    first = pl.multiple_of(lax.axis_index("tp") * sub, sub)
+    move = pltpu.make_async_copy(lat_in.at[pl.ds(first, sub), :], own_ref, sem)
+    move.start()
+    move.wait()
+
+
+def context_kernel(
+    mod_ref, ctx_ref, wk_in, wv_in, gain_ref, kgain_ref, kv_ref, vec_ref, wkv_ref, sems
+):
+    moves = [
+        pltpu.make_async_copy(wk_in, wkv_ref.at[:, :HEAD_DIM], sems.at[0]),
+        pltpu.make_async_copy(wv_in, wkv_ref.at[:, HEAD_DIM:], sems.at[1]),
+    ]
+    for move in moves:
+        move.start()
     shift_lat, scale_lat, shift_ctx, scale_ctx, gate = vectors_of(mod_ref)
     gain = gain_ref[...]
     vec_ref[0:1, :] = gain * (1.0 + scale_lat)
     vec_ref[1:2, :] = shift_lat
     vec_ref[2:3, :] = gate
     rows = (normed(ctx_ref[...]) * (gain * (1.0 + scale_ctx)) + shift_ctx).astype(BF16)
-    keys = head_norm(jnp.dot(rows, wk_ref[...], preferred_element_type=F32), kgain_ref[...])
-    values = jnp.dot(rows, wv_ref[...], preferred_element_type=F32)
-    both = jnp.concatenate([keys, values], axis=1).astype(BF16)
+    for move in moves:
+        move.wait()
+    both = jnp.dot(rows, wkv_ref[...], preferred_element_type=F32)
+    keys = head_norm(both[:, :HEAD_DIM], kgain_ref[...])
+    both = jnp.concatenate([keys, both[:, HEAD_DIM:]], axis=1).astype(BF16)
     kv_ref[...] = jnp.broadcast_to(both[None], kv_ref.shape)
 
 
 def qkv_kernel(
     lat_in, before_in, after_in, wq_in, wk_in, wv_in,
     vec_ref, qgain_ref, kgain_ref, rcos_ref, rsin_ref, ccos_ref, csin_ref,
-    q_ref, near_ref, sum_ref,
-    lat_ref, wq_ref, wk_ref, wv_ref, k_ref, v_ref, even_ref, odd_ref, sems,
+    out_ref, lat_ref, wq_ref, wkv_ref, k_ref, v_ref, even_ref, odd_ref, sum_ref, sems,
 ):
     step = 256
     tok = lat_in.shape[0]
@@ -171,7 +185,7 @@
     sources += [
         (before_in, lat_ref.at[pl.ds(tok, WINDOW), :]),
         (after_in, lat_ref.at[pl.ds(tok + WINDOW, WINDOW), :]),
-        (wk_in, wk_ref), (wv_in, wv_ref), (wq_in, wq_ref),
+        (wk_in, wkv_ref.at[:, :HEAD_DIM]), (wv_in, wkv_ref.at[:, HEAD_DIM:]), (wq_in, wq_ref),
     ]
     moves = [
         pltpu.make_async_copy(source, to, sems.at[i]) for i, (source, to) in enumerate(sources)
@@ -190,9 +204,9 @@
         to[...] = (values * inverse * vec_ref[0:1, :] + vec_ref[1:2, :]).astype(BF16)
 
     def keys_of(rows_ref, cosine, sine):
-        keys = jnp.dot(rows_ref[...], wk_ref[...], preferred_element_type=F32)
-        keys = rotated(head_norm(keys, kgain), cosine, sine).astype(BF16)
-        return keys, jnp.dot(rows_ref[...], wv_ref[...], preferred_element_type=F32).astype(BF16)
+        both = jnp.dot(rows_ref[...], wkv_ref[...], preferred_element_type=F32)
+        keys = rotated(head_norm(both[:, :HEAD_DIM], kgain), cosine, sine).astype(BF16)
+        return keys, both[:, HEAD_DIM:].astype(BF16)
 
     def project(i, rows_ref):
         to = pl.ds(pl.multiple_of(i * step + WINDOW, WINDOW), step)
@@ -204,7 +218,7 @@
             head = slice(h * HEAD_DIM, (h + 1) * HEAD_DIM)
             turned = rotated(head_norm(queries[:, head], qgain), cosine, sine).astype(BF16)
             for half in range(2):
-                q_ref[i * 2 + half, h * WINDOW : (h + 1) * WINDOW, :] = turned[
+                out_ref[i * 2 + half, h * WINDOW : (h + 1) * WINDOW, :HEAD_DIM] = turned[
                     half * WINDOW : (half + 1) * WINDOW
                 ]
 
@@ -240,7 +254,7 @@
     for ref, rows in ((k_ref, keys), (v_ref, values)):
         ref[:WINDOW, :] = rows[:WINDOW]
         ref[tok + WINDOW :, :] = rows[WINDOW:]
-    local_pass(q_ref, k_ref, v_ref, near_ref, sum_ref)
+    local_pass(out_ref, k_ref, v_ref, sum_ref)
 
 
 def contract_last(a, b):
@@ -254,9 +268,9 @@
     return parts[0]
 
 
-def local_pass(q_ref, k_ref, v_ref, out_ref, sum_ref):
+def local_pass(out_ref, k_ref, v_ref, sum_ref):
     sp = sp_index()
-    blocks = q_ref.shape[0]
+    blocks = out_ref.shape[0] - 1
     query_at = lax.broadcasted_iota(jnp.int32, (4 * WINDOW, WINDOW), 0) % WINDOW
     key_at = lax.broadcasted_iota(jnp.int32, (4 * WINDOW, WINDOW), 1)
     in_before, in_after = key_at >= query_at, key_at <= query_at
@@ -267,7 +281,7 @@
         near = pl.ds(pl.multiple_of(block * WINDOW, WINDOW), 3 * WINDOW)
         no_before = (block == 0) & (sp == 0)
         no_after = (block == blocks - 1) & (sp == NZ * NY - 1)
-        local = jnp.exp2(contract_last(q_ref[block], k_ref[near, :]))
+        local = jnp.exp2(contract_last(out_ref[block, :, :HEAD_DIM], k_ref[near, :]))
         local = jnp.concatenate(
             [
                 jnp.where(in_before & jnp.logical_not(no_before), local[:, :WINDOW], 0.0),
@@ -279,52 +293,69 @@
         total = jnp.sum(lanes_summed(local), axis=-1, keepdims=True)
         sum_ref[...] = jnp.where(key_at == block, total, sum_ref[...])
         mixed = jnp.dot(local.astype(BF16), v_ref[near, :], preferred_element_type=F32)
-        out_ref[block] = mixed.astype(BF16)
+        out_ref[block, :, HEAD_DIM:] = mixed.astype(BF16)
         return carry
 
     lax.fori_loop(0, blocks, body, 0)
-
-
-def attend_kernel(by, q_ref, near_ref, sum_ref, ctx_ref, sink_ref, out_ref):
-    quarter = (lax.axis_index("tp") + by) % NX
+    high = sum_ref[...].astype(BF16)
+    out_ref[blocks, :, :HEAD_DIM] = high
+    out_ref[blocks, :, HEAD_DIM:] = (sum_ref[...] - high.astype(F32)).astype(BF16)
+
+
+def attend_kernel(shifts, packed_ref, ctx_ref, sink_ref, *out_refs):
     head = HEAD_DIM
+    last = packed_ref.shape[0] - 1
+    tp = lax.axis_index("tp")
     sink = jnp.concatenate(
         [jnp.exp(jnp.full((WINDOW, 1), sink_ref[0, h], F32)) for h in range(4)], axis=0
     )
-
-    lane = lax.broadcasted_iota(jnp.int32, sum_ref.shape, 1)
-
-    def body(i, carry):
-        block = quarter * 2 + i
-        base = pl.ds(pl.multiple_of(i * WINDOW, WINDOW), WINDOW)
-        far = jnp.exp2(contract_last(q_ref[block], ctx_ref[:, :head]))
-        near_sum = jnp.where(lane == block, sum_ref[...], 0.0)
-        total = jnp.sum(lanes_summed(far) + near_sum, axis=-1, keepdims=True) + sink
-        mixed = near_ref[block].astype(F32) + jnp.dot(
-            far.astype(BF16), ctx_ref[:, head:], preferred_element_type=F32
-        )
-        mixed = (mixed * (1.0 / total)).astype(BF16)
-        for h in range(4):
-            out_ref[base, h * head : (h + 1) * head] = mixed[h * WINDOW : (h + 1) * WINDOW]
-        return carry
-
-    lax.fori_loop(0, 2, body, 0)
+    lane = lax.broadcasted_iota(jnp.int32, (4 * WINDOW, 128), 1)
+    sums = packed_ref[last, :, :head].astype(F32) + packed_ref[last, :, head:].astype(F32)
+
+    for by, out_ref in zip(shifts, out_refs):
+        quarter = (tp + by) % NX
+
+        def body(i, carry, quarter=quarter, out_ref=out_ref):
+            block = quarter * 2 + i
+            base = pl.ds(pl.multiple_of(i * WINDOW, WINDOW), WINDOW)
+            far = jnp.exp2(contract_last(packed_ref[block, :, :head], ctx_ref[:, :head]))
+            near_sum = jnp.where(lane == block, sums, 0.0)
+            total = jnp.sum(lanes_summed(far) + near_sum, axis=-1, keepdims=True) + sink
+            mixed = packed_ref[block, :, head:].astype(F32) + jnp.dot(
+                far.astype(BF16), ctx_ref[:, head:], preferred_element_type=F32
+            )
+            mixed = (mixed * (1.0 / total)).astype(BF16)
+            for h in range(4):
+                out_ref[base, h * head : (h + 1) * head] = mixed[h * WINDOW : (h + 1) * WINDOW]
+            return carry
+
+        lax.fori_loop(0, 2, body, 0)
 
 
 def project_kernel(
     vec_ref, a0_ref, a1_ref, a2_ref, a3_ref, w0_ref,
-    m1_ref, m2_ref, m3_ref, o1_ref, o2_ref, o3_ref, lat_ref, out_ref, done_ref, sems,
+    m1_in, m2_in, m3_in, o1_ref, o2_ref, o3_ref, lat_ref, out_ref,
+    m1_ref, m2_ref, m3_ref, done_ref, sems,
 ):
     dp = lax.axis_index("dp")
     col = 512
+    moves = [
+        pltpu.make_async_copy(source, to, sems.at[4 + i])
+        for i, (source, to) in enumerate(((m1_in, m1_ref), (m2_in, m2_ref), (m3_in, m3_ref)))
+    ]
+    for move in moves:
+        move.start()
 
     def copy(slot, column):
         return pltpu.make_async_copy(
             done_ref.at[slot], out_ref.at[:, pl.ds(column, col)], sems.at[slot]
         )
 
-    for part, weights in enumerate(((m1_ref, m2_ref, m3_ref), (o1_ref, o2_ref, o3_ref))):
-        half = dp if part == 0 else 1 - dp
+    for part, weights in enumerate(((o1_ref, o2_ref, o3_ref), (m1_ref, m2_ref, m3_ref))):
+        half = 1 - dp if part == 0 else dp
+        if part == 1:
+            for move in moves:
+                move.wait()
 
         def body(j, carry, part=part, weights=weights, half=half):
             column = pl.multiple_of(half * (D // 2) + j * col, col)
@@ -392,11 +423,15 @@
     part = call(resum_kernel, [((NZ, NX * VECS, 128), BF16)], (part,), cost(1 << 20, 1 << 18), 4)
     mod = lax.all_to_all(part, "z", 0, 0, tiled=True)
 
-    half, first_rows, last_rows, own = call(
+    half, first_rows, last_rows = call(
         stage_kernel,
-        [((width, D // 2), BF16), ((WINDOW, D), BF16), ((WINDOW, D), BF16), ((sub, D), BF16)],
+        [((width, D // 2), BF16), ((WINDOW, D), BF16), ((WINDOW, D), BF16)],
         (w_out, lat), cost(1 << 24, 4 << 20), 60,
-        scratch=[pltpu.SemaphoreType.DMA((4,))], in_specs=[HBM] * 2,
+        scratch=[pltpu.SemaphoreType.DMA((3,))], in_specs=[HBM] * 2,
+    )
+    own = call(
+        own_kernel, [((sub, D), BF16)], (lat,), cost(1 << 24, 2 << 20), 62,
+        scratch=[pltpu.SemaphoreType.DMA], in_specs=[HBM],
     )
     peers = NZ * NY
     up = [(i, i + 1) for i in range(peers - 1)]
@@ -429,15 +464,13 @@
         [((peers, n_ctx, 2 * HEAD_DIM), BF16), ((8, D), F32)],
         (mod, context[0], w_key, w_value, gain, kgain),
         cost(2 * n_ctx * D * 256, D * 512), 63,
+        scratch=[pltpu.VMEM((D, 2 * HEAD_DIM), BF16), pltpu.SemaphoreType.DMA((2,))],
+        in_specs=[VMEM, VMEM, HBM, HBM, VMEM, VMEM],
     )
     ctx_all = lax.all_to_all(ctx_kv, SP, 0, 0, tiled=True).reshape(-1, 2 * HEAD_DIM)
 
-    queries, near, sums = call(
-        qkv_kernel,
-        [
-            ((tok // WINDOW, 4 * WINDOW, HEAD_DIM), BF16),
-            ((tok // WINDOW, 4 * WINDOW, HEAD_DIM), BF16), ((4 * WINDOW, 128), F32),
-        ],
+    packed = call(
+        qkv_kernel, [((tok // WINDOW + 1, 4 * WINDOW, 2 * HEAD_DIM), BF16)],
         (
             lat, before, after, w_query, w_key, w_value, vec, qgain, kgain,
             row_cos, row_sin, col_cos, col_sin,
@@ -445,26 +478,28 @@
         cost(2 * tok * D * 768 + 16 * tok * 384 * HEAD_DIM, tok * D * 2 + D * 768 * 2), 60,
         scratch=[
             pltpu.VMEM((rows, D), BF16), pltpu.VMEM((D, width), BF16),
-            pltpu.VMEM((D, HEAD_DIM), BF16), pltpu.VMEM((D, HEAD_DIM), BF16),
+            pltpu.VMEM((D, 2 * HEAD_DIM), BF16),
             pltpu.VMEM((rows, HEAD_DIM), BF16), pltpu.VMEM((rows, HEAD_DIM), BF16),
             pltpu.VMEM((256, D), BF16), pltpu.VMEM((256, D), BF16),
+            pltpu.VMEM((4 * WINDOW, 128), F32),
             pltpu.SemaphoreType.DMA((tok // 256 + 5,)),
         ],
         in_specs=[HBM] * 6 + [VMEM] * 7,
     )
 
     arrived = {}
-    for s in (2, 1, 3, 0):
-        piece = call(
-            lambda *refs, s=s: attend_kernel(s, *refs), [((sub, width), BF16)],
-            (queries, near, sums, ctx_all, sinks[None]),
-            cost(4 * 4 * sub * 768 * HEAD_DIM, 2 << 20, 4 * sub * 768), 8,
-            in_specs=[VMEM] * 4 + [SMEM],
+    for shifts in ((2,), (1, 3), (0,)):
+        pieces = call(
+            lambda *refs, shifts=shifts: attend_kernel(shifts, *refs),
+            [((sub, width), BF16)] * len(shifts), (packed, ctx_all, sinks[None]),
+            cost(16 * len(shifts) * sub * 768 * HEAD_DIM, 2 << 20, 4 * len(shifts) * sub * 768), 8,
+            in_specs=[VMEM] * 2 + [SMEM],
         )
-        if s == 0:
-            arrived[s] = piece
-        else:
-            arrived[s] = shifted(piece, "tp", s)
+        for s, piece in zip(shifts, pieces if len(shifts) > 1 else [pieces]):
+            if s == 0:
+                arrived[s] = piece
+            else:
+                arrived[s] = shifted(piece, "tp", s)
 
     result = call(
         project_kernel, [((sub, D), BF16)],
@@ -472,10 +507,12 @@
             vec, arrived[0], arrived[1], arrived[2], arrived[3], w_out,
             mine[1], mine[2], mine[3], other[1], other[2], other[3], own,
         ),
-        cost(2 * sub * D * D, D * D * 2), 8,
+        cost(2 * sub * D * D, D * D * 2), 24,
         scratch=[
-            pltpu.VMEM((4, sub, 512), BF16), pltpu.SemaphoreType.DMA((4,)),
+            *[pltpu.VMEM((width, D // 2), BF16)] * 3,
+            pltpu.VMEM((4, sub, 512), BF16), pltpu.SemaphoreType.DMA((7,)),
         ],
+        in_specs=[VMEM] * 6 + [HBM] * 3 + [VMEM] * 4,
         out_specs=HBM,
     )
     return result[None]

time: 137 us -> 136 us (level)
  the two profiles are of different devices: /device:TPU:120 before, /device:TPU:32 now
where the time goes in v4:
time: 136 us; the launch traced here: 135 us
  blocking collectives  48 us (35%)
  Pallas kernels  41 us (30%)
  starting transfers between devices  32.3 us (24%)
  local copies, waits for them, and re-layouts  5.99 us (4%)
  waiting for transfers between devices  5.93 us (4%)
  other arithmetic  1.54 us (1%)
    all_to_all x1, blocking collectives, per_device(): part = lax.all_to_all(part, ('y', 'tp'), 0, 0, tiled=True)  48 us
    pallas_call x10, Pallas kernels, call(): pl.pallas_call(kernel, in_specs=in_specs or [VMEM] * len(args), out_specs...  41 us
    all_to_all x1, starting transfers between devices, per_device(): mod = lax.all_to_all(part, 'z', 0, 0, tiled=True)  8.57 us
    all_to_all x1, starting transfers between devices, per_device(): lax.all_to_all(ctx_kv, SP, 0, 0, tiled=True).reshape(-1, 2 * HEAD_DIM)  8.51 us
    ppermute x9, starting transfers between devices, shifted(): lax.ppermute(array, axis, [(i, (i + by) % peers) for i in range(peers)])  7.27 us
    unnamed x16, local copies, waits for them, and re-layouts  5.99 us
    ppermute x9, waiting for transfers between devices, shifted(): lax.ppermute(array, axis, [(i, (i + by) % peers) for i in range(peers)])  5.83 us
    ppermute x1, starting transfers between devices, per_device(): after = lax.ppermute(first_rows, SP, [(j, i) for i, j in up])  5.37 us
  transfers between devices with their start and end apart: 13, of which 3 were waited for; matrix products, arithmetic and copies ran while one was open for 1% of the time, Pallas kernels for 24%

profile of v4, /device:TPU:32, one launch (start us, length us, event | category | flops | bytes accessed | tf_op | source)
XLA Modules:
  0.0 135.1 jit_solution(14837554824456714975)
XLA Ops:
  0.0 2.9 %shard_map.148 = (bf16[512,1024]{1,0:T(8,128)(2,1)}, bf16[128,2048]{1,0:T(8,128)(2,1)}, bf16[128,2048]{1,0:T(8,128)(2,1)}) custom-call(bf16[512,2048]{1,0:T(8,128)(2,1)} %w0_ref.1, bf16[1024,2048]{1,0:T(8,128)(2,1)} %bitcast.15), custom_call_target="tpu_custom_call" | custom-call | flops 16777216 | bytes 4194304 | tf_op jit(solution)/shard_map/pallas_call | solution.py:391
  2.9 2.8 %collective-permute-start.7 = (bf16[512,1024]{1,0:T(8,128)(2,1)}, bf16[512,1024]{1,0:T(8,128)(2,1)}, u32[]{:S(2)}, u32[]{:S(2)}) collective-permute-start(bf16[512,1024]{1,0:T(8,128)(2,1)} %get-tuple-element.18), channel_id=1, source_target_pairs={{0,6},{2,0},{4,2},{6,4},{1,7},{3,1},{5,3},{7,5},{8,14},{10,8},{12,... | collective-permute-start | bytes 3145736 | tf_op jit(solution)/shard_map/ppermute | solution.py:380
  5.7 2.3 %collective-permute-start.6 = (bf16[512,1024]{1,0:T(8,128)(2,1)}, bf16[512,1024]{1,0:T(8,128)(2,1)}, u32[]{:S(2)}, u32[]{:S(2)}) collective-permute-start(bf16[512,1024]{1,0:T(8,128)(2,1)} %get-tuple-element.18), channel_id=1, source_target_pairs={{0,4},{2,6},{4,0},{6,2},{1,5},{3,7},{5,1},{7,3},{8,12},{10,14},{12... | collective-permute-start | bytes 3145736 | tf_op jit(solution)/shard_map/ppermute | solution.py:380
  8.0 1.8 %shard_map.145 = bf16[16,24,128]{2,1,0:T(8,128)(2,1)} custom-call(f32[1,2048]{1,0:T(1,128)} %cond_in.1, f32[1,2048]{1,0:T(1,128)} %bitcast.20, bf16[64,512]{1,0:T(8,128)(2,1)} %shift_in.1, bf16[64,512]{1,0:T(8,128)(2,1)} %scale_in.1, bf16[64,512]{1,0:T(8,128)(2,1)} %gate_in.1), custom_call_target="tpu_custom_call" | custom-call | flops 1048576 | bytes 262144 | tf_op jit(solution)/shard_map/pallas_call | solution.py:391
  9.8 48.0 %all_to_all.15.in_ref = bf16[16,24,128]{2,1,0:T(8,128)(2,1)S(1)} all-to-all(bf16[16,24,128]{2,1,0:T(8,128)(2,1)} %shard_map.145), channel_id=1, replica_groups=mesh['z'=8,'y'=4,'tp'=4,'dp'=2] {'y','tp'}, dimensions={0} | all-to-all | bytes 196608 | tf_op jit(solution)/shard_map/all_to_all | solution.py:422
  58.5 8.6 %all-to-all-start.1 = ((bf16[8,80,128]{2,1,0:T(8,128)(2,1)}), bf16[8,80,128]{2,1,0:T(8,128)(2,1)S(1)}, u32[]{:S(2)}, u32[]{:S(2)}) async-start(bf16[8,80,128]{2,1,0:T(8,128)(2,1)} %shard_map.146), calls=%async_computation.1 | async-start | bytes 327680 | tf_op jit(solution)/shard_map/all_to_all | solution.py:424
  67.0 2.6 %collective-permute-start = (bf16[128,2048]{1,0:T(8,128)(2,1)}, bf16[128,2048]{1,0:T(8,128)(2,1)S(1)}, u32[]{:S(2)}, u32[]{:S(2)}) collective-permute-start(bf16[128,2048]{1,0:T(8,128)(2,1)} %get-tuple-element.13), channel_id=1, source_target_pairs={{0,8},{8,16},{16,24},{24,32},{32,40},{40,48},{48,56},{56,64},{64,7... | collective-permute-start | bytes 1572872 | tf_op jit(solution)/shard_map/ppermute | solution.py:438
  69.6 5.4 %collective-permute-start.1 = (bf16[128,2048]{1,0:T(8,128)(2,1)}, bf16[128,2048]{1,0:T(8,128)(2,1)}, u32[]{:S(2)}, u32[]{:S(2)}) collective-permute-start(bf16[128,2048]{1,0:T(8,128)(2,1)} %get-tuple-element.14), channel_id=1, source_target_pairs={{8,0},{16,8},{24,16},{32,24},{40,32},{48,40},{56,48},{64,56},{72,6... | collective-permute-start | bytes 1572872 | tf_op jit(solution)/shard_map/ppermute | solution.py:439
  75.8 3.3 %shard_map.147 = (bf16[32,24,256]{2,1,0:T(8,128)(2,1)}, f32[8,2048]{1,0:T(8,128)}) custom-call(bf16[8,80,128]{2,1,0:T(8,128)(2,1)} %copy-done.6, bf16[24,2048]{1,0:T(8,128)(2,1)} %bitcast.18, bf16[2048,128]{1,0:T(8,128)(2,1)} %wk_in.3, bf16[2048,128]{1,0:T(8,128)(2,1)} %wv_in.3, f32[1,2048]{1,0:T(1,128)} %bitcast.19, f32[1,128]{1,0:T(1,128)} %bitcast.21), custom_call_target="tpu_custom_call" | custom-call | flops 25165824 | bytes 1048576 | tf_op jit(solution)/shard_map/pallas_call | solution.py:391
  79.1 8.5 %all-to-all-start.2 = ((bf16[32,24,256]{2,1,0:T(8,128)(2,1)}), bf16[32,24,256]{2,1,0:T(8,128)(2,1)S(1)}, u32[]{:S(2)}, u32[]{:S(2)}) async-start(bf16[32,24,256]{2,1,0:T(8,128)(2,1)} %get-tuple-element.15), calls=%async_computation.2 | async-start | bytes 786432 | tf_op jit(solution)/shard_map/all_to_all | solution.py:470
  87.6 0.8 multiply_select_fusion
  89.9 0.8 copy-done.7
  90.7 14.7 %shard_map.149.refs_0_ = bf16[9,512,256]{2,1,0:T(8,128)(2,1)} custom-call(bf16[1024,2048]{1,0:T(8,128)(2,1)} %bitcast.16, bf16[128,2048]{1,0:T(8,128)(2,1)} %copy-done.7, bf16[128,2048]{1,0:T(8,128)(2,1)} %collective-permute-done.1.after_in, bf16[2048,512]{1,0:T(8,128)(2,1)} %wq_in.1, bf16[2048,128]{1,0:T(8,128)(2,1)} %wk_in.3, bf16[2048,128]{1,0:T(8,128)(2,1)} %wv_in.3, ...), custom_call_target="tpu_custom_call" | custom-call | flops 4026531840 | bytes 7340032 | tf_op jit(solution)/shard_map/pallas_call | solution.py:391
  105.4 1.7 %copy-done = bf16[9,512,256]{2,1,0:T(8,128)(2,1)S(1)} copy-done((bf16[9,512,256]{2,1,0:T(8,128)(2,1)S(1)}, bf16[9,512,256]{2,1,0:T(8,128)(2,1)}, u32[]{:S(2)}) %copy-start) | copy-done | bytes 2359320
  107.1 2.3 %shard_map.152 = bf16[256,512]{1,0:T(8,128)(2,1)S(1)} custom-call(bf16[9,512,256]{2,1,0:T(8,128)(2,1)S(1)} %copy-done, bf16[768,256]{1,0:T(8,128)(2,1)S(1)} %bitcast.9, f32[1,4]{1,0:T(1,128)S(1)} %bitcast.12), custom_call_target="tpu_custom_call" | custom-call | flops 402653184 | bytes 2097152 | tf_op jit(solution)/shard_map/pallas_call | solution.py:391
  110.0 4.9 %shard_map.151 = (bf16[256,512]{1,0:T(8,128)(2,1)}, bf16[256,512]{1,0:T(8,128)(2,1)}) custom-call(bf16[9,512,256]{2,1,0:T(8,128)(2,1)S(1)} %copy-done, bf16[768,256]{1,0:T(8,128)(2,1)S(1)} %bitcast.10, f32[1,4]{1,0:T(1,128)S(1)} %bitcast.13), custom_call_target="tpu_custom_call" | custom-call | flops 805306368 | bytes 2097152 | tf_op jit(solution)/shard_map/pallas_call | solution.py:391
  115.0 0.9 collective-permute-start.2
  115.9 4.4 %collective-permute-done.3.a2_ref = bf16[256,512]{1,0:T(8,128)(2,1)S(1)} collective-permute-done((bf16[256,512]{1,0:T(8,128)(2,1)S(1)}, bf16[256,512]{1,0:T(8,128)(2,1)S(1)}, u32[]{:S(2)}, u32[]{:S(2)}) %collective-permute-start.3) | collective-permute-done | bytes 262176 | tf_op jit(solution)/shard_map/ppermute | solution.py:380
  120.3 2.2 %shard_map.153.lat_ref = bf16[256,2048]{1,0:T(8,128)(2,1)} custom-call(bf16[1024,2048]{1,0:T(8,128)(2,1)} %bitcast.17), custom_call_target="tpu_custom_call" | custom-call | flops 16777216 | bytes 2097152 | tf_op jit(solution)/shard_map/pallas_call | solution.py:391
  122.5 1.7 %copy-done.1 = bf16[9,512,256]{2,1,0:T(8,128)(2,1)S(1)} copy-done((bf16[9,512,256]{2,1,0:T(8,128)(2,1)S(1)}, bf16[9,512,256]{2,1,0:T(8,128)(2,1)}, u32[]{:S(2)}) %copy-start.1) | copy-done | bytes 2359320
  124.2 2.3 %shard_map.150.a0_ref = bf16[256,512]{1,0:T(8,128)(2,1)S(1)} custom-call(bf16[9,512,256]{2,1,0:T(8,128)(2,1)S(1)} %copy-done.1, bf16[768,256]{1,0:T(8,128)(2,1)S(1)} %bitcast.11, f32[1,4]{1,0:T(1,128)S(1)} %bitcast.14), custom_call_target="tpu_custom_call" | custom-call | flops 402653184 | bytes 2097152 | tf_op jit(solution)/shard_map/pallas_call | solution.py:391
  126.5 1.4 %collective-permute-done.4.a3_ref = bf16[256,512]{1,0:T(8,128)(2,1)} collective-permute-done((bf16[256,512]{1,0:T(8,128)(2,1)}, bf16[256,512]{1,0:T(8,128)(2,1)}, u32[]{:S(2)}, u32[]{:S(2)}) %collective-permute-start.4) | collective-permute-done | bytes 262176 | tf_op jit(solution)/shard_map/ppermute | solution.py:380
  127.9 1.2 copy-done.3
  129.2 5.8 %shard_map.154 = bf16[256,2048]{1,0:T(8,128)(2,1)} custom-call(f32[8,2048]{1,0:T(8,128)S(1)} %copy-done.4, bf16[256,512]{1,0:T(8,128)(2,1)S(1)} %shard_map.150.a0_ref, bf16[256,512]{1,0:T(8,128)(2,1)S(1)} %collective-permute-done.2.a1_ref, bf16[256,512]{1,0:T(8,128)(2,1)S(1)} %collective-permute-done.3.a2_ref, ...), custom_call_target="tpu_custom_call" | custom-call | flops 2147483648 | bytes 8388608 | tf_op jit(solution)/shard_map/pallas_call | solution.py:391
  (34 shorter events, 3.5 us)
Async XLA Ops:
  2.9 85.5 %collective-permute-start.7 = (bf16[512,1024]{1,0:T(8,128)(2,1)}, bf16[512,1024]{1,0:T(8,128)(2,1)}, u32[]{:S(2)}, u32[]{:S(2)}) collective-permute-start(bf16[512,1024]{1,0:T(8,128)(2,1)} %get-tuple-element.18), channel_id=1, source_target_pairs={{0,6},{2,0},{4,2},{6,4},{1,7},{3,1},{5,3},{7,5},{8,14},{10,8},{12,... | collective-permute-start | bytes 3145736 | tf_op jit(solution)/shard_map/ppermute | solution.py:380
  5.7 82.8 %collective-permute-start.5 = (bf16[512,1024]{1,0:T(8,128)(2,1)}, bf16[512,1024]{1,0:T(8,128)(2,1)}, u32[]{:S(2)}, u32[]{:S(2)}) collective-permute-start(bf16[512,1024]{1,0:T(8,128)(2,1)} %get-tuple-element.18), channel_id=1, source_target_pairs={{0,2},{2,4},{4,6},{6,0},{1,3},{3,5},{5,7},{7,1},{8,10},{10,12},{12... | collective-permute-start | bytes 3145736 | tf_op jit(solution)/shard_map/ppermute | solution.py:380
  5.7 83.3 %collective-permute-start.6 = (bf16[512,1024]{1,0:T(8,128)(2,1)}, bf16[512,1024]{1,0:T(8,128)(2,1)}, u32[]{:S(2)}, u32[]{:S(2)}) collective-permute-start(bf16[512,1024]{1,0:T(8,128)(2,1)} %get-tuple-element.18), channel_id=1, source_target_pairs={{0,4},{2,6},{4,0},{6,2},{1,5},{3,7},{5,1},{7,3},{8,12},{10,14},{12... | collective-permute-start | bytes 3145736 | tf_op jit(solution)/shard_map/ppermute | solution.py:380
  58.5 16.6 %all-to-all-start.1 = ((bf16[8,80,128]{2,1,0:T(8,128)(2,1)}), bf16[8,80,128]{2,1,0:T(8,128)(2,1)S(1)}, u32[]{:S(2)}, u32[]{:S(2)}) async-start(bf16[8,80,128]{2,1,0:T(8,128)(2,1)} %shard_map.146), calls=%async_computation.1 | async-start | bytes 327680 | tf_op jit(solution)/shard_map/all_to_all | solution.py:424
  67.0 22.9 %collective-permute-start = (bf16[128,2048]{1,0:T(8,128)(2,1)}, bf16[128,2048]{1,0:T(8,128)(2,1)S(1)}, u32[]{:S(2)}, u32[]{:S(2)}) collective-permute-start(bf16[128,2048]{1,0:T(8,128)(2,1)} %get-tuple-element.13), channel_id=1, source_target_pairs={{0,8},{8,16},{16,24},{24,32},{32,40},{40,48},{48,56},{56,64},{64,7... | collective-permute-start | bytes 1572872 | tf_op jit(solution)/shard_map/ppermute | solution.py:438
  69.6 20.3 %collective-permute-start.1 = (bf16[128,2048]{1,0:T(8,128)(2,1)}, bf16[128,2048]{1,0:T(8,128)(2,1)}, u32[]{:S(2)}, u32[]{:S(2)}) collective-permute-start(bf16[128,2048]{1,0:T(8,128)(2,1)} %get-tuple-element.14), channel_id=1, source_target_pairs={{8,0},{16,8},{24,16},{32,24},{40,32},{48,40},{56,48},{64,56},{72,6... | collective-permute-start | bytes 1572872 | tf_op jit(solution)/shard_map/ppermute | solution.py:439
  75.1 0.7 copy-start.6
  79.1 26.3 %all-to-all-start.2 = ((bf16[32,24,256]{2,1,0:T(8,128)(2,1)}), bf16[32,24,256]{2,1,0:T(8,128)(2,1)S(1)}, u32[]{:S(2)}, u32[]{:S(2)}) async-start(bf16[32,24,256]{2,1,0:T(8,128)(2,1)} %get-tuple-element.15), calls=%async_computation.2 | async-start | bytes 786432 | tf_op jit(solution)/shard_map/all_to_all | solution.py:470
  88.4 39.5 %collective-permute-start.10 = (bf16[512,1024]{1,0:T(8,128)(2,1)}, bf16[512,1024]{1,0:T(8,128)(2,1)S(1)}, u32[]{:S(2)}, u32[]{:S(2)}) collective-permute-start(bf16[512,1024]{1,0:T(8,128)(2,1)} %collective-permute-done.7.m3_in), channel_id=1, source_target_pairs={{0,1},{1,0},{2,3},{3,2},{4,5},{5,4},{6,7},{7,6},{8,9},{9,8},{10,11... | collective-permute-start | bytes 3145736 | tf_op jit(solution)/shard_map/ppermute | solution.py:380
  88.5 39.4 %collective-permute-start.8 = (bf16[512,1024]{1,0:T(8,128)(2,1)}, bf16[512,1024]{1,0:T(8,128)(2,1)}, u32[]{:S(2)}, u32[]{:S(2)}) collective-permute-start(bf16[512,1024]{1,0:T(8,128)(2,1)} %collective-permute-done.5.m1_in), channel_id=1, source_target_pairs={{0,1},{1,0},{2,3},{3,2},{4,5},{5,4},{6,7},{7,6},{8,9},{9,8},{10,11... | collective-permute-start | bytes 3145736 | tf_op jit(solution)/shard_map/ppermute | solution.py:380
  89.0 38.9 %collective-permute-start.9 = (bf16[512,1024]{1,0:T(8,128)(2,1)}, bf16[512,1024]{1,0:T(8,128)(2,1)}, u32[]{:S(2)}, u32[]{:S(2)}) collective-permute-start(bf16[512,1024]{1,0:T(8,128)(2,1)} %collective-permute-done.6.m2_in), channel_id=1, source_target_pairs={{0,1},{1,0},{2,3},{3,2},{4,5},{5,4},{6,7},{7,6},{8,9},{9,8},{10,11... | collective-permute-start | bytes 3145736 | tf_op jit(solution)/shard_map/ppermute | solution.py:380
  89.9 0.8 copy-start.7
  90.7 14.8 %copy-start.5 = (f32[4]{0:T(128)S(1)}, f32[4]{0:T(128)}, u32[]{:S(2)}) copy-start(f32[4]{0:T(128)} %param.29) | copy-start | bytes 52
  105.4 1.7 %copy-start = (bf16[9,512,256]{2,1,0:T(8,128)(2,1)S(1)}, bf16[9,512,256]{2,1,0:T(8,128)(2,1)}, u32[]{:S(2)}) copy-start(bf16[9,512,256]{2,1,0:T(8,128)(2,1)} %shard_map.149.refs_0_) | copy-start | bytes 7077892
  109.5 10.8 %collective-permute-start.3 = (bf16[256,512]{1,0:T(8,128)(2,1)S(1)}, bf16[256,512]{1,0:T(8,128)(2,1)S(1)}, u32[]{:S(2)}, u32[]{:S(2)}) collective-permute-start(bf16[256,512]{1,0:T(8,128)(2,1)S(1)} %shard_map.152), channel_id=1, source_target_pairs={{0,4},{2,6},{4,0},{6,2},{1,5},{3,7},{5,1},{7,3},{8,12},{10,14},{12... | collective-permute-start | bytes 786440 | tf_op jit(solution)/shard_map/ppermute | solution.py:380
  115.0 11.5 %collective-permute-start.2 = (bf16[256,512]{1,0:T(8,128)(2,1)}, bf16[256,512]{1,0:T(8,128)(2,1)S(1)}, u32[]{:S(2)}, u32[]{:S(2)}) collective-permute-start(bf16[256,512]{1,0:T(8,128)(2,1)} %get-tuple-element.16), channel_id=1, source_target_pairs={{0,2},{2,4},{4,6},{6,0},{1,3},{3,5},{5,7},{7,1},{8,10},{10,12},{12... | collective-permute-start | bytes 786440 | tf_op jit(solution)/shard_map/ppermute | solution.py:380
  120.3 7.6 %collective-permute-start.4 = (bf16[256,512]{1,0:T(8,128)(2,1)}, bf16[256,512]{1,0:T(8,128)(2,1)}, u32[]{:S(2)}, u32[]{:S(2)}) collective-permute-start(bf16[256,512]{1,0:T(8,128)(2,1)} %get-tuple-element.17), channel_id=1, source_target_pairs={{0,6},{2,0},{4,2},{6,4},{1,7},{3,1},{5,3},{7,5},{8,14},{10,8},{12,... | collective-permute-start | bytes 786440 | tf_op jit(solution)/shard_map/ppermute | solution.py:380
  122.5 1.7 %copy-start.1 = (bf16[9,512,256]{2,1,0:T(8,128)(2,1)S(1)}, bf16[9,512,256]{2,1,0:T(8,128)(2,1)}, u32[]{:S(2)}) copy-start(bf16[9,512,256]{2,1,0:T(8,128)(2,1)} %shard_map.149.refs_0_) | copy-start | bytes 7077892
  124.2 3.8 %copy-start.2 = (bf16[512,2048]{1,0:T(8,128)(2,1)S(1)}, bf16[512,2048]{1,0:T(8,128)(2,1)}, u32[]{:S(2)}) copy-start(bf16[512,2048]{1,0:T(8,128)(2,1)} %w0_ref.1) | copy-start | bytes 6291460
  124.2 3.8 %copy-start.4 = (f32[8,2048]{1,0:T(8,128)S(1)}, f32[8,2048]{1,0:T(8,128)}, u32[]{:S(2)}) copy-start(f32[8,2048]{1,0:T(8,128)} %get-tuple-element.12.vec_ref) | copy-start | bytes 196612
  127.9 1.2 copy-start.3

commit v5 on v4

--- a/solution.py
+++ b/solution.py
@@ -14,7 +14,6 @@
 NORM_EPSILON = 1e-06
 ROPE_BASE = 10000.0
 D = 2048
-VECS = 20
 NZ, NY, NX = 8, 4, 4
 SP = ("z", "y")
 
@@ -35,18 +34,38 @@
     return pl.CostEstimate(flops=flops, bytes_accessed=nbytes, transcendentals=trans)
 
 
-def partial_kernel(cond_in, ctx_in, shift_in, scale_in, gate_in, out_ref,
-                   cond_ref, ctx_ref, shift_ref, scale_ref, gate_ref, sems):
-    moves = [
-        pltpu.make_async_copy(source, to, sems.at[i])
-        for i, (source, to) in enumerate(
-            (
-                (cond_in, cond_ref), (ctx_in, ctx_ref), (shift_in, shift_ref),
-                (scale_in, scale_ref), (gate_in, gate_ref),
-            )
-        )
-    ]
-    for move in moves:
+def partial_kernel(
+    cond_in, ctx_in, shift_in, scale_in, gate_in, w_in, lat_in,
+    out_ref, half_out, first_out, last_out,
+    cond_ref, ctx_ref, shift_ref, scale_ref, gate_ref, half_ref, first_ref, last_ref, sems,
+):
+    tok = lat_in.shape[0]
+    column = pl.multiple_of(lax.axis_index("dp") * (D // 2), D // 2)
+
+    def moves_of(pairs, base):
+        return [
+            pltpu.make_async_copy(source, to, sems.at[base + i])
+            for i, (source, to) in enumerate(pairs)
+        ]
+
+    moves = moves_of(
+        (
+            (cond_in, cond_ref), (ctx_in, ctx_ref), (shift_in, shift_ref),
+            (scale_in, scale_ref), (gate_in, gate_ref),
+        ),
+        0,
+    )
+    stage_in = moves_of(
+        (
+            (w_in.at[:, pl.ds(column, D // 2)], half_ref),
+            (lat_in.at[:WINDOW, :], first_ref), (lat_in.at[tok - WINDOW :, :], last_ref),
+        ),
+        5,
+    )
+    stage_out = moves_of(
+        ((half_ref, half_out), (first_ref, first_out), (last_ref, last_out)), 8
+    )
+    for move in moves + stage_in:
         move.start()
     for move in moves:
         move.wait()
@@ -76,32 +95,27 @@
     pieces.append(jnp.zeros((4, 128), F32))
     stacked = jnp.concatenate(pieces, axis=0).astype(BF16)
     out_ref[...] = jnp.broadcast_to(stacked[None], out_ref.shape)
-
-
-def resum_kernel(in_ref, out_ref):
-    pieces = []
+    for arrived, move in zip(stage_in, stage_out):
+        arrived.wait()
+        move.start()
+    for move in stage_out:
+        move.wait()
+
+
+def vectors_of(mod_ref):
+    totals = []
     for t in range(NX):
         rows = None
-        for y in range(NY):
-            part = in_ref[y * NX + t].astype(F32)
+        for p in range(NZ * NY):
+            part = mod_ref[p * NX + t].astype(F32)
             rows = part if rows is None else rows + part
-        pieces.append(rows[:VECS])
-    total = jnp.concatenate(pieces, axis=0).astype(BF16)
-    out_ref[...] = jnp.broadcast_to(total[None], out_ref.shape)
-
-
-def vectors_of(mod_ref):
-    rows = None
-    for z in range(NZ):
-        part = mod_ref[z].astype(F32)
-        rows = part if rows is None else rows + part
+        totals.append(rows)
     found = []
     for v in range(5):
         pieces = []
         for t in range(NX):
             for i in range(4):
-                at = t * VECS + v * 4 + i
-                pieces.append(rows[at : at + 1, :])
+                pieces.append(totals[t][v * 4 + i : v * 4 + i + 1, :])
         found.append(jnp.concatenate(pieces, axis=1))
     return found
 
@@ -122,55 +136,25 @@
     return v * cosine + swapped * sine
 
 
-def stage_kernel(w_in, lat_in, half_ref, first_ref, last_ref, sems):
-    tok = lat_in.shape[0]
-    start = pl.multiple_of(lax.axis_index("dp") * (D // 2), D // 2)
-    moves = [
-        pltpu.make_async_copy(w_in.at[:, pl.ds(start, D // 2)], half_ref, sems.at[0]),
-        pltpu.make_async_copy(lat_in.at[:WINDOW, :], first_ref, sems.at[1]),
-        pltpu.make_async_copy(lat_in.at[tok - WINDOW :, :], last_ref, sems.at[2]),
-    ]
-    for move in moves:
-        move.start()
-    for move in moves:
-        move.wait()
-
-
-def own_kernel(lat_in, own_ref, sem):
-    sub = own_ref.shape[0]
-    first = pl.multiple_of(lax.axis_index("tp") * sub, sub)
-    move = pltpu.make_async_copy(lat_in.at[pl.ds(first, sub), :], own_ref, sem)
-    move.start()
-    move.wait()
-
-
 def context_kernel(
-    mod_ref, ctx_ref, wk_in, wv_in, gain_ref, kgain_ref, kv_ref, vec_ref, wkv_ref, sems
+    mod_ref, ctx_ref, wk_ref, wv_ref, gain_ref, kgain_ref, kv_ref, vec_ref
 ):
-    moves = [
-        pltpu.make_async_copy(wk_in, wkv_ref.at[:, :HEAD_DIM], sems.at[0]),
-        pltpu.make_async_copy(wv_in, wkv_ref.at[:, HEAD_DIM:], sems.at[1]),
-    ]
-    for move in moves:
-        move.start()
     shift_lat, scale_lat, shift_ctx, scale_ctx, gate = vectors_of(mod_ref)
     gain = gain_ref[...]
     vec_ref[0:1, :] = gain * (1.0 + scale_lat)
     vec_ref[1:2, :] = shift_lat
     vec_ref[2:3, :] = gate
     rows = (normed(ctx_ref[...]) * (gain * (1.0 + scale_ctx)) + shift_ctx).astype(BF16)
-    for move in moves:
-        move.wait()
-    both = jnp.dot(rows, wkv_ref[...], preferred_element_type=F32)
-    keys = head_norm(both[:, :HEAD_DIM], kgain_ref[...])
-    both = jnp.concatenate([keys, both[:, HEAD_DIM:]], axis=1).astype(BF16)
+    keys = head_norm(jnp.dot(rows, wk_ref[...], preferred_element_type=F32), kgain_ref[...])
+    values = jnp.dot(rows, wv_ref[...], preferred_element_type=F32)
+    both = jnp.concatenate([keys, values], axis=1).astype(BF16)
     kv_ref[...] = jnp.broadcast_to(both[None], kv_ref.shape)
 
 
 def qkv_kernel(
     lat_in, before_in, after_in, wq_in, wk_in, wv_in,
     vec_ref, qgain_ref, kgain_ref, rcos_ref, rsin_ref, ccos_ref, csin_ref,
-    out_ref, lat_ref, wq_ref, wkv_ref, k_ref, v_ref, even_ref, odd_ref, sum_ref, sems,
+    out_ref, own_ref, lat_ref, wq_ref, wkv_ref, k_ref, v_ref, even_ref, odd_ref, sum_ref, sems,
 ):
     step = 256
     tok = lat_in.shape[0]
@@ -249,12 +233,17 @@
         return carry
 
     lax.fori_loop(0, steps // 2, body, 0)
+    own_move = pltpu.make_async_copy(
+        lat_ref.at[at(lax.axis_index("tp"), own_ref.shape[0]), :], own_ref, sems.at[steps + 5]
+    )
+    own_move.start()
     beyond = (tok + WINDOW) // GRID_W
     keys, values = keys_of(even_ref, *tables([0, 1, beyond, beyond + 1]))
     for ref, rows in ((k_ref, keys), (v_ref, values)):
         ref[:WINDOW, :] = rows[:WINDOW]
         ref[tok + WINDOW :, :] = rows[WINDOW:]
     local_pass(out_ref, k_ref, v_ref, sum_ref)
+    own_move.wait()
 
 
 def contract_last(a, b):
@@ -409,31 +398,24 @@
     sp = sp_index()
     width = 4 * HEAD_DIM
 
-    part = call(
-        partial_kernel, [((NY * NX, 24, 128), BF16)],
-        (cond, ctx_cond[None], mod_shift, mod_scale, mod_gate), cost(1 << 20, 1 << 18), 62,
+    peers = NZ * NY
+    small = pltpu.VMEM((64, 512), BF16)
+    edge_rows = ((WINDOW, D), BF16)
+    part, half, first_rows, last_rows = call(
+        partial_kernel,
+        [((peers * NX, 24, 128), BF16), ((width, D // 2), BF16), edge_rows, edge_rows],
+        (cond, ctx_cond[None], mod_shift, mod_scale, mod_gate, w_out, lat),
+        cost(1 << 20, 1 << 18), 62,
         scratch=[
-            pltpu.VMEM((1, D), F32), pltpu.VMEM((1, D), F32), pltpu.VMEM((64, 512), BF16),
-            pltpu.VMEM((64, 512), BF16), pltpu.VMEM((64, 512), BF16),
-            pltpu.SemaphoreType.DMA((5,)),
+            pltpu.VMEM((1, D), F32), pltpu.VMEM((1, D), F32), small, small, small,
+            pltpu.VMEM((width, D // 2), BF16), pltpu.VMEM((WINDOW, D), BF16),
+            pltpu.VMEM((WINDOW, D), BF16), pltpu.SemaphoreType.DMA((11,)),
         ],
-        in_specs=[HBM] * 5,
-    )
-    part = lax.all_to_all(part, ("y", "tp"), 0, 0, tiled=True)
-    part = call(resum_kernel, [((NZ, NX * VECS, 128), BF16)], (part,), cost(1 << 20, 1 << 18), 4)
-    mod = lax.all_to_all(part, "z", 0, 0, tiled=True)
-
-    half, first_rows, last_rows = call(
-        stage_kernel,
-        [((width, D // 2), BF16), ((WINDOW, D), BF16), ((WINDOW, D), BF16)],
-        (w_out, lat), cost(1 << 24, 4 << 20), 60,
-        scratch=[pltpu.SemaphoreType.DMA((3,))], in_specs=[HBM] * 2,
-    )
-    own = call(
-        own_kernel, [((sub, D), BF16)], (lat,), cost(1 << 24, 2 << 20), 62,
-        scratch=[pltpu.SemaphoreType.DMA], in_specs=[HBM],
-    )
-    peers = NZ * NY
+        in_specs=[HBM] * 7,
+        out_specs=[VMEM, HBM, HBM, HBM],
+    )
+    mod = lax.all_to_all(part, ("z", "y", "tp"), 0, 0, tiled=True)
+
     up = [(i, i + 1) for i in range(peers - 1)]
     before = lax.ppermute(last_rows, SP, up)
     after = lax.ppermute(first_rows, SP, [(j, i) for i, j in up])
@@ -463,14 +445,13 @@
         context_kernel,
         [((peers, n_ctx, 2 * HEAD_DIM), BF16), ((8, D), F32)],
         (mod, context[0], w_key, w_value, gain, kgain),
-        cost(2 * n_ctx * D * 256, D * 512), 63,
-        scratch=[pltpu.VMEM((D, 2 * HEAD_DIM), BF16), pltpu.SemaphoreType.DMA((2,))],
-        in_specs=[VMEM, VMEM, HBM, HBM, VMEM, VMEM],
+        cost(2 * n_ctx * D * 256, D * 512), 58,
     )
     ctx_all = lax.all_to_all(ctx_kv, SP, 0, 0, tiled=True).reshape(-1, 2 * HEAD_DIM)
 
-    packed = call(
-        qkv_kernel, [((tok // WINDOW + 1, 4 * WINDOW, 2 * HEAD_DIM), BF16)],
+    packed, own = call(
+        qkv_kernel,
+        [((tok // WINDOW + 1, 4 * WINDOW, 2 * HEAD_DIM), BF16), ((sub, D), BF16)],
         (
             lat, before, after, w_query, w_key, w_value, vec, qgain, kgain,
             row_cos, row_sin, col_cos, col_sin,
@@ -482,9 +463,10 @@
             pltpu.VMEM((rows, HEAD_DIM), BF16), pltpu.VMEM((rows, HEAD_DIM), BF16),
             pltpu.VMEM((256, D), BF16), pltpu.VMEM((256, D), BF16),
             pltpu.VMEM((4 * WINDOW, 128), F32),
-            pltpu.SemaphoreType.DMA((tok // 256 + 5,)),
+            pltpu.SemaphoreType.DMA((tok // 256 + 6,)),
         ],
         in_specs=[HBM] * 6 + [VMEM] * 7,
+        out_specs=[VMEM, HBM],
     )
 
     arrived = {}

time: 136 us -> 131 us (0.963)
  blocking collectives: 48 us -> 0 us
  waiting for transfers between devices: 5.93 us -> 48.6 us
  starting transfers between devices: 32.3 us -> 42.1 us
  Pallas kernels: 41 us -> 35.6 us
  local copies, waits for them, and re-layouts: 5.99 us -> 1.67 us
    all_to_all x1 -> x0, blocking collectives: 48 us -> none  [per_device(): part = lax.all_to_all(part, ('y', 'tp'), 0, 0, tiled=True)]
    ppermute x9, waiting for transfers between devices: 5.83 us -> 48.6 us  [shifted(): lax.ppermute(array, axis, [(i, (i + by) % peers) for i in range(peers)])]
    all_to_all x1, starting transfers between devices: 8.57 us -> 15.4 us  [per_device(): mod = lax.all_to_all(part, ('z', 'y', 'tp'), 0, 0, tiled=True)]
    pallas_call x10 -> x7, Pallas kernels: 41 us -> 35.6 us  [call(): pl.pallas_call(kernel, in_specs=in_specs or [VMEM] * len(args), out_specs...]
    unnamed x16 -> x10, local copies, waits for them, and re-layouts: 5.99 us -> 1.67 us
    ppermute x9, starting transfers between devices: 7.27 us -> 9.39 us  [shifted(): lax.ppermute(array, axis, [(i, (i + by) % peers) for i in range(peers)])]
  transfers between devices with their start and end apart: 13 -> 13, of which waited for: 3 -> 4; matrix products, arithmetic and copies ran while one was open for 1% -> 1% of each run, Pallas kernels for 24% -> 20%
where the time goes in v5:
time: 131 us; the launch traced here: 130 us
  waiting for transfers between devices  48.6 us (37%)
  starting transfers between devices  42.1 us (32%)
  Pallas kernels  35.6 us (27%)
  local copies, waits for them, and re-layouts  1.67 us (1%)
  other arithmetic  1.54 us (1%)
    ppermute x9, waiting for transfers between devices, shifted(): lax.ppermute(array, axis, [(i, (i + by) % peers) for i in range(peers)])  48.6 us
    pallas_call x7, Pallas kernels, call(): pl.pallas_call(kernel, in_specs=in_specs or [VMEM] * len(args), out_specs...  35.6 us
    all_to_all x1, starting transfers between devices, per_device(): mod = lax.all_to_all(part, ('z', 'y', 'tp'), 0, 0, tiled=True)  15.4 us
    ppermute x9, starting transfers between devices, shifted(): lax.ppermute(array, axis, [(i, (i + by) % peers) for i in range(peers)])  9.39 us
    all_to_all x1, starting transfers between devices, per_device(): lax.all_to_all(ctx_kv, SP, 0, 0, tiled=True).reshape(-1, 2 * HEAD_DIM)  9.33 us
    ppermute x1, starting transfers between devices, per_device(): after = lax.ppermute(first_rows, SP, [(j, i) for i, j in up])  4.56 us
    ppermute x1, starting transfers between devices, per_device(): before = lax.ppermute(last_rows, SP, up)  3.38 us
  transfers between devices with their start and end apart: 13, of which 4 were waited for; matrix products, arithmetic and copies ran while one was open for 1% of the time, Pallas kernels for 20%

profile of v5, /device:TPU:32, one launch (start us, length us, event | category | flops | bytes accessed | tf_op | source)
XLA Modules:
  0.0 129.9 jit_solution(12657511363741182275)
XLA Ops:
  0.0 3.7 %shard_map.145 = (bf16[128,24,128]{2,1,0:T(8,128)(2,1)}, bf16[512,1024]{1,0:T(8,128)(2,1)}, bf16[128,2048]{1,0:T(8,128)(2,1)}, bf16[128,2048]{1,0:T(8,128)(2,1)}) custom-call(f32[1,2048]{1,0:T(1,128)} %cond_in.1, f32[1,2048]{1,0:T(1,128)} %bitcast.18, bf16[64,512]{1,0:T(8,128)(2,1)} %shift_in.1, bf16[64,512]{1,0:T(8,128)(2,1)} %scale_in.1, ...), custom_call_target="tpu_custom_call" | custom-call | flops 1048576 | bytes 262144 | tf_op jit(solution)/shard_map/pallas_call | solution.py:380
  3.7 15.4 %all-to-all-start = ((bf16[128,24,128]{2,1,0:T(8,128)(2,1)}), bf16[128,24,128]{2,1,0:T(8,128)(2,1)}, u32[]{:S(2)}, u32[]{:S(2)}) async-start(bf16[128,24,128]{2,1,0:T(8,128)(2,1)} %get-tuple-element.15), calls=%async_computation | async-start | bytes 1572864 | tf_op jit(solution)/shard_map/all_to_all | solution.py:417
  19.2 2.8 %collective-permute-start.7 = (bf16[512,1024]{1,0:T(8,128)(2,1)}, bf16[512,1024]{1,0:T(8,128)(2,1)S(1)}, u32[]{:S(2)}, u32[]{:S(2)}) collective-permute-start(bf16[512,1024]{1,0:T(8,128)(2,1)} %get-tuple-element.23), channel_id=1, source_target_pairs={{0,6},{2,0},{4,2},{6,4},{1,7},{3,1},{5,3},{7,5},{8,14},{10,8},{12,... | collective-permute-start | bytes 3145736 | tf_op jit(solution)/shard_map/ppermute | solution.py:369
  21.9 2.3 %collective-permute-start.6 = (bf16[512,1024]{1,0:T(8,128)(2,1)}, bf16[512,1024]{1,0:T(8,128)(2,1)S(1)}, u32[]{:S(2)}, u32[]{:S(2)}) collective-permute-start(bf16[512,1024]{1,0:T(8,128)(2,1)} %get-tuple-element.23), channel_id=1, source_target_pairs={{0,4},{2,6},{4,0},{6,2},{1,5},{3,7},{5,1},{7,3},{8,12},{10,14},{12... | collective-permute-start | bytes 3145736 | tf_op jit(solution)/shard_map/ppermute | solution.py:369
  24.2 3.4 %collective-permute-start = (bf16[128,2048]{1,0:T(8,128)(2,1)}, bf16[128,2048]{1,0:T(8,128)(2,1)}, u32[]{:S(2)}, u32[]{:S(2)}) collective-permute-start(bf16[128,2048]{1,0:T(8,128)(2,1)} %get-tuple-element.17), channel_id=1, source_target_pairs={{0,8},{8,16},{16,24},{24,32},{32,40},{40,48},{48,56},{56,64},{64,7... | collective-permute-start | bytes 1572872 | tf_op jit(solution)/shard_map/ppermute | solution.py:420
  27.6 4.6 %collective-permute-start.1 = (bf16[128,2048]{1,0:T(8,128)(2,1)}, bf16[128,2048]{1,0:T(8,128)(2,1)}, u32[]{:S(2)}, u32[]{:S(2)}) collective-permute-start(bf16[128,2048]{1,0:T(8,128)(2,1)} %get-tuple-element.18), channel_id=1, source_target_pairs={{8,0},{16,8},{24,16},{32,24},{40,32},{48,40},{56,48},{64,56},{72,6... | collective-permute-start | bytes 1572872 | tf_op jit(solution)/shard_map/ppermute | solution.py:421
  32.2 19.7 %collective-permute-done.7.m3_in = bf16[512,1024]{1,0:T(8,128)(2,1)S(1)} collective-permute-done((bf16[512,1024]{1,0:T(8,128)(2,1)}, bf16[512,1024]{1,0:T(8,128)(2,1)S(1)}, u32[]{:S(2)}, u32[]{:S(2)}) %collective-permute-start.7) | collective-permute-done | bytes 1048608 | tf_op jit(solution)/shard_map/ppermute | solution.py:369
  51.9 24.2 %collective-permute-done.5.m1_in = bf16[512,1024]{1,0:T(8,128)(2,1)S(1)} collective-permute-done((bf16[512,1024]{1,0:T(8,128)(2,1)}, bf16[512,1024]{1,0:T(8,128)(2,1)S(1)}, u32[]{:S(2)}, u32[]{:S(2)}) %collective-permute-start.5) | collective-permute-done | bytes 1048608 | tf_op jit(solution)/shard_map/ppermute | solution.py:369
  76.1 0.5 collective-permute-start.9
  76.6 2.7 %shard_map.146 = (bf16[32,24,256]{2,1,0:T(8,128)(2,1)}, f32[8,2048]{1,0:T(8,128)}) custom-call(bf16[128,24,128]{2,1,0:T(8,128)(2,1)} %all-to-all-done.mod_ref, bf16[24,2048]{1,0:T(8,128)(2,1)} %bitcast.17, bf16[2048,128]{1,0:T(8,128)(2,1)} %wk_in.1, bf16[2048,128]{1,0:T(8,128)(2,1)} %wv_in.1, f32[1,2048]{1,0:T(1,128)} %bitcast.19, f32[1,128]{1,0:T(1,128)} %bitcast.20), custom_call_target="tpu_custom_call" | custom-call | flops 25165824 | bytes 1048576 | tf_op jit(solution)/shard_map/pallas_call | solution.py:380
  79.3 9.3 %all-to-all-start.1 = ((bf16[32,24,256]{2,1,0:T(8,128)(2,1)}), bf16[32,24,256]{2,1,0:T(8,128)(2,1)S(1)}, u32[]{:S(2)}, u32[]{:S(2)}) async-start(bf16[32,24,256]{2,1,0:T(8,128)(2,1)} %get-tuple-element.20), calls=%async_computation.1 | async-start | bytes 786432 | tf_op jit(solution)/shard_map/all_to_all | solution.py:450
  88.6 0.7 fusion.2
  89.4 0.8 multiply_select_fusion
  90.2 14.8 %shard_map.147 = (bf16[9,512,256]{2,1,0:T(8,128)(2,1)}, bf16[256,2048]{1,0:T(8,128)(2,1)}) custom-call(bf16[1024,2048]{1,0:T(8,128)(2,1)} %bitcast.16, bf16[128,2048]{1,0:T(8,128)(2,1)} %collective-permute-done.before_in, bf16[128,2048]{1,0:T(8,128)(2,1)} %collective-permute-done.1.after_in, bf16[2048,512]{1,0:T(8,128)(2,1)} %wq_in.1, ...), custom_call_target="tpu_custom_call" | custom-call | flops 4026531840 | bytes 7340032 | tf_op jit(solution)/shard_map/pallas_call | solution.py:380
  105.0 1.7 %copy-done = bf16[9,512,256]{2,1,0:T(8,128)(2,1)S(1)} copy-done((bf16[9,512,256]{2,1,0:T(8,128)(2,1)S(1)}, bf16[9,512,256]{2,1,0:T(8,128)(2,1)}, u32[]{:S(2)}) %copy-start) | copy-done | bytes 2359320
  106.6 2.3 %shard_map.150 = bf16[256,512]{1,0:T(8,128)(2,1)S(1)} custom-call(bf16[9,512,256]{2,1,0:T(8,128)(2,1)S(1)} %copy-done, bf16[768,256]{1,0:T(8,128)(2,1)S(1)} %bitcast.9, f32[1,4]{1,0:T(1,128)S(1)} %bitcast.12), custom_call_target="tpu_custom_call" | custom-call | flops 402653184 | bytes 2097152 | tf_op jit(solution)/shard_map/pallas_call | solution.py:380
  109.0 0.5 collective-permute-start.3
  109.5 4.1 %shard_map.149 = (bf16[256,512]{1,0:T(8,128)(2,1)S(1)}, bf16[256,512]{1,0:T(8,128)(2,1)S(1)}) custom-call(bf16[9,512,256]{2,1,0:T(8,128)(2,1)S(1)} %copy-done, bf16[768,256]{1,0:T(8,128)(2,1)S(1)} %bitcast.10, f32[1,4]{1,0:T(1,128)S(1)} %bitcast.13), custom_call_target="tpu_custom_call" | custom-call | flops 805306368 | bytes 2097152 | tf_op jit(solution)/shard_map/pallas_call | solution.py:380
  113.6 1.4 %collective-permute-start.2 = (bf16[256,512]{1,0:T(8,128)(2,1)S(1)}, bf16[256,512]{1,0:T(8,128)(2,1)S(1)}, u32[]{:S(2)}, u32[]{:S(2)}) collective-permute-start(bf16[256,512]{1,0:T(8,128)(2,1)S(1)} %get-tuple-element.21), channel_id=1, source_target_pairs={{0,2},{2,4},{4,6},{6,0},{1,3},{3,5},{5,7},{7,1},{8,10},{10,12},{12... | collective-permute-start | bytes 786440 | tf_op jit(solution)/shard_map/ppermute | solution.py:369
  115.0 1.9 %collective-permute-start.4 = (bf16[256,512]{1,0:T(8,128)(2,1)S(1)}, bf16[256,512]{1,0:T(8,128)(2,1)S(1)}, u32[]{:S(2)}, u32[]{:S(2)}) collective-permute-start(bf16[256,512]{1,0:T(8,128)(2,1)S(1)} %get-tuple-element.22), channel_id=1, source_target_pairs={{0,6},{2,0},{4,2},{6,4},{1,7},{3,1},{5,3},{7,5},{8,14},{10,8},{12,... | collective-permute-start | bytes 786440 | tf_op jit(solution)/shard_map/ppermute | solution.py:369
  116.9 2.3 %shard_map.148.a0_ref = bf16[256,512]{1,0:T(8,128)(2,1)S(1)} custom-call(bf16[9,512,256]{2,1,0:T(8,128)(2,1)S(1)} %copy-done, bf16[768,256]{1,0:T(8,128)(2,1)S(1)} %bitcast.11, f32[1,4]{1,0:T(1,128)S(1)} %bitcast.14), custom_call_target="tpu_custom_call" | custom-call | flops 402653184 | bytes 2097152 | tf_op jit(solution)/shard_map/pallas_call | solution.py:380
  119.3 0.2 collective-permute-done.3.a2_ref
  119.5 4.6 %collective-permute-done.2.a1_ref = bf16[256,512]{1,0:T(8,128)(2,1)S(1)} collective-permute-done((bf16[256,512]{1,0:T(8,128)(2,1)S(1)}, bf16[256,512]{1,0:T(8,128)(2,1)S(1)}, u32[]{:S(2)}, u32[]{:S(2)}) %collective-permute-start.2) | collective-permute-done | bytes 262176 | tf_op jit(solution)/shard_map/ppermute | solution.py:369
  124.0 5.7 %shard_map.151 = bf16[256,2048]{1,0:T(8,128)(2,1)} custom-call(f32[8,2048]{1,0:T(8,128)S(1)} %copy-done.3, bf16[256,512]{1,0:T(8,128)(2,1)S(1)} %shard_map.148.a0_ref, bf16[256,512]{1,0:T(8,128)(2,1)S(1)} %collective-permute-done.2.a1_ref, bf16[256,512]{1,0:T(8,128)(2,1)S(1)} %collective-permute-done.3.a2_ref, ...), custom_call_target="tpu_custom_call" | custom-call | flops 2147483648 | bytes 8388608 | tf_op jit(solution)/shard_map/pallas_call | solution.py:380
  (24 shorter events, 0.1 us)
Async XLA Ops:
  3.7 72.9 %all-to-all-start = ((bf16[128,24,128]{2,1,0:T(8,128)(2,1)}), bf16[128,24,128]{2,1,0:T(8,128)(2,1)}, u32[]{:S(2)}, u32[]{:S(2)}) async-start(bf16[128,24,128]{2,1,0:T(8,128)(2,1)} %get-tuple-element.15), calls=%async_computation | async-start | bytes 1572864 | tf_op jit(solution)/shard_map/all_to_all | solution.py:417
  19.2 32.7 %collective-permute-start.7 = (bf16[512,1024]{1,0:T(8,128)(2,1)}, bf16[512,1024]{1,0:T(8,128)(2,1)S(1)}, u32[]{:S(2)}, u32[]{:S(2)}) collective-permute-start(bf16[512,1024]{1,0:T(8,128)(2,1)} %get-tuple-element.23), channel_id=1, source_target_pairs={{0,6},{2,0},{4,2},{6,4},{1,7},{3,1},{5,3},{7,5},{8,14},{10,8},{12,... | collective-permute-start | bytes 3145736 | tf_op jit(solution)/shard_map/ppermute | solution.py:369
  21.9 54.2 %collective-permute-start.5 = (bf16[512,1024]{1,0:T(8,128)(2,1)}, bf16[512,1024]{1,0:T(8,128)(2,1)S(1)}, u32[]{:S(2)}, u32[]{:S(2)}) collective-permute-start(bf16[512,1024]{1,0:T(8,128)(2,1)} %get-tuple-element.23), channel_id=1, source_target_pairs={{0,2},{2,4},{4,6},{6,0},{1,3},{3,5},{5,7},{7,1},{8,10},{10,12},{12... | collective-permute-start | bytes 3145736 | tf_op jit(solution)/shard_map/ppermute | solution.py:369
  21.9 54.2 %collective-permute-start.6 = (bf16[512,1024]{1,0:T(8,128)(2,1)}, bf16[512,1024]{1,0:T(8,128)(2,1)S(1)}, u32[]{:S(2)}, u32[]{:S(2)}) collective-permute-start(bf16[512,1024]{1,0:T(8,128)(2,1)} %get-tuple-element.23), channel_id=1, source_target_pairs={{0,4},{2,6},{4,0},{6,2},{1,5},{3,7},{5,1},{7,3},{8,12},{10,14},{12... | collective-permute-start | bytes 3145736 | tf_op jit(solution)/shard_map/ppermute | solution.py:369
  24.2 65.9 %collective-permute-start = (bf16[128,2048]{1,0:T(8,128)(2,1)}, bf16[128,2048]{1,0:T(8,128)(2,1)}, u32[]{:S(2)}, u32[]{:S(2)}) collective-permute-start(bf16[128,2048]{1,0:T(8,128)(2,1)} %get-tuple-element.17), channel_id=1, source_target_pairs={{0,8},{8,16},{16,24},{24,32},{32,40},{40,48},{48,56},{56,64},{64,7... | collective-permute-start | bytes 1572872 | tf_op jit(solution)/shard_map/ppermute | solution.py:420
  27.6 62.5 %collective-permute-start.1 = (bf16[128,2048]{1,0:T(8,128)(2,1)}, bf16[128,2048]{1,0:T(8,128)(2,1)}, u32[]{:S(2)}, u32[]{:S(2)}) collective-permute-start(bf16[128,2048]{1,0:T(8,128)(2,1)} %get-tuple-element.18), channel_id=1, source_target_pairs={{8,0},{16,8},{24,16},{32,24},{40,32},{48,40},{56,48},{64,56},{72,6... | collective-permute-start | bytes 1572872 | tf_op jit(solution)/shard_map/ppermute | solution.py:421
  51.9 63.1 %collective-permute-start.10 = (bf16[512,1024]{1,0:T(8,128)(2,1)S(1)}, bf16[512,1024]{1,0:T(8,128)(2,1)}, u32[]{:S(2)}, u32[]{:S(2)}) collective-permute-start(bf16[512,1024]{1,0:T(8,128)(2,1)S(1)} %collective-permute-done.7.m3_in), channel_id=1, source_target_pairs={{0,1},{1,0},{2,3},{3,2},{4,5},{5,4},{6,7},{7,6},{8,9},{9,8},{10,11... | collective-permute-start | bytes 3145736 | tf_op jit(solution)/shard_map/ppermute | solution.py:369
  76.1 43.2 %collective-permute-start.8 = (bf16[512,1024]{1,0:T(8,128)(2,1)S(1)}, bf16[512,1024]{1,0:T(8,128)(2,1)}, u32[]{:S(2)}, u32[]{:S(2)}) collective-permute-start(bf16[512,1024]{1,0:T(8,128)(2,1)S(1)} %collective-permute-done.5.m1_in), channel_id=1, source_target_pairs={{0,1},{1,0},{2,3},{3,2},{4,5},{5,4},{6,7},{7,6},{8,9},{9,8},{10,11... | collective-permute-start | bytes 3145736 | tf_op jit(solution)/shard_map/ppermute | solution.py:369
  76.1 43.2 %collective-permute-start.9 = (bf16[512,1024]{1,0:T(8,128)(2,1)S(1)}, bf16[512,1024]{1,0:T(8,128)(2,1)}, u32[]{:S(2)}, u32[]{:S(2)}) collective-permute-start(bf16[512,1024]{1,0:T(8,128)(2,1)S(1)} %collective-permute-done.6.m2_in), channel_id=1, source_target_pairs={{0,1},{1,0},{2,3},{3,2},{4,5},{5,4},{6,7},{7,6},{8,9},{9,8},{10,11... | collective-permute-start | bytes 3145736 | tf_op jit(solution)/shard_map/ppermute | solution.py:369
  79.3 25.6 %all-to-all-start.1 = ((bf16[32,24,256]{2,1,0:T(8,128)(2,1)}), bf16[32,24,256]{2,1,0:T(8,128)(2,1)S(1)}, u32[]{:S(2)}, u32[]{:S(2)}) async-start(bf16[32,24,256]{2,1,0:T(8,128)(2,1)} %get-tuple-element.20), calls=%async_computation.1 | async-start | bytes 786432 | tf_op jit(solution)/shard_map/all_to_all | solution.py:450
  90.2 14.8 %copy-start.4 = (f32[4]{0:T(128)S(1)}, f32[4]{0:T(128)}, u32[]{:S(2)}) copy-start(f32[4]{0:T(128)} %param.29) | copy-start | bytes 52
  105.0 1.7 %copy-start = (bf16[9,512,256]{2,1,0:T(8,128)(2,1)S(1)}, bf16[9,512,256]{2,1,0:T(8,128)(2,1)}, u32[]{:S(2)}) copy-start(bf16[9,512,256]{2,1,0:T(8,128)(2,1)} %get-tuple-element.19.refs_0_) | copy-start | bytes 7077892
  109.0 15.1 %copy-start.1 = (bf16[512,2048]{1,0:T(8,128)(2,1)S(1)}, bf16[512,2048]{1,0:T(8,128)(2,1)}, u32[]{:S(2)}) copy-start(bf16[512,2048]{1,0:T(8,128)(2,1)} %w0_ref.1) | copy-start | bytes 6291460
  109.0 15.1 %copy-start.2 = (bf16[256,2048]{1,0:T(8,128)(2,1)S(1)}, bf16[256,2048]{1,0:T(8,128)(2,1)}, u32[]{:S(2)}) copy-start(bf16[256,2048]{1,0:T(8,128)(2,1)} %get-tuple-element.24.lat_ref) | copy-start | bytes 3145732
  109.0 15.1 %copy-start.3 = (f32[8,2048]{1,0:T(8,128)S(1)}, f32[8,2048]{1,0:T(8,128)}, u32[]{:S(2)}) copy-start(f32[8,2048]{1,0:T(8,128)} %get-tuple-element.16.vec_ref) | copy-start | bytes 196612
  109.0 10.5 %collective-permute-start.3 = (bf16[256,512]{1,0:T(8,128)(2,1)S(1)}, bf16[256,512]{1,0:T(8,128)(2,1)S(1)}, u32[]{:S(2)}, u32[]{:S(2)}) collective-permute-start(bf16[256,512]{1,0:T(8,128)(2,1)S(1)} %shard_map.150), channel_id=1, source_target_pairs={{0,4},{2,6},{4,0},{6,2},{1,5},{3,7},{5,1},{7,3},{8,12},{10,14},{12... | collective-permute-start | bytes 786440 | tf_op jit(solution)/shard_map/ppermute | solution.py:369
  113.6 10.4 %collective-permute-start.2 = (bf16[256,512]{1,0:T(8,128)(2,1)S(1)}, bf16[256,512]{1,0:T(8,128)(2,1)S(1)}, u32[]{:S(2)}, u32[]{:S(2)}) collective-permute-start(bf16[256,512]{1,0:T(8,128)(2,1)S(1)} %get-tuple-element.21), channel_id=1, source_target_pairs={{0,2},{2,4},{4,6},{6,0},{1,3},{3,5},{5,7},{7,1},{8,10},{10,12},{12... | collective-permute-start | bytes 786440 | tf_op jit(solution)/shard_map/ppermute | solution.py:369
  115.0 9.0 %collective-permute-start.4 = (bf16[256,512]{1,0:T(8,128)(2,1)S(1)}, bf16[256,512]{1,0:T(8,128)(2,1)S(1)}, u32[]{:S(2)}, u32[]{:S(2)}) collective-permute-start(bf16[256,512]{1,0:T(8,128)(2,1)S(1)} %get-tuple-element.22), channel_id=1, source_target_pairs={{0,6},{2,0},{4,2},{6,4},{1,7},{3,1},{5,3},{7,5},{8,14},{10,8},{12,... | collective-permute-start | bytes 786440 | tf_op jit(solution)/shard_map/ppermute | solution.py:369

commit v6 on v4

--- a/solution.py
+++ b/solution.py
@@ -122,13 +122,18 @@
     return v * cosine + swapped * sine
 
 
-def stage_kernel(w_in, lat_in, half_ref, first_ref, last_ref, sems):
+def stage_weight_kernel(w_in, half_ref, sem):
+    start = pl.multiple_of(lax.axis_index("dp") * (D // 2), D // 2)
+    move = pltpu.make_async_copy(w_in.at[:, pl.ds(start, D // 2)], half_ref, sem)
+    move.start()
+    move.wait()
+
+
+def stage_rows_kernel(lat_in, first_ref, last_ref, sems):
     tok = lat_in.shape[0]
-    start = pl.multiple_of(lax.axis_index("dp") * (D // 2), D // 2)
     moves = [
-        pltpu.make_async_copy(w_in.at[:, pl.ds(start, D // 2)], half_ref, sems.at[0]),
-        pltpu.make_async_copy(lat_in.at[:WINDOW, :], first_ref, sems.at[1]),
-        pltpu.make_async_copy(lat_in.at[tok - WINDOW :, :], last_ref, sems.at[2]),
+        pltpu.make_async_copy(lat_in.at[:WINDOW, :], first_ref, sems.at[0]),
+        pltpu.make_async_copy(lat_in.at[tok - WINDOW :, :], last_ref, sems.at[1]),
     ]
     for move in moves:
         move.start()
@@ -136,41 +141,26 @@
         move.wait()
 
 
-def own_kernel(lat_in, own_ref, sem):
-    sub = own_ref.shape[0]
-    first = pl.multiple_of(lax.axis_index("tp") * sub, sub)
-    move = pltpu.make_async_copy(lat_in.at[pl.ds(first, sub), :], own_ref, sem)
-    move.start()
-    move.wait()
-
-
 def context_kernel(
-    mod_ref, ctx_ref, wk_in, wv_in, gain_ref, kgain_ref, kv_ref, vec_ref, wkv_ref, sems
+    mod_ref, ctx_ref, wk_ref, wv_ref, gain_ref, kgain_ref, kv_ref, vec_ref
 ):
-    moves = [
-        pltpu.make_async_copy(wk_in, wkv_ref.at[:, :HEAD_DIM], sems.at[0]),
-        pltpu.make_async_copy(wv_in, wkv_ref.at[:, HEAD_DIM:], sems.at[1]),
-    ]
-    for move in moves:
-        move.start()
     shift_lat, scale_lat, shift_ctx, scale_ctx, gate = vectors_of(mod_ref)
     gain = gain_ref[...]
     vec_ref[0:1, :] = gain * (1.0 + scale_lat)
     vec_ref[1:2, :] = shift_lat
     vec_ref[2:3, :] = gate
     rows = (normed(ctx_ref[...]) * (gain * (1.0 + scale_ctx)) + shift_ctx).astype(BF16)
-    for move in moves:
-        move.wait()
-    both = jnp.dot(rows, wkv_ref[...], preferred_element_type=F32)
-    keys = head_norm(both[:, :HEAD_DIM], kgain_ref[...])
-    both = jnp.concatenate([keys, both[:, HEAD_DIM:]], axis=1).astype(BF16)
+    keys = head_norm(jnp.dot(rows, wk_ref[...], preferred_element_type=F32), kgain_ref[...])
+    values = jnp.dot(rows, wv_ref[...], preferred_element_type=F32)
+    both = jnp.concatenate([keys, values], axis=1).astype(BF16)
     kv_ref[...] = jnp.broadcast_to(both[None], kv_ref.shape)
 
 
 def qkv_kernel(
     lat_in, before_in, after_in, wq_in, wk_in, wv_in,
     vec_ref, qgain_ref, kgain_ref, rcos_ref, rsin_ref, ccos_ref, csin_ref,
-    out_ref, lat_ref, wq_ref, wkv_ref, k_ref, v_ref, even_ref, odd_ref, sum_ref, sems,
+    packed_out, own_ref, out_ref, lat_ref, wq_ref, wkv_ref, k_ref, v_ref, even_ref, odd_ref,
+    sum_ref, sems,
 ):
     step = 256
     tok = lat_in.shape[0]
@@ -249,12 +239,25 @@
         return carry
 
     lax.fori_loop(0, steps // 2, body, 0)
+    own_move = pltpu.make_async_copy(
+        lat_ref.at[at(lax.axis_index("tp"), own_ref.shape[0]), :], own_ref, sems.at[steps + 5]
+    )
+    own_move.start()
     beyond = (tok + WINDOW) // GRID_W
     keys, values = keys_of(even_ref, *tables([0, 1, beyond, beyond + 1]))
     for ref, rows in ((k_ref, keys), (v_ref, values)):
         ref[:WINDOW, :] = rows[:WINDOW]
         ref[tok + WINDOW :, :] = rows[WINDOW:]
-    local_pass(out_ref, k_ref, v_ref, sum_ref)
+
+    def block_move(block):
+        return pltpu.make_async_copy(
+            out_ref.at[block], packed_out.at[block], sems.at[steps + 6 + block]
+        )
+
+    local_pass(out_ref, k_ref, v_ref, sum_ref, block_move)
+    for block in range(packed_out.shape[0]):
+        block_move(block).wait()
+    own_move.wait()
 
 
 def contract_last(a, b):
@@ -268,7 +271,7 @@
     return parts[0]
 
 
-def local_pass(out_ref, k_ref, v_ref, sum_ref):
+def local_pass(out_ref, k_ref, v_ref, sum_ref, block_move):
     sp = sp_index()
     blocks = out_ref.shape[0] - 1
     query_at = lax.broadcasted_iota(jnp.int32, (4 * WINDOW, WINDOW), 0) % WINDOW
@@ -294,12 +297,14 @@
         sum_ref[...] = jnp.where(key_at == block, total, sum_ref[...])
         mixed = jnp.dot(local.astype(BF16), v_ref[near, :], preferred_element_type=F32)
         out_ref[block, :, HEAD_DIM:] = mixed.astype(BF16)
+        block_move(block).start()
         return carry
 
     lax.fori_loop(0, blocks, body, 0)
     high = sum_ref[...].astype(BF16)
     out_ref[blocks, :, :HEAD_DIM] = high
     out_ref[blocks, :, HEAD_DIM:] = (sum_ref[...] - high.astype(F32)).astype(BF16)
+    block_move(blocks).start()
 
 
 def attend_kernel(shifts, packed_ref, ctx_ref, sink_ref, *out_refs):
@@ -423,15 +428,13 @@
     part = call(resum_kernel, [((NZ, NX * VECS, 128), BF16)], (part,), cost(1 << 20, 1 << 18), 4)
     mod = lax.all_to_all(part, "z", 0, 0, tiled=True)
 
-    half, first_rows, last_rows = call(
-        stage_kernel,
-        [((width, D // 2), BF16), ((WINDOW, D), BF16), ((WINDOW, D), BF16)],
-        (w_out, lat), cost(1 << 24, 4 << 20), 60,
-        scratch=[pltpu.SemaphoreType.DMA((3,))], in_specs=[HBM] * 2,
-    )
-    own = call(
-        own_kernel, [((sub, D), BF16)], (lat,), cost(1 << 24, 2 << 20), 62,
-        scratch=[pltpu.SemaphoreType.DMA], in_specs=[HBM],
+    half = call(
+        stage_weight_kernel, [((width, D // 2), BF16)], (w_out,),
+        cost(1 << 24, 2 << 20), 60, scratch=[pltpu.SemaphoreType.DMA], in_specs=[HBM],
+    )
+    first_rows, last_rows = call(
+        stage_rows_kernel, [((WINDOW, D), BF16)] * 2, (lat,),
+        cost(1 << 24, 2 << 20), 60, scratch=[pltpu.SemaphoreType.DMA((2,))], in_specs=[HBM],
     )
     peers = NZ * NY
     up = [(i, i + 1) for i in range(peers - 1)]
@@ -464,27 +467,28 @@
         [((peers, n_ctx, 2 * HEAD_DIM), BF16), ((8, D), F32)],
         (mod, context[0], w_key, w_value, gain, kgain),
         cost(2 * n_ctx * D * 256, D * 512), 63,
-        scratch=[pltpu.VMEM((D, 2 * HEAD_DIM), BF16), pltpu.SemaphoreType.DMA((2,))],
-        in_specs=[VMEM, VMEM, HBM, HBM, VMEM, VMEM],
     )
     ctx_all = lax.all_to_all(ctx_kv, SP, 0, 0, tiled=True).reshape(-1, 2 * HEAD_DIM)
 
-    packed = call(
-        qkv_kernel, [((tok // WINDOW + 1, 4 * WINDOW, 2 * HEAD_DIM), BF16)],
+    packed_shape = (tok // WINDOW + 1, 4 * WINDOW, 2 * HEAD_DIM)
+    packed, own = call(
+        qkv_kernel, [(packed_shape, BF16), ((sub, D), BF16)],
         (
             lat, before, after, w_query, w_key, w_value, vec, qgain, kgain,
             row_cos, row_sin, col_cos, col_sin,
         ),
         cost(2 * tok * D * 768 + 16 * tok * 384 * HEAD_DIM, tok * D * 2 + D * 768 * 2), 60,
         scratch=[
+            pltpu.VMEM(packed_shape, BF16),
             pltpu.VMEM((rows, D), BF16), pltpu.VMEM((D, width), BF16),
             pltpu.VMEM((D, 2 * HEAD_DIM), BF16),
             pltpu.VMEM((rows, HEAD_DIM), BF16), pltpu.VMEM((rows, HEAD_DIM), BF16),
             pltpu.VMEM((256, D), BF16), pltpu.VMEM((256, D), BF16),
             pltpu.VMEM((4 * WINDOW, 128), F32),
-            pltpu.SemaphoreType.DMA((tok // 256 + 5,)),
+            pltpu.SemaphoreType.DMA((tok // 256 + 6 + packed_shape[0],)),
         ],
         in_specs=[HBM] * 6 + [VMEM] * 7,
+        out_specs=[HBM, HBM],
     )
 
     arrived = {}

time: 136 us -> 132 us (0.971)
  Pallas kernels: 41 us -> 36.5 us
  waiting for transfers between devices: 5.93 us -> 10.2 us
  local copies, waits for them, and re-layouts: 5.99 us -> 2.31 us
    pallas_call x10, Pallas kernels: 41 us -> 36.5 us  [call(): pl.pallas_call(kernel, in_specs=in_specs or [VMEM] * len(args), out_specs...]
    ppermute x9, waiting for transfers between devices: 5.83 us -> 10.1 us  [shifted(): lax.ppermute(array, axis, [(i, (i + by) % peers) for i in range(peers)])]
    unnamed x16 -> x12, local copies, waits for them, and re-layouts: 5.99 us -> 2.31 us
  transfers between devices with their start and end apart: 13 -> 13, of which waited for: 3 -> 3; matrix products, arithmetic and copies ran while one was open for 1% -> 1% of each run, Pallas kernels for 24% -> 23%
where the time goes in v6:
time: 132 us; the launch traced here: 131 us
  blocking collectives  48 us (36%)
  Pallas kernels  36.5 us (28%)
  starting transfers between devices  32.4 us (25%)
  waiting for transfers between devices  10.2 us (8%)
  local copies, waits for them, and re-layouts  2.31 us (2%)
  other arithmetic  1.5 us (1%)
    all_to_all x1, blocking collectives, per_device(): part = lax.all_to_all(part, ('y', 'tp'), 0, 0, tiled=True)  48 us
    pallas_call x10, Pallas kernels, call(): pl.pallas_call(kernel, in_specs=in_specs or [VMEM] * len(args), out_specs...  36.5 us
    ppermute x9, waiting for transfers between devices, shifted(): lax.ppermute(array, axis, [(i, (i + by) % peers) for i in range(peers)])  10.1 us
    all_to_all x1, starting transfers between devices, per_device(): lax.all_to_all(ctx_kv, SP, 0, 0, tiled=True).reshape(-1, 2 * HEAD_DIM)  8.57 us
    all_to_all x1, starting transfers between devices, per_device(): mod = lax.all_to_all(part, 'z', 0, 0, tiled=True)  8.57 us
    ppermute x9, starting transfers between devices, shifted(): lax.ppermute(array, axis, [(i, (i + by) % peers) for i in range(peers)])  7.35 us
    ppermute x1, starting transfers between devices, per_device(): after = lax.ppermute(first_rows, SP, [(j, i) for i, j in up])  5.37 us
  transfers between devices with their start and end apart: 13, of which 3 were waited for; matrix products, arithmetic and copies ran while one was open for 1% of the time, Pallas kernels for 23%

profile of v6, /device:TPU:32, one launch (start us, length us, event | category | flops | bytes accessed | tf_op | source)
XLA Modules:
  0.0 131.2 jit_solution(4234373575077730792)
XLA Ops:
  0.0 2.2 %shard_map.153 = bf16[512,1024]{1,0:T(8,128)(2,1)} custom-call(bf16[512,2048]{1,0:T(8,128)(2,1)} %w0_ref.1), custom_call_target="tpu_custom_call" | custom-call | flops 16777216 | bytes 2097152 | tf_op jit(solution)/shard_map/pallas_call | solution.py:396
  2.2 2.8 %collective-permute-start.7 = (bf16[512,1024]{1,0:T(8,128)(2,1)}, bf16[512,1024]{1,0:T(8,128)(2,1)}, u32[]{:S(2)}, u32[]{:S(2)}) collective-permute-start(bf16[512,1024]{1,0:T(8,128)(2,1)} %shard_map.153), channel_id=1, source_target_pairs={{0,6},{2,0},{4,2},{6,4},{1,7},{3,1},{5,3},{7,5},{8,14},{10,8},{12,... | collective-permute-start | bytes 3145736 | tf_op jit(solution)/shard_map/ppermute | solution.py:385
  5.0 2.3 %collective-permute-start.6 = (bf16[512,1024]{1,0:T(8,128)(2,1)}, bf16[512,1024]{1,0:T(8,128)(2,1)}, u32[]{:S(2)}, u32[]{:S(2)}) collective-permute-start(bf16[512,1024]{1,0:T(8,128)(2,1)} %shard_map.153), channel_id=1, source_target_pairs={{0,4},{2,6},{4,0},{6,2},{1,5},{3,7},{5,1},{7,3},{8,12},{10,14},{12... | collective-permute-start | bytes 3145736 | tf_op jit(solution)/shard_map/ppermute | solution.py:385
  7.3 1.8 %shard_map.145 = bf16[16,24,128]{2,1,0:T(8,128)(2,1)} custom-call(f32[1,2048]{1,0:T(1,128)} %cond_in.1, f32[1,2048]{1,0:T(1,128)} %bitcast.19, bf16[64,512]{1,0:T(8,128)(2,1)} %shift_in.1, bf16[64,512]{1,0:T(8,128)(2,1)} %scale_in.1, bf16[64,512]{1,0:T(8,128)(2,1)} %gate_in.1), custom_call_target="tpu_custom_call" | custom-call | flops 1048576 | bytes 262144 | tf_op jit(solution)/shard_map/pallas_call | solution.py:396
  9.1 48.0 %all_to_all.15.in_ref = bf16[16,24,128]{2,1,0:T(8,128)(2,1)S(1)} all-to-all(bf16[16,24,128]{2,1,0:T(8,128)(2,1)} %shard_map.145), channel_id=1, replica_groups=mesh['z'=8,'y'=4,'tp'=4,'dp'=2] {'y','tp'}, dimensions={0} | all-to-all | bytes 196608 | tf_op jit(solution)/shard_map/all_to_all | solution.py:427
  57.1 0.7 shard_map.146
  57.8 8.6 %all-to-all-start.1 = ((bf16[8,80,128]{2,1,0:T(8,128)(2,1)}), bf16[8,80,128]{2,1,0:T(8,128)(2,1)S(1)}, u32[]{:S(2)}, u32[]{:S(2)}) async-start(bf16[8,80,128]{2,1,0:T(8,128)(2,1)} %shard_map.146), calls=%async_computation.1 | async-start | bytes 327680 | tf_op jit(solution)/shard_map/all_to_all | solution.py:429
  66.3 2.2 %shard_map.148 = (bf16[128,2048]{1,0:T(8,128)(2,1)}, bf16[128,2048]{1,0:T(8,128)(2,1)}) custom-call(bf16[1024,2048]{1,0:T(8,128)(2,1)} %bitcast.15), custom_call_target="tpu_custom_call" | custom-call | flops 16777216 | bytes 2097152 | tf_op jit(solution)/shard_map/pallas_call | solution.py:396
  68.6 2.6 %collective-permute-start = (bf16[128,2048]{1,0:T(8,128)(2,1)}, bf16[128,2048]{1,0:T(8,128)(2,1)}, u32[]{:S(2)}, u32[]{:S(2)}) collective-permute-start(bf16[128,2048]{1,0:T(8,128)(2,1)} %get-tuple-element.14), channel_id=1, source_target_pairs={{0,8},{8,16},{16,24},{24,32},{32,40},{40,48},{48,56},{56,64},{64,7... | collective-permute-start | bytes 1572872 | tf_op jit(solution)/shard_map/ppermute | solution.py:441
  71.2 5.4 %collective-permute-start.1 = (bf16[128,2048]{1,0:T(8,128)(2,1)}, bf16[128,2048]{1,0:T(8,128)(2,1)}, u32[]{:S(2)}, u32[]{:S(2)}) collective-permute-start(bf16[128,2048]{1,0:T(8,128)(2,1)} %get-tuple-element.15), channel_id=1, source_target_pairs={{8,0},{16,8},{24,16},{32,24},{40,32},{48,40},{56,48},{64,56},{72,6... | collective-permute-start | bytes 1572872 | tf_op jit(solution)/shard_map/ppermute | solution.py:442
  77.2 2.5 %shard_map.147 = (bf16[32,24,256]{2,1,0:T(8,128)(2,1)}, f32[8,2048]{1,0:T(8,128)}) custom-call(bf16[8,80,128]{2,1,0:T(8,128)(2,1)} %copy-done.5, bf16[24,2048]{1,0:T(8,128)(2,1)} %bitcast.17, bf16[2048,128]{1,0:T(8,128)(2,1)} %wk_in.1, bf16[2048,128]{1,0:T(8,128)(2,1)} %wv_in.1, f32[1,2048]{1,0:T(1,128)} %bitcast.18, f32[1,128]{1,0:T(1,128)} %bitcast.20), custom_call_target="tpu_custom_call" | custom-call | flops 25165824 | bytes 1048576 | tf_op jit(solution)/shard_map/pallas_call | solution.py:396
  79.7 8.6 %all-to-all-start.2 = ((bf16[32,24,256]{2,1,0:T(8,128)(2,1)}), bf16[32,24,256]{2,1,0:T(8,128)(2,1)S(1)}, u32[]{:S(2)}, u32[]{:S(2)}) async-start(bf16[32,24,256]{2,1,0:T(8,128)(2,1)} %get-tuple-element.17), calls=%async_computation.2 | async-start | bytes 786432 | tf_op jit(solution)/shard_map/all_to_all | solution.py:471
  88.3 0.8 multiply_select_fusion
  89.8 0.7 fusion.2
  90.5 14.1 %shard_map.149 = (bf16[9,512,256]{2,1,0:T(8,128)(2,1)}, bf16[256,2048]{1,0:T(8,128)(2,1)}) custom-call(bf16[1024,2048]{1,0:T(8,128)(2,1)} %bitcast.16, bf16[128,2048]{1,0:T(8,128)(2,1)} %collective-permute-done.before_in, bf16[128,2048]{1,0:T(8,128)(2,1)} %collective-permute-done.1.after_in, bf16[2048,512]{1,0:T(8,128)(2,1)} %wq_in.1, ...), custom_call_target="tpu_custom_call" | custom-call | flops 4026531840 | bytes 7340032 | tf_op jit(solution)/shard_map/pallas_call | solution.py:396
  104.7 1.7 %copy-done = bf16[9,512,256]{2,1,0:T(8,128)(2,1)S(1)} copy-done((bf16[9,512,256]{2,1,0:T(8,128)(2,1)S(1)}, bf16[9,512,256]{2,1,0:T(8,128)(2,1)}, u32[]{:S(2)}) %copy-start) | copy-done | bytes 2359320
  106.4 2.3 %shard_map.152 = bf16[256,512]{1,0:T(8,128)(2,1)S(1)} custom-call(bf16[9,512,256]{2,1,0:T(8,128)(2,1)S(1)} %copy-done, bf16[768,256]{1,0:T(8,128)(2,1)S(1)} %bitcast.9, f32[1,4]{1,0:T(1,128)S(1)} %bitcast.12), custom_call_target="tpu_custom_call" | custom-call | flops 402653184 | bytes 2097152 | tf_op jit(solution)/shard_map/pallas_call | solution.py:396
  109.3 4.1 %shard_map.151 = (bf16[256,512]{1,0:T(8,128)(2,1)S(1)}, bf16[256,512]{1,0:T(8,128)(2,1)S(1)}) custom-call(bf16[9,512,256]{2,1,0:T(8,128)(2,1)S(1)} %copy-done, bf16[768,256]{1,0:T(8,128)(2,1)S(1)} %bitcast.10, f32[1,4]{1,0:T(1,128)S(1)} %bitcast.13), custom_call_target="tpu_custom_call" | custom-call | flops 805306368 | bytes 2097152 | tf_op jit(solution)/shard_map/pallas_call | solution.py:396
  113.5 0.9 collective-permute-start.2
  114.4 5.3 %collective-permute-done.3.a2_ref = bf16[256,512]{1,0:T(8,128)(2,1)S(1)} collective-permute-done((bf16[256,512]{1,0:T(8,128)(2,1)S(1)}, bf16[256,512]{1,0:T(8,128)(2,1)S(1)}, u32[]{:S(2)}, u32[]{:S(2)}) %collective-permute-start.3) | collective-permute-done | bytes 262176 | tf_op jit(solution)/shard_map/ppermute | solution.py:385
  119.7 2.3 %shard_map.150.a0_ref = bf16[256,512]{1,0:T(8,128)(2,1)S(1)} custom-call(bf16[9,512,256]{2,1,0:T(8,128)(2,1)S(1)} %copy-done, bf16[768,256]{1,0:T(8,128)(2,1)S(1)} %bitcast.11, f32[1,4]{1,0:T(1,128)S(1)} %bitcast.14), custom_call_target="tpu_custom_call" | custom-call | flops 402653184 | bytes 2097152 | tf_op jit(solution)/shard_map/pallas_call | solution.py:396
  122.0 2.7 %collective-permute-done.2.a1_ref = bf16[256,512]{1,0:T(8,128)(2,1)S(1)} collective-permute-done((bf16[256,512]{1,0:T(8,128)(2,1)S(1)}, bf16[256,512]{1,0:T(8,128)(2,1)S(1)}, u32[]{:S(2)}, u32[]{:S(2)}) %collective-permute-start.2) | collective-permute-done | bytes 262176 | tf_op jit(solution)/shard_map/ppermute | solution.py:385
  124.7 2.1 %collective-permute-done.4.a3_ref = bf16[256,512]{1,0:T(8,128)(2,1)S(1)} collective-permute-done((bf16[256,512]{1,0:T(8,128)(2,1)S(1)}, bf16[256,512]{1,0:T(8,128)(2,1)S(1)}, u32[]{:S(2)}, u32[]{:S(2)}) %collective-permute-start.4) | collective-permute-done | bytes 262176 | tf_op jit(solution)/shard_map/ppermute | solution.py:385
  126.9 4.1 %shard_map.154 = bf16[256,2048]{1,0:T(8,128)(2,1)} custom-call(f32[8,2048]{1,0:T(8,128)S(1)} %copy-done.3, bf16[256,512]{1,0:T(8,128)(2,1)S(1)} %shard_map.150.a0_ref, bf16[256,512]{1,0:T(8,128)(2,1)S(1)} %collective-permute-done.2.a1_ref, bf16[256,512]{1,0:T(8,128)(2,1)S(1)} %collective-permute-done.3.a2_ref, ...), custom_call_target="tpu_custom_call" | custom-call | flops 2147483648 | bytes 8388608 | tf_op jit(solution)/shard_map/pallas_call | solution.py:396
  (30 shorter events, 2.0 us)
Async XLA Ops:
  2.2 86.9 %collective-permute-start.7 = (bf16[512,1024]{1,0:T(8,128)(2,1)}, bf16[512,1024]{1,0:T(8,128)(2,1)}, u32[]{:S(2)}, u32[]{:S(2)}) collective-permute-start(bf16[512,1024]{1,0:T(8,128)(2,1)} %shard_map.153), channel_id=1, source_target_pairs={{0,6},{2,0},{4,2},{6,4},{1,7},{3,1},{5,3},{7,5},{8,14},{10,8},{12,... | collective-permute-start | bytes 3145736 | tf_op jit(solution)/shard_map/ppermute | solution.py:385
  5.0 84.1 %collective-permute-start.5 = (bf16[512,1024]{1,0:T(8,128)(2,1)}, bf16[512,1024]{1,0:T(8,128)(2,1)}, u32[]{:S(2)}, u32[]{:S(2)}) collective-permute-start(bf16[512,1024]{1,0:T(8,128)(2,1)} %shard_map.153), channel_id=1, source_target_pairs={{0,2},{2,4},{4,6},{6,0},{1,3},{3,5},{5,7},{7,1},{8,10},{10,12},{12... | collective-permute-start | bytes 3145736 | tf_op jit(solution)/shard_map/ppermute | solution.py:385
  5.0 84.6 %collective-permute-start.6 = (bf16[512,1024]{1,0:T(8,128)(2,1)}, bf16[512,1024]{1,0:T(8,128)(2,1)}, u32[]{:S(2)}, u32[]{:S(2)}) collective-permute-start(bf16[512,1024]{1,0:T(8,128)(2,1)} %shard_map.153), channel_id=1, source_target_pairs={{0,4},{2,6},{4,0},{6,2},{1,5},{3,7},{5,1},{7,3},{8,12},{10,14},{12... | collective-permute-start | bytes 3145736 | tf_op jit(solution)/shard_map/ppermute | solution.py:385
  57.8 18.8 %all-to-all-start.1 = ((bf16[8,80,128]{2,1,0:T(8,128)(2,1)}), bf16[8,80,128]{2,1,0:T(8,128)(2,1)S(1)}, u32[]{:S(2)}, u32[]{:S(2)}) async-start(bf16[8,80,128]{2,1,0:T(8,128)(2,1)} %shard_map.146), calls=%async_computation.1 | async-start | bytes 327680 | tf_op jit(solution)/shard_map/all_to_all | solution.py:429
  68.6 21.9 %collective-permute-start = (bf16[128,2048]{1,0:T(8,128)(2,1)}, bf16[128,2048]{1,0:T(8,128)(2,1)}, u32[]{:S(2)}, u32[]{:S(2)}) collective-permute-start(bf16[128,2048]{1,0:T(8,128)(2,1)} %get-tuple-element.14), channel_id=1, source_target_pairs={{0,8},{8,16},{16,24},{24,32},{32,40},{40,48},{48,56},{56,64},{64,7... | collective-permute-start | bytes 1572872 | tf_op jit(solution)/shard_map/ppermute | solution.py:441
  71.2 19.3 %collective-permute-start.1 = (bf16[128,2048]{1,0:T(8,128)(2,1)}, bf16[128,2048]{1,0:T(8,128)(2,1)}, u32[]{:S(2)}, u32[]{:S(2)}) collective-permute-start(bf16[128,2048]{1,0:T(8,128)(2,1)} %get-tuple-element.15), channel_id=1, source_target_pairs={{8,0},{16,8},{24,16},{32,24},{40,32},{48,40},{56,48},{64,56},{72,6... | collective-permute-start | bytes 1572872 | tf_op jit(solution)/shard_map/ppermute | solution.py:442
  76.6 0.6 copy-start.5
  79.7 24.9 %all-to-all-start.2 = ((bf16[32,24,256]{2,1,0:T(8,128)(2,1)}), bf16[32,24,256]{2,1,0:T(8,128)(2,1)S(1)}, u32[]{:S(2)}, u32[]{:S(2)}) async-start(bf16[32,24,256]{2,1,0:T(8,128)(2,1)} %get-tuple-element.17), calls=%async_computation.2 | async-start | bytes 786432 | tf_op jit(solution)/shard_map/all_to_all | solution.py:471
  89.1 37.8 %collective-permute-start.10 = (bf16[512,1024]{1,0:T(8,128)(2,1)}, bf16[512,1024]{1,0:T(8,128)(2,1)S(1)}, u32[]{:S(2)}, u32[]{:S(2)}) collective-permute-start(bf16[512,1024]{1,0:T(8,128)(2,1)} %collective-permute-done.7.m3_in), channel_id=1, source_target_pairs={{0,1},{1,0},{2,3},{3,2},{4,5},{5,4},{6,7},{7,6},{8,9},{9,8},{10,11... | collective-permute-start | bytes 3145736 | tf_op jit(solution)/shard_map/ppermute | solution.py:385
  89.2 37.7 %collective-permute-start.8 = (bf16[512,1024]{1,0:T(8,128)(2,1)}, bf16[512,1024]{1,0:T(8,128)(2,1)S(1)}, u32[]{:S(2)}, u32[]{:S(2)}) collective-permute-start(bf16[512,1024]{1,0:T(8,128)(2,1)} %collective-permute-done.5.m1_in), channel_id=1, source_target_pairs={{0,1},{1,0},{2,3},{3,2},{4,5},{5,4},{6,7},{7,6},{8,9},{9,8},{10,11... | collective-permute-start | bytes 3145736 | tf_op jit(solution)/shard_map/ppermute | solution.py:385
  89.7 37.2 %collective-permute-start.9 = (bf16[512,1024]{1,0:T(8,128)(2,1)}, bf16[512,1024]{1,0:T(8,128)(2,1)S(1)}, u32[]{:S(2)}, u32[]{:S(2)}) collective-permute-start(bf16[512,1024]{1,0:T(8,128)(2,1)} %collective-permute-done.6.m2_in), channel_id=1, source_target_pairs={{0,1},{1,0},{2,3},{3,2},{4,5},{5,4},{6,7},{7,6},{8,9},{9,8},{10,11... | collective-permute-start | bytes 3145736 | tf_op jit(solution)/shard_map/ppermute | solution.py:385
  90.5 14.2 %copy-start.4 = (f32[4]{0:T(128)S(1)}, f32[4]{0:T(128)}, u32[]{:S(2)}) copy-start(f32[4]{0:T(128)} %param.29) | copy-start | bytes 52
  104.7 1.7 %copy-start = (bf16[9,512,256]{2,1,0:T(8,128)(2,1)S(1)}, bf16[9,512,256]{2,1,0:T(8,128)(2,1)}, u32[]{:S(2)}) copy-start(bf16[9,512,256]{2,1,0:T(8,128)(2,1)} %get-tuple-element.16.refs_0_) | copy-start | bytes 7077892
  108.7 18.2 %copy-start.1 = (bf16[512,2048]{1,0:T(8,128)(2,1)S(1)}, bf16[512,2048]{1,0:T(8,128)(2,1)}, u32[]{:S(2)}) copy-start(bf16[512,2048]{1,0:T(8,128)(2,1)} %w0_ref.1) | copy-start | bytes 6291460
  108.7 18.2 %copy-start.2 = (bf16[256,2048]{1,0:T(8,128)(2,1)S(1)}, bf16[256,2048]{1,0:T(8,128)(2,1)}, u32[]{:S(2)}) copy-start(bf16[256,2048]{1,0:T(8,128)(2,1)} %get-tuple-element.20.lat_ref) | copy-start | bytes 3145732
  108.7 18.2 %copy-start.3 = (f32[8,2048]{1,0:T(8,128)S(1)}, f32[8,2048]{1,0:T(8,128)}, u32[]{:S(2)}) copy-start(f32[8,2048]{1,0:T(8,128)} %get-tuple-element.13.vec_ref) | copy-start | bytes 196612
  108.7 10.9 %collective-permute-start.3 = (bf16[256,512]{1,0:T(8,128)(2,1)S(1)}, bf16[256,512]{1,0:T(8,128)(2,1)S(1)}, u32[]{:S(2)}, u32[]{:S(2)}) collective-permute-start(bf16[256,512]{1,0:T(8,128)(2,1)S(1)} %shard_map.152), channel_id=1, source_target_pairs={{0,4},{2,6},{4,0},{6,2},{1,5},{3,7},{5,1},{7,3},{8,12},{10,14},{12... | collective-permute-start | bytes 786440 | tf_op jit(solution)/shard_map/ppermute | solution.py:385
  113.5 11.3 %collective-permute-start.2 = (bf16[256,512]{1,0:T(8,128)(2,1)S(1)}, bf16[256,512]{1,0:T(8,128)(2,1)S(1)}, u32[]{:S(2)}, u32[]{:S(2)}) collective-permute-start(bf16[256,512]{1,0:T(8,128)(2,1)S(1)} %get-tuple-element.18), channel_id=1, source_target_pairs={{0,2},{2,4},{4,6},{6,0},{1,3},{3,5},{5,7},{7,1},{8,10},{10,12},{12... | collective-permute-start | bytes 786440 | tf_op jit(solution)/shard_map/ppermute | solution.py:385
  119.7 7.2 %collective-permute-start.4 = (bf16[256,512]{1,0:T(8,128)(2,1)S(1)}, bf16[256,512]{1,0:T(8,128)(2,1)S(1)}, u32[]{:S(2)}, u32[]{:S(2)}) collective-permute-start(bf16[256,512]{1,0:T(8,128)(2,1)S(1)} %get-tuple-element.19), channel_id=1, source_target_pairs={{0,6},{2,0},{4,2},{6,4},{1,7},{3,1},{5,3},{7,5},{8,14},{10,8},{12,... | collective-permute-start | bytes 786440 | tf_op jit(solution)/shard_map/ppermute | solution.py:385

commit v7 on v6

--- a/solution.py
+++ b/solution.py
@@ -129,35 +129,58 @@
     move.wait()
 
 
-def stage_rows_kernel(lat_in, first_ref, last_ref, sems):
+def rotation(refs, groups):
+    row_cos, row_sin, col_cos, col_sin = refs
+    cosines = [row_cos[pl.ds(g, 1), :] + col_cos[...] for g in groups]
+    sines = [row_sin[pl.ds(g, 1), :] + col_sin[...] for g in groups]
+    return jnp.concatenate(cosines), jnp.concatenate(sines)
+
+
+def context_kernel(
+    mod_ref, ctx_ref, wk_ref, wv_ref, gain_ref, kgain_ref, rcos_ref, rsin_ref, ccos_ref, csin_ref,
+    lat_in, kv_ref, vec_ref, first_ref, last_ref, edge_ref, rows_ref, sems,
+):
     tok = lat_in.shape[0]
     moves = [
-        pltpu.make_async_copy(lat_in.at[:WINDOW, :], first_ref, sems.at[0]),
-        pltpu.make_async_copy(lat_in.at[tok - WINDOW :, :], last_ref, sems.at[1]),
+        pltpu.make_async_copy(lat_in.at[:WINDOW, :], edge_ref.at[:WINDOW], sems.at[0]),
+        pltpu.make_async_copy(lat_in.at[tok - WINDOW :, :], edge_ref.at[WINDOW:], sems.at[1]),
     ]
     for move in moves:
         move.start()
-    for move in moves:
-        move.wait()
-
-
-def context_kernel(
-    mod_ref, ctx_ref, wk_ref, wv_ref, gain_ref, kgain_ref, kv_ref, vec_ref
-):
     shift_lat, scale_lat, shift_ctx, scale_ctx, gate = vectors_of(mod_ref)
     gain = gain_ref[...]
     vec_ref[0:1, :] = gain * (1.0 + scale_lat)
     vec_ref[1:2, :] = shift_lat
     vec_ref[2:3, :] = gate
-    rows = (normed(ctx_ref[...]) * (gain * (1.0 + scale_ctx)) + shift_ctx).astype(BF16)
-    keys = head_norm(jnp.dot(rows, wk_ref[...], preferred_element_type=F32), kgain_ref[...])
-    values = jnp.dot(rows, wv_ref[...], preferred_element_type=F32)
-    both = jnp.concatenate([keys, values], axis=1).astype(BF16)
+    rows_ref[2 * WINDOW :, :] = (
+        normed(ctx_ref[...]) * (gain * (1.0 + scale_ctx)) + shift_ctx
+    ).astype(BF16)
+    for move in moves:
+        move.wait()
+    step = 64
+
+    def body(i, carry):
+        at = pl.ds(pl.multiple_of(i * step, step), step)
+        rows_ref[at, :] = (normed(edge_ref[at, :]) * vec_ref[0:1, :] + vec_ref[1:2, :]).astype(BF16)
+        return carry
+
+    lax.fori_loop(0, 2 * WINDOW // step, body, 0)
+    keys = head_norm(
+        jnp.dot(rows_ref[...], wk_ref[...], preferred_element_type=F32), kgain_ref[...]
+    )
+    values = jnp.dot(rows_ref[...], wv_ref[...], preferred_element_type=F32).astype(BF16)
+    refs = (rcos_ref, rsin_ref, ccos_ref, csin_ref)
+    final = tok // GRID_W
+    for ref, base, groups in ((first_ref, 0, (2, 3)), (last_ref, WINDOW, (final, final + 1))):
+        at = slice(base, base + WINDOW)
+        ref[:, :HEAD_DIM] = rotated(keys[at], *rotation(refs, groups)).astype(BF16)
+        ref[:, HEAD_DIM:] = values[at]
+    both = jnp.concatenate([keys[2 * WINDOW :].astype(BF16), values[2 * WINDOW :]], axis=1)
     kv_ref[...] = jnp.broadcast_to(both[None], kv_ref.shape)
 
 
 def qkv_kernel(
-    lat_in, before_in, after_in, wq_in, wk_in, wv_in,
+    lat_in, wq_in, wk_in, wv_in, before_ref, after_ref,
     vec_ref, qgain_ref, kgain_ref, rcos_ref, rsin_ref, ccos_ref, csin_ref,
     packed_out, own_ref, out_ref, lat_ref, wq_ref, wkv_ref, k_ref, v_ref, even_ref, odd_ref,
     sum_ref, sems,
@@ -173,20 +196,17 @@
 
     sources = [(lat_in.at[at(i), :], lat_ref.at[at(i), :]) for i in range(steps)]
     sources += [
-        (before_in, lat_ref.at[pl.ds(tok, WINDOW), :]),
-        (after_in, lat_ref.at[pl.ds(tok + WINDOW, WINDOW), :]),
         (wk_in, wkv_ref.at[:, :HEAD_DIM]), (wv_in, wkv_ref.at[:, HEAD_DIM:]), (wq_in, wq_ref),
     ]
     moves = [
         pltpu.make_async_copy(source, to, sems.at[i]) for i, (source, to) in enumerate(sources)
     ]
-    for i in (0, steps + 2, steps + 3, steps + 4, *range(1, steps + 2)):
+    for i in (0, steps, steps + 1, steps + 2, *range(1, steps)):
         moves[i].start()
-
-    def tables(groups):
-        cosines = [rcos_ref[pl.ds(g, 1), :] + ccos_ref[...] for g in groups]
-        sines = [rsin_ref[pl.ds(g, 1), :] + csin_ref[...] for g in groups]
-        return jnp.concatenate(cosines), jnp.concatenate(sines)
+    for ref, edge in ((k_ref, slice(0, HEAD_DIM)), (v_ref, slice(HEAD_DIM, 2 * HEAD_DIM))):
+        ref[:WINDOW, :] = before_ref[:, edge]
+        ref[tok + WINDOW :, :] = after_ref[:, edge]
+    refs = (rcos_ref, rsin_ref, ccos_ref, csin_ref)
 
     def fill(i, to):
         values = lat_ref[at(i), :].astype(F32)
@@ -201,7 +221,7 @@
     def project(i, rows_ref):
         to = pl.ds(pl.multiple_of(i * step + WINDOW, WINDOW), step)
         first = 2 + i * (step // GRID_W)
-        cosine, sine = tables([first + g for g in range(step // GRID_W)])
+        cosine, sine = rotation(refs, [first + g for g in range(step // GRID_W)])
         queries = jnp.dot(rows_ref[...], wq_ref[...], preferred_element_type=F32)
         k_ref[to, :], v_ref[to, :] = keys_of(rows_ref, cosine, sine)
         for h in range(4):
@@ -214,7 +234,7 @@
 
     moves[0].wait()
     fill(0, even_ref)
-    for i in range(steps + 2, steps + 5):
+    for i in range(steps, steps + 3):
         moves[i].wait()
 
     def wait_rows(i):
@@ -227,31 +247,21 @@
         def _():
             wait_rows(2)
 
-        @pl.when(j == 1)
-        def _():
-            moves[steps].wait()
-            moves[steps + 1].wait()
-
         fill(2 * j + 1, odd_ref)
         project(2 * j, even_ref)
-        fill(2 * j + 2, even_ref)
+        fill(jnp.minimum(2 * j + 2, steps - 1), even_ref)
         project(2 * j + 1, odd_ref)
         return carry
 
     lax.fori_loop(0, steps // 2, body, 0)
     own_move = pltpu.make_async_copy(
-        lat_ref.at[at(lax.axis_index("tp"), own_ref.shape[0]), :], own_ref, sems.at[steps + 5]
+        lat_ref.at[at(lax.axis_index("tp"), own_ref.shape[0]), :], own_ref, sems.at[steps + 3]
     )
     own_move.start()
-    beyond = (tok + WINDOW) // GRID_W
-    keys, values = keys_of(even_ref, *tables([0, 1, beyond, beyond + 1]))
-    for ref, rows in ((k_ref, keys), (v_ref, values)):
-        ref[:WINDOW, :] = rows[:WINDOW]
-        ref[tok + WINDOW :, :] = rows[WINDOW:]
 
     def block_move(block):
         return pltpu.make_async_copy(
-            out_ref.at[block], packed_out.at[block], sems.at[steps + 6 + block]
+            out_ref.at[block], packed_out.at[block], sems.at[steps + 4 + block]
         )
 
     local_pass(out_ref, k_ref, v_ref, sum_ref, block_move)
@@ -414,6 +424,7 @@
     sp = sp_index()
     width = 4 * HEAD_DIM
 
+    peers = NZ * NY
     part = call(
         partial_kernel, [((NY * NX, 24, 128), BF16)],
         (cond, ctx_cond[None], mod_shift, mod_scale, mod_gate), cost(1 << 20, 1 << 18), 62,
@@ -432,15 +443,6 @@
         stage_weight_kernel, [((width, D // 2), BF16)], (w_out,),
         cost(1 << 24, 2 << 20), 60, scratch=[pltpu.SemaphoreType.DMA], in_specs=[HBM],
     )
-    first_rows, last_rows = call(
-        stage_rows_kernel, [((WINDOW, D), BF16)] * 2, (lat,),
-        cost(1 << 24, 2 << 20), 60, scratch=[pltpu.SemaphoreType.DMA((2,))], in_specs=[HBM],
-    )
-    peers = NZ * NY
-    up = [(i, i + 1) for i in range(peers - 1)]
-    before = lax.ppermute(last_rows, SP, up)
-    after = lax.ppermute(first_rows, SP, [(j, i) for i, j in up])
-
     mine, other = {}, {}
     for s in (1, 3, 2):
         mine[s] = shifted(half, "tp", s)
@@ -462,32 +464,44 @@
     rows = tok + 2 * WINDOW
     gain, qgain, kgain = norm_gain[None], q_gain[None], k_gain[None]
     n_ctx = context.shape[1]
-    ctx_kv, vec = call(
+    edge = ((WINDOW, 2 * HEAD_DIM), BF16)
+    ctx_kv, vec, first_kv, last_kv = call(
         context_kernel,
-        [((peers, n_ctx, 2 * HEAD_DIM), BF16), ((8, D), F32)],
-        (mod, context[0], w_key, w_value, gain, kgain),
-        cost(2 * n_ctx * D * 256, D * 512), 63,
-    )
+        [((peers, n_ctx, 2 * HEAD_DIM), BF16), ((8, D), F32), edge, edge],
+        (
+            mod, context[0], w_key, w_value, gain, kgain,
+            row_cos, row_sin, col_cos, col_sin, lat,
+        ),
+        cost(2 * (n_ctx + 2 * WINDOW) * D * 256, D * 512), 63,
+        scratch=[
+            pltpu.VMEM((2 * WINDOW, D), BF16), pltpu.VMEM((2 * WINDOW + n_ctx, D), BF16),
+            pltpu.SemaphoreType.DMA((2,)),
+        ],
+        in_specs=[VMEM] * 10 + [HBM],
+    )
+    up = [(i, i + 1) for i in range(peers - 1)]
+    before = lax.ppermute(last_kv, SP, up)
+    after = lax.ppermute(first_kv, SP, [(j, i) for i, j in up])
     ctx_all = lax.all_to_all(ctx_kv, SP, 0, 0, tiled=True).reshape(-1, 2 * HEAD_DIM)
 
     packed_shape = (tok // WINDOW + 1, 4 * WINDOW, 2 * HEAD_DIM)
     packed, own = call(
         qkv_kernel, [(packed_shape, BF16), ((sub, D), BF16)],
         (
-            lat, before, after, w_query, w_key, w_value, vec, qgain, kgain,
+            lat, w_query, w_key, w_value, before, after, vec, qgain, kgain,
             row_cos, row_sin, col_cos, col_sin,
         ),
         cost(2 * tok * D * 768 + 16 * tok * 384 * HEAD_DIM, tok * D * 2 + D * 768 * 2), 60,
         scratch=[
             pltpu.VMEM(packed_shape, BF16),
-            pltpu.VMEM((rows, D), BF16), pltpu.VMEM((D, width), BF16),
+            pltpu.VMEM((tok, D), BF16), pltpu.VMEM((D, width), BF16),
             pltpu.VMEM((D, 2 * HEAD_DIM), BF16),
             pltpu.VMEM((rows, HEAD_DIM), BF16), pltpu.VMEM((rows, HEAD_DIM), BF16),
             pltpu.VMEM((256, D), BF16), pltpu.VMEM((256, D), BF16),
             pltpu.VMEM((4 * WINDOW, 128), F32),
-            pltpu.SemaphoreType.DMA((tok // 256 + 6 + packed_shape[0],)),
+            pltpu.SemaphoreType.DMA((tok // 256 + 4 + packed_shape[0],)),
         ],
-        in_specs=[HBM] * 6 + [VMEM] * 7,
+        in_specs=[HBM] * 4 + [VMEM] * 9,
         out_specs=[HBM, HBM],
     )
 

time: 132 us -> 139 us (1.053)
  the two profiles are of different devices: /device:TPU:32 before, /device:TPU:120 now
where the time goes in v7:
time: 139 us; the launch traced here: 138 us
  waiting for transfers between devices  61 us (44%)
  Pallas kernels  36.3 us (26%)
  starting transfers between devices  36.2 us (26%)
  local copies, waits for them, and re-layouts  2.97 us (2%)
  other arithmetic  1.52 us (1%)
    all_to_all x1, waiting for transfers between devices, per_device(): part = lax.all_to_all(part, ('y', 'tp'), 0, 0, tiled=True)  40 us
    pallas_call x9, Pallas kernels, call(): pl.pallas_call(kernel, in_specs=in_specs or [VMEM] * len(args), out_specs...  36.3 us
    ppermute x9, waiting for transfers between devices, shifted(): lax.ppermute(array, axis, [(i, (i + by) % peers) for i in range(peers)])  8.77 us
    all_to_all x1, starting transfers between devices, per_device(): lax.all_to_all(ctx_kv, SP, 0, 0, tiled=True).reshape(-1, 2 * HEAD_DIM)  8.73 us
    all_to_all x1, starting transfers between devices, per_device(): mod = lax.all_to_all(part, 'z', 0, 0, tiled=True)  7.66 us
    ppermute x9, starting transfers between devices, shifted(): lax.ppermute(array, axis, [(i, (i + by) % peers) for i in range(peers)])  7.33 us
    ppermute x1, waiting for transfers between devices, per_device(): after = lax.ppermute(first_kv, SP, [(j, i) for i, j in up])  7.13 us
    all_to_all x1, starting transfers between devices, per_device(): part = lax.all_to_all(part, ('y', 'tp'), 0, 0, tiled=True)  5.96 us
  transfers between devices with their start and end apart: 14, of which 7 were waited for; matrix products, arithmetic and copies ran while one was open for 1% of the time, Pallas kernels for 22%

profile of v7, /device:TPU:120, one launch (start us, length us, event | category | flops | bytes accessed | tf_op | source)
XLA Modules:
  0.0 138.2 jit_solution(5138597867790221539)
XLA Ops:
  0.0 2.2 %shard_map.152 = bf16[512,1024]{1,0:T(8,128)(2,1)} custom-call(bf16[512,2048]{1,0:T(8,128)(2,1)} %w0_ref.1), custom_call_target="tpu_custom_call" | custom-call | flops 16777216 | bytes 2097152 | tf_op jit(solution)/shard_map/pallas_call | solution.py:406
  2.2 2.8 %collective-permute-start.7 = (bf16[512,1024]{1,0:T(8,128)(2,1)}, bf16[512,1024]{1,0:T(8,128)(2,1)}, u32[]{:S(2)}, u32[]{:S(2)}) collective-permute-start(bf16[512,1024]{1,0:T(8,128)(2,1)} %shard_map.152), channel_id=1, source_target_pairs={{0,6},{2,0},{4,2},{6,4},{1,7},{3,1},{5,3},{7,5},{8,14},{10,8},{12,... | collective-permute-start | bytes 3145736 | tf_op jit(solution)/shard_map/ppermute | solution.py:395
  5.0 2.3 %collective-permute-start.6 = (bf16[512,1024]{1,0:T(8,128)(2,1)}, bf16[512,1024]{1,0:T(8,128)(2,1)}, u32[]{:S(2)}, u32[]{:S(2)}) collective-permute-start(bf16[512,1024]{1,0:T(8,128)(2,1)} %shard_map.152), channel_id=1, source_target_pairs={{0,4},{2,6},{4,0},{6,2},{1,5},{3,7},{5,1},{7,3},{8,12},{10,14},{12... | collective-permute-start | bytes 3145736 | tf_op jit(solution)/shard_map/ppermute | solution.py:395
  7.3 1.8 %shard_map.145 = bf16[16,24,128]{2,1,0:T(8,128)(2,1)} custom-call(f32[1,2048]{1,0:T(1,128)} %cond_in.1, f32[1,2048]{1,0:T(1,128)} %bitcast.19, bf16[64,512]{1,0:T(8,128)(2,1)} %shift_in.1, bf16[64,512]{1,0:T(8,128)(2,1)} %scale_in.1, bf16[64,512]{1,0:T(8,128)(2,1)} %gate_in.1), custom_call_target="tpu_custom_call" | custom-call | flops 1048576 | bytes 262144 | tf_op jit(solution)/shard_map/pallas_call | solution.py:406
  9.2 6.0 %all-to-all-start = ((bf16[16,24,128]{2,1,0:T(8,128)(2,1)}), bf16[16,24,128]{2,1,0:T(8,128)(2,1)S(1)}, u32[]{:S(2)}, u32[]{:S(2)}) async-start(bf16[16,24,128]{2,1,0:T(8,128)(2,1)} %shard_map.145), calls=%async_computation | async-start | bytes 196608 | tf_op jit(solution)/shard_map/all_to_all | solution.py:438
  15.2 40.0 %all-to-all-done.in_ref = bf16[16,24,128]{2,1,0:T(8,128)(2,1)S(1)} async-done(((bf16[16,24,128]{2,1,0:T(8,128)(2,1)}), bf16[16,24,128]{2,1,0:T(8,128)(2,1)S(1)}, u32[]{:S(2)}, u32[]{:S(2)}) %all-to-all-start) | async-done | bytes 98336 | tf_op jit(solution)/shard_map/all_to_all | solution.py:438
  55.8 7.7 %all-to-all-start.1 = ((bf16[8,80,128]{2,1,0:T(8,128)(2,1)}), bf16[8,80,128]{2,1,0:T(8,128)(2,1)S(1)}, u32[]{:S(2)}, u32[]{:S(2)}) async-start(bf16[8,80,128]{2,1,0:T(8,128)(2,1)} %shard_map.146), calls=%async_computation.1 | async-start | bytes 327680 | tf_op jit(solution)/shard_map/all_to_all | solution.py:440
  64.2 0.8 multiply_select_fusion
  65.0 4.5 %all-to-all-done.1.mod_ref = bf16[8,80,128]{2,1,0:T(8,128)(2,1)S(1)} async-done(((bf16[8,80,128]{2,1,0:T(8,128)(2,1)}), bf16[8,80,128]{2,1,0:T(8,128)(2,1)S(1)}, u32[]{:S(2)}, u32[]{:S(2)}) %all-to-all-start.1) | async-done | bytes 163872 | tf_op jit(solution)/shard_map/all_to_all | solution.py:440
  70.1 5.0 %shard_map.147 = (bf16[32,24,256]{2,1,0:T(8,128)(2,1)}, f32[8,2048]{1,0:T(8,128)}, bf16[128,256]{1,0:T(8,128)(2,1)}, bf16[128,256]{1,0:T(8,128)(2,1)}) custom-call(bf16[8,80,128]{2,1,0:T(8,128)(2,1)} %copy-done.5, bf16[24,2048]{1,0:T(8,128)(2,1)} %bitcast.17, bf16[2048,128]{1,0:T(8,128)(2,1)} %wk_in.1, bf16[2048,128]{1,0:T(8,128)(2,1)} %wv_in.1, ...), custom_call_target="tpu_custom_call" | custom-call | flops 293601280 | bytes 1048576 | tf_op jit(solution)/shard_map/pallas_call | solution.py:406
  75.1 8.7 %all-to-all-start.2 = ((bf16[32,24,256]{2,1,0:T(8,128)(2,1)}), bf16[32,24,256]{2,1,0:T(8,128)(2,1)S(1)}, u32[]{:S(2)}, u32[]{:S(2)}) async-start(bf16[32,24,256]{2,1,0:T(8,128)(2,1)} %get-tuple-element.17), calls=%async_computation.2 | async-start | bytes 786432 | tf_op jit(solution)/shard_map/all_to_all | solution.py:485
  84.6 4.6 %collective-permute-start = (bf16[128,256]{1,0:T(8,128)(2,1)}, bf16[128,256]{1,0:T(8,128)(2,1)S(1)}, u32[]{:S(2)}, u32[]{:S(2)}) collective-permute-start(bf16[128,256]{1,0:T(8,128)(2,1)} %get-tuple-element.14), channel_id=1, source_target_pairs={{0,8},{8,16},{16,24},{24,32},{32,40},{40,48},{48,56},{56,64},{64,7... | collective-permute-start | bytes 196616 | tf_op jit(solution)/shard_map/ppermute | solution.py:483
  89.2 1.9 %collective-permute-start.1 = (bf16[128,256]{1,0:T(8,128)(2,1)}, bf16[128,256]{1,0:T(8,128)(2,1)S(1)}, u32[]{:S(2)}, u32[]{:S(2)}) collective-permute-start(bf16[128,256]{1,0:T(8,128)(2,1)} %get-tuple-element.15), channel_id=1, source_target_pairs={{8,0},{16,8},{24,16},{32,24},{40,32},{48,40},{56,48},{64,56},{72,6... | collective-permute-start | bytes 196616 | tf_op jit(solution)/shard_map/ppermute | solution.py:484
  91.7 7.1 %collective-permute-done.1.after_ref = bf16[128,256]{1,0:T(8,128)(2,1)S(1)} collective-permute-done((bf16[128,256]{1,0:T(8,128)(2,1)}, bf16[128,256]{1,0:T(8,128)(2,1)S(1)}, u32[]{:S(2)}, u32[]{:S(2)}) %collective-permute-start.1) | collective-permute-done | bytes 65568 | tf_op jit(solution)/shard_map/ppermute | solution.py:484
  99.5 13.6 %shard_map.148 = (bf16[9,512,256]{2,1,0:T(8,128)(2,1)}, bf16[256,2048]{1,0:T(8,128)(2,1)}) custom-call(bf16[1024,2048]{1,0:T(8,128)(2,1)} %bitcast.16, bf16[2048,512]{1,0:T(8,128)(2,1)} %wq_in.1, bf16[2048,128]{1,0:T(8,128)(2,1)} %wk_in.1, bf16[2048,128]{1,0:T(8,128)(2,1)} %wv_in.1, bf16[128,256]{1,0:T(8,128)(2,1)} %copy-done.6, bf16[128,256]{1,0:T(8,128)(2,1)} %copy-done.7, ...), custom_call_target="tpu_custom_call" | custom-call | flops 4026531840 | bytes 7340032 | tf_op jit(solution)/shard_map/pallas_call | solution.py:406
  113.1 1.7 %copy-done = bf16[9,512,256]{2,1,0:T(8,128)(2,1)S(1)} copy-done((bf16[9,512,256]{2,1,0:T(8,128)(2,1)S(1)}, bf16[9,512,256]{2,1,0:T(8,128)(2,1)}, u32[]{:S(2)}) %copy-start) | copy-done | bytes 2359320
  114.8 2.3 %shard_map.151 = bf16[256,512]{1,0:T(8,128)(2,1)S(1)} custom-call(bf16[9,512,256]{2,1,0:T(8,128)(2,1)S(1)} %copy-done, bf16[768,256]{1,0:T(8,128)(2,1)S(1)} %bitcast.9, f32[1,4]{1,0:T(1,128)S(1)} %bitcast.12), custom_call_target="tpu_custom_call" | custom-call | flops 402653184 | bytes 2097152 | tf_op jit(solution)/shard_map/pallas_call | solution.py:406
  117.8 4.1 %shard_map.150 = (bf16[256,512]{1,0:T(8,128)(2,1)S(1)}, bf16[256,512]{1,0:T(8,128)(2,1)S(1)}) custom-call(bf16[9,512,256]{2,1,0:T(8,128)(2,1)S(1)} %copy-done, bf16[768,256]{1,0:T(8,128)(2,1)S(1)} %bitcast.10, f32[1,4]{1,0:T(1,128)S(1)} %bitcast.13), custom_call_target="tpu_custom_call" | custom-call | flops 805306368 | bytes 2097152 | tf_op jit(solution)/shard_map/pallas_call | solution.py:406
  121.9 0.9 collective-permute-start.2
  122.8 4.7 %collective-permute-done.3.a2_ref = bf16[256,512]{1,0:T(8,128)(2,1)S(1)} collective-permute-done((bf16[256,512]{1,0:T(8,128)(2,1)S(1)}, bf16[256,512]{1,0:T(8,128)(2,1)S(1)}, u32[]{:S(2)}, u32[]{:S(2)}) %collective-permute-start.3) | collective-permute-done | bytes 262176 | tf_op jit(solution)/shard_map/ppermute | solution.py:395
  127.5 2.3 %shard_map.149.a0_ref = bf16[256,512]{1,0:T(8,128)(2,1)S(1)} custom-call(bf16[9,512,256]{2,1,0:T(8,128)(2,1)S(1)} %copy-done, bf16[768,256]{1,0:T(8,128)(2,1)S(1)} %bitcast.11, f32[1,4]{1,0:T(1,128)S(1)} %bitcast.14), custom_call_target="tpu_custom_call" | custom-call | flops 402653184 | bytes 2097152 | tf_op jit(solution)/shard_map/pallas_call | solution.py:406
  129.9 1.8 %collective-permute-done.2.a1_ref = bf16[256,512]{1,0:T(8,128)(2,1)S(1)} collective-permute-done((bf16[256,512]{1,0:T(8,128)(2,1)S(1)}, bf16[256,512]{1,0:T(8,128)(2,1)S(1)}, u32[]{:S(2)}, u32[]{:S(2)}) %collective-permute-start.2) | collective-permute-done | bytes 262176 | tf_op jit(solution)/shard_map/ppermute | solution.py:395
  131.7 2.2 %collective-permute-done.4.a3_ref = bf16[256,512]{1,0:T(8,128)(2,1)S(1)} collective-permute-done((bf16[256,512]{1,0:T(8,128)(2,1)S(1)}, bf16[256,512]{1,0:T(8,128)(2,1)S(1)}, u32[]{:S(2)}, u32[]{:S(2)}) %collective-permute-start.4) | collective-permute-done | bytes 262176 | tf_op jit(solution)/shard_map/ppermute | solution.py:395
  133.9 4.1 %shard_map.153 = bf16[256,2048]{1,0:T(8,128)(2,1)} custom-call(f32[8,2048]{1,0:T(8,128)S(1)} %copy-done.3, bf16[256,512]{1,0:T(8,128)(2,1)S(1)} %shard_map.149.a0_ref, bf16[256,512]{1,0:T(8,128)(2,1)S(1)} %collective-permute-done.2.a1_ref, bf16[256,512]{1,0:T(8,128)(2,1)S(1)} %collective-permute-done.3.a2_ref, ...), custom_call_target="tpu_custom_call" | custom-call | flops 2147483648 | bytes 8388608 | tf_op jit(solution)/shard_map/pallas_call | solution.py:406
  (34 shorter events, 4.7 us)
Async XLA Ops:
  2.2 81.7 %collective-permute-start.7 = (bf16[512,1024]{1,0:T(8,128)(2,1)}, bf16[512,1024]{1,0:T(8,128)(2,1)}, u32[]{:S(2)}, u32[]{:S(2)}) collective-permute-start(bf16[512,1024]{1,0:T(8,128)(2,1)} %shard_map.152), channel_id=1, source_target_pairs={{0,6},{2,0},{4,2},{6,4},{1,7},{3,1},{5,3},{7,5},{8,14},{10,8},{12,... | collective-permute-start | bytes 3145736 | tf_op jit(solution)/shard_map/ppermute | solution.py:395
  5.0 78.9 %collective-permute-start.5 = (bf16[512,1024]{1,0:T(8,128)(2,1)}, bf16[512,1024]{1,0:T(8,128)(2,1)}, u32[]{:S(2)}, u32[]{:S(2)}) collective-permute-start(bf16[512,1024]{1,0:T(8,128)(2,1)} %shard_map.152), channel_id=1, source_target_pairs={{0,2},{2,4},{4,6},{6,0},{1,3},{3,5},{5,7},{7,1},{8,10},{10,12},{12... | collective-permute-start | bytes 3145736 | tf_op jit(solution)/shard_map/ppermute | solution.py:395
  5.0 79.4 %collective-permute-start.6 = (bf16[512,1024]{1,0:T(8,128)(2,1)}, bf16[512,1024]{1,0:T(8,128)(2,1)}, u32[]{:S(2)}, u32[]{:S(2)}) collective-permute-start(bf16[512,1024]{1,0:T(8,128)(2,1)} %shard_map.152), channel_id=1, source_target_pairs={{0,4},{2,6},{4,0},{6,2},{1,5},{3,7},{5,1},{7,3},{8,12},{10,14},{12... | collective-permute-start | bytes 3145736 | tf_op jit(solution)/shard_map/ppermute | solution.py:395
  9.2 46.0 %all-to-all-start = ((bf16[16,24,128]{2,1,0:T(8,128)(2,1)}), bf16[16,24,128]{2,1,0:T(8,128)(2,1)S(1)}, u32[]{:S(2)}, u32[]{:S(2)}) async-start(bf16[16,24,128]{2,1,0:T(8,128)(2,1)} %shard_map.145), calls=%async_computation | async-start | bytes 196608 | tf_op jit(solution)/shard_map/all_to_all | solution.py:438
  55.8 13.6 %all-to-all-start.1 = ((bf16[8,80,128]{2,1,0:T(8,128)(2,1)}), bf16[8,80,128]{2,1,0:T(8,128)(2,1)S(1)}, u32[]{:S(2)}, u32[]{:S(2)}) async-start(bf16[8,80,128]{2,1,0:T(8,128)(2,1)} %shard_map.146), calls=%async_computation.1 | async-start | bytes 327680 | tf_op jit(solution)/shard_map/all_to_all | solution.py:440
  69.5 0.7 copy-start.5
  75.1 38.0 %all-to-all-start.2 = ((bf16[32,24,256]{2,1,0:T(8,128)(2,1)}), bf16[32,24,256]{2,1,0:T(8,128)(2,1)S(1)}, u32[]{:S(2)}, u32[]{:S(2)}) async-start(bf16[32,24,256]{2,1,0:T(8,128)(2,1)} %get-tuple-element.17), calls=%async_computation.2 | async-start | bytes 786432 | tf_op jit(solution)/shard_map/all_to_all | solution.py:485
  83.9 50.0 %collective-permute-start.10 = (bf16[512,1024]{1,0:T(8,128)(2,1)}, bf16[512,1024]{1,0:T(8,128)(2,1)S(1)}, u32[]{:S(2)}, u32[]{:S(2)}) collective-permute-start(bf16[512,1024]{1,0:T(8,128)(2,1)} %collective-permute-done.7.m3_in), channel_id=1, source_target_pairs={{0,1},{1,0},{2,3},{3,2},{4,5},{5,4},{6,7},{7,6},{8,9},{9,8},{10,11... | collective-permute-start | bytes 3145736 | tf_op jit(solution)/shard_map/ppermute | solution.py:395
  84.0 49.9 %collective-permute-start.8 = (bf16[512,1024]{1,0:T(8,128)(2,1)}, bf16[512,1024]{1,0:T(8,128)(2,1)S(1)}, u32[]{:S(2)}, u32[]{:S(2)}) collective-permute-start(bf16[512,1024]{1,0:T(8,128)(2,1)} %collective-permute-done.5.m1_in), channel_id=1, source_target_pairs={{0,1},{1,0},{2,3},{3,2},{4,5},{5,4},{6,7},{7,6},{8,9},{9,8},{10,11... | collective-permute-start | bytes 3145736 | tf_op jit(solution)/shard_map/ppermute | solution.py:395
  84.5 49.4 %collective-permute-start.9 = (bf16[512,1024]{1,0:T(8,128)(2,1)}, bf16[512,1024]{1,0:T(8,128)(2,1)S(1)}, u32[]{:S(2)}, u32[]{:S(2)}) collective-permute-start(bf16[512,1024]{1,0:T(8,128)(2,1)} %collective-permute-done.6.m2_in), channel_id=1, source_target_pairs={{0,1},{1,0},{2,3},{3,2},{4,5},{5,4},{6,7},{7,6},{8,9},{9,8},{10,11... | collective-permute-start | bytes 3145736 | tf_op jit(solution)/shard_map/ppermute | solution.py:395
  84.6 7.1 %collective-permute-start = (bf16[128,256]{1,0:T(8,128)(2,1)}, bf16[128,256]{1,0:T(8,128)(2,1)S(1)}, u32[]{:S(2)}, u32[]{:S(2)}) collective-permute-start(bf16[128,256]{1,0:T(8,128)(2,1)} %get-tuple-element.14), channel_id=1, source_target_pairs={{0,8},{8,16},{16,24},{24,32},{32,40},{40,48},{48,56},{56,64},{64,7... | collective-permute-start | bytes 196616 | tf_op jit(solution)/shard_map/ppermute | solution.py:483
  89.2 9.7 %collective-permute-start.1 = (bf16[128,256]{1,0:T(8,128)(2,1)}, bf16[128,256]{1,0:T(8,128)(2,1)S(1)}, u32[]{:S(2)}, u32[]{:S(2)}) collective-permute-start(bf16[128,256]{1,0:T(8,128)(2,1)} %get-tuple-element.15), channel_id=1, source_target_pairs={{8,0},{16,8},{24,16},{32,24},{40,32},{48,40},{56,48},{64,56},{72,6... | collective-permute-start | bytes 196616 | tf_op jit(solution)/shard_map/ppermute | solution.py:484
  91.7 7.1 %copy-start.6 = (bf16[128,256]{1,0:T(8,128)(2,1)}, bf16[128,256]{1,0:T(8,128)(2,1)S(1)}, u32[]{:S(2)}) copy-start(bf16[128,256]{1,0:T(8,128)(2,1)S(1)} %collective-permute-done.before_ref) | copy-start | bytes 196612
  98.9 0.6 copy-start.7
  99.5 13.6 %copy-start.4 = (f32[4]{0:T(128)S(1)}, f32[4]{0:T(128)}, u32[]{:S(2)}) copy-start(f32[4]{0:T(128)} %param.29) | copy-start | bytes 52
  113.1 1.7 %copy-start = (bf16[9,512,256]{2,1,0:T(8,128)(2,1)S(1)}, bf16[9,512,256]{2,1,0:T(8,128)(2,1)}, u32[]{:S(2)}) copy-start(bf16[9,512,256]{2,1,0:T(8,128)(2,1)} %get-tuple-element.16.refs_0_) | copy-start | bytes 7077892
  117.1 16.8 %copy-start.1 = (bf16[512,2048]{1,0:T(8,128)(2,1)S(1)}, bf16[512,2048]{1,0:T(8,128)(2,1)}, u32[]{:S(2)}) copy-start(bf16[512,2048]{1,0:T(8,128)(2,1)} %w0_ref.1) | copy-start | bytes 6291460
  117.1 16.8 %copy-start.2 = (bf16[256,2048]{1,0:T(8,128)(2,1)S(1)}, bf16[256,2048]{1,0:T(8,128)(2,1)}, u32[]{:S(2)}) copy-start(bf16[256,2048]{1,0:T(8,128)(2,1)} %get-tuple-element.20.lat_ref) | copy-start | bytes 3145732
  117.1 16.8 %copy-start.3 = (f32[8,2048]{1,0:T(8,128)S(1)}, f32[8,2048]{1,0:T(8,128)}, u32[]{:S(2)}) copy-start(f32[8,2048]{1,0:T(8,128)} %get-tuple-element.13.vec_ref) | copy-start | bytes 196612
  117.1 10.4 %collective-permute-start.3 = (bf16[256,512]{1,0:T(8,128)(2,1)S(1)}, bf16[256,512]{1,0:T(8,128)(2,1)S(1)}, u32[]{:S(2)}, u32[]{:S(2)}) collective-permute-start(bf16[256,512]{1,0:T(8,128)(2,1)S(1)} %shard_map.151), channel_id=1, source_target_pairs={{0,4},{2,6},{4,0},{6,2},{1,5},{3,7},{5,1},{7,3},{8,12},{10,14},{12... | collective-permute-start | bytes 786440 | tf_op jit(solution)/shard_map/ppermute | solution.py:395
  121.9 9.8 %collective-permute-start.2 = (bf16[256,512]{1,0:T(8,128)(2,1)S(1)}, bf16[256,512]{1,0:T(8,128)(2,1)S(1)}, u32[]{:S(2)}, u32[]{:S(2)}) collective-permute-start(bf16[256,512]{1,0:T(8,128)(2,1)S(1)} %get-tuple-element.18), channel_id=1, source_target_pairs={{0,2},{2,4},{4,6},{6,0},{1,3},{3,5},{5,7},{7,1},{8,10},{10,12},{12... | collective-permute-start | bytes 786440 | tf_op jit(solution)/shard_map/ppermute | solution.py:395
  127.5 6.4 %collective-permute-start.4 = (bf16[256,512]{1,0:T(8,128)(2,1)S(1)}, bf16[256,512]{1,0:T(8,128)(2,1)S(1)}, u32[]{:S(2)}, u32[]{:S(2)}) collective-permute-start(bf16[256,512]{1,0:T(8,128)(2,1)S(1)} %get-tuple-element.19), channel_id=1, source_target_pairs={{0,6},{2,0},{4,2},{6,4},{1,7},{3,1},{5,3},{7,5},{8,14},{10,8},{12,... | collective-permute-start | bytes 786440 | tf_op jit(solution)/shard_map/ppermute | solution.py:395

commit v8 on v7

--- a/solution.py
+++ b/solution.py
@@ -136,41 +136,63 @@
     return jnp.concatenate(cosines), jnp.concatenate(sines)
 
 
-def context_kernel(
-    mod_ref, ctx_ref, wk_ref, wv_ref, gain_ref, kgain_ref, rcos_ref, rsin_ref, ccos_ref, csin_ref,
-    lat_in, kv_ref, vec_ref, first_ref, last_ref, edge_ref, rows_ref, sems,
-):
+def prepare_kernel(lat_in, ctx_in, wk_in, wv_in, rows_ref, wkv_ref, edge_ref, ctx_ref, sems):
     tok = lat_in.shape[0]
     moves = [
-        pltpu.make_async_copy(lat_in.at[:WINDOW, :], edge_ref.at[:WINDOW], sems.at[0]),
-        pltpu.make_async_copy(lat_in.at[tok - WINDOW :, :], edge_ref.at[WINDOW:], sems.at[1]),
+        pltpu.make_async_copy(source, to, sems.at[i])
+        for i, (source, to) in enumerate(
+            (
+                (lat_in.at[:WINDOW, :], edge_ref.at[:WINDOW]),
+                (lat_in.at[tok - WINDOW :, :], edge_ref.at[WINDOW:]),
+                (ctx_in, ctx_ref),
+                (wk_in, wkv_ref.at[:, :HEAD_DIM]),
+                (wv_in, wkv_ref.at[:, HEAD_DIM:]),
+            )
+        )
     ]
     for move in moves:
         move.start()
+    for move in moves[:3]:
+        move.wait()
+    step = 64
+
+    def body(i, carry):
+        at = pl.ds(pl.multiple_of(i * step, step), step)
+        rows_ref[at, :] = normed(edge_ref[at, :]).astype(BF16)
+        return carry
+
+    lax.fori_loop(0, 2 * WINDOW // step, body, 0)
+    rows_ref[2 * WINDOW :, :] = normed(ctx_ref[...]).astype(BF16)
+    for move in moves[3:]:
+        move.wait()
+
+
+def context_kernel(
+    mod_ref, rows_in, wkv_ref, gain_ref, kgain_ref, rcos_ref, rsin_ref, ccos_ref, csin_ref,
+    kv_ref, vec_ref, first_ref, last_ref, rows_ref,
+):
     shift_lat, scale_lat, shift_ctx, scale_ctx, gate = vectors_of(mod_ref)
     gain = gain_ref[...]
     vec_ref[0:1, :] = gain * (1.0 + scale_lat)
     vec_ref[1:2, :] = shift_lat
     vec_ref[2:3, :] = gate
     rows_ref[2 * WINDOW :, :] = (
-        normed(ctx_ref[...]) * (gain * (1.0 + scale_ctx)) + shift_ctx
+        rows_in[2 * WINDOW :, :].astype(F32) * (gain * (1.0 + scale_ctx)) + shift_ctx
     ).astype(BF16)
-    for move in moves:
-        move.wait()
     step = 64
 
     def body(i, carry):
         at = pl.ds(pl.multiple_of(i * step, step), step)
-        rows_ref[at, :] = (normed(edge_ref[at, :]) * vec_ref[0:1, :] + vec_ref[1:2, :]).astype(BF16)
+        rows = rows_in[at, :].astype(F32) * vec_ref[0:1, :] + vec_ref[1:2, :]
+        rows_ref[at, :] = rows.astype(BF16)
         return carry
 
     lax.fori_loop(0, 2 * WINDOW // step, body, 0)
-    keys = head_norm(
-        jnp.dot(rows_ref[...], wk_ref[...], preferred_element_type=F32), kgain_ref[...]
-    )
-    values = jnp.dot(rows_ref[...], wv_ref[...], preferred_element_type=F32).astype(BF16)
+    both = jnp.dot(rows_ref[...], wkv_ref[...], preferred_element_type=F32)
+    keys = head_norm(both[:, :HEAD_DIM], kgain_ref[...])
+    values = both[:, HEAD_DIM:].astype(BF16)
     refs = (rcos_ref, rsin_ref, ccos_ref, csin_ref)
-    final = tok // GRID_W
+    final = 1024 // GRID_W
     for ref, base, groups in ((first_ref, 0, (2, 3)), (last_ref, WINDOW, (final, final + 1))):
         at = slice(base, base + WINDOW)
         ref[:, :HEAD_DIM] = rotated(keys[at], *rotation(refs, groups)).astype(BF16)
@@ -180,7 +202,7 @@
 
 
 def qkv_kernel(
-    lat_in, wq_in, wk_in, wv_in, before_ref, after_ref,
+    lat_in, wq_in, wkv_in, before_ref, after_ref,
     vec_ref, qgain_ref, kgain_ref, rcos_ref, rsin_ref, ccos_ref, csin_ref,
     packed_out, own_ref, out_ref, lat_ref, wq_ref, wkv_ref, k_ref, v_ref, even_ref, odd_ref,
     sum_ref, sems,
@@ -196,12 +218,12 @@
 
     sources = [(lat_in.at[at(i), :], lat_ref.at[at(i), :]) for i in range(steps)]
     sources += [
-        (wk_in, wkv_ref.at[:, :HEAD_DIM]), (wv_in, wkv_ref.at[:, HEAD_DIM:]), (wq_in, wq_ref),
+        (wkv_in, wkv_ref), (wq_in, wq_ref),
     ]
     moves = [
         pltpu.make_async_copy(source, to, sems.at[i]) for i, (source, to) in enumerate(sources)
     ]
-    for i in (0, steps, steps + 1, steps + 2, *range(1, steps)):
+    for i in (0, steps, steps + 1, *range(1, steps)):
         moves[i].start()
     for ref, edge in ((k_ref, slice(0, HEAD_DIM)), (v_ref, slice(HEAD_DIM, 2 * HEAD_DIM))):
         ref[:WINDOW, :] = before_ref[:, edge]
@@ -234,7 +256,7 @@
 
     moves[0].wait()
     fill(0, even_ref)
-    for i in range(steps, steps + 3):
+    for i in range(steps, steps + 2):
         moves[i].wait()
 
     def wait_rows(i):
@@ -290,7 +312,7 @@
 
     sum_ref[...] = jnp.zeros(sum_ref.shape, F32)
 
-    def body(block, carry):
+    def one(block):
         near = pl.ds(pl.multiple_of(block * WINDOW, WINDOW), 3 * WINDOW)
         no_before = (block == 0) & (sp == 0)
         no_after = (block == blocks - 1) & (sp == NZ * NY - 1)
@@ -304,13 +326,22 @@
             axis=1,
         )
         total = jnp.sum(lanes_summed(local), axis=-1, keepdims=True)
-        sum_ref[...] = jnp.where(key_at == block, total, sum_ref[...])
         mixed = jnp.dot(local.astype(BF16), v_ref[near, :], preferred_element_type=F32)
-        out_ref[block, :, HEAD_DIM:] = mixed.astype(BF16)
-        block_move(block).start()
+        return total, mixed.astype(BF16)
+
+    def body(i, carry):
+        pair = (2 * i, 2 * i + 1)
+        found = [one(block) for block in pair]
+        sums = sum_ref[...]
+        for block, (total, mixed) in zip(pair, found):
+            sums = jnp.where(key_at == block, total, sums)
+            out_ref[block, :, HEAD_DIM:] = mixed
+        sum_ref[...] = sums
+        for block in pair:
+            block_move(block).start()
         return carry
 
-    lax.fori_loop(0, blocks, body, 0)
+    lax.fori_loop(0, blocks // 2, body, 0)
     high = sum_ref[...].astype(BF16)
     out_ref[blocks, :, :HEAD_DIM] = high
     out_ref[blocks, :, HEAD_DIM:] = (sum_ref[...] - high.astype(F32)).astype(BF16)
@@ -347,16 +378,36 @@
         lax.fori_loop(0, 2, body, 0)
 
 
+def early_kernel(a0_ref, a2_ref, w0_ref, m2_in, o2_ref, sum_ref, m2_ref, sem):
+    dp = lax.axis_index("dp")
+    col = 512
+    move = pltpu.make_async_copy(m2_in, m2_ref, sem)
+    move.start()
+    for part, weight in enumerate((o2_ref, m2_ref)):
+        half = 1 - dp if part == 0 else dp
+        if part == 1:
+            move.wait()
+
+        def body(j, carry, weight=weight, half=half):
+            wide = pl.ds(pl.multiple_of(half * (D // 2) + j * col, col), col)
+            sub = pl.ds(pl.multiple_of(j * col, col), col)
+            sum_ref[:, wide] = jnp.dot(
+                a0_ref[...], w0_ref[:, wide], preferred_element_type=F32
+            ) + jnp.dot(a2_ref[...], weight[:, sub], preferred_element_type=F32)
+            return carry
+
+        lax.fori_loop(0, 2, body, 0)
+
+
 def project_kernel(
-    vec_ref, a0_ref, a1_ref, a2_ref, a3_ref, w0_ref,
-    m1_in, m2_in, m3_in, o1_ref, o2_ref, o3_ref, lat_ref, out_ref,
-    m1_ref, m2_ref, m3_ref, done_ref, sems,
+    vec_ref, sum_ref, a1_ref, a3_ref, m1_in, m3_in, o1_ref, o3_ref, lat_ref, out_ref,
+    m1_ref, m3_ref, done_ref, sems,
 ):
     dp = lax.axis_index("dp")
     col = 512
     moves = [
         pltpu.make_async_copy(source, to, sems.at[4 + i])
-        for i, (source, to) in enumerate(((m1_in, m1_ref), (m2_in, m2_ref), (m3_in, m3_ref)))
+        for i, (source, to) in enumerate(((m1_in, m1_ref), (m3_in, m3_ref)))
     ]
     for move in moves:
         move.start()
@@ -366,7 +417,7 @@
             done_ref.at[slot], out_ref.at[:, pl.ds(column, col)], sems.at[slot]
         )
 
-    for part, weights in enumerate(((o1_ref, o2_ref, o3_ref), (m1_ref, m2_ref, m3_ref))):
+    for part, weights in enumerate(((o1_ref, o3_ref), (m1_ref, m3_ref))):
         half = 1 - dp if part == 0 else dp
         if part == 1:
             for move in moves:
@@ -376,8 +427,8 @@
             column = pl.multiple_of(half * (D // 2) + j * col, col)
             wide = pl.ds(column, col)
             sub = pl.ds(pl.multiple_of(j * col, col), col)
-            mixed = jnp.dot(a0_ref[...], w0_ref[:, wide], preferred_element_type=F32)
-            for a, w in zip((a1_ref, a2_ref, a3_ref), weights):
+            mixed = sum_ref[:, wide]
+            for a, w in zip((a1_ref, a3_ref), weights):
                 mixed = mixed + jnp.dot(a[...], w[:, sub], preferred_element_type=F32)
             slot = part * 2 + j
             result = lat_ref[:, wide].astype(F32) + vec_ref[2:3, wide] * mixed
@@ -464,20 +515,23 @@
     rows = tok + 2 * WINDOW
     gain, qgain, kgain = norm_gain[None], q_gain[None], k_gain[None]
     n_ctx = context.shape[1]
+    prepared, w_kv = call(
+        prepare_kernel,
+        [((2 * WINDOW + n_ctx, D), BF16), ((D, 2 * HEAD_DIM), BF16)],
+        (lat, context[0], w_key, w_value), cost(1 << 24, 4 << 20), 60,
+        scratch=[
+            pltpu.VMEM((2 * WINDOW, D), BF16), pltpu.VMEM((n_ctx, D), BF16),
+            pltpu.SemaphoreType.DMA((5,)),
+        ],
+        in_specs=[HBM] * 4,
+    )
     edge = ((WINDOW, 2 * HEAD_DIM), BF16)
     ctx_kv, vec, first_kv, last_kv = call(
         context_kernel,
         [((peers, n_ctx, 2 * HEAD_DIM), BF16), ((8, D), F32), edge, edge],
-        (
-            mod, context[0], w_key, w_value, gain, kgain,
-            row_cos, row_sin, col_cos, col_sin, lat,
-        ),
+        (mod, prepared, w_kv, gain, kgain, row_cos, row_sin, col_cos, col_sin),
         cost(2 * (n_ctx + 2 * WINDOW) * D * 256, D * 512), 63,
-        scratch=[
-            pltpu.VMEM((2 * WINDOW, D), BF16), pltpu.VMEM((2 * WINDOW + n_ctx, D), BF16),
-            pltpu.SemaphoreType.DMA((2,)),
-        ],
-        in_specs=[VMEM] * 10 + [HBM],
+        scratch=[pltpu.VMEM((2 * WINDOW + n_ctx, D), BF16)],
     )
     up = [(i, i + 1) for i in range(peers - 1)]
     before = lax.ppermute(last_kv, SP, up)
@@ -488,7 +542,7 @@
     packed, own = call(
         qkv_kernel, [(packed_shape, BF16), ((sub, D), BF16)],
         (
-            lat, w_query, w_key, w_value, before, after, vec, qgain, kgain,
+            lat, w_query, w_kv, before, after, vec, qgain, kgain,
             row_cos, row_sin, col_cos, col_sin,
         ),
         cost(2 * tok * D * 768 + 16 * tok * 384 * HEAD_DIM, tok * D * 2 + D * 768 * 2), 60,
@@ -501,7 +555,7 @@
             pltpu.VMEM((4 * WINDOW, 128), F32),
             pltpu.SemaphoreType.DMA((tok // 256 + 4 + packed_shape[0],)),
         ],
-        in_specs=[HBM] * 4 + [VMEM] * 9,
+        in_specs=[HBM] * 3 + [VMEM] * 9,
         out_specs=[HBM, HBM],
     )
 
@@ -519,18 +573,23 @@
             else:
                 arrived[s] = shifted(piece, "tp", s)
 
+    matrix = pltpu.VMEM((width, D // 2), BF16)
+    early = call(
+        early_kernel, [((sub, D), F32)],
+        (arrived[0], arrived[2], w_out, mine[2], other[2]),
+        cost(sub * D * D, D * D), 24,
+        scratch=[matrix, pltpu.SemaphoreType.DMA], in_specs=[VMEM] * 3 + [HBM, VMEM],
+    )
     result = call(
         project_kernel, [((sub, D), BF16)],
         (
-            vec, arrived[0], arrived[1], arrived[2], arrived[3], w_out,
-            mine[1], mine[2], mine[3], other[1], other[2], other[3], own,
+            vec, early, arrived[1], arrived[3], mine[1], mine[3], other[1], other[3], own,
         ),
-        cost(2 * sub * D * D, D * D * 2), 24,
+        cost(sub * D * D, D * D), 24,
         scratch=[
-            *[pltpu.VMEM((width, D // 2), BF16)] * 3,
-            pltpu.VMEM((4, sub, 512), BF16), pltpu.SemaphoreType.DMA((7,)),
+            matrix, matrix, pltpu.VMEM((4, sub, 512), BF16), pltpu.SemaphoreType.DMA((6,)),
         ],
-        in_specs=[VMEM] * 6 + [HBM] * 3 + [VMEM] * 4,
+        in_specs=[VMEM] * 4 + [HBM] * 2 + [VMEM] * 3,
         out_specs=HBM,
     )
     return result[None]

time: 139 us -> 134 us (0.964)
  the two profiles are of different devices: /device:TPU:120 before, /device:TPU:126 now
where the time goes in v8:
time: 134 us; the launch traced here: 133 us
  waiting for transfers between devices  48.8 us (36%)
  starting transfers between devices  40.7 us (30%)
  Pallas kernels  38.6 us (29%)
  local copies, waits for them, and re-layouts  2.95 us (2%)
  other arithmetic  1.51 us (1%)
    pallas_call x11, Pallas kernels, call(): pl.pallas_call(kernel, in_specs=in_specs or [VMEM] * len(args), out_specs...  38.6 us
    all_to_all x1, waiting for transfers between devices, per_device(): part = lax.all_to_all(part, ('y', 'tp'), 0, 0, tiled=True)  37.4 us
    ppermute x9, starting transfers between devices, shifted(): lax.ppermute(array, axis, [(i, (i + by) % peers) for i in range(peers)])  11.1 us
    all_to_all x1, starting transfers between devices, per_device(): lax.all_to_all(ctx_kv, SP, 0, 0, tiled=True).reshape(-1, 2 * HEAD_DIM)  8.54 us
    all_to_all x1, starting transfers between devices, per_device(): mod = lax.all_to_all(part, 'z', 0, 0, tiled=True)  7.66 us
    all_to_all x1, starting transfers between devices, per_device(): part = lax.all_to_all(part, ('y', 'tp'), 0, 0, tiled=True)  6.83 us
    ppermute x1, waiting for transfers between devices, per_device(): after = lax.ppermute(first_kv, SP, [(j, i) for i, j in up])  6.12 us
    ppermute x1, starting transfers between devices, per_device(): before = lax.ppermute(last_kv, SP, up)  4.58 us
  transfers between devices with their start and end apart: 14, of which 6 were waited for; matrix products, arithmetic and copies ran while one was open for 1% of the time, Pallas kernels for 25%

profile of v8, /device:TPU:126, one launch (start us, length us, event | category | flops | bytes accessed | tf_op | source)
XLA Modules:
  0.0 132.9 jit_solution(3057979253712520465)
XLA Ops:
  0.0 2.2 %shard_map.152 = bf16[512,1024]{1,0:T(8,128)(2,1)} custom-call(bf16[512,2048]{1,0:T(8,128)(2,1)} %w0_ref.1), custom_call_target="tpu_custom_call" | custom-call | flops 16777216 | bytes 2097152 | tf_op jit(solution)/shard_map/pallas_call | solution.py:457
  3.7 3.2 %collective-permute-start.7 = (bf16[512,1024]{1,0:T(8,128)(2,1)}, bf16[512,1024]{1,0:T(8,128)(2,1)}, u32[]{:S(2)}, u32[]{:S(2)}) collective-permute-start(bf16[512,1024]{1,0:T(8,128)(2,1)} %shard_map.152), channel_id=1, source_target_pairs={{0,2},{2,4},{4,6},{6,0},{1,3},{3,5},{5,7},{7,1},{8,10},{10,12},{12... | collective-permute-start | bytes 3145736 | tf_op jit(solution)/shard_map/ppermute | solution.py:446
  6.9 1.8 %shard_map.145 = bf16[16,24,128]{2,1,0:T(8,128)(2,1)} custom-call(f32[1,2048]{1,0:T(1,128)} %cond_in.1, f32[1,2048]{1,0:T(1,128)} %bitcast.19, bf16[64,512]{1,0:T(8,128)(2,1)} %shift_in.1, bf16[64,512]{1,0:T(8,128)(2,1)} %scale_in.1, bf16[64,512]{1,0:T(8,128)(2,1)} %gate_in.1), custom_call_target="tpu_custom_call" | custom-call | flops 1048576 | bytes 262144 | tf_op jit(solution)/shard_map/pallas_call | solution.py:457
  8.8 6.8 %all-to-all-start = ((bf16[16,24,128]{2,1,0:T(8,128)(2,1)}), bf16[16,24,128]{2,1,0:T(8,128)(2,1)S(1)}, u32[]{:S(2)}, u32[]{:S(2)}) async-start(bf16[16,24,128]{2,1,0:T(8,128)(2,1)} %shard_map.145), calls=%async_computation | async-start | bytes 196608 | tf_op jit(solution)/shard_map/all_to_all | solution.py:489
  15.6 37.4 %all-to-all-done.in_ref = bf16[16,24,128]{2,1,0:T(8,128)(2,1)S(1)} async-done(((bf16[16,24,128]{2,1,0:T(8,128)(2,1)}), bf16[16,24,128]{2,1,0:T(8,128)(2,1)S(1)}, u32[]{:S(2)}, u32[]{:S(2)}) %all-to-all-start) | async-done | bytes 98336 | tf_op jit(solution)/shard_map/all_to_all | solution.py:489
  53.7 7.7 %all-to-all-start.1 = ((bf16[8,80,128]{2,1,0:T(8,128)(2,1)}), bf16[8,80,128]{2,1,0:T(8,128)(2,1)S(1)}, u32[]{:S(2)}, u32[]{:S(2)}) async-start(bf16[8,80,128]{2,1,0:T(8,128)(2,1)} %shard_map.146), calls=%async_computation.1 | async-start | bytes 327680 | tf_op jit(solution)/shard_map/all_to_all | solution.py:491
  62.0 3.3 %shard_map.147 = (bf16[280,2048]{1,0:T(8,128)(2,1)}, bf16[2048,256]{1,0:T(8,128)(2,1)}) custom-call(bf16[1024,2048]{1,0:T(8,128)(2,1)} %bitcast.15, bf16[24,2048]{1,0:T(8,128)(2,1)} %bitcast.17, bf16[2048,128]{1,0:T(8,128)(2,1)} %wk_in.1, bf16[2048,128]{1,0:T(8,128)(2,1)} %wv_in.1), custom_call_target="tpu_custom_call" | custom-call | flops 16777216 | bytes 4194304 | tf_op jit(solution)/shard_map/pallas_call | solution.py:457
  66.1 1.6 %all-to-all-done.1.mod_ref = bf16[8,80,128]{2,1,0:T(8,128)(2,1)S(1)} async-done(((bf16[8,80,128]{2,1,0:T(8,128)(2,1)}), bf16[8,80,128]{2,1,0:T(8,128)(2,1)S(1)}, u32[]{:S(2)}, u32[]{:S(2)}) %all-to-all-start.1) | async-done | bytes 163872 | tf_op jit(solution)/shard_map/all_to_all | solution.py:491
  68.4 3.4 %shard_map.148 = (bf16[32,24,256]{2,1,0:T(8,128)(2,1)}, f32[8,2048]{1,0:T(8,128)}, bf16[128,256]{1,0:T(8,128)(2,1)}, bf16[128,256]{1,0:T(8,128)(2,1)}) custom-call(bf16[8,80,128]{2,1,0:T(8,128)(2,1)} %copy-done.5, bf16[280,2048]{1,0:T(8,128)(2,1)} %get-tuple-element.15.rows_in, bf16[2048,256]{1,0:T(8,128)(2,1)} %get-tuple-element.16.wkv_ref.wkv_in, ...), custom_call_target="tpu_custom_call" | custom-call | flops 293601280 | bytes 1048576 | tf_op jit(solution)/shard_map/pallas_call | solution.py:457
  71.8 8.5 %all-to-all-start.2 = ((bf16[32,24,256]{2,1,0:T(8,128)(2,1)}), bf16[32,24,256]{2,1,0:T(8,128)(2,1)S(1)}, u32[]{:S(2)}, u32[]{:S(2)}) async-start(bf16[32,24,256]{2,1,0:T(8,128)(2,1)} %get-tuple-element.21), calls=%async_computation.2 | async-start | bytes 786432 | tf_op jit(solution)/shard_map/all_to_all | solution.py:539
  81.1 4.6 %collective-permute-start = (bf16[128,256]{1,0:T(8,128)(2,1)}, bf16[128,256]{1,0:T(8,128)(2,1)S(1)}, u32[]{:S(2)}, u32[]{:S(2)}) collective-permute-start(bf16[128,256]{1,0:T(8,128)(2,1)} %get-tuple-element.18), channel_id=1, source_target_pairs={{0,8},{8,16},{16,24},{24,32},{32,40},{40,48},{48,56},{56,64},{64,7... | collective-permute-start | bytes 196616 | tf_op jit(solution)/shard_map/ppermute | solution.py:537
  85.7 1.9 %collective-permute-start.1 = (bf16[128,256]{1,0:T(8,128)(2,1)}, bf16[128,256]{1,0:T(8,128)(2,1)S(1)}, u32[]{:S(2)}, u32[]{:S(2)}) collective-permute-start(bf16[128,256]{1,0:T(8,128)(2,1)} %get-tuple-element.19), channel_id=1, source_target_pairs={{8,0},{16,8},{24,16},{32,24},{40,32},{48,40},{56,48},{64,56},{72,6... | collective-permute-start | bytes 196616 | tf_op jit(solution)/shard_map/ppermute | solution.py:538
  87.6 1.6 %collective-permute-done.before_ref = bf16[128,256]{1,0:T(8,128)(2,1)S(1)} collective-permute-done((bf16[128,256]{1,0:T(8,128)(2,1)}, bf16[128,256]{1,0:T(8,128)(2,1)S(1)}, u32[]{:S(2)}, u32[]{:S(2)}) %collective-permute-start) | collective-permute-done | bytes 65568 | tf_op jit(solution)/shard_map/ppermute | solution.py:537
  89.2 6.1 %collective-permute-done.1.after_ref = bf16[128,256]{1,0:T(8,128)(2,1)S(1)} collective-permute-done((bf16[128,256]{1,0:T(8,128)(2,1)}, bf16[128,256]{1,0:T(8,128)(2,1)S(1)}, u32[]{:S(2)}, u32[]{:S(2)}) %collective-permute-start.1) | collective-permute-done | bytes 65568 | tf_op jit(solution)/shard_map/ppermute | solution.py:538
  96.0 12.9 %shard_map.149 = (bf16[9,512,256]{2,1,0:T(8,128)(2,1)}, bf16[256,2048]{1,0:T(8,128)(2,1)}) custom-call(bf16[1024,2048]{1,0:T(8,128)(2,1)} %bitcast.16, bf16[2048,512]{1,0:T(8,128)(2,1)} %wq_in.1, bf16[2048,256]{1,0:T(8,128)(2,1)} %get-tuple-element.16.wkv_ref.wkv_in, bf16[128,256]{1,0:T(8,128)(2,1)} %copy-done.6, bf16[128,256]{1,0:T(8,128)(2,1)} %copy-done.7, ...), custom_call_target="tpu_custom_call" | custom-call | flops 4026531840 | bytes 7340032 | tf_op jit(solution)/shard_map/pallas_call | solution.py:457
  108.9 1.7 %copy-done = bf16[9,512,256]{2,1,0:T(8,128)(2,1)S(1)} copy-done((bf16[9,512,256]{2,1,0:T(8,128)(2,1)S(1)}, bf16[9,512,256]{2,1,0:T(8,128)(2,1)}, u32[]{:S(2)}) %copy-start) | copy-done | bytes 2359320
  110.5 2.3 %shard_map.151 = bf16[256,512]{1,0:T(8,128)(2,1)S(1)} custom-call(bf16[9,512,256]{2,1,0:T(8,128)(2,1)S(1)} %copy-done, bf16[768,256]{1,0:T(8,128)(2,1)S(1)} %bitcast.9, f32[1,4]{1,0:T(1,128)S(1)} %bitcast.12), custom_call_target="tpu_custom_call" | custom-call | flops 402653184 | bytes 2097152 | tf_op jit(solution)/shard_map/pallas_call | solution.py:457
  112.9 1.5 %collective-permute-start.2 = (bf16[256,512]{1,0:T(8,128)(2,1)S(1)}, bf16[256,512]{1,0:T(8,128)(2,1)S(1)}, u32[]{:S(2)}, u32[]{:S(2)}) collective-permute-start(bf16[256,512]{1,0:T(8,128)(2,1)S(1)} %shard_map.151), channel_id=1, source_target_pairs={{0,4},{2,6},{4,0},{6,2},{1,5},{3,7},{5,1},{7,3},{8,12},{10,14},{12... | collective-permute-start | bytes 786440 | tf_op jit(solution)/shard_map/ppermute | solution.py:446
  114.4 4.1 %shard_map.154 = (bf16[256,512]{1,0:T(8,128)(2,1)S(1)}, bf16[256,512]{1,0:T(8,128)(2,1)S(1)}) custom-call(bf16[9,512,256]{2,1,0:T(8,128)(2,1)S(1)} %copy-done, bf16[768,256]{1,0:T(8,128)(2,1)S(1)} %bitcast.10, f32[1,4]{1,0:T(1,128)S(1)} %bitcast.13), custom_call_target="tpu_custom_call" | custom-call | flops 805306368 | bytes 2097152 | tf_op jit(solution)/shard_map/pallas_call | solution.py:457
  118.5 2.3 %collective-permute-start.5 = (bf16[256,512]{1,0:T(8,128)(2,1)S(1)}, bf16[256,512]{1,0:T(8,128)(2,1)S(1)}, u32[]{:S(2)}, u32[]{:S(2)}) collective-permute-start(bf16[256,512]{1,0:T(8,128)(2,1)S(1)} %get-tuple-element.22), channel_id=1, source_target_pairs={{0,2},{2,4},{4,6},{6,0},{1,3},{3,5},{5,7},{7,1},{8,10},{10,12},{12... | collective-permute-start | bytes 786440 | tf_op jit(solution)/shard_map/ppermute | solution.py:446
  121.8 1.9 %collective-permute-start.6 = (bf16[256,512]{1,0:T(8,128)(2,1)S(1)}, bf16[256,512]{1,0:T(8,128)(2,1)S(1)}, u32[]{:S(2)}, u32[]{:S(2)}) collective-permute-start(bf16[256,512]{1,0:T(8,128)(2,1)S(1)} %get-tuple-element.23), channel_id=1, source_target_pairs={{0,6},{2,0},{4,2},{6,4},{1,7},{3,1},{5,3},{7,5},{8,14},{10,8},{12,... | collective-permute-start | bytes 786440 | tf_op jit(solution)/shard_map/ppermute | solution.py:446
  123.7 2.3 %shard_map.150.a0_ref = bf16[256,512]{1,0:T(8,128)(2,1)S(1)} custom-call(bf16[9,512,256]{2,1,0:T(8,128)(2,1)S(1)} %copy-done, bf16[768,256]{1,0:T(8,128)(2,1)S(1)} %bitcast.11, f32[1,4]{1,0:T(1,128)S(1)} %bitcast.14), custom_call_target="tpu_custom_call" | custom-call | flops 402653184 | bytes 2097152 | tf_op jit(solution)/shard_map/pallas_call | solution.py:457
  126.1 2.2 %shard_map.153.sum_ref = f32[256,2048]{1,0:T(8,128)S(1)} custom-call(bf16[256,512]{1,0:T(8,128)(2,1)S(1)} %shard_map.150.a0_ref, bf16[256,512]{1,0:T(8,128)(2,1)S(1)} %collective-permute-done.2.a2_ref, bf16[512,2048]{1,0:T(8,128)(2,1)S(1)} %copy-done.1, bf16[512,1024]{1,0:T(8,128)(2,1)} %collective-permute-done.3.m2_in, ...), custom_call_target="tpu_custom_call" | custom-call | flops 1073741824 | bytes 4194304 | tf_op jit(solution)/shard_map/pallas_call | solution.py:457
  129.4 3.3 %shard_map.155 = bf16[256,2048]{1,0:T(8,128)(2,1)} custom-call(f32[8,2048]{1,0:T(8,128)S(1)} %copy-done.3, f32[256,2048]{1,0:T(8,128)S(1)} %shard_map.153.sum_ref, bf16[256,512]{1,0:T(8,128)(2,1)S(1)} %collective-permute-done.5.a1_ref, bf16[256,512]{1,0:T(8,128)(2,1)S(1)} %collective-permute-done.6.a3_ref, bf16[512,1024]{1,0:T(8,128)(2,1)} %collective-permute-done.7.m1_in, ...), custom_call_target="tpu_custom_call" | custom-call | flops 1073741824 | bytes 4194304 | tf_op jit(solution)/shard_map/pallas_call | solution.py:457
  (36 shorter events, 7.8 us)
Async XLA Ops:
  2.2 78.1 %collective-permute-start.3 = (bf16[512,1024]{1,0:T(8,128)(2,1)}, bf16[512,1024]{1,0:T(8,128)(2,1)}, u32[]{:S(2)}, u32[]{:S(2)}) collective-permute-start(bf16[512,1024]{1,0:T(8,128)(2,1)} %shard_map.152), channel_id=1, source_target_pairs={{0,4},{2,6},{4,0},{6,2},{1,5},{3,7},{5,1},{7,3},{8,12},{10,14},{12... | collective-permute-start | bytes 3145736 | tf_op jit(solution)/shard_map/ppermute | solution.py:446
  3.7 76.8 %collective-permute-start.8 = (bf16[512,1024]{1,0:T(8,128)(2,1)}, bf16[512,1024]{1,0:T(8,128)(2,1)}, u32[]{:S(2)}, u32[]{:S(2)}) collective-permute-start(bf16[512,1024]{1,0:T(8,128)(2,1)} %shard_map.152), channel_id=1, source_target_pairs={{0,6},{2,0},{4,2},{6,4},{1,7},{3,1},{5,3},{7,5},{8,14},{10,8},{12,... | collective-permute-start | bytes 3145736 | tf_op jit(solution)/shard_map/ppermute | solution.py:446
  3.7 77.3 %collective-permute-start.7 = (bf16[512,1024]{1,0:T(8,128)(2,1)}, bf16[512,1024]{1,0:T(8,128)(2,1)}, u32[]{:S(2)}, u32[]{:S(2)}) collective-permute-start(bf16[512,1024]{1,0:T(8,128)(2,1)} %shard_map.152), channel_id=1, source_target_pairs={{0,2},{2,4},{4,6},{6,0},{1,3},{3,5},{5,7},{7,1},{8,10},{10,12},{12... | collective-permute-start | bytes 3145736 | tf_op jit(solution)/shard_map/ppermute | solution.py:446
  8.8 44.2 %all-to-all-start = ((bf16[16,24,128]{2,1,0:T(8,128)(2,1)}), bf16[16,24,128]{2,1,0:T(8,128)(2,1)S(1)}, u32[]{:S(2)}, u32[]{:S(2)}) async-start(bf16[16,24,128]{2,1,0:T(8,128)(2,1)} %shard_map.145), calls=%async_computation | async-start | bytes 196608 | tf_op jit(solution)/shard_map/all_to_all | solution.py:489
  53.7 14.1 %all-to-all-start.1 = ((bf16[8,80,128]{2,1,0:T(8,128)(2,1)}), bf16[8,80,128]{2,1,0:T(8,128)(2,1)S(1)}, u32[]{:S(2)}, u32[]{:S(2)}) async-start(bf16[8,80,128]{2,1,0:T(8,128)(2,1)} %shard_map.146), calls=%async_computation.1 | async-start | bytes 327680 | tf_op jit(solution)/shard_map/all_to_all | solution.py:491
  67.7 0.7 copy-start.5
  71.8 37.0 %all-to-all-start.2 = ((bf16[32,24,256]{2,1,0:T(8,128)(2,1)}), bf16[32,24,256]{2,1,0:T(8,128)(2,1)S(1)}, u32[]{:S(2)}, u32[]{:S(2)}) async-start(bf16[32,24,256]{2,1,0:T(8,128)(2,1)} %get-tuple-element.21), calls=%async_computation.2 | async-start | bytes 786432 | tf_op jit(solution)/shard_map/all_to_all | solution.py:539
  80.4 45.7 %collective-permute-start.4 = (bf16[512,1024]{1,0:T(8,128)(2,1)}, bf16[512,1024]{1,0:T(8,128)(2,1)S(1)}, u32[]{:S(2)}, u32[]{:S(2)}) collective-permute-start(bf16[512,1024]{1,0:T(8,128)(2,1)} %collective-permute-done.3.m2_in), channel_id=1, source_target_pairs={{0,1},{1,0},{2,3},{3,2},{4,5},{5,4},{6,7},{7,6},{8,9},{9,8},{10,11... | collective-permute-start | bytes 3145736 | tf_op jit(solution)/shard_map/ppermute | solution.py:446
  80.5 48.9 %collective-permute-start.10 = (bf16[512,1024]{1,0:T(8,128)(2,1)}, bf16[512,1024]{1,0:T(8,128)(2,1)S(1)}, u32[]{:S(2)}, u32[]{:S(2)}) collective-permute-start(bf16[512,1024]{1,0:T(8,128)(2,1)} %collective-permute-done.8.m3_in), channel_id=1, source_target_pairs={{0,1},{1,0},{2,3},{3,2},{4,5},{5,4},{6,7},{7,6},{8,9},{9,8},{10,11... | collective-permute-start | bytes 3145736 | tf_op jit(solution)/shard_map/ppermute | solution.py:446
  81.0 48.4 %collective-permute-start.9 = (bf16[512,1024]{1,0:T(8,128)(2,1)}, bf16[512,1024]{1,0:T(8,128)(2,1)S(1)}, u32[]{:S(2)}, u32[]{:S(2)}) collective-permute-start(bf16[512,1024]{1,0:T(8,128)(2,1)} %collective-permute-done.7.m1_in), channel_id=1, source_target_pairs={{0,1},{1,0},{2,3},{3,2},{4,5},{5,4},{6,7},{7,6},{8,9},{9,8},{10,11... | collective-permute-start | bytes 3145736 | tf_op jit(solution)/shard_map/ppermute | solution.py:446
  81.1 8.2 %collective-permute-start = (bf16[128,256]{1,0:T(8,128)(2,1)}, bf16[128,256]{1,0:T(8,128)(2,1)S(1)}, u32[]{:S(2)}, u32[]{:S(2)}) collective-permute-start(bf16[128,256]{1,0:T(8,128)(2,1)} %get-tuple-element.18), channel_id=1, source_target_pairs={{0,8},{8,16},{16,24},{24,32},{32,40},{40,48},{48,56},{56,64},{64,7... | collective-permute-start | bytes 196616 | tf_op jit(solution)/shard_map/ppermute | solution.py:537
  85.7 9.7 %collective-permute-start.1 = (bf16[128,256]{1,0:T(8,128)(2,1)}, bf16[128,256]{1,0:T(8,128)(2,1)S(1)}, u32[]{:S(2)}, u32[]{:S(2)}) collective-permute-start(bf16[128,256]{1,0:T(8,128)(2,1)} %get-tuple-element.19), channel_id=1, source_target_pairs={{8,0},{16,8},{24,16},{32,24},{40,32},{48,40},{56,48},{64,56},{72,6... | collective-permute-start | bytes 196616 | tf_op jit(solution)/shard_map/ppermute | solution.py:538
  89.2 6.1 %copy-start.6 = (bf16[128,256]{1,0:T(8,128)(2,1)}, bf16[128,256]{1,0:T(8,128)(2,1)S(1)}, u32[]{:S(2)}) copy-start(bf16[128,256]{1,0:T(8,128)(2,1)S(1)} %collective-permute-done.before_ref) | copy-start | bytes 196612
  95.3 0.6 copy-start.7
  96.0 12.9 %copy-start.4 = (f32[4]{0:T(128)S(1)}, f32[4]{0:T(128)}, u32[]{:S(2)}) copy-start(f32[4]{0:T(128)} %param.29) | copy-start | bytes 52
  108.8 1.7 %copy-start = (bf16[9,512,256]{2,1,0:T(8,128)(2,1)S(1)}, bf16[9,512,256]{2,1,0:T(8,128)(2,1)}, u32[]{:S(2)}) copy-start(bf16[9,512,256]{2,1,0:T(8,128)(2,1)} %get-tuple-element.20.refs_0_) | copy-start | bytes 7077892
  112.9 8.9 %collective-permute-start.2 = (bf16[256,512]{1,0:T(8,128)(2,1)S(1)}, bf16[256,512]{1,0:T(8,128)(2,1)S(1)}, u32[]{:S(2)}, u32[]{:S(2)}) collective-permute-start(bf16[256,512]{1,0:T(8,128)(2,1)S(1)} %shard_map.151), channel_id=1, source_target_pairs={{0,4},{2,6},{4,0},{6,2},{1,5},{3,7},{5,1},{7,3},{8,12},{10,14},{12... | collective-permute-start | bytes 786440 | tf_op jit(solution)/shard_map/ppermute | solution.py:446
  118.5 7.6 %copy-start.1 = (bf16[512,2048]{1,0:T(8,128)(2,1)S(1)}, bf16[512,2048]{1,0:T(8,128)(2,1)}, u32[]{:S(2)}) copy-start(bf16[512,2048]{1,0:T(8,128)(2,1)} %w0_ref.1) | copy-start | bytes 6291460
  118.5 9.8 %collective-permute-start.5 = (bf16[256,512]{1,0:T(8,128)(2,1)S(1)}, bf16[256,512]{1,0:T(8,128)(2,1)S(1)}, u32[]{:S(2)}, u32[]{:S(2)}) collective-permute-start(bf16[256,512]{1,0:T(8,128)(2,1)S(1)} %get-tuple-element.22), channel_id=1, source_target_pairs={{0,2},{2,4},{4,6},{6,0},{1,3},{3,5},{5,7},{7,1},{8,10},{10,12},{12... | collective-permute-start | bytes 786440 | tf_op jit(solution)/shard_map/ppermute | solution.py:446
  121.8 7.6 %collective-permute-start.6 = (bf16[256,512]{1,0:T(8,128)(2,1)S(1)}, bf16[256,512]{1,0:T(8,128)(2,1)S(1)}, u32[]{:S(2)}, u32[]{:S(2)}) collective-permute-start(bf16[256,512]{1,0:T(8,128)(2,1)S(1)} %get-tuple-element.23), channel_id=1, source_target_pairs={{0,6},{2,0},{4,2},{6,4},{1,7},{3,1},{5,3},{7,5},{8,14},{10,8},{12,... | collective-permute-start | bytes 786440 | tf_op jit(solution)/shard_map/ppermute | solution.py:446
  126.1 3.3 %copy-start.2 = (bf16[256,2048]{1,0:T(8,128)(2,1)S(1)}, bf16[256,2048]{1,0:T(8,128)(2,1)}, u32[]{:S(2)}) copy-start(bf16[256,2048]{1,0:T(8,128)(2,1)} %get-tuple-element.24.lat_ref) | copy-start | bytes 3145732
  126.1 3.3 %copy-start.3 = (f32[8,2048]{1,0:T(8,128)S(1)}, f32[8,2048]{1,0:T(8,128)}, u32[]{:S(2)}) copy-start(f32[8,2048]{1,0:T(8,128)} %get-tuple-element.17.vec_ref) | copy-start | bytes 196612

commit v9 on v8

--- a/solution.py
+++ b/solution.py
@@ -136,7 +136,23 @@
     return jnp.concatenate(cosines), jnp.concatenate(sines)
 
 
-def prepare_kernel(lat_in, ctx_in, wk_in, wv_in, rows_ref, wkv_ref, edge_ref, ctx_ref, sems):
+def fill_tables(first_row, cos_ref, sin_ref, rows):
+    shape = cos_ref.shape
+    quarter = HEAD_DIM // 4
+    at = lax.broadcasted_iota(jnp.int32, shape, 0) + first_row
+    lane = lax.broadcasted_iota(jnp.int32, shape, 1)
+    frequency = jnp.exp((lane % quarter).astype(F32) * (-math.log(ROPE_BASE) / quarter))
+    angle = at.astype(F32) * frequency
+    wanted = (lane < HEAD_DIM // 2) == rows
+    sign = jnp.where((lane // quarter) % 2 == 0, -1.0, 1.0)
+    cos_ref[...] = jnp.where(wanted, jnp.cos(angle), 0.0)
+    sin_ref[...] = jnp.where(wanted, jnp.sin(angle) * sign, 0.0)
+
+
+def prepare_kernel(
+    lat_in, ctx_in, wk_in, wv_in,
+    rows_ref, wkv_ref, rcos_ref, rsin_ref, ccos_ref, csin_ref, edge_ref, ctx_ref, sems,
+):
     tok = lat_in.shape[0]
     moves = [
         pltpu.make_async_copy(source, to, sems.at[i])
@@ -152,6 +168,8 @@
     ]
     for move in moves:
         move.start()
+    fill_tables((sp_index() * tok - WINDOW) // GRID_W, rcos_ref, rsin_ref, True)
+    fill_tables(0, ccos_ref, csin_ref, False)
     for move in moves[:3]:
         move.wait()
     step = 64
@@ -472,7 +490,6 @@
     lat = latent[0]
     tok = lat.shape[0]
     sub = tok // NX
-    sp = sp_index()
     width = 4 * HEAD_DIM
 
     peers = NZ * NY
@@ -499,25 +516,16 @@
         mine[s] = shifted(half, "tp", s)
         other[s] = shifted(mine[s], "dp", 1)
 
-    quarter = HEAD_DIM // 4
-    lane = jnp.arange(HEAD_DIM)
-    frequency = ROPE_BASE ** (-(lane % quarter).astype(F32) / quarter)
-    sign = jnp.where((lane // quarter) % 2 == 0, -1.0, 1.0).astype(F32)
-    by_row = lane < HEAD_DIM // 2
-    grid_row = (sp * tok - WINDOW) // GRID_W + jnp.arange(24, dtype=jnp.int32)
-    row_angle = grid_row.astype(F32)[:, None] * frequency
-    col_angle = jnp.arange(GRID_W, dtype=F32)[:, None] * frequency
-    row_cos = jnp.where(by_row, jnp.cos(row_angle), 0.0)
-    row_sin = jnp.where(by_row, jnp.sin(row_angle) * sign, 0.0)
-    col_cos = jnp.where(by_row, 0.0, jnp.cos(col_angle))
-    col_sin = jnp.where(by_row, 0.0, jnp.sin(col_angle) * sign)
-
     rows = tok + 2 * WINDOW
     gain, qgain, kgain = norm_gain[None], q_gain[None], k_gain[None]
     n_ctx = context.shape[1]
-    prepared, w_kv = call(
+    table, column_table = ((24, HEAD_DIM), F32), ((GRID_W, HEAD_DIM), F32)
+    prepared, w_kv, row_cos, row_sin, col_cos, col_sin = call(
         prepare_kernel,
-        [((2 * WINDOW + n_ctx, D), BF16), ((D, 2 * HEAD_DIM), BF16)],
+        [
+            ((2 * WINDOW + n_ctx, D), BF16), ((D, 2 * HEAD_DIM), BF16),
+            table, table, column_table, column_table,
+        ],
         (lat, context[0], w_key, w_value), cost(1 << 24, 4 << 20), 60,
         scratch=[
             pltpu.VMEM((2 * WINDOW, D), BF16), pltpu.VMEM((n_ctx, D), BF16),

time: 134 us -> 134 us (level)
  blocking collectives: 0 us -> 44.2 us
  waiting for transfers between devices: 48.8 us -> 12.9 us
  starting transfers between devices: 40.7 us -> 33.9 us
  other arithmetic: 1.51 us -> 0 us
    all_to_all x0 -> x1, blocking collectives: none -> 44.2 us  [per_device(): part = lax.all_to_all(part, ('y', 'tp'), 0, 0, tiled=True)]
    all_to_all x1 -> x0, waiting for transfers between devices: 37.4 us -> none  [per_device(): part = lax.all_to_all(part, ('y', 'tp'), 0, 0, tiled=True)]
    all_to_all x1 -> x0, starting transfers between devices: 6.83 us -> none  [per_device(): part = lax.all_to_all(part, ('y', 'tp'), 0, 0, tiled=True)]
    select_n x3 -> x0, other arithmetic: 1.5 us -> none  [the longest x1 0.76 us: per_device(): col_sin = jnp.where(by_row, 0.0, jnp.sin(col_angle) * sign)]
    all_to_all x1, waiting for transfers between devices: 1.59 us -> 3.06 us  [per_device(): mod = lax.all_to_all(part, 'z', 0, 0, tiled=True)]
  transfers between devices with their start and end apart: 14 -> 13, of which waited for: 6 -> 5; matrix products, arithmetic and copies ran while one was open for 1% -> 0% of each run, Pallas kernels for 25% -> 25%
where the time goes in v9:
time: 134 us; the launch traced here: 133 us
  blocking collectives  44.2 us (33%)
  Pallas kernels  38.6 us (29%)
  starting transfers between devices  33.9 us (25%)
  waiting for transfers between devices  12.9 us (10%)
  local copies, waits for them, and re-layouts  2.96 us (2%)
    all_to_all x1, blocking collectives, per_device(): part = lax.all_to_all(part, ('y', 'tp'), 0, 0, tiled=True)  44.2 us
    pallas_call x11, Pallas kernels, call(): pl.pallas_call(kernel, in_specs=in_specs or [VMEM] * len(args), out_specs...  38.6 us
    ppermute x9, starting transfers between devices, shifted(): lax.ppermute(array, axis, [(i, (i + by) % peers) for i in range(peers)])  11.2 us
    all_to_all x1, starting transfers between devices, per_device(): lax.all_to_all(ctx_kv, SP, 0, 0, tiled=True).reshape(-1, 2 * HEAD_DIM)  8.54 us
    all_to_all x1, starting transfers between devices, per_device(): mod = lax.all_to_all(part, 'z', 0, 0, tiled=True)  7.66 us
    ppermute x1, waiting for transfers between devices, per_device(): after = lax.ppermute(first_kv, SP, [(j, i) for i, j in up])  6.64 us
    ppermute x1, starting transfers between devices, per_device(): before = lax.ppermute(last_kv, SP, up)  4.58 us
    all_to_all x1, waiting for transfers between devices, per_device(): mod = lax.all_to_all(part, 'z', 0, 0, tiled=True)  3.06 us
  transfers between devices with their start and end apart: 13, of which 5 were waited for; matrix products, arithmetic and copies ran while one was open for 0% of the time, Pallas kernels for 25%

profile of v9, /device:TPU:126, one launch (start us, length us, event | category | flops | bytes accessed | tf_op | source)
XLA Modules:
  0.0 132.9 jit_solution(13652575150288075558)
XLA Ops:
  0.0 2.2 %shard_map.152 = bf16[512,1024]{1,0:T(8,128)(2,1)} custom-call(bf16[512,2048]{1,0:T(8,128)(2,1)} %w0_ref.1), custom_call_target="tpu_custom_call" | custom-call | flops 16777216 | bytes 2097152 | tf_op jit(solution)/shard_map/pallas_call | solution.py:475
  2.2 1.5 %collective-permute-start.3 = (bf16[512,1024]{1,0:T(8,128)(2,1)}, bf16[512,1024]{1,0:T(8,128)(2,1)}, u32[]{:S(2)}, u32[]{:S(2)}) collective-permute-start(bf16[512,1024]{1,0:T(8,128)(2,1)} %shard_map.152), channel_id=1, source_target_pairs={{0,4},{2,6},{4,0},{6,2},{1,5},{3,7},{5,1},{7,3},{8,12},{10,14},{12... | collective-permute-start | bytes 3145736 | tf_op jit(solution)/shard_map/ppermute | solution.py:464
  3.7 3.2 %collective-permute-start.7 = (bf16[512,1024]{1,0:T(8,128)(2,1)}, bf16[512,1024]{1,0:T(8,128)(2,1)}, u32[]{:S(2)}, u32[]{:S(2)}) collective-permute-start(bf16[512,1024]{1,0:T(8,128)(2,1)} %shard_map.152), channel_id=1, source_target_pairs={{0,2},{2,4},{4,6},{6,0},{1,3},{3,5},{5,7},{7,1},{8,10},{10,12},{12... | collective-permute-start | bytes 3145736 | tf_op jit(solution)/shard_map/ppermute | solution.py:464
  6.9 1.8 %shard_map.145 = bf16[16,24,128]{2,1,0:T(8,128)(2,1)} custom-call(f32[1,2048]{1,0:T(1,128)} %cond_in.1, f32[1,2048]{1,0:T(1,128)} %bitcast.19, bf16[64,512]{1,0:T(8,128)(2,1)} %shift_in.1, bf16[64,512]{1,0:T(8,128)(2,1)} %scale_in.1, bf16[64,512]{1,0:T(8,128)(2,1)} %gate_in.1), custom_call_target="tpu_custom_call" | custom-call | flops 1048576 | bytes 262144 | tf_op jit(solution)/shard_map/pallas_call | solution.py:475
  8.8 44.2 %all_to_all.15.in_ref = bf16[16,24,128]{2,1,0:T(8,128)(2,1)S(1)} all-to-all(bf16[16,24,128]{2,1,0:T(8,128)(2,1)} %shard_map.145), channel_id=1, replica_groups=mesh['z'=8,'y'=4,'tp'=4,'dp'=2] {'y','tp'}, dimensions={0} | all-to-all | bytes 196608 | tf_op jit(solution)/shard_map/all_to_all | solution.py:506
  53.7 7.7 %all-to-all-start.1 = ((bf16[8,80,128]{2,1,0:T(8,128)(2,1)}), bf16[8,80,128]{2,1,0:T(8,128)(2,1)S(1)}, u32[]{:S(2)}, u32[]{:S(2)}) async-start(bf16[8,80,128]{2,1,0:T(8,128)(2,1)} %shard_map.146), calls=%async_computation.1 | async-start | bytes 327680 | tf_op jit(solution)/shard_map/all_to_all | solution.py:508
  61.3 3.3 %shard_map.147 = (bf16[280,2048]{1,0:T(8,128)(2,1)}, bf16[2048,256]{1,0:T(8,128)(2,1)}, f32[24,128]{1,0:T(8,128)}, f32[24,128]{1,0:T(8,128)}, f32[64,128]{1,0:T(8,128)}, /*index=5*/f32[64,128]{1,0:T(8,128)}) custom-call(bf16[1024,2048]{1,0:T(8,128)(2,1)} %bitcast.15, bf16[24,2048]{1,0:T(8,128)(2,1)} %bitcast.17, bf16[2048,128]{1,0:T(8,128)(2,1)} %wk_in.1, ...), custom_call_target="tpu_custom_call" | custom-call | flops 16777216 | bytes 4194304 | tf_op jit(solution)/shard_map/pallas_call | solution.py:475
  64.7 3.1 %all-to-all-done.1.mod_ref = bf16[8,80,128]{2,1,0:T(8,128)(2,1)S(1)} async-done(((bf16[8,80,128]{2,1,0:T(8,128)(2,1)}), bf16[8,80,128]{2,1,0:T(8,128)(2,1)S(1)}, u32[]{:S(2)}, u32[]{:S(2)}) %all-to-all-start.1) | async-done | bytes 163872 | tf_op jit(solution)/shard_map/all_to_all | solution.py:508
  68.4 3.4 %shard_map.148 = (bf16[32,24,256]{2,1,0:T(8,128)(2,1)}, f32[8,2048]{1,0:T(8,128)}, bf16[128,256]{1,0:T(8,128)(2,1)}, bf16[128,256]{1,0:T(8,128)(2,1)}) custom-call(bf16[8,80,128]{2,1,0:T(8,128)(2,1)} %copy-done.5, bf16[280,2048]{1,0:T(8,128)(2,1)} %get-tuple-element.19.rows_in, bf16[2048,256]{1,0:T(8,128)(2,1)} %get-tuple-element.20.wkv_ref.wkv_in, ...), custom_call_target="tpu_custom_call" | custom-call | flops 293601280 | bytes 1048576 | tf_op jit(solution)/shard_map/pallas_call | solution.py:475
  71.8 8.5 %all-to-all-start.2 = ((bf16[32,24,256]{2,1,0:T(8,128)(2,1)}), bf16[32,24,256]{2,1,0:T(8,128)(2,1)S(1)}, u32[]{:S(2)}, u32[]{:S(2)}) async-start(bf16[32,24,256]{2,1,0:T(8,128)(2,1)} %get-tuple-element.29), calls=%async_computation.2 | async-start | bytes 786432 | tf_op jit(solution)/shard_map/all_to_all | solution.py:547
  81.1 4.6 %collective-permute-start = (bf16[128,256]{1,0:T(8,128)(2,1)}, bf16[128,256]{1,0:T(8,128)(2,1)S(1)}, u32[]{:S(2)}, u32[]{:S(2)}) collective-permute-start(bf16[128,256]{1,0:T(8,128)(2,1)} %get-tuple-element.26), channel_id=1, source_target_pairs={{0,8},{8,16},{16,24},{24,32},{32,40},{40,48},{48,56},{56,64},{64,7... | collective-permute-start | bytes 196616 | tf_op jit(solution)/shard_map/ppermute | solution.py:545
  85.7 1.9 %collective-permute-start.1 = (bf16[128,256]{1,0:T(8,128)(2,1)}, bf16[128,256]{1,0:T(8,128)(2,1)S(1)}, u32[]{:S(2)}, u32[]{:S(2)}) collective-permute-start(bf16[128,256]{1,0:T(8,128)(2,1)} %get-tuple-element.27), channel_id=1, source_target_pairs={{8,0},{16,8},{24,16},{32,24},{40,32},{48,40},{56,48},{64,56},{72,6... | collective-permute-start | bytes 196616 | tf_op jit(solution)/shard_map/ppermute | solution.py:546
  87.6 1.1 collective-permute-done.before_ref
  88.7 6.6 %collective-permute-done.1.after_ref = bf16[128,256]{1,0:T(8,128)(2,1)S(1)} collective-permute-done((bf16[128,256]{1,0:T(8,128)(2,1)}, bf16[128,256]{1,0:T(8,128)(2,1)S(1)}, u32[]{:S(2)}, u32[]{:S(2)}) %collective-permute-start.1) | collective-permute-done | bytes 65568 | tf_op jit(solution)/shard_map/ppermute | solution.py:546
  96.0 12.8 %shard_map.149 = (bf16[9,512,256]{2,1,0:T(8,128)(2,1)}, bf16[256,2048]{1,0:T(8,128)(2,1)}) custom-call(bf16[1024,2048]{1,0:T(8,128)(2,1)} %bitcast.16, bf16[2048,512]{1,0:T(8,128)(2,1)} %wq_in.1, bf16[2048,256]{1,0:T(8,128)(2,1)} %get-tuple-element.20.wkv_ref.wkv_in, bf16[128,256]{1,0:T(8,128)(2,1)} %copy-done.6, bf16[128,256]{1,0:T(8,128)(2,1)} %copy-done.7, ...), custom_call_target="tpu_custom_call" | custom-call | flops 4026531840 | bytes 7340032 | tf_op jit(solution)/shard_map/pallas_call | solution.py:475
  108.9 1.7 %copy-done = bf16[9,512,256]{2,1,0:T(8,128)(2,1)S(1)} copy-done((bf16[9,512,256]{2,1,0:T(8,128)(2,1)S(1)}, bf16[9,512,256]{2,1,0:T(8,128)(2,1)}, u32[]{:S(2)}) %copy-start) | copy-done | bytes 2359320
  110.5 2.3 %shard_map.151 = bf16[256,512]{1,0:T(8,128)(2,1)S(1)} custom-call(bf16[9,512,256]{2,1,0:T(8,128)(2,1)S(1)} %copy-done, bf16[768,256]{1,0:T(8,128)(2,1)S(1)} %bitcast.9, f32[1,4]{1,0:T(1,128)S(1)} %bitcast.12), custom_call_target="tpu_custom_call" | custom-call | flops 402653184 | bytes 2097152 | tf_op jit(solution)/shard_map/pallas_call | solution.py:475
  112.9 1.5 %collective-permute-start.2 = (bf16[256,512]{1,0:T(8,128)(2,1)S(1)}, bf16[256,512]{1,0:T(8,128)(2,1)S(1)}, u32[]{:S(2)}, u32[]{:S(2)}) collective-permute-start(bf16[256,512]{1,0:T(8,128)(2,1)S(1)} %shard_map.151), channel_id=1, source_target_pairs={{0,4},{2,6},{4,0},{6,2},{1,5},{3,7},{5,1},{7,3},{8,12},{10,14},{12... | collective-permute-start | bytes 786440 | tf_op jit(solution)/shard_map/ppermute | solution.py:464
  114.4 4.1 %shard_map.154 = (bf16[256,512]{1,0:T(8,128)(2,1)S(1)}, bf16[256,512]{1,0:T(8,128)(2,1)S(1)}) custom-call(bf16[9,512,256]{2,1,0:T(8,128)(2,1)S(1)} %copy-done, bf16[768,256]{1,0:T(8,128)(2,1)S(1)} %bitcast.10, f32[1,4]{1,0:T(1,128)S(1)} %bitcast.13), custom_call_target="tpu_custom_call" | custom-call | flops 805306368 | bytes 2097152 | tf_op jit(solution)/shard_map/pallas_call | solution.py:475
  118.5 2.3 %collective-permute-start.5 = (bf16[256,512]{1,0:T(8,128)(2,1)S(1)}, bf16[256,512]{1,0:T(8,128)(2,1)S(1)}, u32[]{:S(2)}, u32[]{:S(2)}) collective-permute-start(bf16[256,512]{1,0:T(8,128)(2,1)S(1)} %get-tuple-element.30), channel_id=1, source_target_pairs={{0,2},{2,4},{4,6},{6,0},{1,3},{3,5},{5,7},{7,1},{8,10},{10,12},{12... | collective-permute-start | bytes 786440 | tf_op jit(solution)/shard_map/ppermute | solution.py:464
  121.8 1.9 %collective-permute-start.6 = (bf16[256,512]{1,0:T(8,128)(2,1)S(1)}, bf16[256,512]{1,0:T(8,128)(2,1)S(1)}, u32[]{:S(2)}, u32[]{:S(2)}) collective-permute-start(bf16[256,512]{1,0:T(8,128)(2,1)S(1)} %get-tuple-element.31), channel_id=1, source_target_pairs={{0,6},{2,0},{4,2},{6,4},{1,7},{3,1},{5,3},{7,5},{8,14},{10,8},{12,... | collective-permute-start | bytes 786440 | tf_op jit(solution)/shard_map/ppermute | solution.py:464
  123.7 2.3 %shard_map.150.a0_ref = bf16[256,512]{1,0:T(8,128)(2,1)S(1)} custom-call(bf16[9,512,256]{2,1,0:T(8,128)(2,1)S(1)} %copy-done, bf16[768,256]{1,0:T(8,128)(2,1)S(1)} %bitcast.11, f32[1,4]{1,0:T(1,128)S(1)} %bitcast.14), custom_call_target="tpu_custom_call" | custom-call | flops 402653184 | bytes 2097152 | tf_op jit(solution)/shard_map/pallas_call | solution.py:475
  126.1 2.2 %shard_map.153.sum_ref = f32[256,2048]{1,0:T(8,128)S(1)} custom-call(bf16[256,512]{1,0:T(8,128)(2,1)S(1)} %shard_map.150.a0_ref, bf16[256,512]{1,0:T(8,128)(2,1)S(1)} %collective-permute-done.2.a2_ref, bf16[512,2048]{1,0:T(8,128)(2,1)S(1)} %copy-done.1, bf16[512,1024]{1,0:T(8,128)(2,1)} %collective-permute-done.3.m2_in, ...), custom_call_target="tpu_custom_call" | custom-call | flops 1073741824 | bytes 4194304 | tf_op jit(solution)/shard_map/pallas_call | solution.py:475
  129.4 3.3 %shard_map.155 = bf16[256,2048]{1,0:T(8,128)(2,1)} custom-call(f32[8,2048]{1,0:T(8,128)S(1)} %copy-done.3, f32[256,2048]{1,0:T(8,128)S(1)} %shard_map.153.sum_ref, bf16[256,512]{1,0:T(8,128)(2,1)S(1)} %collective-permute-done.5.a1_ref, bf16[256,512]{1,0:T(8,128)(2,1)S(1)} %collective-permute-done.6.a3_ref, bf16[512,1024]{1,0:T(8,128)(2,1)} %collective-permute-done.7.m1_in, ...), custom_call_target="tpu_custom_call" | custom-call | flops 1073741824 | bytes 4194304 | tf_op jit(solution)/shard_map/pallas_call | solution.py:475
  (30 shorter events, 4.7 us)
Async XLA Ops:
  2.2 78.2 %collective-permute-start.3 = (bf16[512,1024]{1,0:T(8,128)(2,1)}, bf16[512,1024]{1,0:T(8,128)(2,1)}, u32[]{:S(2)}, u32[]{:S(2)}) collective-permute-start(bf16[512,1024]{1,0:T(8,128)(2,1)} %shard_map.152), channel_id=1, source_target_pairs={{0,4},{2,6},{4,0},{6,2},{1,5},{3,7},{5,1},{7,3},{8,12},{10,14},{12... | collective-permute-start | bytes 3145736 | tf_op jit(solution)/shard_map/ppermute | solution.py:464
  3.7 76.8 %collective-permute-start.8 = (bf16[512,1024]{1,0:T(8,128)(2,1)}, bf16[512,1024]{1,0:T(8,128)(2,1)}, u32[]{:S(2)}, u32[]{:S(2)}) collective-permute-start(bf16[512,1024]{1,0:T(8,128)(2,1)} %shard_map.152), channel_id=1, source_target_pairs={{0,6},{2,0},{4,2},{6,4},{1,7},{3,1},{5,3},{7,5},{8,14},{10,8},{12,... | collective-permute-start | bytes 3145736 | tf_op jit(solution)/shard_map/ppermute | solution.py:464
  3.7 77.3 %collective-permute-start.7 = (bf16[512,1024]{1,0:T(8,128)(2,1)}, bf16[512,1024]{1,0:T(8,128)(2,1)}, u32[]{:S(2)}, u32[]{:S(2)}) collective-permute-start(bf16[512,1024]{1,0:T(8,128)(2,1)} %shard_map.152), channel_id=1, source_target_pairs={{0,2},{2,4},{4,6},{6,0},{1,3},{3,5},{5,7},{7,1},{8,10},{10,12},{12... | collective-permute-start | bytes 3145736 | tf_op jit(solution)/shard_map/ppermute | solution.py:464
  53.7 14.1 %all-to-all-start.1 = ((bf16[8,80,128]{2,1,0:T(8,128)(2,1)}), bf16[8,80,128]{2,1,0:T(8,128)(2,1)S(1)}, u32[]{:S(2)}, u32[]{:S(2)}) async-start(bf16[8,80,128]{2,1,0:T(8,128)(2,1)} %shard_map.146), calls=%async_computation.1 | async-start | bytes 327680 | tf_op jit(solution)/shard_map/all_to_all | solution.py:508
  67.7 0.7 copy-start.5
  71.8 37.0 %all-to-all-start.2 = ((bf16[32,24,256]{2,1,0:T(8,128)(2,1)}), bf16[32,24,256]{2,1,0:T(8,128)(2,1)S(1)}, u32[]{:S(2)}, u32[]{:S(2)}) async-start(bf16[32,24,256]{2,1,0:T(8,128)(2,1)} %get-tuple-element.29), calls=%async_computation.2 | async-start | bytes 786432 | tf_op jit(solution)/shard_map/all_to_all | solution.py:547
  80.4 45.7 %collective-permute-start.4 = (bf16[512,1024]{1,0:T(8,128)(2,1)}, bf16[512,1024]{1,0:T(8,128)(2,1)S(1)}, u32[]{:S(2)}, u32[]{:S(2)}) collective-permute-start(bf16[512,1024]{1,0:T(8,128)(2,1)} %collective-permute-done.3.m2_in), channel_id=1, source_target_pairs={{0,1},{1,0},{2,3},{3,2},{4,5},{5,4},{6,7},{7,6},{8,9},{9,8},{10,11... | collective-permute-start | bytes 3145736 | tf_op jit(solution)/shard_map/ppermute | solution.py:464
  80.5 48.9 %collective-permute-start.10 = (bf16[512,1024]{1,0:T(8,128)(2,1)}, bf16[512,1024]{1,0:T(8,128)(2,1)S(1)}, u32[]{:S(2)}, u32[]{:S(2)}) collective-permute-start(bf16[512,1024]{1,0:T(8,128)(2,1)} %collective-permute-done.8.m3_in), channel_id=1, source_target_pairs={{0,1},{1,0},{2,3},{3,2},{4,5},{5,4},{6,7},{7,6},{8,9},{9,8},{10,11... | collective-permute-start | bytes 3145736 | tf_op jit(solution)/shard_map/ppermute | solution.py:464
  81.0 48.4 %collective-permute-start.9 = (bf16[512,1024]{1,0:T(8,128)(2,1)}, bf16[512,1024]{1,0:T(8,128)(2,1)S(1)}, u32[]{:S(2)}, u32[]{:S(2)}) collective-permute-start(bf16[512,1024]{1,0:T(8,128)(2,1)} %collective-permute-done.7.m1_in), channel_id=1, source_target_pairs={{0,1},{1,0},{2,3},{3,2},{4,5},{5,4},{6,7},{7,6},{8,9},{9,8},{10,11... | collective-permute-start | bytes 3145736 | tf_op jit(solution)/shard_map/ppermute | solution.py:464
  81.1 7.6 %collective-permute-start = (bf16[128,256]{1,0:T(8,128)(2,1)}, bf16[128,256]{1,0:T(8,128)(2,1)S(1)}, u32[]{:S(2)}, u32[]{:S(2)}) collective-permute-start(bf16[128,256]{1,0:T(8,128)(2,1)} %get-tuple-element.26), channel_id=1, source_target_pairs={{0,8},{8,16},{16,24},{24,32},{32,40},{40,48},{48,56},{56,64},{64,7... | collective-permute-start | bytes 196616 | tf_op jit(solution)/shard_map/ppermute | solution.py:545
  85.7 9.7 %collective-permute-start.1 = (bf16[128,256]{1,0:T(8,128)(2,1)}, bf16[128,256]{1,0:T(8,128)(2,1)S(1)}, u32[]{:S(2)}, u32[]{:S(2)}) collective-permute-start(bf16[128,256]{1,0:T(8,128)(2,1)} %get-tuple-element.27), channel_id=1, source_target_pairs={{8,0},{16,8},{24,16},{32,24},{40,32},{48,40},{56,48},{64,56},{72,6... | collective-permute-start | bytes 196616 | tf_op jit(solution)/shard_map/ppermute | solution.py:546
  88.7 6.6 %copy-start.6 = (bf16[128,256]{1,0:T(8,128)(2,1)}, bf16[128,256]{1,0:T(8,128)(2,1)S(1)}, u32[]{:S(2)}) copy-start(bf16[128,256]{1,0:T(8,128)(2,1)S(1)} %collective-permute-done.before_ref) | copy-start | bytes 196612
  95.4 0.6 copy-start.7
  96.0 12.9 %copy-start.4 = (f32[4]{0:T(128)S(1)}, f32[4]{0:T(128)}, u32[]{:S(2)}) copy-start(f32[4]{0:T(128)} %param.29) | copy-start | bytes 52
  108.9 1.7 %copy-start = (bf16[9,512,256]{2,1,0:T(8,128)(2,1)S(1)}, bf16[9,512,256]{2,1,0:T(8,128)(2,1)}, u32[]{:S(2)}) copy-start(bf16[9,512,256]{2,1,0:T(8,128)(2,1)} %get-tuple-element.28.refs_0_) | copy-start | bytes 7077892
  112.9 8.9 %collective-permute-start.2 = (bf16[256,512]{1,0:T(8,128)(2,1)S(1)}, bf16[256,512]{1,0:T(8,128)(2,1)S(1)}, u32[]{:S(2)}, u32[]{:S(2)}) collective-permute-start(bf16[256,512]{1,0:T(8,128)(2,1)S(1)} %shard_map.151), channel_id=1, source_target_pairs={{0,4},{2,6},{4,0},{6,2},{1,5},{3,7},{5,1},{7,3},{8,12},{10,14},{12... | collective-permute-start | bytes 786440 | tf_op jit(solution)/shard_map/ppermute | solution.py:464
  118.5 7.6 %copy-start.1 = (bf16[512,2048]{1,0:T(8,128)(2,1)S(1)}, bf16[512,2048]{1,0:T(8,128)(2,1)}, u32[]{:S(2)}) copy-start(bf16[512,2048]{1,0:T(8,128)(2,1)} %w0_ref.1) | copy-start | bytes 6291460
  118.5 9.8 %collective-permute-start.5 = (bf16[256,512]{1,0:T(8,128)(2,1)S(1)}, bf16[256,512]{1,0:T(8,128)(2,1)S(1)}, u32[]{:S(2)}, u32[]{:S(2)}) collective-permute-start(bf16[256,512]{1,0:T(8,128)(2,1)S(1)} %get-tuple-element.30), channel_id=1, source_target_pairs={{0,2},{2,4},{4,6},{6,0},{1,3},{3,5},{5,7},{7,1},{8,10},{10,12},{12... | collective-permute-start | bytes 786440 | tf_op jit(solution)/shard_map/ppermute | solution.py:464
  121.8 7.6 %collective-permute-start.6 = (bf16[256,512]{1,0:T(8,128)(2,1)S(1)}, bf16[256,512]{1,0:T(8,128)(2,1)S(1)}, u32[]{:S(2)}, u32[]{:S(2)}) collective-permute-start(bf16[256,512]{1,0:T(8,128)(2,1)S(1)} %get-tuple-element.31), channel_id=1, source_target_pairs={{0,6},{2,0},{4,2},{6,4},{1,7},{3,1},{5,3},{7,5},{8,14},{10,8},{12,... | collective-permute-start | bytes 786440 | tf_op jit(solution)/shard_map/ppermute | solution.py:464
  126.1 3.3 %copy-start.2 = (bf16[256,2048]{1,0:T(8,128)(2,1)S(1)}, bf16[256,2048]{1,0:T(8,128)(2,1)}, u32[]{:S(2)}) copy-start(bf16[256,2048]{1,0:T(8,128)(2,1)} %get-tuple-element.32.lat_ref) | copy-start | bytes 3145732
  126.1 3.3 %copy-start.3 = (f32[8,2048]{1,0:T(8,128)S(1)}, f32[8,2048]{1,0:T(8,128)}, u32[]{:S(2)}) copy-start(f32[8,2048]{1,0:T(8,128)} %get-tuple-element.25.vec_ref) | copy-start | bytes 196612

commit v10 on v9

--- a/solution.py
+++ b/solution.py
@@ -379,9 +379,9 @@
     for by, out_ref in zip(shifts, out_refs):
         quarter = (tp + by) % NX
 
-        def body(i, carry, quarter=quarter, out_ref=out_ref):
+        for i in range(2):
             block = quarter * 2 + i
-            base = pl.ds(pl.multiple_of(i * WINDOW, WINDOW), WINDOW)
+            base = slice(i * WINDOW, (i + 1) * WINDOW)
             far = jnp.exp2(contract_last(packed_ref[block, :, :head], ctx_ref[:, :head]))
             near_sum = jnp.where(lane == block, sums, 0.0)
             total = jnp.sum(lanes_summed(far) + near_sum, axis=-1, keepdims=True) + sink
@@ -391,9 +391,6 @@
             mixed = (mixed * (1.0 / total)).astype(BF16)
             for h in range(4):
                 out_ref[base, h * head : (h + 1) * head] = mixed[h * WINDOW : (h + 1) * WINDOW]
-            return carry
-
-        lax.fori_loop(0, 2, body, 0)
 
 
 def early_kernel(a0_ref, a2_ref, w0_ref, m2_in, o2_ref, sum_ref, m2_ref, sem):

time: 134 us -> 134 us (level)
  the two profiles are of different devices: /device:TPU:126 before, /device:TPU:124 now
where the time goes in v10:
time: 134 us; the launch traced here: 133 us
  blocking collectives  46.2 us (34%)
  Pallas kernels  36.8 us (27%)
  starting transfers between devices  28.9 us (22%)
  waiting for transfers between devices  18.1 us (14%)
  local copies, waits for them, and re-layouts  2.96 us (2%)
    all_to_all x1, blocking collectives, per_device(): part = lax.all_to_all(part, ('y', 'tp'), 0, 0, tiled=True)  46.2 us
    pallas_call x11, Pallas kernels, call(): pl.pallas_call(kernel, in_specs=in_specs or [VMEM] * len(args), out_specs...  36.8 us
    all_to_all x1, starting transfers between devices, per_device(): lax.all_to_all(ctx_kv, SP, 0, 0, tiled=True).reshape(-1, 2 * HEAD_DIM)  8.54 us
    all_to_all x1, starting transfers between devices, per_device(): mod = lax.all_to_all(part, 'z', 0, 0, tiled=True)  7.66 us
    ppermute x9, waiting for transfers between devices, shifted(): lax.ppermute(array, axis, [(i, (i + by) % peers) for i in range(peers)])  7.25 us
    ppermute x1, waiting for transfers between devices, per_device(): after = lax.ppermute(first_kv, SP, [(j, i) for i, j in up])  6.64 us
    ppermute x9, starting transfers between devices, shifted(): lax.ppermute(array, axis, [(i, (i + by) % peers) for i in range(peers)])  6.22 us
    ppermute x1, starting transfers between devices, per_device(): before = lax.ppermute(last_kv, SP, up)  4.58 us
  transfers between devices with their start and end apart: 13, of which 5 were waited for; matrix products, arithmetic and copies ran while one was open for 0% of the time, Pallas kernels for 23%

profile of v10, /device:TPU:124, one launch (start us, length us, event | category | flops | bytes accessed | tf_op | source)
XLA Modules:
  0.0 133.2 jit_solution(11319805016767366688)
XLA Ops:
  0.0 2.2 %shard_map.152 = bf16[512,1024]{1,0:T(8,128)(2,1)} custom-call(bf16[512,2048]{1,0:T(8,128)(2,1)} %w0_ref.1), custom_call_target="tpu_custom_call" | custom-call | flops 16777216 | bytes 2097152 | tf_op jit(solution)/shard_map/pallas_call | solution.py:472
  2.8 2.2 %collective-permute-start.8 = (bf16[512,1024]{1,0:T(8,128)(2,1)}, bf16[512,1024]{1,0:T(8,128)(2,1)}, u32[]{:S(2)}, u32[]{:S(2)}) collective-permute-start(bf16[512,1024]{1,0:T(8,128)(2,1)} %shard_map.152), channel_id=1, source_target_pairs={{0,6},{2,0},{4,2},{6,4},{1,7},{3,1},{5,3},{7,5},{8,14},{10,8},{12,... | collective-permute-start | bytes 3145736 | tf_op jit(solution)/shard_map/ppermute | solution.py:461
  5.0 1.8 %shard_map.145 = bf16[16,24,128]{2,1,0:T(8,128)(2,1)} custom-call(f32[1,2048]{1,0:T(1,128)} %cond_in.1, f32[1,2048]{1,0:T(1,128)} %bitcast.19, bf16[64,512]{1,0:T(8,128)(2,1)} %shift_in.1, bf16[64,512]{1,0:T(8,128)(2,1)} %scale_in.1, bf16[64,512]{1,0:T(8,128)(2,1)} %gate_in.1), custom_call_target="tpu_custom_call" | custom-call | flops 1048576 | bytes 262144 | tf_op jit(solution)/shard_map/pallas_call | solution.py:472
  6.8 46.2 %all_to_all.15.in_ref = bf16[16,24,128]{2,1,0:T(8,128)(2,1)S(1)} all-to-all(bf16[16,24,128]{2,1,0:T(8,128)(2,1)} %shard_map.145), channel_id=1, replica_groups=mesh['z'=8,'y'=4,'tp'=4,'dp'=2] {'y','tp'}, dimensions={0} | all-to-all | bytes 196608 | tf_op jit(solution)/shard_map/all_to_all | solution.py:503
  53.0 0.7 shard_map.146
  53.7 7.7 %all-to-all-start.1 = ((bf16[8,80,128]{2,1,0:T(8,128)(2,1)}), bf16[8,80,128]{2,1,0:T(8,128)(2,1)S(1)}, u32[]{:S(2)}, u32[]{:S(2)}) async-start(bf16[8,80,128]{2,1,0:T(8,128)(2,1)} %shard_map.146), calls=%async_computation.1 | async-start | bytes 327680 | tf_op jit(solution)/shard_map/all_to_all | solution.py:505
  61.3 3.3 %shard_map.147 = (bf16[280,2048]{1,0:T(8,128)(2,1)}, bf16[2048,256]{1,0:T(8,128)(2,1)}, f32[24,128]{1,0:T(8,128)}, f32[24,128]{1,0:T(8,128)}, f32[64,128]{1,0:T(8,128)}, /*index=5*/f32[64,128]{1,0:T(8,128)}) custom-call(bf16[1024,2048]{1,0:T(8,128)(2,1)} %bitcast.15, bf16[24,2048]{1,0:T(8,128)(2,1)} %bitcast.17, bf16[2048,128]{1,0:T(8,128)(2,1)} %wk_in.1, ...), custom_call_target="tpu_custom_call" | custom-call | flops 16777216 | bytes 4194304 | tf_op jit(solution)/shard_map/pallas_call | solution.py:472
  64.7 3.1 %all-to-all-done.1.mod_ref = bf16[8,80,128]{2,1,0:T(8,128)(2,1)S(1)} async-done(((bf16[8,80,128]{2,1,0:T(8,128)(2,1)}), bf16[8,80,128]{2,1,0:T(8,128)(2,1)S(1)}, u32[]{:S(2)}, u32[]{:S(2)}) %all-to-all-start.1) | async-done | bytes 163872 | tf_op jit(solution)/shard_map/all_to_all | solution.py:505
  68.4 3.4 %shard_map.148 = (bf16[32,24,256]{2,1,0:T(8,128)(2,1)}, f32[8,2048]{1,0:T(8,128)}, bf16[128,256]{1,0:T(8,128)(2,1)}, bf16[128,256]{1,0:T(8,128)(2,1)}) custom-call(bf16[8,80,128]{2,1,0:T(8,128)(2,1)} %copy-done.5, bf16[280,2048]{1,0:T(8,128)(2,1)} %get-tuple-element.19.rows_in, bf16[2048,256]{1,0:T(8,128)(2,1)} %get-tuple-element.20.wkv_ref.wkv_in, ...), custom_call_target="tpu_custom_call" | custom-call | flops 293601280 | bytes 1048576 | tf_op jit(solution)/shard_map/pallas_call | solution.py:472
  71.8 8.5 %all-to-all-start.2 = ((bf16[32,24,256]{2,1,0:T(8,128)(2,1)}), bf16[32,24,256]{2,1,0:T(8,128)(2,1)S(1)}, u32[]{:S(2)}, u32[]{:S(2)}) async-start(bf16[32,24,256]{2,1,0:T(8,128)(2,1)} %get-tuple-element.29), calls=%async_computation.2 | async-start | bytes 786432 | tf_op jit(solution)/shard_map/all_to_all | solution.py:544
  81.1 4.6 %collective-permute-start = (bf16[128,256]{1,0:T(8,128)(2,1)}, bf16[128,256]{1,0:T(8,128)(2,1)S(1)}, u32[]{:S(2)}, u32[]{:S(2)}) collective-permute-start(bf16[128,256]{1,0:T(8,128)(2,1)} %get-tuple-element.26), channel_id=1, source_target_pairs={{0,8},{8,16},{16,24},{24,32},{32,40},{40,48},{48,56},{56,64},{64,7... | collective-permute-start | bytes 196616 | tf_op jit(solution)/shard_map/ppermute | solution.py:542
  85.7 1.9 %collective-permute-start.1 = (bf16[128,256]{1,0:T(8,128)(2,1)}, bf16[128,256]{1,0:T(8,128)(2,1)S(1)}, u32[]{:S(2)}, u32[]{:S(2)}) collective-permute-start(bf16[128,256]{1,0:T(8,128)(2,1)} %get-tuple-element.27), channel_id=1, source_target_pairs={{8,0},{16,8},{24,16},{32,24},{40,32},{48,40},{56,48},{64,56},{72,6... | collective-permute-start | bytes 196616 | tf_op jit(solution)/shard_map/ppermute | solution.py:543
  87.6 1.1 collective-permute-done.before_ref
  88.7 6.6 %collective-permute-done.1.after_ref = bf16[128,256]{1,0:T(8,128)(2,1)S(1)} collective-permute-done((bf16[128,256]{1,0:T(8,128)(2,1)}, bf16[128,256]{1,0:T(8,128)(2,1)S(1)}, u32[]{:S(2)}, u32[]{:S(2)}) %collective-permute-start.1) | collective-permute-done | bytes 65568 | tf_op jit(solution)/shard_map/ppermute | solution.py:543
  96.0 12.8 %shard_map.149 = (bf16[9,512,256]{2,1,0:T(8,128)(2,1)}, bf16[256,2048]{1,0:T(8,128)(2,1)}) custom-call(bf16[1024,2048]{1,0:T(8,128)(2,1)} %bitcast.16, bf16[2048,512]{1,0:T(8,128)(2,1)} %wq_in.1, bf16[2048,256]{1,0:T(8,128)(2,1)} %get-tuple-element.20.wkv_ref.wkv_in, bf16[128,256]{1,0:T(8,128)(2,1)} %copy-done.6, bf16[128,256]{1,0:T(8,128)(2,1)} %copy-done.7, ...), custom_call_target="tpu_custom_call" | custom-call | flops 4026531840 | bytes 7340032 | tf_op jit(solution)/shard_map/pallas_call | solution.py:472
  108.9 1.7 %copy-done = bf16[9,512,256]{2,1,0:T(8,128)(2,1)S(1)} copy-done((bf16[9,512,256]{2,1,0:T(8,128)(2,1)S(1)}, bf16[9,512,256]{2,1,0:T(8,128)(2,1)}, u32[]{:S(2)}) %copy-start) | copy-done | bytes 2359320
  110.5 2.0 %shard_map.151 = bf16[256,512]{1,0:T(8,128)(2,1)S(1)} custom-call(bf16[9,512,256]{2,1,0:T(8,128)(2,1)S(1)} %copy-done, bf16[768,256]{1,0:T(8,128)(2,1)S(1)} %bitcast.9, f32[1,4]{1,0:T(1,128)S(1)} %bitcast.12), custom_call_target="tpu_custom_call" | custom-call | flops 402653184 | bytes 2097152 | tf_op jit(solution)/shard_map/pallas_call | solution.py:472
  113.1 3.1 %shard_map.154 = (bf16[256,512]{1,0:T(8,128)(2,1)S(1)}, bf16[256,512]{1,0:T(8,128)(2,1)S(1)}) custom-call(bf16[9,512,256]{2,1,0:T(8,128)(2,1)S(1)} %copy-done, bf16[768,256]{1,0:T(8,128)(2,1)S(1)} %bitcast.10, f32[1,4]{1,0:T(1,128)S(1)} %bitcast.13), custom_call_target="tpu_custom_call" | custom-call | flops 805306368 | bytes 2097152 | tf_op jit(solution)/shard_map/pallas_call | solution.py:472
  116.2 2.1 %collective-permute-start.5 = (bf16[256,512]{1,0:T(8,128)(2,1)S(1)}, bf16[256,512]{1,0:T(8,128)(2,1)S(1)}, u32[]{:S(2)}, u32[]{:S(2)}) collective-permute-start(bf16[256,512]{1,0:T(8,128)(2,1)S(1)} %get-tuple-element.30), channel_id=1, source_target_pairs={{0,2},{2,4},{4,6},{6,0},{1,3},{3,5},{5,7},{7,1},{8,10},{10,12},{12... | collective-permute-start | bytes 786440 | tf_op jit(solution)/shard_map/ppermute | solution.py:461
  118.3 5.1 %collective-permute-done.2.a2_ref = bf16[256,512]{1,0:T(8,128)(2,1)S(1)} collective-permute-done((bf16[256,512]{1,0:T(8,128)(2,1)S(1)}, bf16[256,512]{1,0:T(8,128)(2,1)S(1)}, u32[]{:S(2)}, u32[]{:S(2)}) %collective-permute-start.2) | collective-permute-done | bytes 262176 | tf_op jit(solution)/shard_map/ppermute | solution.py:461
  123.4 2.0 %shard_map.150.a0_ref = bf16[256,512]{1,0:T(8,128)(2,1)S(1)} custom-call(bf16[9,512,256]{2,1,0:T(8,128)(2,1)S(1)} %copy-done, bf16[768,256]{1,0:T(8,128)(2,1)S(1)} %bitcast.11, f32[1,4]{1,0:T(1,128)S(1)} %bitcast.14), custom_call_target="tpu_custom_call" | custom-call | flops 402653184 | bytes 2097152 | tf_op jit(solution)/shard_map/pallas_call | solution.py:472
  125.4 2.2 %shard_map.153.sum_ref = f32[256,2048]{1,0:T(8,128)S(1)} custom-call(bf16[256,512]{1,0:T(8,128)(2,1)S(1)} %shard_map.150.a0_ref, bf16[256,512]{1,0:T(8,128)(2,1)S(1)} %collective-permute-done.2.a2_ref, bf16[512,2048]{1,0:T(8,128)(2,1)S(1)} %copy-done.1, bf16[512,1024]{1,0:T(8,128)(2,1)} %collective-permute-done.3.m2_in, ...), custom_call_target="tpu_custom_call" | custom-call | flops 1073741824 | bytes 4194304 | tf_op jit(solution)/shard_map/pallas_call | solution.py:472
  127.6 2.2 %collective-permute-done.6.a3_ref = bf16[256,512]{1,0:T(8,128)(2,1)S(1)} collective-permute-done((bf16[256,512]{1,0:T(8,128)(2,1)S(1)}, bf16[256,512]{1,0:T(8,128)(2,1)S(1)}, u32[]{:S(2)}, u32[]{:S(2)}) %collective-permute-start.6) | collective-permute-done | bytes 262176 | tf_op jit(solution)/shard_map/ppermute | solution.py:461
  129.8 3.3 %shard_map.155 = bf16[256,2048]{1,0:T(8,128)(2,1)} custom-call(f32[8,2048]{1,0:T(8,128)S(1)} %copy-done.3, f32[256,2048]{1,0:T(8,128)S(1)} %shard_map.153.sum_ref, bf16[256,512]{1,0:T(8,128)(2,1)S(1)} %collective-permute-done.5.a1_ref, bf16[256,512]{1,0:T(8,128)(2,1)S(1)} %collective-permute-done.6.a3_ref, bf16[512,1024]{1,0:T(8,128)(2,1)} %collective-permute-done.7.m1_in, ...), custom_call_target="tpu_custom_call" | custom-call | flops 1073741824 | bytes 4194304 | tf_op jit(solution)/shard_map/pallas_call | solution.py:472
  (30 shorter events, 3.2 us)
Async XLA Ops:
  2.2 78.2 %collective-permute-start.3 = (bf16[512,1024]{1,0:T(8,128)(2,1)}, bf16[512,1024]{1,0:T(8,128)(2,1)}, u32[]{:S(2)}, u32[]{:S(2)}) collective-permute-start(bf16[512,1024]{1,0:T(8,128)(2,1)} %shard_map.152), channel_id=1, source_target_pairs={{0,4},{2,6},{4,0},{6,2},{1,5},{3,7},{5,1},{7,3},{8,12},{10,14},{12... | collective-permute-start | bytes 3145736 | tf_op jit(solution)/shard_map/ppermute | solution.py:461
  2.8 77.7 %collective-permute-start.8 = (bf16[512,1024]{1,0:T(8,128)(2,1)}, bf16[512,1024]{1,0:T(8,128)(2,1)}, u32[]{:S(2)}, u32[]{:S(2)}) collective-permute-start(bf16[512,1024]{1,0:T(8,128)(2,1)} %shard_map.152), channel_id=1, source_target_pairs={{0,6},{2,0},{4,2},{6,4},{1,7},{3,1},{5,3},{7,5},{8,14},{10,8},{12,... | collective-permute-start | bytes 3145736 | tf_op jit(solution)/shard_map/ppermute | solution.py:461
  5.0 76.0 %collective-permute-start.7 = (bf16[512,1024]{1,0:T(8,128)(2,1)}, bf16[512,1024]{1,0:T(8,128)(2,1)}, u32[]{:S(2)}, u32[]{:S(2)}) collective-permute-start(bf16[512,1024]{1,0:T(8,128)(2,1)} %shard_map.152), channel_id=1, source_target_pairs={{0,2},{2,4},{4,6},{6,0},{1,3},{3,5},{5,7},{7,1},{8,10},{10,12},{12... | collective-permute-start | bytes 3145736 | tf_op jit(solution)/shard_map/ppermute | solution.py:461
  53.7 14.1 %all-to-all-start.1 = ((bf16[8,80,128]{2,1,0:T(8,128)(2,1)}), bf16[8,80,128]{2,1,0:T(8,128)(2,1)S(1)}, u32[]{:S(2)}, u32[]{:S(2)}) async-start(bf16[8,80,128]{2,1,0:T(8,128)(2,1)} %shard_map.146), calls=%async_computation.1 | async-start | bytes 327680 | tf_op jit(solution)/shard_map/all_to_all | solution.py:505
  67.7 0.7 copy-start.5
  71.8 37.0 %all-to-all-start.2 = ((bf16[32,24,256]{2,1,0:T(8,128)(2,1)}), bf16[32,24,256]{2,1,0:T(8,128)(2,1)S(1)}, u32[]{:S(2)}, u32[]{:S(2)}) async-start(bf16[32,24,256]{2,1,0:T(8,128)(2,1)} %get-tuple-element.29), calls=%async_computation.2 | async-start | bytes 786432 | tf_op jit(solution)/shard_map/all_to_all | solution.py:544
  80.4 45.0 %collective-permute-start.4 = (bf16[512,1024]{1,0:T(8,128)(2,1)}, bf16[512,1024]{1,0:T(8,128)(2,1)S(1)}, u32[]{:S(2)}, u32[]{:S(2)}) collective-permute-start(bf16[512,1024]{1,0:T(8,128)(2,1)} %collective-permute-done.3.m2_in), channel_id=1, source_target_pairs={{0,1},{1,0},{2,3},{3,2},{4,5},{5,4},{6,7},{7,6},{8,9},{9,8},{10,11... | collective-permute-start | bytes 3145736 | tf_op jit(solution)/shard_map/ppermute | solution.py:461
  80.5 49.3 %collective-permute-start.10 = (bf16[512,1024]{1,0:T(8,128)(2,1)}, bf16[512,1024]{1,0:T(8,128)(2,1)S(1)}, u32[]{:S(2)}, u32[]{:S(2)}) collective-permute-start(bf16[512,1024]{1,0:T(8,128)(2,1)} %collective-permute-done.8.m3_in), channel_id=1, source_target_pairs={{0,1},{1,0},{2,3},{3,2},{4,5},{5,4},{6,7},{7,6},{8,9},{9,8},{10,11... | collective-permute-start | bytes 3145736 | tf_op jit(solution)/shard_map/ppermute | solution.py:461
  81.0 48.8 %collective-permute-start.9 = (bf16[512,1024]{1,0:T(8,128)(2,1)}, bf16[512,1024]{1,0:T(8,128)(2,1)S(1)}, u32[]{:S(2)}, u32[]{:S(2)}) collective-permute-start(bf16[512,1024]{1,0:T(8,128)(2,1)} %collective-permute-done.7.m1_in), channel_id=1, source_target_pairs={{0,1},{1,0},{2,3},{3,2},{4,5},{5,4},{6,7},{7,6},{8,9},{9,8},{10,11... | collective-permute-start | bytes 3145736 | tf_op jit(solution)/shard_map/ppermute | solution.py:461
  81.1 7.6 %collective-permute-start = (bf16[128,256]{1,0:T(8,128)(2,1)}, bf16[128,256]{1,0:T(8,128)(2,1)S(1)}, u32[]{:S(2)}, u32[]{:S(2)}) collective-permute-start(bf16[128,256]{1,0:T(8,128)(2,1)} %get-tuple-element.26), channel_id=1, source_target_pairs={{0,8},{8,16},{16,24},{24,32},{32,40},{40,48},{48,56},{56,64},{64,7... | collective-permute-start | bytes 196616 | tf_op jit(solution)/shard_map/ppermute | solution.py:542
  85.7 9.7 %collective-permute-start.1 = (bf16[128,256]{1,0:T(8,128)(2,1)}, bf16[128,256]{1,0:T(8,128)(2,1)S(1)}, u32[]{:S(2)}, u32[]{:S(2)}) collective-permute-start(bf16[128,256]{1,0:T(8,128)(2,1)} %get-tuple-element.27), channel_id=1, source_target_pairs={{8,0},{16,8},{24,16},{32,24},{40,32},{48,40},{56,48},{64,56},{72,6... | collective-permute-start | bytes 196616 | tf_op jit(solution)/shard_map/ppermute | solution.py:543
  88.7 6.6 %copy-start.6 = (bf16[128,256]{1,0:T(8,128)(2,1)}, bf16[128,256]{1,0:T(8,128)(2,1)S(1)}, u32[]{:S(2)}) copy-start(bf16[128,256]{1,0:T(8,128)(2,1)S(1)} %collective-permute-done.before_ref) | copy-start | bytes 196612
  95.4 0.6 copy-start.7
  96.0 12.9 %copy-start.4 = (f32[4]{0:T(128)S(1)}, f32[4]{0:T(128)}, u32[]{:S(2)}) copy-start(f32[4]{0:T(128)} %param.29) | copy-start | bytes 52
  108.8 1.7 %copy-start = (bf16[9,512,256]{2,1,0:T(8,128)(2,1)S(1)}, bf16[9,512,256]{2,1,0:T(8,128)(2,1)}, u32[]{:S(2)}) copy-start(bf16[9,512,256]{2,1,0:T(8,128)(2,1)} %get-tuple-element.28.refs_0_) | copy-start | bytes 7077892
  112.5 10.9 %collective-permute-start.2 = (bf16[256,512]{1,0:T(8,128)(2,1)S(1)}, bf16[256,512]{1,0:T(8,128)(2,1)S(1)}, u32[]{:S(2)}, u32[]{:S(2)}) collective-permute-start(bf16[256,512]{1,0:T(8,128)(2,1)S(1)} %shard_map.151), channel_id=1, source_target_pairs={{0,4},{2,6},{4,0},{6,2},{1,5},{3,7},{5,1},{7,3},{8,12},{10,14},{12... | collective-permute-start | bytes 786440 | tf_op jit(solution)/shard_map/ppermute | solution.py:461
  116.2 9.2 %copy-start.1 = (bf16[512,2048]{1,0:T(8,128)(2,1)S(1)}, bf16[512,2048]{1,0:T(8,128)(2,1)}, u32[]{:S(2)}) copy-start(bf16[512,2048]{1,0:T(8,128)(2,1)} %w0_ref.1) | copy-start | bytes 6291460
  116.2 11.4 %collective-permute-start.5 = (bf16[256,512]{1,0:T(8,128)(2,1)S(1)}, bf16[256,512]{1,0:T(8,128)(2,1)S(1)}, u32[]{:S(2)}, u32[]{:S(2)}) collective-permute-start(bf16[256,512]{1,0:T(8,128)(2,1)S(1)} %get-tuple-element.30), channel_id=1, source_target_pairs={{0,2},{2,4},{4,6},{6,0},{1,3},{3,5},{5,7},{7,1},{8,10},{10,12},{12... | collective-permute-start | bytes 786440 | tf_op jit(solution)/shard_map/ppermute | solution.py:461
  123.4 6.4 %collective-permute-start.6 = (bf16[256,512]{1,0:T(8,128)(2,1)S(1)}, bf16[256,512]{1,0:T(8,128)(2,1)S(1)}, u32[]{:S(2)}, u32[]{:S(2)}) collective-permute-start(bf16[256,512]{1,0:T(8,128)(2,1)S(1)} %get-tuple-element.31), channel_id=1, source_target_pairs={{0,6},{2,0},{4,2},{6,4},{1,7},{3,1},{5,3},{7,5},{8,14},{10,8},{12,... | collective-permute-start | bytes 786440 | tf_op jit(solution)/shard_map/ppermute | solution.py:461
  125.3 4.4 %copy-start.2 = (bf16[256,2048]{1,0:T(8,128)(2,1)S(1)}, bf16[256,2048]{1,0:T(8,128)(2,1)}, u32[]{:S(2)}) copy-start(bf16[256,2048]{1,0:T(8,128)(2,1)} %get-tuple-element.32.lat_ref) | copy-start | bytes 3145732
  125.3 4.4 %copy-start.3 = (f32[8,2048]{1,0:T(8,128)S(1)}, f32[8,2048]{1,0:T(8,128)}, u32[]{:S(2)}) copy-start(f32[8,2048]{1,0:T(8,128)} %get-tuple-element.25.vec_ref) | copy-start | bytes 196612
